TPU v7x, 256 devices: a whole 4x4x8 slice. The times are simulated.
256 devices in a mesh: sp: 32 (over z, x), tp: 8 (over y, core).
Axes of the slice: x: 4, y: 4, z: 8, core: 2. Of those that a mesh axis runs over, the one named last changes fastest.
Arguments:
- tokens: bfloat16 [32768, 2048], P('sp', 'tp'), may hold values from -70 to 70
- w_query: bfloat16 [2048, 1024], P(None, 'tp'), may hold values from -0.125 to 0.125
- w_key: bfloat16 [2048, 1024], P(None, 'tp'), may hold values from -0.125 to 0.125
- w_value: bfloat16 [2048, 1024], P(None, 'tp'), may hold values from -0.125 to 0.125
- w_delta_gate: bfloat16 [2048, 1024], P(None, 'tp'), may hold values from -0.125 to 0.125
- w_glu_value: bfloat16 [2048, 1024], P(None, 'tp'), may hold values from -0.125 to 0.125
- w_glu_gate: bfloat16 [2048, 1024], P(None, 'tp'), may hold values from -0.125 to 0.125
- w_conv_gate: bfloat16 [2048, 1024], P(None, 'tp'), may hold values from -0.125 to 0.125
- w_beta: bfloat16 [2048, 8], replicated, may hold values from -0.125 to 0.125
- w_decay: bfloat16 [2048, 8], replicated, may hold values from -0.125 to 0.125
- decay_log: float32 [8], replicated, may hold values from -12 to -3
- head_gain: float32 [128], replicated, may hold values from 0.1 to 1.9
- conv_taps: bfloat16 [31, 1024], P(None, 'tp'), may hold values from -2.5 to 2.5
- ln_gain: float32 [1024], P('tp'), may hold values from 0.1 to 1.9
- ln_shift: float32 [1024], P('tp'), may hold values from -3 to 3
- out_delta: bfloat16 [1024, 2048], P('tp'), may hold values from -0.125 to 0.125
- out_conv: bfloat16 [1024, 2048], P('tp'), may hold values from -0.125 to 0.125
Outputs:
- mixed_out: bfloat16 [32768, 2048], P(('sp', 'tp'))
All inputs are finite; a program needn't handle non-finite values.
Results may differ from a plain program's by a relative error of at most 0.024.
Values may be sent and summed in bfloat16 or wider, within the bound.
No kernel may reach another device: no remote copies, remote signals or barrier semaphores. Data moves between devices by JAX's collectives and lax.ppermute only.
A program may use at most 64 MiB of HBM per device.

v0:
```python
import functools

import jax
import jax.numpy as jnp
from jax import lax
from jax.experimental import pallas as pl
from jax.experimental.pallas import tpu as pltpu
from jax.sharding import Mesh
from jax.sharding import PartitionSpec as P


SP = ("z", "x")
TP = ("y", "c")
TINY_NORM = 1e-06
TINY_VAR = 1e-05
CHUNK = 128
F32 = jnp.float32
BF16 = jnp.bfloat16


def whole():
    return pl.BlockSpec(memory_space=pltpu.VMEM)


def scalars():
    return pl.BlockSpec(memory_space=pltpu.SMEM)


def params(mib):
    return pltpu.CompilerParams(vmem_limit_bytes=mib * 1024 * 1024)


def cost(flops, bytes_accessed):
    return pl.CostEstimate(flops=flops, bytes_accessed=bytes_accessed, transcendentals=0)


def dot(a, b):
    return jnp.dot(a, b, preferred_element_type=F32)


def dot_nt(a, b):
    return lax.dot_general(a, b, (((1,), (1,)), ((), ())), preferred_element_type=F32)


def dot_tn(a, b):
    return lax.dot_general(a, b, (((0,), (0,)), ((), ())), preferred_element_type=F32)


def low(a):
    return a.astype(BF16)


def split_two(a):
    high = a.astype(BF16)
    return high, (a - high.astype(F32)).astype(BF16)


def split_three(a):
    high = a.astype(BF16)
    rest = a - high.astype(F32)
    middle = rest.astype(BF16)
    return high, middle, (rest - middle.astype(F32)).astype(BF16)


def dot_fine(a, b):
    a_high, a_low = split_two(a)
    b_high, b_low = split_two(b)
    return dot(a_high, b_high) + (dot(a_high, b_low) + dot(a_low, b_high))


def project_kernel(width_all, head_size, block_ref, rate_ref, *refs):
    own, sw, r1, sr1, l1, sl1, fa, sfa, fb, sfb, weights = refs[:11]
    q_ref, k_ref, v_ref, dg_ref, gu_ref, cg_ref, bl_ref = refs[11:18]
    gathered = refs[18]
    first = pl.program_id(0) == 0
    piece_width = own.shape[1]
    rows = own.shape[0]
    squares = jnp.zeros((rows, 1), F32)

    def put(slot, piece):
        offset = pl.multiple_of(block_ref[slot] * piece_width, piece_width)
        gathered[:, pl.ds(offset, piece_width)] = piece
        wide = piece.astype(F32)
        return jnp.sum(wide * wide, axis=1, keepdims=True)

    for slot, ref in enumerate((own, sw, r1, sr1, l1, sl1)):
        squares = squares + put(slot, ref[...])
    squares = squares + put(6, jnp.where(first, fa[...], fb[...]))
    squares = squares + put(7, jnp.where(first, sfa[...], sfb[...]))
    inv_rms = lax.rsqrt(squares / width_all + TINY_NORM)
    features = gathered[...]

    def pair(n):
        both = dot(features, weights[:, n * 256 : (n + 1) * 256]) * inv_rms
        return both[:, :128], both[:, 128:]

    def unit_rows(raw):
        wide = low(raw).astype(F32)
        return wide * lax.rsqrt(jnp.sum(wide * wide, axis=-1, keepdims=True) + TINY_NORM)

    q, k = pair(0)
    q_ref[...] = low(unit_rows(q) * head_size ** (-0.5))
    k_ref[...] = low(unit_rows(k))
    v, dg = pair(1)
    v_ref[...] = low(v)
    dg_ref[...] = low(dg)
    gv, gg = pair(2)
    gu_ref[...] = low(low(gv).astype(F32) * jax.nn.sigmoid(low(gg).astype(F32)))
    cg, bl = pair(3)
    cg_ref[...] = low(cg)
    lane = lax.broadcasted_iota(jnp.int32, bl.shape, 1)
    bl_ref[...] = jnp.where(lane == 0, jax.nn.sigmoid(bl), -rate_ref[0] * jax.nn.softplus(bl))


def project(pieces, weights, blocks, rate, width_all, head_size):
    rows = pieces[0].shape[0]
    half = rows // 2
    piece_width = pieces[0].shape[1]
    full = pl.BlockSpec((half, piece_width), lambda i: (i, 0))
    fixed = pl.BlockSpec((half, piece_width), lambda i: (0, 0))
    out = pl.BlockSpec((half, 128), lambda i: (i, 0))
    kinds = [BF16] * 6 + [F32]
    return pl.pallas_call(
        functools.partial(project_kernel, width_all, head_size),
        grid=(2,),
        in_specs=[scalars(), scalars()]
        + [full] * 6
        + [fixed] * 4
        + [pl.BlockSpec(weights.shape, lambda i: (0, 0))],
        out_specs=[out] * 7,
        out_shape=[jax.ShapeDtypeStruct((rows, 128), kind) for kind in kinds],
        scratch_shapes=[pltpu.VMEM((half, width_all), BF16)],
        compiler_params=params(28),
        cost_estimate=cost(2 * rows * width_all * 1024, 12 << 20),
        name="project",
    )(blocks, rate, *pieces, weights)


def write_state(ref, state):
    total, lost, made = state
    size = lost.shape[0]
    ref[0:size, 0:size] = low(lost)
    ref[0:size, size:] = low(made)
    row = lax.broadcasted_iota(jnp.int32, (16, 2 * size), 0)
    high, middle, rest = split_three(jnp.broadcast_to(total, (16, 2 * size)))
    packed = jnp.where(
        row == 0,
        high.astype(F32),
        jnp.where(row == 1, middle.astype(F32), rest.astype(F32)),
    )
    ref[size : size + 16, :] = low(packed)


def read_state(ref):
    size = ref.shape[1] // 2
    packed = ref[size : size + 16, 0:128].astype(F32)
    total = packed[0:1, 0:1] + packed[1:2, 0:1] + packed[2:3, 0:1]
    return (total, ref[0:size, 0:size].astype(F32), ref[0:size, size:].astype(F32))


def compose(later, earlier):
    total2, lost2, made2 = later
    total1, lost1, made1 = earlier
    size = lost1.shape[0]
    both = dot(low(lost2), low(jnp.concatenate([lost1, made1], axis=1)))
    lost = total2 * lost1 + total1 * lost2 - both[:, :size]
    made = total2 * made1 - both[:, size:] + made2
    return (total1 * total2, lost, made)


def delta_kernel(q_ref, k_ref, v_ref, bl_ref, coef_p_ref, coef_q_ref, state_ref):
    rows, size = q_ref.shape
    chunks = rows // CHUNK
    row = lax.broadcasted_iota(jnp.int32, (CHUNK, CHUNK), 0)
    column = lax.broadcasted_iota(jnp.int32, (CHUNK, CHUNK), 1)
    causal = row >= column
    strict = row > column
    ones = jnp.where(causal, 1.0, 0.0).astype(BF16)
    lowers, inverses, scores, grown, tails = [], [], [], [], []
    betas = []
    for n in range(chunks):
        here = slice(n * CHUNK, (n + 1) * CHUNK)
        both = bl_ref[here, :]
        beta = both[:, 0:1]
        high, middle, rest = split_three(both)
        sums = dot(ones, high) + (dot(ones, middle) + dot(ones, rest))
        log_sum = jnp.broadcast_to(sums[:, 1:2], (CHUNK, CHUNK))
        damping = jnp.where(causal, jnp.exp(jnp.minimum(log_sum - log_sum.T, 0.0)), 0.0)
        k = k_ref[here, :]
        lower = jnp.where(strict, dot_nt(k, k) * damping, 0.0) * beta
        scores.append(low(dot_nt(q_ref[here, :], k) * damping))
        lowers.append(lower)
        betas.append(beta)
        grown.append(log_sum)
        tails.append(log_sum[CHUNK - 1 : CHUNK, :])
        below = ((row & 1) == 1) & (column == row - 1)
        inverses.append(jnp.where(row == column, 1.0, 0.0) - jnp.where(below, lower, 0.0))
    level = 2
    while level < CHUNK:
        shift = level.bit_length() - 1
        part = row >> shift
        below = ((part & 1) == 1) & ((column >> shift) == part - 1)
        multiply = dot_fine if level >= 16 else (lambda a, b: dot(low(a), low(b)))
        moved = [
            multiply(inverse, jnp.where(below, lower, 0.0))
            for inverse, lower in zip(inverses, lowers)
        ]
        inverses = [
            inverse - multiply(middle, inverse) for inverse, middle in zip(inverses, moved)
        ]
        level *= 2
    queries, starts, losts, mades = [], [], [], []
    for n in range(chunks):
        here = slice(n * CHUNK, (n + 1) * CHUNK)
        k = k_ref[here, :].astype(F32)
        grow = jnp.exp(grown[n])
        right = jnp.concatenate(
            [v_ref[here, :].astype(F32) * betas[n], k * (betas[n] * grow)], axis=1
        )
        solved = low(dot(low(inverses[n]), low(right)))
        seen = dot(scores[n], solved)
        starts.append(seen[:, :size])
        queries.append(low(q_ref[here, :].astype(F32) * grow - seen[:, size:]))
        weighted = low(k * jnp.exp(tails[n] - grown[n]))
        written = dot_tn(weighted, solved)
        mades.append(written[:, :size])
        losts.append(low(written[:, size:]))
    carried = jnp.where(row == column, 1.0, 0.0)
    made = jnp.zeros((CHUNK, size), F32)
    log_total = jnp.zeros((1, CHUNK), F32)
    for n in range(chunks):
        here = slice(n * CHUNK, (n + 1) * CHUNK)
        rounded = low(jnp.concatenate([carried, made], axis=1))
        seen = dot(queries[n], rounded)
        coef_p_ref[here, :] = low(seen[:, :size])
        coef_q_ref[here, :] = seen[:, size:] + starts[n]
        moved = dot(losts[n], rounded)
        keep = jnp.exp(tails[n])
        carried = carried * keep - moved[:, :size]
        made = made * keep - moved[:, size:] + mades[n]
        log_total = log_total + tails[n]
    total = jnp.exp(log_total)[:, 0:1]
    lost = jnp.where(row == column, total, 0.0) - carried
    write_state(state_ref, (total, lost, made))


def delta(q, k, v, bl):
    rows, size = q.shape
    return pl.pallas_call(
        delta_kernel,
        in_specs=[whole()] * 4,
        out_specs=[whole()] * 3,
        out_shape=[
            jax.ShapeDtypeStruct((rows, size), BF16),
            jax.ShapeDtypeStruct((rows, size), F32),
            jax.ShapeDtypeStruct((size + 16, 2 * size), BF16),
        ],
        compiler_params=params(16),
        cost_estimate=cost(2 * rows * size * size * 60, 3 << 20),
        name="delta",
    )(q, k, v, bl)


def along_kernel(place_ref, p0, p1, p2, p3, before_ref, total_ref, held):
    me = place_ref[0]
    for j, piece in ((0, p0), (2, p1), (3, p2), (1, p3)):
        held[(me - j + 4) & 3] = piece[...]
    size = p0.shape[1] // 2
    nothing = (jnp.ones((1, 1), F32), jnp.zeros((size, size), F32), jnp.zeros((size, size), F32))
    before = nothing
    so_far = read_state(held.at[0])
    for m in range(1, 4):
        before = tuple(jnp.where(me == m, a, b) for a, b in zip(so_far, before))
        so_far = compose(read_state(held.at[m]), so_far)
    write_state(before_ref, before)
    write_state(total_ref, so_far)


def small_call(kernel, shapes, scratch, *args):
    return pl.pallas_call(
        kernel,
        in_specs=[scalars()] + [whole()] * (len(args) - 1),
        out_specs=[whole()] * len(shapes),
        out_shape=[jax.ShapeDtypeStruct(shape, BF16) for shape in shapes],
        scratch_shapes=scratch,
        compiler_params=params(4),
        cost_estimate=cost(16 << 20, 1 << 18),
    )(*args)


def cyclic(block, axis, distance):
    count = lax.axis_size(axis)
    return lax.ppermute(block, axis, [(i, (i + distance) % count) for i in range(count)])


def shifted(block, axis, distance):
    devices = range(lax.axis_size(axis))
    return lax.ppermute(block, axis, [(i, i + distance) for i in devices if i + distance in devices])


def swapped(block):
    return lax.ppermute(block, "c", [(0, 1), (1, 0)])


def finish_kernel(coef_p_ref, coef_q_ref, dg_ref, gain_ref, reach_ref, far_ref, before_ref, out_ref):
    total, lost, made = read_state(reach_ref)
    far = far_ref[...].astype(F32)
    state = total * far - dot(low(lost), far_ref[...]) + made
    total, lost, made = read_state(before_ref)
    state = low(total * state - dot(low(lost), low(state)) + made)
    result = coef_q_ref[...] + dot(coef_p_ref[...], state)
    mean = jnp.sum(result * result, axis=-1, keepdims=True) * (1.0 / result.shape[1])
    result = result * lax.rsqrt(mean + TINY_NORM) * gain_ref[...]
    out_ref[...] = low(result * jax.nn.silu(dg_ref[...].astype(F32)))


def finish(*args):
    return pl.pallas_call(
        finish_kernel,
        in_specs=[whole()] * len(args),
        out_specs=whole(),
        out_shape=jax.ShapeDtypeStruct(args[2].shape, BF16),
        compiler_params=params(4),
        cost_estimate=cost(64 << 20, 2 << 20),
        name="finish",
    )(*args)


def conv_kernel(gu_ref, before_ref, taps_ref, cg_ref, out_ref, padded):
    rows, size = gu_ref.shape
    head = before_ref.shape[0]
    count = taps_ref.shape[0]
    padded[0:head, :] = before_ref[...].astype(F32)
    padded[head:, :] = gu_ref[...].astype(F32)
    taps = taps_ref[...].astype(F32)
    step = 64
    skip = head - (count - 1)
    for base in range(0, rows, step):
        total = jnp.zeros((step, size), F32)
        for j in range(count):
            total = total + padded[base + skip + j : base + skip + j + step, :] * taps[j : j + 1, :]
        out_ref[base : base + step, 0:size] = low(total)
    out_ref[:, size:] = cg_ref[...]


def conv(gu, before, taps, cg):
    rows, size = gu.shape
    return pl.pallas_call(
        conv_kernel,
        in_specs=[whole()] * 4,
        out_specs=whole(),
        out_shape=jax.ShapeDtypeStruct((rows, 2 * size), BF16),
        scratch_shapes=[pltpu.VMEM((rows + before.shape[0], size), F32)],
        compiler_params=params(4),
        cost_estimate=cost(256 << 20, 1 << 20),
        name="conv",
    )(gu, before, taps, cg)


def order_of(weight_refs):
    return list(enumerate(weight_refs))


def conv_out_kernel(block_ref, got_ref, *refs):
    weight_refs, out_ref, mixed = refs[:8], refs[8], refs[9]
    starts = [128] * 6 + [0] * 2
    groups, rows, size = mixed.shape
    total = jnp.zeros((rows, 1), F32)
    total_square = jnp.zeros((rows, 1), F32)
    for g in range(groups):
        part = got_ref[g, :, 0:size].astype(F32)
        total = total + jnp.sum(part, axis=1, keepdims=True)
        total_square = total_square + jnp.sum(part * part, axis=1, keepdims=True)
    scale = 1.0 / (groups * size)
    center = total * scale
    variance = jnp.maximum(total_square * scale - center * center, 0.0)
    factor = lax.rsqrt(variance + TINY_VAR)
    for slot, ref in order_of(weight_refs):
        g = block_ref[slot]
        top = starts[slot] + size
        extra = ref[top : top + 16, :].astype(F32)
        gain = extra[0:1, 0:size] + extra[1:2, 0:size] + extra[2:3, 0:size]
        shift = extra[3:4, 0:size] + extra[4:5, 0:size] + extra[5:6, 0:size]
        normed = (got_ref[g, :, 0:size].astype(F32) - center) * factor * gain + shift
        gate = got_ref[g, :, size:].astype(F32)
        mixed[slot] = low(jax.nn.silu(normed) * jax.nn.silu(gate))
    width = out_ref.shape[1]
    for base in range(0, width, 512):
        acc = jnp.zeros((rows, 512), F32)
        for slot, ref in order_of(weight_refs):
            top = starts[slot]
            acc = acc + dot(mixed[slot], ref[top : top + size, base : base + 512])
        out_ref[:, base : base + 512] = acc


def delta_out_kernel(block_ref, got_ref, conv_ref, *refs):
    weight_refs, out_ref = refs[:8], refs[8]
    width = out_ref.shape[1]
    for base in range(0, width, 512):
        acc = conv_ref[:, base : base + 512]
        for slot, ref in order_of(weight_refs):
            acc = acc + dot(got_ref[block_ref[slot]], ref[0:128, base : base + 512])
        out_ref[:, base : base + 512] = low(acc)


def out_call(kernel, kind, scratch, blocks, *args):
    rows, width = args[0].shape[1], args[-1].shape[1]
    return pl.pallas_call(
        kernel,
        in_specs=[scalars()] + [whole()] * len(args),
        out_specs=whole(),
        out_shape=jax.ShapeDtypeStruct((rows, width), kind),
        scratch_shapes=scratch,
        compiler_params=params(8),
        cost_estimate=cost(2 * rows * 1024 * width, 6 << 20),
    )(blocks, *args)


def local(
    tokens,
    w_query,
    w_key,
    w_value,
    w_delta_gate,
    w_glu_value,
    w_glu_gate,
    w_conv_gate,
    w_beta,
    w_decay,
    decay_log,
    head_gain,
    conv_taps,
    ln_gain,
    ln_shift,
    out_delta,
    out_conv,
):
    rows = tokens.shape[0]
    half = rows // 2
    size = w_query.shape[1]
    y, core = lax.axis_index("y"), lax.axis_index("c")
    x, z = lax.axis_index("x"), lax.axis_index("z")
    count_y = lax.axis_size("y")
    head = y * 2 + core
    chips = [y, (y - 1) % count_y, (y + 1) % count_y, (y + 2) % count_y]
    blocks = jnp.stack([chip * 2 + side for chip in chips for side in (core, 1 - core)])
    blocks = blocks.astype(jnp.int32)

    beta_decay = jnp.concatenate(
        [
            lax.dynamic_slice_in_dim(w_beta, head, 1, 1),
            lax.dynamic_slice_in_dim(w_decay, head, 1, 1),
            jnp.zeros((w_beta.shape[0], 126), BF16),
        ],
        axis=1,
    )
    weights = jnp.concatenate(
        [
            w_query,
            w_key,
            w_value,
            w_delta_gate,
            w_glu_value,
            w_glu_gate,
            w_conv_gate,
            beta_decay,
        ],
        axis=1,
    )
    rate = jnp.exp(lax.dynamic_slice_in_dim(decay_log, head, 1, 0))

    def three(vector):
        high = lax.reduce_precision(vector, 8, 7)
        rest = vector - high
        middle = lax.reduce_precision(rest, 8, 7)
        return [high, middle, rest - middle]

    extra = jnp.stack(three(ln_gain) + three(ln_shift)).astype(BF16)
    extra = jnp.pad(extra, ((0, 10), (0, out_conv.shape[1] - extra.shape[1])))
    last = jnp.concatenate([out_delta, out_conv, extra], axis=0)

    own = tokens
    r1, l1 = cyclic(own, "y", 1), cyclic(own, "y", -1)
    sw = swapped(own)
    r1, l1, weights, last = lax.optimization_barrier((r1, l1, weights, last))
    fa, fb = cyclic(r1[:half], "y", 1), cyclic(l1[half:], "y", -1)
    sr1, sl1 = swapped(r1), swapped(l1)
    sfa, sfb = swapped(fa), swapped(fb)
    pieces = [own, sw, r1, sr1, l1, sl1, fa, sfa, fb, sfb]
    wr, wl = cyclic(last, "y", 1), cyclic(last, "y", -1)
    q, k, v, dg, gu, cg, bl = project(pieces, weights, blocks, rate, 2048, size)

    coef_p, coef_q, state = delta(q, k, v, bl)

    gu, last, state = lax.optimization_barrier((gu, last, state))

    kind = state.shape

    def among_four(place, state, others):
        return small_call(
            along_kernel,
            [kind, kind],
            [pltpu.VMEM((4,) + kind, BF16)],
            place[None].astype(jnp.int32),
            state,
            *others,
        )

    before, total = among_four(x, state, [cyclic(state, "x", j) for j in (2, 3, 1)])
    route = lambda j: [(h + i, h + (i + j) % 4) for h in (0, 4) for i in range(4)]
    around = []
    for j in (2, 3, 1):
        around.append(lax.ppermute(total, "z", route(j)))
    before_z, total_z = among_four(z % 4, total, around)
    far = shifted(total_z[:size, size:], "z", 4)

    ws = swapped(last)
    wfa, wfb = cyclic(wr[:size], "y", 1), cyclic(wl[size:], "y", -1)
    wsr, wsl = swapped(wr), swapped(wl)
    wsfa, wsfb = swapped(wfa), swapped(wfb)
    near = [last, ws, wr, wsr, wl, wsl]
    delta_weights = near + [wfa, wsfa]
    conv_weights = near + [wfb, wsfb]

    halo = lax.ppermute(gu[rows - 32 :], SP, [(i, i + 1) for i in range(31)])
    filtered = conv(gu, halo, conv_taps, cg)
    groups = 8
    got = lax.all_to_all(filtered.reshape(groups, rows // groups, 2 * size), TP, 0, 0, tiled=True)
    conv_part = out_call(
        conv_out_kernel,
        F32,
        [pltpu.VMEM((groups, rows // groups, size), BF16)],
        blocks,
        got,
        *conv_weights,
    )

    mixed = finish(coef_p, coef_q, dg, head_gain[None, :], before_z, far, before)
    mixed = lax.all_to_all(mixed.reshape(groups, rows // groups, size), TP, 0, 0, tiled=True)
    return out_call(delta_out_kernel, BF16, [], blocks, mixed, conv_part, *delta_weights)


def solution(mesh):
    finer = Mesh(mesh.devices.reshape(8, 4, 4, 2), ("z", "x", "y", "c"))
    placed = (
        P(SP, TP),
        P(None, TP),
        P(None, TP),
        P(None, TP),
        P(None, TP),
        P(None, TP),
        P(None, TP),
        P(None, TP),
        P(),
        P(),
        P(),
        P(),
        P(None, TP),
        P(TP),
        P(TP),
        P(TP, None),
        P(TP, None),
    )
    return jax.shard_map(
        local, mesh=finer, in_specs=placed, out_specs=P(SP + TP, None), check_vma=False
    )
```

profile of v0, /device:TPU:1, one launch (start us, length us, event | category | flops | bytes accessed | tf_op | source)
XLA Modules:
  0.0 136.4 jit_solution(2423582023911647874)
XLA Ops:
  0.0 2.2 %collective-permute-start.1 = (bf16[1024,256]{1,0:T(8,128)(2,1)}, bf16[1024,256]{1,0:T(8,128)(2,1)}, u32[]{:S(2)}, u32[]{:S(2)}) collective-permute-start(bf16[1024,256]{1,0:T(8,128)(2,1)} %refs_0_.1), channel_id=1, source_target_pairs={{0,2},{2,4},{4,6},{6,0},{1,3},{3,5},{5,7},{7,1},{8,10},{10,12},{12... | collective-permute-start | bytes 1572872 | tf_op jit(solution)/shard_map/ppermute | solution.py:293
  2.2 1.5 %collective-permute-start.2 = (bf16[1024,256]{1,0:T(8,128)(2,1)}, bf16[1024,256]{1,0:T(8,128)(2,1)}, u32[]{:S(2)}, u32[]{:S(2)}) collective-permute-start(bf16[1024,256]{1,0:T(8,128)(2,1)} %refs_0_.1), channel_id=1, source_target_pairs={{0,6},{2,0},{4,2},{6,4},{1,7},{3,1},{5,3},{7,5},{8,14},{10,8},{12,... | collective-permute-start | bytes 1572872 | tf_op jit(solution)/shard_map/ppermute | solution.py:293
  3.7 2.8 %collective-permute-start = (bf16[1024,256]{1,0:T(8,128)(2,1)}, bf16[1024,256]{1,0:T(8,128)(2,1)S(1)}, u32[]{:S(2)}, u32[]{:S(2)}) collective-permute-start(bf16[1024,256]{1,0:T(8,128)(2,1)} %refs_0_.1), channel_id=1, source_target_pairs={{0,1},{1,0},{2,3},{3,2},{4,5},{5,4},{6,7},{7,6},{8,9},{9,8},{10,11... | collective-permute-start | bytes 1572872 | tf_op jit(solution)/shard_map/ppermute | solution.py:302
  8.1 7.7 %concatenate.6.refs_10_ = bf16[2048,1024]{1,0:T(8,128)(2,1)} concatenate(bf16[2048,128]{1,0:T(8,128)(2,1)S(1)} %copy-done.34, bf16[2048,128]{1,0:T(8,128)(2,1)S(1)} %copy-done.35, bf16[2048,128]{1,0:T(8,128)(2,1)} %param.20, bf16[2048,128]{1,0:T(8,128)(2,1)} %param.21, bf16[2048,128]{1,0:T(8,128)(2,1)} %param.22, bf16[2048,128]{1,0:T(8,128)(2,1)} %param.23, ...), dimensions={1} | concatenate | bytes 8388608 | tf_op jit(solution)/shard_map/concatenate | solution.py:457
  15.8 1.3 fusion.1.refs_0_
  19.2 2.7 %collective-permute-start.7 = (bf16[512,256]{1,0:T(8,128)(2,1)S(1)}, bf16[512,256]{1,0:T(8,128)(2,1)}, u32[]{:S(2)}, u32[]{:S(2)}) collective-permute-start(bf16[512,256]{1,0:T(8,128)(2,1)S(1)} %slice.19), channel_id=1, source_target_pairs={{0,6},{2,0},{4,2},{6,4},{1,7},{3,1},{5,3},{7,5},{8,14},{10,8},{12,... | collective-permute-start | bytes 786440 | tf_op jit(solution)/shard_map/ppermute | solution.py:293
  21.9 5.3 %collective-permute-done.5.refs_6_ = bf16[512,256]{1,0:T(8,128)(2,1)S(1)} collective-permute-done((bf16[512,256]{1,0:T(8,128)(2,1)S(1)}, bf16[512,256]{1,0:T(8,128)(2,1)S(1)}, u32[]{:S(2)}, u32[]{:S(2)}) %collective-permute-start.5) | collective-permute-done | bytes 262176 | tf_op jit(solution)/shard_map/ppermute | solution.py:293
  30.1 1.5 %collective-permute-start.18 = (bf16[272,2048]{1,0:T(8,128)(2,1)S(1)}, bf16[272,2048]{1,0:T(8,128)(2,1)S(1)}, u32[]{:S(2)}, u32[]{:S(2)}) collective-permute-start(bf16[272,2048]{1,0:T(8,128)(2,1)S(1)} %fusion.1.refs_0_), channel_id=1, source_target_pairs={{0,2},{2,4},{4,6},{6,0},{1,3},{3,5},{5,7},{7,1},{8,10},{10,12},{12... | collective-permute-start | bytes 3342344 | tf_op jit(solution)/shard_map/ppermute | solution.py:293
  34.4 2.2 %copy-done.2 = bf16[2048,1024]{1,0:T(8,128)(2,1)S(1)} copy-done((bf16[2048,1024]{1,0:T(8,128)(2,1)S(1)}, bf16[2048,1024]{1,0:T(8,128)(2,1)}, u32[]{:S(2)}) %copy-start.2) | copy-done | bytes 4194328
  36.6 1.0 copy-done.27
  37.7 1.0 copy-done.29
  40.6 7.2 %project.1 = (bf16[1024,128]{1,0:T(8,128)(2,1)S(1)}, bf16[1024,128]{1,0:T(8,128)(2,1)S(1)}, bf16[1024,128]{1,0:T(8,128)(2,1)S(1)}, bf16[1024,128]{1,0:T(8,128)(2...) custom-call(s32[8]{0:T(128)S(1)} %stack.63.block_ref, ...), custom_call_target="tpu_custom_call" | custom-call | flops 4294967296 | bytes 12582912 | tf_op jit(solution)/shard_map/project/pallas_call | solution.py:123
  47.8 5.6 %delta.1 = (bf16[1024,128]{1,0:T(8,128)(2,1)S(1)}, f32[1024,128]{1,0:T(8,128)S(1)}, bf16[144,256]{1,0:T(8,128)(2,1)S(1)}) custom-call(bf16[1024,128]{1,0:T(8,128)(2,1)S(1)} %get-tuple-element.29.q_ref, bf16[1024,128]{1,0:T(8,128)(2,1)S(1)} %get-tuple-element.30.k_ref, bf16[1024,128]{1,0:T(8,128)(2,1)S(1)} %get-tuple-element.31.v_ref, ...), custom_call_target="tpu_custom_call" | custom-call | flops 2013265920 | bytes 3145728 | tf_op jit(solution)/shard_map/delta/pallas_call | solution.py:249
  58.8 1.5 %collective-permute-done.11.p3 = bf16[144,256]{1,0:T(8,128)(2,1)} collective-permute-done((bf16[144,256]{1,0:T(8,128)(2,1)S(1)}, bf16[144,256]{1,0:T(8,128)(2,1)}, u32[]{:S(2)}, u32[]{:S(2)}) %collective-permute-start.11) | collective-permute-done | bytes 73760 | tf_op jit(solution)/shard_map/ppermute | solution.py:293
  60.3 1.0 collective-permute-done.9.p1
  62.2 1.4 %shard_map.163 = (bf16[144,256]{1,0:T(8,128)(2,1)S(1)}, bf16[144,256]{1,0:T(8,128)(2,1)S(1)}) custom-call(s32[1]{0:T(128)} %bitcast.16.place_ref, bf16[144,256]{1,0:T(8,128)(2,1)S(1)} %get-tuple-element.39.p0, bf16[144,256]{1,0:T(8,128)(2,1)} %collective-permute-done.9.p1, bf16[144,256]{1,0:T(8,128)(2,1)S(1)} %copy-done.20, ...), custom_call_target="tpu_custom_call" | custom-call | flops 16777216 | bytes 262144 | tf_op jit(solution)/shard_map/pallas_call | solution.py:280
  64.3 3.3 %collective-permute-start.12 = (bf16[144,256]{1,0:T(8,128)(2,1)S(1)}, bf16[144,256]{1,0:T(8,128)(2,1)S(1)}, u32[]{:S(2)}, u32[]{:S(2)}) collective-permute-start(bf16[144,256]{1,0:T(8,128)(2,1)S(1)} %get-tuple-element.40.p0), channel_id=1, source_target_pairs={{0,64},{32,96},{64,0},{96,32},{128,192},{160,224},{192,128},{224,1... | collective-permute-start | bytes 221192 | tf_op jit(solution)/shard_map/ppermute | solution.py:513
  67.6 1.4 collective-permute-start.13
  69.9 2.5 %collective-permute-start.22 = (bf16[144,2048]{1,0:T(8,128)(2,1)}, bf16[144,2048]{1,0:T(8,128)(2,1)}, u32[]{:S(2)}, u32[]{:S(2)}) collective-permute-start(bf16[144,2048]{1,0:T(8,128)(2,1)} %slice.24), channel_id=1, source_target_pairs={{0,6},{2,0},{4,2},{6,4},{1,7},{3,1},{5,3},{7,5},{8,14},{10,8},{12,... | collective-permute-start | bytes 1769480 | tf_op jit(solution)/shard_map/ppermute | solution.py:293
  72.4 2.2 %collective-permute-start.17 = (bf16[272,2048]{1,0:T(8,128)(2,1)S(1)}, bf16[272,2048]{1,0:T(8,128)(2,1)}, u32[]{:S(2)}, u32[]{:S(2)}) collective-permute-start(bf16[272,2048]{1,0:T(8,128)(2,1)S(1)} %fusion.1.refs_0_), channel_id=1, source_target_pairs={{0,1},{1,0},{2,3},{3,2},{4,5},{5,4},{6,7},{7,6},{8,9},{9,8},{10,11... | collective-permute-start | bytes 3342344 | tf_op jit(solution)/shard_map/ppermute | solution.py:302
  76.8 4.2 %collective-permute-done.14.p3 = bf16[144,256]{1,0:T(8,128)(2,1)S(1)} collective-permute-done((bf16[144,256]{1,0:T(8,128)(2,1)S(1)}, bf16[144,256]{1,0:T(8,128)(2,1)S(1)}, u32[]{:S(2)}, u32[]{:S(2)}) %collective-permute-start.14) | collective-permute-done | bytes 73760 | tf_op jit(solution)/shard_map/ppermute | solution.py:513
  81.7 1.4 %collective-permute-start.16 = (bf16[32,128]{1,0:T(8,128)(2,1)S(1)}, bf16[32,128]{1,0:T(8,128)(2,1)S(1)}, u32[]{:S(2)}, u32[]{:S(2)}) collective-permute-start(bf16[32,128]{1,0:T(8,128)(2,1)S(1)} %slice.21), channel_id=1, source_target_pairs={{0,8},{8,16},{16,24},{24,32},{32,40},{40,48},{48,56},{56,64},{64,7... | collective-permute-start | bytes 24584 | tf_op jit(solution)/shard_map/ppermute | solution.py:525
  86.1 10.8 %collective-permute-start.15 = (bf16[128,128]{1,0:T(8,128)(2,1)S(1)}, bf16[128,128]{1,0:T(8,128)(2,1)S(1)}, u32[]{:S(2)}, u32[]{:S(2)}) collective-permute-start(bf16[128,128]{1,0:T(8,128)(2,1)S(1)} %slice.20), channel_id=1, source_target_pairs={{0,128},{32,160},{64,192},{96,224},{1,129},{33,161},{65,193},{97,2... | collective-permute-start | bytes 98312 | tf_op jit(solution)/shard_map/ppermute | solution.py:298
  98.0 1.1 conv.1
  99.9 7.7 %all-to-all-start.1 = ((bf16[8,128,256]{2,1,0:T(8,128)(2,1)}), bf16[8,128,256]{2,1,0:T(8,128)(2,1)}, u32[]{:S(2)}, u32[]{:S(2)}) async-start(bf16[8,128,256]{2,1,0:T(8,128)(2,1)} %bitcast.25), calls=%async_computation.1 | async-start | bytes 1048576 | tf_op jit(solution)/shard_map/all_to_all | solution.py:528
  107.7 2.1 %collective-permute-done.24.refs_6_ = bf16[128,2048]{1,0:T(8,128)(2,1)} collective-permute-done((bf16[128,2048]{1,0:T(8,128)(2,1)}, bf16[128,2048]{1,0:T(8,128)(2,1)}, u32[]{:S(2)}, u32[]{:S(2)}) %collective-permute-start.24) | collective-permute-done | bytes 524320 | tf_op jit(solution)/shard_map/ppermute | solution.py:293
  109.8 6.1 %collective-permute-start.25 = (bf16[128,2048]{1,0:T(8,128)(2,1)}, bf16[128,2048]{1,0:T(8,128)(2,1)}, u32[]{:S(2)}, u32[]{:S(2)}) collective-permute-start(bf16[128,2048]{1,0:T(8,128)(2,1)} %collective-permute-done.24.refs_6_), channel_id=1, source_target_pairs={{0,1},{1,0},{2,3},{3,2},{4,5},{5,4},{6,7},{7,6},{8,9},{9,8},{10,11... | collective-permute-start | bytes 1572872 | tf_op jit(solution)/shard_map/ppermute | solution.py:302
  120.3 4.0 %all-to-all-start = ((bf16[8,128,128]{2,1,0:T(8,128)(2,1)}), bf16[8,128,128]{2,1,0:T(8,128)(2,1)}, u32[]{:S(2)}, u32[]{:S(2)}) async-start(bf16[8,128,128]{2,1,0:T(8,128)(2,1)} %bitcast.26), calls=%async_computation | async-start | bytes 524288 | tf_op jit(solution)/shard_map/all_to_all | solution.py:539
  124.3 4.0 %shard_map.165.conv_ref = f32[128,2048]{1,0:T(8,128)S(1)} custom-call(s32[8]{0:T(128)S(1)} %stack.63.block_ref, bf16[8,128,256]{2,1,0:T(8,128)(2,1)} %all-to-all-done.1.got_ref, bf16[272,2048]{1,0:T(8,128)(2,1)S(1)} %fusion.1.refs_0_, bf16[272,2048]{1,0:T(8,128)(2,1)} %collective-permute-done.17.refs_1_, ...), custom_call_target="tpu_custom_call" | custom-call | flops 536870912 | bytes 6291456 | tf_op jit(solution)/shard_map/pallas_call | solution.py:408
  129.4 1.5 %all-to-all-done.got_ref = bf16[8,128,128]{2,1,0:T(8,128)(2,1)} async-done(((bf16[8,128,128]{2,1,0:T(8,128)(2,1)}), bf16[8,128,128]{2,1,0:T(8,128)(2,1)}, u32[]{:S(2)}, u32[]{:S(2)}) %all-to-all-start) | async-done | bytes 262176 | tf_op jit(solution)/shard_map/all_to_all | solution.py:539
  130.8 1.2 copy-done.1
  132.1 4.3 %shard_map.166 = bf16[128,2048]{1,0:T(8,128)(2,1)} custom-call(s32[8]{0:T(128)S(1)} %stack.63.block_ref, bf16[8,128,128]{2,1,0:T(8,128)(2,1)} %all-to-all-done.got_ref, f32[128,2048]{1,0:T(8,128)S(1)} %copy-done.1, bf16[272,2048]{1,0:T(8,128)(2,1)S(1)} %fusion.1.refs_0_, bf16[272,2048]{1,0:T(8,128)(2,1)} %collective-permute-done.17.refs_1_, ...), custom_call_target="tpu_custom_call" | custom-call | flops 536870912 | bytes 6291456 | tf_op jit(solution)/shard_map/pallas_call | solution.py:408
  (126 shorter events, 31.3 us)
Async XLA Ops:
  0.0 17.1 %collective-permute-start.1 = (bf16[1024,256]{1,0:T(8,128)(2,1)}, bf16[1024,256]{1,0:T(8,128)(2,1)}, u32[]{:S(2)}, u32[]{:S(2)}) collective-permute-start(bf16[1024,256]{1,0:T(8,128)(2,1)} %refs_0_.1), channel_id=1, source_target_pairs={{0,2},{2,4},{4,6},{6,0},{1,3},{3,5},{5,7},{7,1},{8,10},{10,12},{12... | collective-permute-start | bytes 1572872 | tf_op jit(solution)/shard_map/ppermute | solution.py:293
  2.2 14.9 %collective-permute-start.2 = (bf16[1024,256]{1,0:T(8,128)(2,1)}, bf16[1024,256]{1,0:T(8,128)(2,1)}, u32[]{:S(2)}, u32[]{:S(2)}) collective-permute-start(bf16[1024,256]{1,0:T(8,128)(2,1)} %refs_0_.1), channel_id=1, source_target_pairs={{0,6},{2,0},{4,2},{6,4},{1,7},{3,1},{5,3},{7,5},{8,14},{10,8},{12,... | collective-permute-start | bytes 1572872 | tf_op jit(solution)/shard_map/ppermute | solution.py:293
  3.7 25.6 %collective-permute-start = (bf16[1024,256]{1,0:T(8,128)(2,1)}, bf16[1024,256]{1,0:T(8,128)(2,1)S(1)}, u32[]{:S(2)}, u32[]{:S(2)}) collective-permute-start(bf16[1024,256]{1,0:T(8,128)(2,1)} %refs_0_.1), channel_id=1, source_target_pairs={{0,1},{1,0},{2,3},{3,2},{4,5},{5,4},{6,7},{7,6},{8,9},{9,8},{10,11... | collective-permute-start | bytes 1572872 | tf_op jit(solution)/shard_map/ppermute | solution.py:302
  18.1 9.1 %collective-permute-start.5 = (bf16[512,256]{1,0:T(8,128)(2,1)S(1)}, bf16[512,256]{1,0:T(8,128)(2,1)S(1)}, u32[]{:S(2)}, u32[]{:S(2)}) collective-permute-start(bf16[512,256]{1,0:T(8,128)(2,1)S(1)} %slice.18), channel_id=1, source_target_pairs={{0,2},{2,4},{4,6},{6,0},{1,3},{3,5},{5,7},{7,1},{8,10},{10,12},{12... | collective-permute-start | bytes 786440 | tf_op jit(solution)/shard_map/ppermute | solution.py:293
  19.2 11.0 %collective-permute-start.7 = (bf16[512,256]{1,0:T(8,128)(2,1)S(1)}, bf16[512,256]{1,0:T(8,128)(2,1)}, u32[]{:S(2)}, u32[]{:S(2)}) collective-permute-start(bf16[512,256]{1,0:T(8,128)(2,1)S(1)} %slice.19), channel_id=1, source_target_pairs={{0,6},{2,0},{4,2},{6,4},{1,7},{3,1},{5,3},{7,5},{8,14},{10,8},{12,... | collective-permute-start | bytes 786440 | tf_op jit(solution)/shard_map/ppermute | solution.py:293
  27.3 4.3 %collective-permute-start.6 = (bf16[512,256]{1,0:T(8,128)(2,1)S(1)}, bf16[512,256]{1,0:T(8,128)(2,1)S(1)}, u32[]{:S(2)}, u32[]{:S(2)}) collective-permute-start(bf16[512,256]{1,0:T(8,128)(2,1)S(1)} %collective-permute-done.5.refs_6_), channel_id=1, source_target_pairs={{0,1},{1,0},{2,3},{3,2},{4,5},{5,4},{6,7},{7,6},{8,9},{9,8},{10,11... | collective-permute-start | bytes 786440 | tf_op jit(solution)/shard_map/ppermute | solution.py:302
  28.8 5.6 %collective-permute-start.3 = (bf16[1024,256]{1,0:T(8,128)(2,1)}, bf16[1024,256]{1,0:T(8,128)(2,1)}, u32[]{:S(2)}, u32[]{:S(2)}) collective-permute-start(bf16[1024,256]{1,0:T(8,128)(2,1)} %collective-permute-done.1.refs_2_), channel_id=1, source_target_pairs={{0,1},{1,0},{2,3},{3,2},{4,5},{5,4},{6,7},{7,6},{8,9},{9,8},{10,11... | collective-permute-start | bytes 1572872 | tf_op jit(solution)/shard_map/ppermute | solution.py:302
  28.8 5.6 %collective-permute-start.4 = (bf16[1024,256]{1,0:T(8,128)(2,1)}, bf16[1024,256]{1,0:T(8,128)(2,1)}, u32[]{:S(2)}, u32[]{:S(2)}) collective-permute-start(bf16[1024,256]{1,0:T(8,128)(2,1)} %collective-permute-done.2.refs_4_), channel_id=1, source_target_pairs={{0,1},{1,0},{2,3},{3,2},{4,5},{5,4},{6,7},{7,6},{8,9},{9,8},{10,11... | collective-permute-start | bytes 1572872 | tf_op jit(solution)/shard_map/ppermute | solution.py:302
  30.1 38.8 %collective-permute-start.20 = (bf16[272,2048]{1,0:T(8,128)(2,1)S(1)}, bf16[272,2048]{1,0:T(8,128)(2,1)S(1)}, u32[]{:S(2)}, u32[]{:S(2)}) collective-permute-start(bf16[272,2048]{1,0:T(8,128)(2,1)S(1)} %fusion.1.refs_0_), channel_id=1, source_target_pairs={{0,6},{2,0},{4,2},{6,4},{1,7},{3,1},{5,3},{7,5},{8,14},{10,8},{12,... | collective-permute-start | bytes 3342344 | tf_op jit(solution)/shard_map/ppermute | solution.py:293
  30.1 44.5 %collective-permute-start.18 = (bf16[272,2048]{1,0:T(8,128)(2,1)S(1)}, bf16[272,2048]{1,0:T(8,128)(2,1)S(1)}, u32[]{:S(2)}, u32[]{:S(2)}) collective-permute-start(bf16[272,2048]{1,0:T(8,128)(2,1)S(1)} %fusion.1.refs_0_), channel_id=1, source_target_pairs={{0,2},{2,4},{4,6},{6,0},{1,3},{3,5},{5,7},{7,1},{8,10},{10,12},{12... | collective-permute-start | bytes 3342344 | tf_op jit(solution)/shard_map/ppermute | solution.py:293
  32.4 2.1 %collective-permute-start.8 = (bf16[512,256]{1,0:T(8,128)(2,1)}, bf16[512,256]{1,0:T(8,128)(2,1)}, u32[]{:S(2)}, u32[]{:S(2)}) collective-permute-start(bf16[512,256]{1,0:T(8,128)(2,1)} %collective-permute-done.7.refs_8_), channel_id=1, source_target_pairs={{0,1},{1,0},{2,3},{3,2},{4,5},{5,4},{6,7},{7,6},{8,9},{9,8},{10,11... | collective-permute-start | bytes 786440 | tf_op jit(solution)/shard_map/ppermute | solution.py:302
  55.0 3.2 %collective-permute-start.10 = (bf16[144,256]{1,0:T(8,128)(2,1)S(1)}, bf16[144,256]{1,0:T(8,128)(2,1)S(1)}, u32[]{:S(2)}, u32[]{:S(2)}) collective-permute-start(bf16[144,256]{1,0:T(8,128)(2,1)S(1)} %get-tuple-element.39.p0), channel_id=1, source_target_pairs={{0,24},{8,0},{16,8},{24,16},{1,25},{9,1},{17,9},{25,17},{2,26},{10... | collective-permute-start | bytes 221192 | tf_op jit(solution)/shard_map/ppermute | solution.py:293
  55.8 4.5 %collective-permute-start.11 = (bf16[144,256]{1,0:T(8,128)(2,1)S(1)}, bf16[144,256]{1,0:T(8,128)(2,1)}, u32[]{:S(2)}, u32[]{:S(2)}) collective-permute-start(bf16[144,256]{1,0:T(8,128)(2,1)S(1)} %get-tuple-element.39.p0), channel_id=1, source_target_pairs={{0,8},{8,16},{16,24},{24,0},{1,9},{9,17},{17,25},{25,1},{2,10},{10... | collective-permute-start | bytes 221192 | tf_op jit(solution)/shard_map/ppermute | solution.py:293
  56.5 4.9 %collective-permute-start.9 = (bf16[144,256]{1,0:T(8,128)(2,1)S(1)}, bf16[144,256]{1,0:T(8,128)(2,1)}, u32[]{:S(2)}, u32[]{:S(2)}) collective-permute-start(bf16[144,256]{1,0:T(8,128)(2,1)S(1)} %get-tuple-element.39.p0), channel_id=1, source_target_pairs={{0,16},{8,24},{16,0},{24,8},{1,17},{9,25},{17,1},{25,9},{2,18},{10... | collective-permute-start | bytes 221192 | tf_op jit(solution)/shard_map/ppermute | solution.py:293
  64.3 33.7 %copy-start.25 = (bf16[31,128]{1,0:T(8,128)(2,1)S(1)}, bf16[31,128]{1,0:T(8,128)(2,1)}, u32[]{:S(2)}) copy-start(bf16[31,128]{1,0:T(8,128)(2,1)} %taps_ref.1) | copy-start | bytes 23812
  64.3 10.3 %collective-permute-start.12 = (bf16[144,256]{1,0:T(8,128)(2,1)S(1)}, bf16[144,256]{1,0:T(8,128)(2,1)S(1)}, u32[]{:S(2)}, u32[]{:S(2)}) collective-permute-start(bf16[144,256]{1,0:T(8,128)(2,1)S(1)} %get-tuple-element.40.p0), channel_id=1, source_target_pairs={{0,64},{32,96},{64,0},{96,32},{128,192},{160,224},{192,128},{224,1... | collective-permute-start | bytes 221192 | tf_op jit(solution)/shard_map/ppermute | solution.py:513
  67.6 7.5 %collective-permute-start.13 = (bf16[144,256]{1,0:T(8,128)(2,1)S(1)}, bf16[144,256]{1,0:T(8,128)(2,1)S(1)}, u32[]{:S(2)}, u32[]{:S(2)}) collective-permute-start(bf16[144,256]{1,0:T(8,128)(2,1)S(1)} %get-tuple-element.40.p0), channel_id=1, source_target_pairs={{0,96},{32,0},{64,32},{96,64},{128,224},{160,128},{192,160},{224,1... | collective-permute-start | bytes 221192 | tf_op jit(solution)/shard_map/ppermute | solution.py:513
  69.9 37.7 %collective-permute-start.22 = (bf16[144,2048]{1,0:T(8,128)(2,1)}, bf16[144,2048]{1,0:T(8,128)(2,1)}, u32[]{:S(2)}, u32[]{:S(2)}) collective-permute-start(bf16[144,2048]{1,0:T(8,128)(2,1)} %slice.24), channel_id=1, source_target_pairs={{0,6},{2,0},{4,2},{6,4},{1,7},{3,1},{5,3},{7,5},{8,14},{10,8},{12,... | collective-permute-start | bytes 1769480 | tf_op jit(solution)/shard_map/ppermute | solution.py:293
  72.4 51.9 %collective-permute-start.17 = (bf16[272,2048]{1,0:T(8,128)(2,1)S(1)}, bf16[272,2048]{1,0:T(8,128)(2,1)}, u32[]{:S(2)}, u32[]{:S(2)}) collective-permute-start(bf16[272,2048]{1,0:T(8,128)(2,1)S(1)} %fusion.1.refs_0_), channel_id=1, source_target_pairs={{0,1},{1,0},{2,3},{3,2},{4,5},{5,4},{6,7},{7,6},{8,9},{9,8},{10,11... | collective-permute-start | bytes 3342344 | tf_op jit(solution)/shard_map/ppermute | solution.py:302
  74.6 49.7 %collective-permute-start.19 = (bf16[272,2048]{1,0:T(8,128)(2,1)S(1)}, bf16[272,2048]{1,0:T(8,128)(2,1)}, u32[]{:S(2)}, u32[]{:S(2)}) collective-permute-start(bf16[272,2048]{1,0:T(8,128)(2,1)S(1)} %collective-permute-done.18.refs_2_), channel_id=1, source_target_pairs={{0,1},{1,0},{2,3},{3,2},{4,5},{5,4},{6,7},{7,6},{8,9},{9,8},{10,11... | collective-permute-start | bytes 3342344 | tf_op jit(solution)/shard_map/ppermute | solution.py:302
  74.6 49.7 %collective-permute-start.21 = (bf16[272,2048]{1,0:T(8,128)(2,1)S(1)}, bf16[272,2048]{1,0:T(8,128)(2,1)}, u32[]{:S(2)}, u32[]{:S(2)}) collective-permute-start(bf16[272,2048]{1,0:T(8,128)(2,1)S(1)} %collective-permute-done.20.refs_4_), channel_id=1, source_target_pairs={{0,1},{1,0},{2,3},{3,2},{4,5},{5,4},{6,7},{7,6},{8,9},{9,8},{10,11... | collective-permute-start | bytes 3342344 | tf_op jit(solution)/shard_map/ppermute | solution.py:302
  75.8 5.3 %collective-permute-start.14 = (bf16[144,256]{1,0:T(8,128)(2,1)S(1)}, bf16[144,256]{1,0:T(8,128)(2,1)S(1)}, u32[]{:S(2)}, u32[]{:S(2)}) collective-permute-start(bf16[144,256]{1,0:T(8,128)(2,1)S(1)} %get-tuple-element.40.p0), channel_id=1, source_target_pairs={{0,32},{32,64},{64,96},{96,0},{128,160},{160,192},{192,224},{224,1... | collective-permute-start | bytes 221192 | tf_op jit(solution)/shard_map/ppermute | solution.py:513
  81.7 4.4 %collective-permute-start.16 = (bf16[32,128]{1,0:T(8,128)(2,1)S(1)}, bf16[32,128]{1,0:T(8,128)(2,1)S(1)}, u32[]{:S(2)}, u32[]{:S(2)}) collective-permute-start(bf16[32,128]{1,0:T(8,128)(2,1)S(1)} %slice.21), channel_id=1, source_target_pairs={{0,8},{8,16},{16,24},{24,32},{32,40},{40,48},{48,56},{56,64},{64,7... | collective-permute-start | bytes 24584 | tf_op jit(solution)/shard_map/ppermute | solution.py:525
  86.1 11.8 %collective-permute-start.15 = (bf16[128,128]{1,0:T(8,128)(2,1)S(1)}, bf16[128,128]{1,0:T(8,128)(2,1)S(1)}, u32[]{:S(2)}, u32[]{:S(2)}) collective-permute-start(bf16[128,128]{1,0:T(8,128)(2,1)S(1)} %slice.20), channel_id=1, source_target_pairs={{0,128},{32,160},{64,192},{96,224},{1,129},{33,161},{65,193},{97,2... | collective-permute-start | bytes 98312 | tf_op jit(solution)/shard_map/ppermute | solution.py:298
  97.8 18.1 %copy-start.22 = (bf16[144,256]{1,0:T(8,128)(2,1)S(1)}, bf16[144,256]{1,0:T(8,128)(2,1)}, u32[]{:S(2)}) copy-start(bf16[144,256]{1,0:T(8,128)(2,1)} %copy-done.21) | copy-start | bytes 221188
  97.8 18.1 %copy-start.24 = (bf16[144,256]{1,0:T(8,128)(2,1)S(1)}, bf16[144,256]{1,0:T(8,128)(2,1)}, u32[]{:S(2)}) copy-start(bf16[144,256]{1,0:T(8,128)(2,1)} %copy-done.23) | copy-start | bytes 221188
  97.8 18.1 %copy-start.26 = (f32[128]{0:T(128)S(1)}, f32[128]{0:T(128)}, u32[]{:S(2)}) copy-start(f32[128]{0:T(128)} %param.28) | copy-start | bytes 1540
  98.0 11.8 %collective-permute-start.24 = (bf16[128,2048]{1,0:T(8,128)(2,1)}, bf16[128,2048]{1,0:T(8,128)(2,1)}, u32[]{:S(2)}, u32[]{:S(2)}) collective-permute-start(bf16[128,2048]{1,0:T(8,128)(2,1)} %slice.25), channel_id=1, source_target_pairs={{0,2},{2,4},{4,6},{6,0},{1,3},{3,5},{5,7},{7,1},{8,10},{10,12},{12... | collective-permute-start | bytes 1572872 | tf_op jit(solution)/shard_map/ppermute | solution.py:293
  99.9 20.3 %all-to-all-start.1 = ((bf16[8,128,256]{2,1,0:T(8,128)(2,1)}), bf16[8,128,256]{2,1,0:T(8,128)(2,1)}, u32[]{:S(2)}, u32[]{:S(2)}) async-start(bf16[8,128,256]{2,1,0:T(8,128)(2,1)} %bitcast.25), calls=%async_computation.1 | async-start | bytes 1048576 | tf_op jit(solution)/shard_map/all_to_all | solution.py:528
  107.6 16.7 %collective-permute-start.23 = (bf16[144,2048]{1,0:T(8,128)(2,1)}, bf16[144,2048]{1,0:T(8,128)(2,1)}, u32[]{:S(2)}, u32[]{:S(2)}) collective-permute-start(bf16[144,2048]{1,0:T(8,128)(2,1)} %collective-permute-done.22.refs_6_), channel_id=1, source_target_pairs={{0,1},{1,0},{2,3},{3,2},{4,5},{5,4},{6,7},{7,6},{8,9},{9,8},{10,11... | collective-permute-start | bytes 1769480 | tf_op jit(solution)/shard_map/ppermute | solution.py:302
  109.8 21.0 %collective-permute-start.25 = (bf16[128,2048]{1,0:T(8,128)(2,1)}, bf16[128,2048]{1,0:T(8,128)(2,1)}, u32[]{:S(2)}, u32[]{:S(2)}) collective-permute-start(bf16[128,2048]{1,0:T(8,128)(2,1)} %collective-permute-done.24.refs_6_), channel_id=1, source_target_pairs={{0,1},{1,0},{2,3},{3,2},{4,5},{5,4},{6,7},{7,6},{8,9},{9,8},{10,11... | collective-permute-start | bytes 1572872 | tf_op jit(solution)/shard_map/ppermute | solution.py:302
  120.3 10.6 %all-to-all-start = ((bf16[8,128,128]{2,1,0:T(8,128)(2,1)}), bf16[8,128,128]{2,1,0:T(8,128)(2,1)}, u32[]{:S(2)}, u32[]{:S(2)}) async-start(bf16[8,128,128]{2,1,0:T(8,128)(2,1)} %bitcast.26), calls=%async_computation | async-start | bytes 524288 | tf_op jit(solution)/shard_map/all_to_all | solution.py:539
  (35 other events, 118.3 us)
where the time goes:
time: 138 us; the launch traced here: 136 us
  starting transfers between devices  55.7 us (40%)
  local copies, waits for them, and re-layouts  36.7 us (27%)
  Pallas kernels  24.8 us (18%)
  waiting for transfers between devices  16.9 us (12%)
    unnamed x80, local copies, waits for them, and re-layouts  23.1 us
    ppermute x10, starting transfers between devices, swapped(): return lax.ppermute(block, 'c', [(0, 1), (1, 0)])  13.7 us
    ppermute x11, starting transfers between devices, cyclic(): lax.ppermute(block, axis, [(i, (i + distance) % count) for i in range(cou...  13 us
    ppermute x1, starting transfers between devices, shifted(): lax.ppermute(block, axis, [(i, i + distance) for i in devices if i + dist...  10.8 us
    ppermute x11, waiting for transfers between devices, cyclic(): lax.ppermute(block, axis, [(i, (i + distance) % count) for i in range(cou...  10.7 us
    pallas_call x2, Pallas kernels, out_call(): pl.pallas_call(kernel, in_specs=[scalars()] + [whole()] * len(args), out_...  8.35 us
    all_to_all x1, starting transfers between devices, local(): lax.all_to_all(filtered.reshape(groups, rows // groups, 2 * size), TP, 0,...  7.67 us
    concatenate x1, local copies, waits for them, and re-layouts, local(): jnp.concatenate([w_query, w_key, w_value, w_delta_gate, w_glu_value, w_gl...  7.67 us
  transfers between devices with their start and end apart: 28, of which 9 were waited for; matrix products, arithmetic and copies ran while one was open for 11% of the time, Pallas kernels for 15%

commit v1 on v0

--- a/solution.py
+++ b/solution.py
@@ -22,12 +22,31 @@
     return pl.BlockSpec(memory_space=pltpu.VMEM)
 
 
+def hbm():
+    return pl.BlockSpec(memory_space=pltpu.HBM)
+
+
+def anywhere():
+    return pl.BlockSpec(memory_space=pl.ANY)
+
+
+def home(array):
+    return pltpu.with_memory_space_constraint(array, pltpu.HBM)
+
+
+def fetch(sems, *pairs):
+    copies = [pltpu.make_async_copy(a, b, sems.at[n]) for n, (a, b) in enumerate(pairs)]
+    for one in copies:
+        one.start()
+    return copies
+
+
 def scalars():
     return pl.BlockSpec(memory_space=pltpu.SMEM)
 
 
 def params(mib):
-    return pltpu.CompilerParams(vmem_limit_bytes=mib * 1024 * 1024)
+    return pltpu.CompilerParams(vmem_limit_bytes=min(mib * 1024 * 1024, 67043328))
 
 
 def cost(flops, bytes_accessed):
@@ -69,71 +88,101 @@
 
 
 def project_kernel(width_all, head_size, block_ref, rate_ref, *refs):
-    own, sw, r1, sr1, l1, sl1, fa, sfa, fb, sfb, weights = refs[:11]
-    q_ref, k_ref, v_ref, dg_ref, gu_ref, cg_ref, bl_ref = refs[11:18]
-    gathered = refs[18]
-    first = pl.program_id(0) == 0
-    piece_width = own.shape[1]
-    rows = own.shape[0]
-    squares = jnp.zeros((rows, 1), F32)
-
-    def put(slot, piece):
-        offset = pl.multiple_of(block_ref[slot] * piece_width, piece_width)
-        gathered[:, pl.ds(offset, piece_width)] = piece
-        wide = piece.astype(F32)
-        return jnp.sum(wide * wide, axis=1, keepdims=True)
-
-    for slot, ref in enumerate((own, sw, r1, sr1, l1, sl1)):
-        squares = squares + put(slot, ref[...])
-    squares = squares + put(6, jnp.where(first, fa[...], fb[...]))
-    squares = squares + put(7, jnp.where(first, sfa[...], sfb[...]))
-    inv_rms = lax.rsqrt(squares / width_all + TINY_NORM)
-    features = gathered[...]
-
-    def pair(n):
-        both = dot(features, weights[:, n * 256 : (n + 1) * 256]) * inv_rms
-        return both[:, :128], both[:, 128:]
+    own, sw, r1, sr1, l1, sl1, fa, sfa, fb, sfb = refs[:10]
+    sides = refs[10:18]
+    q_ref, k_ref, v_ref, bl_ref, dg_hbm, gu_hbm, cg_hbm = refs[18:25]
+    gathered, weights, dg_ref, gu_ref, cg_ref, sems, out_sems = refs[25:]
+    rows, piece_width = own.shape[0], own.shape[1]
+    half = rows // 2
+    places = [slice(0, half), slice(half, rows)]
+
+    def columns(slot):
+        return pl.ds(pl.multiple_of(block_ref[slot] * piece_width, piece_width), piece_width)
+
+    moves = [[], []]
+    for n, here in enumerate(places):
+        for slot, ref in enumerate((own, sw, r1, sr1, l1, sl1)):
+            moves[n].append((ref.at[here, :], gathered.at[here, columns(slot)]))
+        for slot, ref in enumerate(((fa, sfa), (fb, sfb))[n]):
+            moves[n].append((ref, gathered.at[here, columns(6 + slot)]))
+    parts = [
+        (ref, weights.at[n // 2, :, pl.ds(n % 2 * 128, 128)]) for n, ref in enumerate(sides)
+    ]
+    first = fetch(sems, *moves[0])
+    loads = fetch(sems.at[pl.ds(16, 2)], *parts[:2])
+    second = fetch(sems.at[pl.ds(8, 8)], *moves[1])
+    loads += fetch(sems.at[pl.ds(18, 6)], *parts[2:])
 
     def unit_rows(raw):
         wide = low(raw).astype(F32)
         return wide * lax.rsqrt(jnp.sum(wide * wide, axis=-1, keepdims=True) + TINY_NORM)
 
-    q, k = pair(0)
-    q_ref[...] = low(unit_rows(q) * head_size ** (-0.5))
-    k_ref[...] = low(unit_rows(k))
-    v, dg = pair(1)
-    v_ref[...] = low(v)
-    dg_ref[...] = low(dg)
-    gv, gg = pair(2)
-    gu_ref[...] = low(low(gv).astype(F32) * jax.nn.sigmoid(low(gg).astype(F32)))
-    cg, bl = pair(3)
-    cg_ref[...] = low(cg)
-    lane = lax.broadcasted_iota(jnp.int32, bl.shape, 1)
-    bl_ref[...] = jnp.where(lane == 0, jax.nn.sigmoid(bl), -rate_ref[0] * jax.nn.softplus(bl))
+    def factor_of(n, pieces):
+        for one in pieces:
+            one.wait()
+        wide = gathered[places[n], :].astype(F32)
+        squares = jnp.sum(wide * wide, axis=1, keepdims=True)
+        return lax.rsqrt(squares / width_all + TINY_NORM)
+
+    def pair(n, here, factor):
+        both = dot(gathered[here, :], weights[n]) * factor
+        return both[:, :128], both[:, 128:]
+
+    factors = []
+    for n, here in enumerate(places):
+        factor = factor_of(n, second if n else first[:8])
+        factors.append(factor)
+        if n == 0:
+            loads[0].wait()
+            loads[1].wait()
+        gv, gg = pair(0, here, factor)
+        gu_ref[here, :] = low(low(gv).astype(F32) * jax.nn.sigmoid(low(gg).astype(F32)))
+    stores = fetch(out_sems, (gu_ref, gu_hbm))
+    for one in loads[2 : 4]:
+        one.wait()
+    for here, factor in zip(places, factors):
+        dg, cg = pair(1, here, factor)
+        dg_ref[here, :] = low(dg)
+        cg_ref[here, :] = low(cg)
+    stores += fetch(out_sems.at[pl.ds(1, 2)], (dg_ref, dg_hbm), (cg_ref, cg_hbm))
+    for one in loads[4 : 6]:
+        one.wait()
+    for here, factor in zip(places, factors):
+        q, k = pair(2, here, factor)
+        q_ref[here, :] = low(unit_rows(q) * head_size ** (-0.5))
+        k_ref[here, :] = low(unit_rows(k))
+    for one in loads[6 : 8]:
+        one.wait()
+    for here, factor in zip(places, factors):
+        v, bl = pair(3, here, factor)
+        v_ref[here, :] = low(v)
+        lane = lax.broadcasted_iota(jnp.int32, bl.shape, 1)
+        bl_ref[here, :] = jnp.where(
+            lane == 0, jax.nn.sigmoid(bl), -rate_ref[0] * jax.nn.softplus(bl)
+        )
+    for one in stores:
+        one.wait()
 
 
 def project(pieces, weights, blocks, rate, width_all, head_size):
     rows = pieces[0].shape[0]
-    half = rows // 2
-    piece_width = pieces[0].shape[1]
-    full = pl.BlockSpec((half, piece_width), lambda i: (i, 0))
-    fixed = pl.BlockSpec((half, piece_width), lambda i: (0, 0))
-    out = pl.BlockSpec((half, 128), lambda i: (i, 0))
-    kinds = [BF16] * 6 + [F32]
+    kinds = [BF16] * 3 + [F32] + [BF16] * 3
     return pl.pallas_call(
         functools.partial(project_kernel, width_all, head_size),
-        grid=(2,),
-        in_specs=[scalars(), scalars()]
-        + [full] * 6
-        + [fixed] * 4
-        + [pl.BlockSpec(weights.shape, lambda i: (0, 0))],
-        out_specs=[out] * 7,
-        out_shape=[jax.ShapeDtypeStruct((rows, 128), kind) for kind in kinds],
-        scratch_shapes=[pltpu.VMEM((half, width_all), BF16)],
+        in_specs=[scalars(), scalars()] + [anywhere()] * 18,
+        out_specs=[whole()] * 4 + [hbm()] * 3,
+        out_shape=[pltpu.VMEM((rows, 128), kind) for kind in kinds[:4]]
+        + [pltpu.HBM((rows, 128), kind) for kind in kinds[4:]],
+        scratch_shapes=[
+            pltpu.VMEM((rows, width_all), BF16),
+            pltpu.VMEM((4, width_all, 256), BF16),
+        ]
+        + [pltpu.VMEM((rows, 128), BF16)] * 3
+        + [pltpu.SemaphoreType.DMA((24,)), pltpu.SemaphoreType.DMA((3,))],
         compiler_params=params(28),
         cost_estimate=cost(2 * rows * width_all * 1024, 12 << 20),
         name="project",
-    )(blocks, rate, *pieces, weights)
+    )(blocks, rate, home(pieces[0]), *pieces[1:], *map(home, weights))
 
 
 def write_state(ref, state):
@@ -168,7 +217,9 @@
     return (total1 * total2, lost, made)
 
 
-def delta_kernel(q_ref, k_ref, v_ref, bl_ref, coef_p_ref, coef_q_ref, state_ref):
+def delta_kernel(
+    q_ref, k_ref, v_ref, bl_ref, coef_p_hbm, coef_q_hbm, state_ref, coef_p_ref, coef_q_ref, sems
+):
     rows, size = q_ref.shape
     chunks = rows // CHUNK
     row = lax.broadcasted_iota(jnp.int32, (CHUNK, CHUNK), 0)
@@ -228,12 +279,18 @@
     carried = jnp.where(row == column, 1.0, 0.0)
     made = jnp.zeros((CHUNK, size), F32)
     log_total = jnp.zeros((1, CHUNK), F32)
+    stores = []
     for n in range(chunks):
         here = slice(n * CHUNK, (n + 1) * CHUNK)
         rounded = low(jnp.concatenate([carried, made], axis=1))
         seen = dot(queries[n], rounded)
         coef_p_ref[here, :] = low(seen[:, :size])
         coef_q_ref[here, :] = seen[:, size:] + starts[n]
+        stores += fetch(
+            sems.at[n],
+            (coef_p_ref.at[here, :], coef_p_hbm.at[here, :]),
+            (coef_q_ref.at[here, :], coef_q_hbm.at[here, :]),
+        )
         moved = dot(losts[n], rounded)
         keep = jnp.exp(tails[n])
         carried = carried * keep - moved[:, :size]
@@ -242,6 +299,8 @@
     total = jnp.exp(log_total)[:, 0:1]
     lost = jnp.where(row == column, total, 0.0) - carried
     write_state(state_ref, (total, lost, made))
+    for one in stores:
+        one.wait()
 
 
 def delta(q, k, v, bl):
@@ -249,11 +308,16 @@
     return pl.pallas_call(
         delta_kernel,
         in_specs=[whole()] * 4,
-        out_specs=[whole()] * 3,
+        out_specs=[hbm(), hbm(), whole()],
         out_shape=[
-            jax.ShapeDtypeStruct((rows, size), BF16),
-            jax.ShapeDtypeStruct((rows, size), F32),
-            jax.ShapeDtypeStruct((size + 16, 2 * size), BF16),
+            pltpu.HBM((rows, size), BF16),
+            pltpu.HBM((rows, size), F32),
+            pltpu.VMEM((size + 16, 2 * size), BF16),
+        ],
+        scratch_shapes=[
+            pltpu.VMEM((rows, size), BF16),
+            pltpu.VMEM((rows, size), F32),
+            pltpu.SemaphoreType.DMA((rows // CHUNK, 2)),
         ],
         compiler_params=params(16),
         cost_estimate=cost(2 * rows * size * size * 60, 3 << 20),
@@ -261,10 +325,11 @@
     )(q, k, v, bl)
 
 
-def along_kernel(place_ref, p0, p1, p2, p3, before_ref, total_ref, held):
+def along_kernel(place_ref, p0, p1, p2, p3, before_hbm, total_ref, held, kept, sems, out_sem):
     me = place_ref[0]
-    for j, piece in ((0, p0), (2, p1), (3, p2), (1, p3)):
-        held[(me - j + 4) & 3] = piece[...]
+    pieces = ((0, p0), (2, p1), (3, p2), (1, p3))
+    for one in fetch(sems, *((piece, held.at[(me - j + 4) & 3]) for j, piece in pieces)):
+        one.wait()
     size = p0.shape[1] // 2
     nothing = (jnp.ones((1, 1), F32), jnp.zeros((size, size), F32), jnp.zeros((size, size), F32))
     before = nothing
@@ -272,20 +337,28 @@
     for m in range(1, 4):
         before = tuple(jnp.where(me == m, a, b) for a, b in zip(so_far, before))
         so_far = compose(read_state(held.at[m]), so_far)
-    write_state(before_ref, before)
+    write_state(kept, before)
+    (store,) = fetch(out_sem, (kept, before_hbm))
     write_state(total_ref, so_far)
-
-
-def small_call(kernel, shapes, scratch, *args):
+    store.wait()
+
+
+def along(place, state, *others):
     return pl.pallas_call(
-        kernel,
-        in_specs=[scalars()] + [whole()] * (len(args) - 1),
-        out_specs=[whole()] * len(shapes),
-        out_shape=[jax.ShapeDtypeStruct(shape, BF16) for shape in shapes],
-        scratch_shapes=scratch,
+        along_kernel,
+        in_specs=[scalars()] + [anywhere()] * 4,
+        out_specs=[hbm(), whole()],
+        out_shape=[pltpu.HBM(state.shape, BF16), pltpu.VMEM(state.shape, BF16)],
+        scratch_shapes=[
+            pltpu.VMEM((4,) + state.shape, BF16),
+            pltpu.VMEM(state.shape, BF16),
+            pltpu.SemaphoreType.DMA((4,)),
+            pltpu.SemaphoreType.DMA((1,)),
+        ],
         compiler_params=params(4),
         cost_estimate=cost(16 << 20, 1 << 18),
-    )(*args)
+        name="along",
+    )(place[None].astype(jnp.int32), state, *others)
 
 
 def cyclic(block, axis, distance):
@@ -302,69 +375,117 @@
     return lax.ppermute(block, "c", [(0, 1), (1, 0)])
 
 
-def finish_kernel(coef_p_ref, coef_q_ref, dg_ref, gain_ref, reach_ref, far_ref, before_ref, out_ref):
+def finish_kernel(
+    coef_p_hbm, coef_q_hbm, dg_hbm, gain_ref, reach_any, far_any, before_hbm, out_hbm, *scratch
+):
+    coef_p_ref, coef_q_ref, dg_ref, reach_ref, far_ref, before_ref, out_ref, sems, out_sems = scratch
+    loads = fetch(
+        sems,
+        (reach_any, reach_ref),
+        (far_any, far_ref),
+        (before_hbm, before_ref),
+        (coef_p_hbm, coef_p_ref),
+        (coef_q_hbm, coef_q_ref),
+        (dg_hbm, dg_ref),
+    )
+    for one in loads[:3]:
+        one.wait()
     total, lost, made = read_state(reach_ref)
-    far = far_ref[...].astype(F32)
-    state = total * far - dot(low(lost), far_ref[...]) + made
+    state = total * far_ref[...].astype(F32) - dot(low(lost), far_ref[...]) + made
     total, lost, made = read_state(before_ref)
     state = low(total * state - dot(low(lost), low(state)) + made)
-    result = coef_q_ref[...] + dot(coef_p_ref[...], state)
-    mean = jnp.sum(result * result, axis=-1, keepdims=True) * (1.0 / result.shape[1])
-    result = result * lax.rsqrt(mean + TINY_NORM) * gain_ref[...]
-    out_ref[...] = low(result * jax.nn.silu(dg_ref[...].astype(F32)))
-
-
-def finish(*args):
+    for one in loads[3:]:
+        one.wait()
+    stores = []
+    step = out_ref.shape[0] // 4
+    for n in range(4):
+        here = slice(n * step, (n + 1) * step)
+        result = coef_q_ref[here, :] + dot(coef_p_ref[here, :], state)
+        mean = jnp.sum(result * result, axis=-1, keepdims=True) * (1.0 / result.shape[1])
+        result = result * lax.rsqrt(mean + TINY_NORM) * gain_ref[...]
+        out_ref[here, :] = low(result * jax.nn.silu(dg_ref[here, :].astype(F32)))
+        stores += fetch(out_sems.at[pl.ds(n, 1)], (out_ref.at[here, :], out_hbm.at[here, :]))
+    for one in stores:
+        one.wait()
+
+
+def finish(coef_p, coef_q, dg, gain, reach, far, before):
+    coef_p, coef_q, dg, before, reach = map(home, (coef_p, coef_q, dg, before, reach))
+    args = (coef_p, coef_q, dg, gain, reach, far, before)
+    copied = (coef_p, coef_q, dg, reach, far, before, dg)
     return pl.pallas_call(
         finish_kernel,
-        in_specs=[whole()] * len(args),
-        out_specs=whole(),
-        out_shape=jax.ShapeDtypeStruct(args[2].shape, BF16),
-        compiler_params=params(4),
+        in_specs=[hbm(), hbm(), hbm(), whole(), anywhere(), anywhere(), hbm()],
+        out_specs=hbm(),
+        out_shape=pltpu.HBM(dg.shape, BF16),
+        scratch_shapes=[pltpu.VMEM(a.shape, a.dtype) for a in copied]
+        + [pltpu.SemaphoreType.DMA((6,)), pltpu.SemaphoreType.DMA((4,))],
+        compiler_params=params(8),
         cost_estimate=cost(64 << 20, 2 << 20),
         name="finish",
     )(*args)
 
 
-def conv_kernel(gu_ref, before_ref, taps_ref, cg_ref, out_ref, padded):
+def conv_kernel(gu_hbm, before_any, taps_ref, cg_hbm, out_hbm, gu_ref, before_ref, padded, out_ref, sems, out_sems):
     rows, size = gu_ref.shape
     head = before_ref.shape[0]
     count = taps_ref.shape[0]
+    gate = pltpu.make_async_copy(cg_hbm, out_ref.at[:, pl.ds(size, size)], sems.at[2])
+    gate.start()
+    for one in fetch(sems, (gu_hbm, gu_ref), (before_any, before_ref)):
+        one.wait()
     padded[0:head, :] = before_ref[...].astype(F32)
     padded[head:, :] = gu_ref[...].astype(F32)
     taps = taps_ref[...].astype(F32)
     step = 64
     skip = head - (count - 1)
-    for base in range(0, rows, step):
+    gate.wait()
+    stores = []
+    for n, base in enumerate(range(0, rows, step)):
         total = jnp.zeros((step, size), F32)
         for j in range(count):
             total = total + padded[base + skip + j : base + skip + j + step, :] * taps[j : j + 1, :]
-        out_ref[base : base + step, 0:size] = low(total)
-    out_ref[:, size:] = cg_ref[...]
+        here = slice(base, base + step)
+        out_ref[here, 0:size] = low(total)
+        stores += fetch(out_sems.at[pl.ds(n, 1)], (out_ref.at[here, :], out_hbm.at[here, :]))
+    for one in stores:
+        one.wait()
 
 
 def conv(gu, before, taps, cg):
     rows, size = gu.shape
     return pl.pallas_call(
         conv_kernel,
-        in_specs=[whole()] * 4,
-        out_specs=whole(),
-        out_shape=jax.ShapeDtypeStruct((rows, 2 * size), BF16),
-        scratch_shapes=[pltpu.VMEM((rows + before.shape[0], size), F32)],
-        compiler_params=params(4),
+        in_specs=[hbm(), anywhere(), whole(), hbm()],
+        out_specs=hbm(),
+        out_shape=pltpu.HBM((rows, 2 * size), BF16),
+        scratch_shapes=[
+            pltpu.VMEM(gu.shape, BF16),
+            pltpu.VMEM(before.shape, BF16),
+            pltpu.VMEM((rows + before.shape[0], size), F32),
+            pltpu.VMEM((rows, 2 * size), BF16),
+            pltpu.SemaphoreType.DMA((3,)),
+            pltpu.SemaphoreType.DMA((rows // 64,)),
+        ],
+        compiler_params=params(8),
         cost_estimate=cost(256 << 20, 1 << 20),
         name="conv",
-    )(gu, before, taps, cg)
-
-
-def order_of(weight_refs):
-    return list(enumerate(weight_refs))
-
-
-def conv_out_kernel(block_ref, got_ref, *refs):
-    weight_refs, out_ref, mixed = refs[:8], refs[8], refs[9]
-    starts = [128] * 6 + [0] * 2
+    )(home(gu), before, taps, home(cg))
+
+
+def conv_out_kernel(block_ref, got_hbm, *refs):
+    sources, out_hbm = refs[:8], refs[8]
+    got_ref, weights, mixed, out_ref, sems, out_sems = refs[9:]
     groups, rows, size = mixed.shape
+    (load,) = fetch(sems.at[pl.ds(8, 1)], (got_hbm, got_ref))
+    loads = fetch(
+        sems,
+        *(
+            (ref.at[pl.ds(0 if ref.shape[0] == size + 16 else size, size + 16), :], weights.at[slot])
+            for slot, ref in enumerate(sources)
+        ),
+    )
+    load.wait()
     total = jnp.zeros((rows, 1), F32)
     total_square = jnp.zeros((rows, 1), F32)
     for g in range(groups):
@@ -375,45 +496,89 @@
     center = total * scale
     variance = jnp.maximum(total_square * scale - center * center, 0.0)
     factor = lax.rsqrt(variance + TINY_VAR)
-    for slot, ref in order_of(weight_refs):
+    for one in loads:
+        one.wait()
+    for slot in range(groups):
         g = block_ref[slot]
-        top = starts[slot] + size
-        extra = ref[top : top + 16, :].astype(F32)
+        extra = weights[slot, size : size + 16, :].astype(F32)
         gain = extra[0:1, 0:size] + extra[1:2, 0:size] + extra[2:3, 0:size]
         shift = extra[3:4, 0:size] + extra[4:5, 0:size] + extra[5:6, 0:size]
         normed = (got_ref[g, :, 0:size].astype(F32) - center) * factor * gain + shift
         gate = got_ref[g, :, size:].astype(F32)
         mixed[slot] = low(jax.nn.silu(normed) * jax.nn.silu(gate))
     width = out_ref.shape[1]
-    for base in range(0, width, 512):
+    stores = []
+    for n, base in enumerate(range(0, width, 512)):
         acc = jnp.zeros((rows, 512), F32)
-        for slot, ref in order_of(weight_refs):
-            top = starts[slot]
-            acc = acc + dot(mixed[slot], ref[top : top + size, base : base + 512])
-        out_ref[:, base : base + 512] = acc
-
-
-def delta_out_kernel(block_ref, got_ref, conv_ref, *refs):
-    weight_refs, out_ref = refs[:8], refs[8]
+        for slot in range(groups):
+            acc = acc + dot(mixed[slot], weights[slot, 0:size, base : base + 512])
+        here = slice(base, base + 512)
+        out_ref[:, here] = acc
+        stores += fetch(out_sems.at[pl.ds(n, 1)], (out_ref.at[:, here], out_hbm.at[:, here]))
+    for one in stores:
+        one.wait()
+
+
+def conv_out(blocks, got, *sources):
+    groups, rows, both = got.shape
+    size, width = both // 2, sources[0].shape[1]
+    return pl.pallas_call(
+        conv_out_kernel,
+        in_specs=[scalars()] + [anywhere()] * 9,
+        out_specs=hbm(),
+        out_shape=pltpu.HBM((rows, width), F32),
+        scratch_shapes=[
+            pltpu.VMEM(got.shape, BF16),
+            pltpu.VMEM((groups, size + 16, width), BF16),
+            pltpu.VMEM((groups, rows, size), BF16),
+            pltpu.VMEM((rows, width), F32),
+            pltpu.SemaphoreType.DMA((9,)),
+            pltpu.SemaphoreType.DMA((4,)),
+        ],
+        compiler_params=params(12),
+        cost_estimate=cost(2 * rows * 1024 * width, 6 << 20),
+        name="conv_out",
+    )(blocks, got, *sources)
+
+
+def delta_out_kernel(block_ref, got_hbm, conv_hbm, *refs):
+    sources, out_ref = refs[:8], refs[8]
+    got_ref, weights, conv_ref, sems = refs[9:]
+    size = got_ref.shape[1]
+    loads = fetch(
+        sems,
+        (got_hbm, got_ref),
+        *((ref.at[pl.ds(0, size), :], weights.at[slot]) for slot, ref in enumerate(sources)),
+        (conv_hbm, conv_ref),
+    )
+    for one in loads:
+        one.wait()
     width = out_ref.shape[1]
     for base in range(0, width, 512):
         acc = conv_ref[:, base : base + 512]
-        for slot, ref in order_of(weight_refs):
-            acc = acc + dot(got_ref[block_ref[slot]], ref[0:128, base : base + 512])
+        for slot in range(len(sources)):
+            acc = acc + dot(got_ref[block_ref[slot]], weights[slot, :, base : base + 512])
         out_ref[:, base : base + 512] = low(acc)
 
 
-def out_call(kernel, kind, scratch, blocks, *args):
-    rows, width = args[0].shape[1], args[-1].shape[1]
+def delta_out(blocks, got, conv_part, *sources):
+    groups, rows, size = got.shape
+    width = conv_part.shape[1]
     return pl.pallas_call(
-        kernel,
-        in_specs=[scalars()] + [whole()] * len(args),
+        delta_out_kernel,
+        in_specs=[scalars()] + [anywhere()] * 10,
         out_specs=whole(),
-        out_shape=jax.ShapeDtypeStruct((rows, width), kind),
-        scratch_shapes=scratch,
-        compiler_params=params(8),
+        out_shape=jax.ShapeDtypeStruct((rows, width), BF16),
+        scratch_shapes=[
+            pltpu.VMEM(got.shape, BF16),
+            pltpu.VMEM((groups, size, width), BF16),
+            pltpu.VMEM(conv_part.shape, F32),
+            pltpu.SemaphoreType.DMA((10,)),
+        ],
+        compiler_params=params(12),
         cost_estimate=cost(2 * rows * 1024 * width, 6 << 20),
-    )(blocks, *args)
+        name="delta_out",
+    )(blocks, got, home(conv_part), *sources)
 
 
 def local(
@@ -454,18 +619,15 @@
         ],
         axis=1,
     )
-    weights = jnp.concatenate(
-        [
-            w_query,
-            w_key,
-            w_value,
-            w_delta_gate,
-            w_glu_value,
-            w_glu_gate,
-            w_conv_gate,
-            beta_decay,
-        ],
-        axis=1,
+    weights = (
+        w_glu_value,
+        w_glu_gate,
+        w_delta_gate,
+        w_conv_gate,
+        w_query,
+        w_key,
+        w_value,
+        beta_decay,
     )
     rate = jnp.exp(lax.dynamic_slice_in_dim(decay_log, head, 1, 0))
 
@@ -482,36 +644,24 @@
     own = tokens
     r1, l1 = cyclic(own, "y", 1), cyclic(own, "y", -1)
     sw = swapped(own)
-    r1, l1, weights, last = lax.optimization_barrier((r1, l1, weights, last))
+    r1, l1, beta_decay, last = lax.optimization_barrier((r1, l1, beta_decay, last))
+    weights = weights[:7] + (beta_decay,)
     fa, fb = cyclic(r1[:half], "y", 1), cyclic(l1[half:], "y", -1)
     sr1, sl1 = swapped(r1), swapped(l1)
     sfa, sfb = swapped(fa), swapped(fb)
     pieces = [own, sw, r1, sr1, l1, sl1, fa, sfa, fb, sfb]
     wr, wl = cyclic(last, "y", 1), cyclic(last, "y", -1)
-    q, k, v, dg, gu, cg, bl = project(pieces, weights, blocks, rate, 2048, size)
+    q, k, v, bl, dg, gu, cg = project(pieces, weights, blocks, rate, 2048, size)
 
     coef_p, coef_q, state = delta(q, k, v, bl)
 
-    gu, last, state = lax.optimization_barrier((gu, last, state))
-
-    kind = state.shape
-
-    def among_four(place, state, others):
-        return small_call(
-            along_kernel,
-            [kind, kind],
-            [pltpu.VMEM((4,) + kind, BF16)],
-            place[None].astype(jnp.int32),
-            state,
-            *others,
-        )
-
-    before, total = among_four(x, state, [cyclic(state, "x", j) for j in (2, 3, 1)])
+
+    before, total = along(x, state, *(cyclic(state, "x", j) for j in (2, 3, 1)))
     route = lambda j: [(h + i, h + (i + j) % 4) for h in (0, 4) for i in range(4)]
     around = []
     for j in (2, 3, 1):
         around.append(lax.ppermute(total, "z", route(j)))
-    before_z, total_z = among_four(z % 4, total, around)
+    before_z, total_z = along(z % 4, total, *around)
     far = shifted(total_z[:size, size:], "z", 4)
 
     ws = swapped(last)
@@ -526,18 +676,11 @@
     filtered = conv(gu, halo, conv_taps, cg)
     groups = 8
     got = lax.all_to_all(filtered.reshape(groups, rows // groups, 2 * size), TP, 0, 0, tiled=True)
-    conv_part = out_call(
-        conv_out_kernel,
-        F32,
-        [pltpu.VMEM((groups, rows // groups, size), BF16)],
-        blocks,
-        got,
-        *conv_weights,
-    )
+    conv_part = conv_out(blocks, got, *conv_weights)
 
     mixed = finish(coef_p, coef_q, dg, head_gain[None, :], before_z, far, before)
     mixed = lax.all_to_all(mixed.reshape(groups, rows // groups, size), TP, 0, 0, tiled=True)
-    return out_call(delta_out_kernel, BF16, [], blocks, mixed, conv_part, *delta_weights)
+    return delta_out(blocks, mixed, conv_part, *delta_weights)
 
 
 def solution(mesh):

time: 138 us -> 134 us (0.971)
  local copies, waits for them, and re-layouts: 36.7 us -> 14.9 us
  Pallas kernels: 24.8 us -> 34.2 us
  waiting for transfers between devices: 16.9 us -> 24.5 us
  starting transfers between devices: 55.7 us -> 57.4 us
    unnamed x80 -> x36, local copies, waits for them, and re-layouts: 23.1 us -> 8.86 us
    pallas_call x8, Pallas kernels: 24.8 us -> 34.2 us  [the longest x1 9.4 us: project(): pl.pallas_call(functools.partial(project_kernel, width_all, head_size), i...]
    concatenate x1, local copies, waits for them, and re-layouts: 7.67 us -> 0.08 us  [local(): jnp.concatenate([lax.dynamic_slice_in_dim(w_beta, head, 1, 1), lax.dynami...]
    ppermute x11, waiting for transfers between devices: 10.7 us -> 16.9 us  [cyclic(): lax.ppermute(block, axis, [(i, (i + distance) % count) for i in range(cou...]
  transfers between devices with their start and end apart: 28 -> 28, of which waited for: 9 -> 11; matrix products, arithmetic and copies ran while one was open for 11% -> 6% of each run, Pallas kernels for 15% -> 22%
where the time goes in v1:
time: 134 us; the launch traced here: 133 us
  starting transfers between devices  57.4 us (43%)
  Pallas kernels  34.2 us (26%)
  waiting for transfers between devices  24.5 us (18%)
  local copies, waits for them, and re-layouts  14.9 us (11%)
    ppermute x11, waiting for transfers between devices, cyclic(): lax.ppermute(block, axis, [(i, (i + distance) % count) for i in range(cou...  16.9 us
    ppermute x10, starting transfers between devices, swapped(): return lax.ppermute(block, 'c', [(0, 1), (1, 0)])  14.8 us
    ppermute x11, starting transfers between devices, cyclic(): lax.ppermute(block, axis, [(i, (i + distance) % count) for i in range(cou...  13.2 us
    ppermute x1, starting transfers between devices, shifted(): lax.ppermute(block, axis, [(i, i + distance) for i in devices if i + dist...  10.7 us
    pallas_call x1, Pallas kernels, project(): pl.pallas_call(functools.partial(project_kernel, width_all, head_size), i...  9.4 us
    unnamed x36, local copies, waits for them, and re-layouts  8.86 us
    all_to_all x1, starting transfers between devices, local(): lax.all_to_all(filtered.reshape(groups, rows // groups, 2 * size), TP, 0,...  7.47 us
    pallas_call x1, Pallas kernels, delta(): pl.pallas_call(delta_kernel, in_specs=[whole()] * 4, out_specs=[hbm(), hb...  6.4 us
  transfers between devices with their start and end apart: 28, of which 11 were waited for; matrix products, arithmetic and copies ran while one was open for 6% of the time, Pallas kernels for 22%

profile of v1, /device:TPU:1, one launch (start us, length us, event | category | flops | bytes accessed | tf_op | source)
XLA Modules:
  0.0 133.3 jit_solution(8689547558426115690)
XLA Ops:
  0.0 3.2 %collective-permute-start = (bf16[1024,256]{1,0:T(8,128)(2,1)}, bf16[1024,256]{1,0:T(8,128)(2,1)S(1)}, u32[]{:S(2)}, u32[]{:S(2)}) collective-permute-start(bf16[1024,256]{1,0:T(8,128)(2,1)} %refs_0_.1), channel_id=1, source_target_pairs={{0,1},{1,0},{2,3},{3,2},{4,5},{5,4},{6,7},{7,6},{8,9},{9,8},{10,11... | collective-permute-start | bytes 1572872 | tf_op jit(solution)/shard_map/ppermute | solution.py:375
  3.2 2.7 %collective-permute-start.2 = (bf16[1024,256]{1,0:T(8,128)(2,1)}, bf16[1024,256]{1,0:T(8,128)(2,1)}, u32[]{:S(2)}, u32[]{:S(2)}) collective-permute-start(bf16[1024,256]{1,0:T(8,128)(2,1)} %refs_0_.1), channel_id=1, source_target_pairs={{0,6},{2,0},{4,2},{6,4},{1,7},{3,1},{5,3},{7,5},{8,14},{10,8},{12,... | collective-permute-start | bytes 1572872 | tf_op jit(solution)/shard_map/ppermute | solution.py:366
  7.5 1.1 maximum_maximum_fusion.refs_17_
  8.7 9.5 %collective-permute-done.1.refs_2_ = bf16[1024,256]{1,0:T(8,128)(2,1)} collective-permute-done((bf16[1024,256]{1,0:T(8,128)(2,1)}, bf16[1024,256]{1,0:T(8,128)(2,1)}, u32[]{:S(2)}, u32[]{:S(2)}) %collective-permute-start.1) | collective-permute-done | bytes 524320 | tf_op jit(solution)/shard_map/ppermute | solution.py:366
  21.1 2.8 %collective-permute-start.7 = (bf16[512,256]{1,0:T(8,128)(2,1)S(1)}, bf16[512,256]{1,0:T(8,128)(2,1)}, u32[]{:S(2)}, u32[]{:S(2)}) collective-permute-start(bf16[512,256]{1,0:T(8,128)(2,1)S(1)} %slice.19), channel_id=1, source_target_pairs={{0,6},{2,0},{4,2},{6,4},{1,7},{3,1},{5,3},{7,5},{8,14},{10,8},{12,... | collective-permute-start | bytes 786440 | tf_op jit(solution)/shard_map/ppermute | solution.py:366
  25.2 1.5 %collective-permute-start.20 = (bf16[272,2048]{1,0:T(8,128)(2,1)S(1)}, bf16[272,2048]{1,0:T(8,128)(2,1)S(1)}, u32[]{:S(2)}, u32[]{:S(2)}) collective-permute-start(bf16[272,2048]{1,0:T(8,128)(2,1)S(1)} %fusion.1.refs_0_), channel_id=1, source_target_pairs={{0,6},{2,0},{4,2},{6,4},{1,7},{3,1},{5,3},{7,5},{8,14},{10,8},{12,... | collective-permute-start | bytes 3342344 | tf_op jit(solution)/shard_map/ppermute | solution.py:366
  26.7 2.6 %collective-permute-done.5.refs_6_ = bf16[512,256]{1,0:T(8,128)(2,1)} collective-permute-done((bf16[512,256]{1,0:T(8,128)(2,1)S(1)}, bf16[512,256]{1,0:T(8,128)(2,1)}, u32[]{:S(2)}, u32[]{:S(2)}) %collective-permute-start.5) | collective-permute-done | bytes 262176 | tf_op jit(solution)/shard_map/ppermute | solution.py:366
  29.3 1.8 %collective-permute-start.6 = (bf16[512,256]{1,0:T(8,128)(2,1)}, bf16[512,256]{1,0:T(8,128)(2,1)}, u32[]{:S(2)}, u32[]{:S(2)}) collective-permute-start(bf16[512,256]{1,0:T(8,128)(2,1)} %collective-permute-done.5.refs_6_), channel_id=1, source_target_pairs={{0,1},{1,0},{2,3},{3,2},{4,5},{5,4},{6,7},{7,6},{8,9},{9,8},{10,11... | collective-permute-start | bytes 786440 | tf_op jit(solution)/shard_map/ppermute | solution.py:375
  33.8 1.0 copy-done.9
  34.8 1.0 copy-done.11
  35.9 9.4 %project.1 = (bf16[1024,128]{1,0:T(8,128)(2,1)S(1)}, bf16[1024,128]{1,0:T(8,128)(2,1)S(1)}, bf16[1024,128]{1,0:T(8,128)(2,1)S(1)}, f32[1024,128]{1,0:T(8,128)S(1...) custom-call(s32[8]{0:T(128)S(1)} %stack.63.block_ref, f32[1]{0:T(128)S(6)} %exp.3.rate_ref, ...), custom_call_target="tpu_custom_call" | custom-call | flops 4294967296 | bytes 12582912 | tf_op jit(solution)/shard_map/project/pallas_call | solution.py:170
  45.3 6.4 %delta.1 = (bf16[1024,128]{1,0:T(8,128)(2,1)}, f32[1024,128]{1,0:T(8,128)}, bf16[144,256]{1,0:T(8,128)(2,1)S(1)}) custom-call(bf16[1024,128]{1,0:T(8,128)(2,1)S(1)} %get-tuple-element.26.q_ref, bf16[1024,128]{1,0:T(8,128)(2,1)S(1)} %get-tuple-element.27.k_ref, bf16[1024,128]{1,0:T(8,128)(2,1)S(1)} %get-tuple-element.28.v_ref, ...), custom_call_target="tpu_custom_call" | custom-call | flops 2013265920 | bytes 3145728 | tf_op jit(solution)/shard_map/delta/pallas_call | solution.py:308
  51.7 2.1 %collective-permute-start.9 = (bf16[144,256]{1,0:T(8,128)(2,1)S(1)}, bf16[144,256]{1,0:T(8,128)(2,1)S(1)}, u32[]{:S(2)}, u32[]{:S(2)}) collective-permute-start(bf16[144,256]{1,0:T(8,128)(2,1)S(1)} %get-tuple-element.33.p0), channel_id=1, source_target_pairs={{0,16},{8,24},{16,0},{24,8},{1,17},{9,25},{17,1},{25,9},{2,18},{10... | collective-permute-start | bytes 221192 | tf_op jit(solution)/shard_map/ppermute | solution.py:366
  55.3 1.7 %collective-permute-done.9.p1 = bf16[144,256]{1,0:T(8,128)(2,1)S(1)} collective-permute-done((bf16[144,256]{1,0:T(8,128)(2,1)S(1)}, bf16[144,256]{1,0:T(8,128)(2,1)S(1)}, u32[]{:S(2)}, u32[]{:S(2)}) %collective-permute-start.9) | collective-permute-done | bytes 73760 | tf_op jit(solution)/shard_map/ppermute | solution.py:366
  60.1 2.1 %along.2 = (bf16[144,256]{1,0:T(8,128)(2,1)}, bf16[144,256]{1,0:T(8,128)(2,1)S(1)}) custom-call(s32[1]{0:T(128)} %bitcast.16.place_ref, bf16[144,256]{1,0:T(8,128)(2,1)S(1)} %get-tuple-element.33.p0, bf16[144,256]{1,0:T(8,128)(2,1)S(1)} %copy-done.5, bf16[144,256]{1,0:T(8,128)(2,1)} %collective-permute-done.10.p2, bf16[144,256]{1,0:T(8,128)(2,1)} %collective-permute-done.11.p3), custom_call_target="tpu_custom_call" | custom-call | flops 16777216 | bytes 262144 | tf_op jit(solution)/shard_map/along/pallas_call | solution.py:347
  62.2 3.3 %collective-permute-start.12 = (bf16[144,256]{1,0:T(8,128)(2,1)S(1)}, bf16[144,256]{1,0:T(8,128)(2,1)S(1)}, u32[]{:S(2)}, u32[]{:S(2)}) collective-permute-start(bf16[144,256]{1,0:T(8,128)(2,1)S(1)} %get-tuple-element.34.p0), channel_id=1, source_target_pairs={{0,64},{32,96},{64,0},{96,32},{128,192},{160,224},{192,128},{224,1... | collective-permute-start | bytes 221192 | tf_op jit(solution)/shard_map/ppermute | solution.py:663
  65.5 1.4 %collective-permute-start.13 = (bf16[144,256]{1,0:T(8,128)(2,1)S(1)}, bf16[144,256]{1,0:T(8,128)(2,1)S(1)}, u32[]{:S(2)}, u32[]{:S(2)}) collective-permute-start(bf16[144,256]{1,0:T(8,128)(2,1)S(1)} %get-tuple-element.34.p0), channel_id=1, source_target_pairs={{0,96},{32,0},{64,32},{96,64},{128,224},{160,128},{192,160},{224,1... | collective-permute-start | bytes 221192 | tf_op jit(solution)/shard_map/ppermute | solution.py:663
  67.8 2.6 %collective-permute-start.22 = (bf16[144,2048]{1,0:T(8,128)(2,1)}, bf16[144,2048]{1,0:T(8,128)(2,1)}, u32[]{:S(2)}, u32[]{:S(2)}) collective-permute-start(bf16[144,2048]{1,0:T(8,128)(2,1)} %slice.24), channel_id=1, source_target_pairs={{0,6},{2,0},{4,2},{6,4},{1,7},{3,1},{5,3},{7,5},{8,14},{10,8},{12,... | collective-permute-start | bytes 1769480 | tf_op jit(solution)/shard_map/ppermute | solution.py:366
  70.4 2.4 %collective-permute-start.17 = (bf16[272,2048]{1,0:T(8,128)(2,1)S(1)}, bf16[272,2048]{1,0:T(8,128)(2,1)}, u32[]{:S(2)}, u32[]{:S(2)}) collective-permute-start(bf16[272,2048]{1,0:T(8,128)(2,1)S(1)} %fusion.1.refs_0_), channel_id=1, source_target_pairs={{0,1},{1,0},{2,3},{3,2},{4,5},{5,4},{6,7},{7,6},{8,9},{9,8},{10,11... | collective-permute-start | bytes 3342344 | tf_op jit(solution)/shard_map/ppermute | solution.py:375
  75.0 4.5 %collective-permute-done.14.p3 = bf16[144,256]{1,0:T(8,128)(2,1)S(1)} collective-permute-done((bf16[144,256]{1,0:T(8,128)(2,1)S(1)}, bf16[144,256]{1,0:T(8,128)(2,1)S(1)}, u32[]{:S(2)}, u32[]{:S(2)}) %collective-permute-start.14) | collective-permute-done | bytes 73760 | tf_op jit(solution)/shard_map/ppermute | solution.py:663
  80.1 1.3 collective-permute-start.16
  83.2 1.4 %along.3 = (bf16[144,256]{1,0:T(8,128)(2,1)}, bf16[144,256]{1,0:T(8,128)(2,1)S(1)}) custom-call(s32[1]{0:T(128)} %bitcast.15.place_ref, bf16[144,256]{1,0:T(8,128)(2,1)S(1)} %get-tuple-element.34.p0, bf16[144,256]{1,0:T(8,128)(2,1)S(1)} %collective-permute-done.12.p1, bf16[144,256]{1,0:T(8,128)(2,1)S(1)} %copy-done.1, bf16[144,256]{1,0:T(8,128)(2,1)S(1)} %copy-done.3), custom_call_target="tpu_custom_call" | custom-call | flops 16777216 | bytes 262144 | tf_op jit(solution)/shard_map/along/pallas_call | solution.py:347
  84.6 10.7 %collective-permute-start.15 = (bf16[128,128]{1,0:T(8,128)(2,1)S(1)}, bf16[128,128]{1,0:T(8,128)(2,1)S(1)}, u32[]{:S(2)}, u32[]{:S(2)}) collective-permute-start(bf16[128,128]{1,0:T(8,128)(2,1)S(1)} %slice.20), channel_id=1, source_target_pairs={{0,128},{32,160},{64,192},{96,224},{1,129},{33,161},{65,193},{97,2... | collective-permute-start | bytes 98312 | tf_op jit(solution)/shard_map/ppermute | solution.py:371
  96.3 3.0 %conv.1 = bf16[1024,256]{1,0:T(8,128)(2,1)} custom-call(bf16[1024,128]{1,0:T(8,128)(2,1)} %get-tuple-element.38.gu_hbm, bf16[32,128]{1,0:T(8,128)(2,1)S(1)} %collective-permute-done.16.before_any, bf16[31,128]{1,0:T(8,128)(2,1)S(1)} %copy-done.6, bf16[1024,128]{1,0:T(8,128)(2,1)} %get-tuple-element.39.cg_hbm), custom_call_target="tpu_custom_call" | custom-call | flops 268435456 | bytes 1048576 | tf_op jit(solution)/shard_map/conv/pallas_call | solution.py:457
  99.3 7.5 %all-to-all-start.1 = ((bf16[8,128,256]{2,1,0:T(8,128)(2,1)}), bf16[8,128,256]{2,1,0:T(8,128)(2,1)}, u32[]{:S(2)}, u32[]{:S(2)}) async-start(bf16[8,128,256]{2,1,0:T(8,128)(2,1)} %bitcast.26), calls=%async_computation.1 | async-start | bytes 1048576 | tf_op jit(solution)/shard_map/all_to_all | solution.py:678
  106.9 1.5 %collective-permute-done.24.refs_6_ = bf16[128,2048]{1,0:T(8,128)(2,1)} collective-permute-done((bf16[128,2048]{1,0:T(8,128)(2,1)}, bf16[128,2048]{1,0:T(8,128)(2,1)}, u32[]{:S(2)}, u32[]{:S(2)}) %collective-permute-start.24) | collective-permute-done | bytes 524320 | tf_op jit(solution)/shard_map/ppermute | solution.py:366
  108.4 5.4 %collective-permute-start.25 = (bf16[128,2048]{1,0:T(8,128)(2,1)}, bf16[128,2048]{1,0:T(8,128)(2,1)}, u32[]{:S(2)}, u32[]{:S(2)}) collective-permute-start(bf16[128,2048]{1,0:T(8,128)(2,1)} %collective-permute-done.24.refs_6_), channel_id=1, source_target_pairs={{0,1},{1,0},{2,3},{3,2},{4,5},{5,4},{6,7},{7,6},{8,9},{9,8},{10,11... | collective-permute-start | bytes 1572872 | tf_op jit(solution)/shard_map/ppermute | solution.py:375
  113.7 2.4 %finish.1 = bf16[1024,128]{1,0:T(8,128)(2,1)} custom-call(bf16[1024,128]{1,0:T(8,128)(2,1)} %get-tuple-element.30.coef_p_hbm, f32[1024,128]{1,0:T(8,128)} %get-tuple-element.31.coef_q_hbm, bf16[1024,128]{1,0:T(8,128)(2,1)} %get-tuple-element.32.dg_hbm, f32[1,128]{1,0:T(1,128)S(1)} %bitcast.25, bf16[144,256]{1,0:T(8,128)(2,1)} %get-tuple-element.35.reach_any, ...), custom_call_target="tpu_custom_call" | custom-call | flops 67108864 | bytes 2097152 | tf_op jit(solution)/shard_map/finish/pallas_call | solution.py:416
  116.8 5.0 %all-to-all-start = ((bf16[8,128,128]{2,1,0:T(8,128)(2,1)}), bf16[8,128,128]{2,1,0:T(8,128)(2,1)}, u32[]{:S(2)}, u32[]{:S(2)}) async-start(bf16[8,128,128]{2,1,0:T(8,128)(2,1)} %bitcast.27), calls=%async_computation | async-start | bytes 524288 | tf_op jit(solution)/shard_map/all_to_all | solution.py:682
  121.8 4.7 %conv_out.1.conv_hbm = f32[128,2048]{1,0:T(8,128)} custom-call(s32[8]{0:T(128)S(1)} %stack.63.block_ref, bf16[8,128,256]{2,1,0:T(8,128)(2,1)} %all-to-all-done.1.got_hbm, bf16[272,2048]{1,0:T(8,128)(2,1)S(1)} %fusion.1.refs_0_, bf16[272,2048]{1,0:T(8,128)(2,1)} %collective-permute-done.17.refs_1_, bf16[272,2048]{1,0:T(8,128)(2,1)S(1)} %collective-permute-done.18.refs_2_, ...), custom_call_target="tpu_custom_call" | custom-call | flops 536870912 | bytes 6291456 | tf_op jit(solution)/shard_map/conv_out/pallas_call | solution.py:525
  126.5 1.8 %all-to-all-done.got_hbm = bf16[8,128,128]{2,1,0:T(8,128)(2,1)} async-done(((bf16[8,128,128]{2,1,0:T(8,128)(2,1)}), bf16[8,128,128]{2,1,0:T(8,128)(2,1)}, u32[]{:S(2)}, u32[]{:S(2)}) %all-to-all-start) | async-done | bytes 262176 | tf_op jit(solution)/shard_map/all_to_all | solution.py:682
  128.3 4.8 %delta_out.1 = bf16[128,2048]{1,0:T(8,128)(2,1)} custom-call(s32[8]{0:T(128)S(1)} %stack.63.block_ref, bf16[8,128,128]{2,1,0:T(8,128)(2,1)} %all-to-all-done.got_hbm, f32[128,2048]{1,0:T(8,128)} %conv_out.1.conv_hbm, bf16[272,2048]{1,0:T(8,128)(2,1)S(1)} %fusion.1.refs_0_, bf16[272,2048]{1,0:T(8,128)(2,1)} %collective-permute-done.17.refs_1_, ...), custom_call_target="tpu_custom_call" | custom-call | flops 536870912 | bytes 6291456 | tf_op jit(solution)/shard_map/delta_out/pallas_call | solution.py:567
  (83 shorter events, 19.7 us)
Async XLA Ops:
  0.0 7.4 %copy-start.15 = (f32[128]{0:T(128)S(1)}, f32[128]{0:T(128)}, u32[]{:S(2)}) copy-start(f32[128]{0:T(128)} %param.31) | copy-start | bytes 1540
  0.0 24.4 %collective-permute-start = (bf16[1024,256]{1,0:T(8,128)(2,1)}, bf16[1024,256]{1,0:T(8,128)(2,1)S(1)}, u32[]{:S(2)}, u32[]{:S(2)}) collective-permute-start(bf16[1024,256]{1,0:T(8,128)(2,1)} %refs_0_.1), channel_id=1, source_target_pairs={{0,1},{1,0},{2,3},{3,2},{4,5},{5,4},{6,7},{7,6},{8,9},{9,8},{10,11... | collective-permute-start | bytes 1572872 | tf_op jit(solution)/shard_map/ppermute | solution.py:375
  3.2 15.0 %collective-permute-start.1 = (bf16[1024,256]{1,0:T(8,128)(2,1)}, bf16[1024,256]{1,0:T(8,128)(2,1)}, u32[]{:S(2)}, u32[]{:S(2)}) collective-permute-start(bf16[1024,256]{1,0:T(8,128)(2,1)} %refs_0_.1), channel_id=1, source_target_pairs={{0,2},{2,4},{4,6},{6,0},{1,3},{3,5},{5,7},{7,1},{8,10},{10,12},{12... | collective-permute-start | bytes 1572872 | tf_op jit(solution)/shard_map/ppermute | solution.py:366
  3.2 15.0 %collective-permute-start.2 = (bf16[1024,256]{1,0:T(8,128)(2,1)}, bf16[1024,256]{1,0:T(8,128)(2,1)}, u32[]{:S(2)}, u32[]{:S(2)}) collective-permute-start(bf16[1024,256]{1,0:T(8,128)(2,1)} %refs_0_.1), channel_id=1, source_target_pairs={{0,6},{2,0},{4,2},{6,4},{1,7},{3,1},{5,3},{7,5},{8,14},{10,8},{12,... | collective-permute-start | bytes 1572872 | tf_op jit(solution)/shard_map/ppermute | solution.py:366
  8.6 23.3 %copy-start.16 = (f32[8]{0:T(128)S(1)}, f32[8]{0:T(128)}, u32[]{:S(2)}) copy-start(f32[8]{0:T(128)} %param.27) | copy-start | bytes 100
  18.2 12.9 %collective-permute-start.3 = (bf16[1024,256]{1,0:T(8,128)(2,1)}, bf16[1024,256]{1,0:T(8,128)(2,1)S(1)}, u32[]{:S(2)}, u32[]{:S(2)}) collective-permute-start(bf16[1024,256]{1,0:T(8,128)(2,1)} %collective-permute-done.1.refs_2_), channel_id=1, source_target_pairs={{0,1},{1,0},{2,3},{3,2},{4,5},{5,4},{6,7},{7,6},{8,9},{9,8},{10,11... | collective-permute-start | bytes 1572872 | tf_op jit(solution)/shard_map/ppermute | solution.py:375
  20.0 9.3 %collective-permute-start.5 = (bf16[512,256]{1,0:T(8,128)(2,1)S(1)}, bf16[512,256]{1,0:T(8,128)(2,1)}, u32[]{:S(2)}, u32[]{:S(2)}) collective-permute-start(bf16[512,256]{1,0:T(8,128)(2,1)S(1)} %slice.18), channel_id=1, source_target_pairs={{0,2},{2,4},{4,6},{6,0},{1,3},{3,5},{5,7},{7,1},{8,10},{10,12},{12... | collective-permute-start | bytes 786440 | tf_op jit(solution)/shard_map/ppermute | solution.py:366
  21.1 8.2 %collective-permute-start.7 = (bf16[512,256]{1,0:T(8,128)(2,1)S(1)}, bf16[512,256]{1,0:T(8,128)(2,1)}, u32[]{:S(2)}, u32[]{:S(2)}) collective-permute-start(bf16[512,256]{1,0:T(8,128)(2,1)S(1)} %slice.19), channel_id=1, source_target_pairs={{0,6},{2,0},{4,2},{6,4},{1,7},{3,1},{5,3},{7,5},{8,14},{10,8},{12,... | collective-permute-start | bytes 786440 | tf_op jit(solution)/shard_map/ppermute | solution.py:366
  23.9 9.4 %collective-permute-start.4 = (bf16[1024,256]{1,0:T(8,128)(2,1)}, bf16[1024,256]{1,0:T(8,128)(2,1)}, u32[]{:S(2)}, u32[]{:S(2)}) collective-permute-start(bf16[1024,256]{1,0:T(8,128)(2,1)} %collective-permute-done.2.refs_4_), channel_id=1, source_target_pairs={{0,1},{1,0},{2,3},{3,2},{4,5},{5,4},{6,7},{7,6},{8,9},{9,8},{10,11... | collective-permute-start | bytes 1572872 | tf_op jit(solution)/shard_map/ppermute | solution.py:375
  25.2 41.7 %collective-permute-start.20 = (bf16[272,2048]{1,0:T(8,128)(2,1)S(1)}, bf16[272,2048]{1,0:T(8,128)(2,1)S(1)}, u32[]{:S(2)}, u32[]{:S(2)}) collective-permute-start(bf16[272,2048]{1,0:T(8,128)(2,1)S(1)} %fusion.1.refs_0_), channel_id=1, source_target_pairs={{0,6},{2,0},{4,2},{6,4},{1,7},{3,1},{5,3},{7,5},{8,14},{10,8},{12,... | collective-permute-start | bytes 3342344 | tf_op jit(solution)/shard_map/ppermute | solution.py:366
  29.3 43.5 %collective-permute-start.18 = (bf16[272,2048]{1,0:T(8,128)(2,1)S(1)}, bf16[272,2048]{1,0:T(8,128)(2,1)S(1)}, u32[]{:S(2)}, u32[]{:S(2)}) collective-permute-start(bf16[272,2048]{1,0:T(8,128)(2,1)S(1)} %fusion.1.refs_0_), channel_id=1, source_target_pairs={{0,2},{2,4},{4,6},{6,0},{1,3},{3,5},{5,7},{7,1},{8,10},{10,12},{12... | collective-permute-start | bytes 3342344 | tf_op jit(solution)/shard_map/ppermute | solution.py:366
  29.3 4.0 %collective-permute-start.6 = (bf16[512,256]{1,0:T(8,128)(2,1)}, bf16[512,256]{1,0:T(8,128)(2,1)}, u32[]{:S(2)}, u32[]{:S(2)}) collective-permute-start(bf16[512,256]{1,0:T(8,128)(2,1)} %collective-permute-done.5.refs_6_), channel_id=1, source_target_pairs={{0,1},{1,0},{2,3},{3,2},{4,5},{5,4},{6,7},{7,6},{8,9},{9,8},{10,11... | collective-permute-start | bytes 786440 | tf_op jit(solution)/shard_map/ppermute | solution.py:375
  31.9 1.9 %collective-permute-start.8 = (bf16[512,256]{1,0:T(8,128)(2,1)}, bf16[512,256]{1,0:T(8,128)(2,1)}, u32[]{:S(2)}, u32[]{:S(2)}) collective-permute-start(bf16[512,256]{1,0:T(8,128)(2,1)} %collective-permute-done.7.refs_8_), channel_id=1, source_target_pairs={{0,1},{1,0},{2,3},{3,2},{4,5},{5,4},{6,7},{7,6},{8,9},{9,8},{10,11... | collective-permute-start | bytes 786440 | tf_op jit(solution)/shard_map/ppermute | solution.py:375
  51.7 5.3 %collective-permute-start.9 = (bf16[144,256]{1,0:T(8,128)(2,1)S(1)}, bf16[144,256]{1,0:T(8,128)(2,1)S(1)}, u32[]{:S(2)}, u32[]{:S(2)}) collective-permute-start(bf16[144,256]{1,0:T(8,128)(2,1)S(1)} %get-tuple-element.33.p0), channel_id=1, source_target_pairs={{0,16},{8,24},{16,0},{24,8},{1,17},{9,25},{17,1},{25,9},{2,18},{10... | collective-permute-start | bytes 221192 | tf_op jit(solution)/shard_map/ppermute | solution.py:366
  53.8 4.4 %collective-permute-start.10 = (bf16[144,256]{1,0:T(8,128)(2,1)S(1)}, bf16[144,256]{1,0:T(8,128)(2,1)}, u32[]{:S(2)}, u32[]{:S(2)}) collective-permute-start(bf16[144,256]{1,0:T(8,128)(2,1)S(1)} %get-tuple-element.33.p0), channel_id=1, source_target_pairs={{0,24},{8,0},{16,8},{24,16},{1,25},{9,1},{17,9},{25,17},{2,26},{10... | collective-permute-start | bytes 221192 | tf_op jit(solution)/shard_map/ppermute | solution.py:366
  54.7 4.5 %collective-permute-start.11 = (bf16[144,256]{1,0:T(8,128)(2,1)S(1)}, bf16[144,256]{1,0:T(8,128)(2,1)}, u32[]{:S(2)}, u32[]{:S(2)}) collective-permute-start(bf16[144,256]{1,0:T(8,128)(2,1)S(1)} %get-tuple-element.33.p0), channel_id=1, source_target_pairs={{0,8},{8,16},{16,24},{24,0},{1,9},{9,17},{17,25},{25,1},{2,10},{10... | collective-permute-start | bytes 221192 | tf_op jit(solution)/shard_map/ppermute | solution.py:366
  62.2 34.1 %copy-start.6 = (bf16[31,128]{1,0:T(8,128)(2,1)S(1)}, bf16[31,128]{1,0:T(8,128)(2,1)}, u32[]{:S(2)}) copy-start(bf16[31,128]{1,0:T(8,128)(2,1)} %taps_ref.1) | copy-start | bytes 23812
  62.2 10.6 %collective-permute-start.12 = (bf16[144,256]{1,0:T(8,128)(2,1)S(1)}, bf16[144,256]{1,0:T(8,128)(2,1)S(1)}, u32[]{:S(2)}, u32[]{:S(2)}) collective-permute-start(bf16[144,256]{1,0:T(8,128)(2,1)S(1)} %get-tuple-element.34.p0), channel_id=1, source_target_pairs={{0,64},{32,96},{64,0},{96,32},{128,192},{160,224},{192,128},{224,1... | collective-permute-start | bytes 221192 | tf_op jit(solution)/shard_map/ppermute | solution.py:663
  65.5 7.8 %collective-permute-start.13 = (bf16[144,256]{1,0:T(8,128)(2,1)S(1)}, bf16[144,256]{1,0:T(8,128)(2,1)S(1)}, u32[]{:S(2)}, u32[]{:S(2)}) collective-permute-start(bf16[144,256]{1,0:T(8,128)(2,1)S(1)} %get-tuple-element.34.p0), channel_id=1, source_target_pairs={{0,96},{32,0},{64,32},{96,64},{128,224},{160,128},{192,160},{224,1... | collective-permute-start | bytes 221192 | tf_op jit(solution)/shard_map/ppermute | solution.py:663
  67.8 39.0 %collective-permute-start.22 = (bf16[144,2048]{1,0:T(8,128)(2,1)}, bf16[144,2048]{1,0:T(8,128)(2,1)}, u32[]{:S(2)}, u32[]{:S(2)}) collective-permute-start(bf16[144,2048]{1,0:T(8,128)(2,1)} %slice.24), channel_id=1, source_target_pairs={{0,6},{2,0},{4,2},{6,4},{1,7},{3,1},{5,3},{7,5},{8,14},{10,8},{12,... | collective-permute-start | bytes 1769480 | tf_op jit(solution)/shard_map/ppermute | solution.py:366
  70.4 51.3 %collective-permute-start.17 = (bf16[272,2048]{1,0:T(8,128)(2,1)S(1)}, bf16[272,2048]{1,0:T(8,128)(2,1)}, u32[]{:S(2)}, u32[]{:S(2)}) collective-permute-start(bf16[272,2048]{1,0:T(8,128)(2,1)S(1)} %fusion.1.refs_0_), channel_id=1, source_target_pairs={{0,1},{1,0},{2,3},{3,2},{4,5},{5,4},{6,7},{7,6},{8,9},{9,8},{10,11... | collective-permute-start | bytes 3342344 | tf_op jit(solution)/shard_map/ppermute | solution.py:375
  72.8 48.9 %collective-permute-start.19 = (bf16[272,2048]{1,0:T(8,128)(2,1)S(1)}, bf16[272,2048]{1,0:T(8,128)(2,1)}, u32[]{:S(2)}, u32[]{:S(2)}) collective-permute-start(bf16[272,2048]{1,0:T(8,128)(2,1)S(1)} %collective-permute-done.18.refs_2_), channel_id=1, source_target_pairs={{0,1},{1,0},{2,3},{3,2},{4,5},{5,4},{6,7},{7,6},{8,9},{9,8},{10,11... | collective-permute-start | bytes 3342344 | tf_op jit(solution)/shard_map/ppermute | solution.py:375
  72.8 48.9 %collective-permute-start.21 = (bf16[272,2048]{1,0:T(8,128)(2,1)S(1)}, bf16[272,2048]{1,0:T(8,128)(2,1)}, u32[]{:S(2)}, u32[]{:S(2)}) collective-permute-start(bf16[272,2048]{1,0:T(8,128)(2,1)S(1)} %collective-permute-done.20.refs_4_), channel_id=1, source_target_pairs={{0,1},{1,0},{2,3},{3,2},{4,5},{5,4},{6,7},{7,6},{8,9},{9,8},{10,11... | collective-permute-start | bytes 3342344 | tf_op jit(solution)/shard_map/ppermute | solution.py:375
  74.0 5.5 %collective-permute-start.14 = (bf16[144,256]{1,0:T(8,128)(2,1)S(1)}, bf16[144,256]{1,0:T(8,128)(2,1)S(1)}, u32[]{:S(2)}, u32[]{:S(2)}) collective-permute-start(bf16[144,256]{1,0:T(8,128)(2,1)S(1)} %get-tuple-element.34.p0), channel_id=1, source_target_pairs={{0,32},{32,64},{64,96},{96,0},{128,160},{160,192},{192,224},{224,1... | collective-permute-start | bytes 221192 | tf_op jit(solution)/shard_map/ppermute | solution.py:663
  80.1 4.5 %collective-permute-start.16 = (bf16[32,128]{1,0:T(8,128)(2,1)S(1)}, bf16[32,128]{1,0:T(8,128)(2,1)S(1)}, u32[]{:S(2)}, u32[]{:S(2)}) collective-permute-start(bf16[32,128]{1,0:T(8,128)(2,1)S(1)} %slice.21), channel_id=1, source_target_pairs={{0,8},{8,16},{16,24},{24,32},{32,40},{40,48},{48,56},{56,64},{64,7... | collective-permute-start | bytes 24584 | tf_op jit(solution)/shard_map/ppermute | solution.py:675
  84.6 11.7 %collective-permute-start.15 = (bf16[128,128]{1,0:T(8,128)(2,1)S(1)}, bf16[128,128]{1,0:T(8,128)(2,1)S(1)}, u32[]{:S(2)}, u32[]{:S(2)}) collective-permute-start(bf16[128,128]{1,0:T(8,128)(2,1)S(1)} %slice.20), channel_id=1, source_target_pairs={{0,128},{32,160},{64,192},{96,224},{1,129},{33,161},{65,193},{97,2... | collective-permute-start | bytes 98312 | tf_op jit(solution)/shard_map/ppermute | solution.py:371
  96.2 17.5 %copy-start.7 = (f32[128]{0:T(128)S(1)}, f32[128]{0:T(128)}, u32[]{:S(2)}) copy-start(f32[128]{0:T(128)} %param.28) | copy-start | bytes 1540
  96.3 12.1 %collective-permute-start.24 = (bf16[128,2048]{1,0:T(8,128)(2,1)}, bf16[128,2048]{1,0:T(8,128)(2,1)}, u32[]{:S(2)}, u32[]{:S(2)}) collective-permute-start(bf16[128,2048]{1,0:T(8,128)(2,1)} %slice.25), channel_id=1, source_target_pairs={{0,2},{2,4},{4,6},{6,0},{1,3},{3,5},{5,7},{7,1},{8,10},{10,12},{12... | collective-permute-start | bytes 1572872 | tf_op jit(solution)/shard_map/ppermute | solution.py:366
  99.3 17.4 %all-to-all-start.1 = ((bf16[8,128,256]{2,1,0:T(8,128)(2,1)}), bf16[8,128,256]{2,1,0:T(8,128)(2,1)}, u32[]{:S(2)}, u32[]{:S(2)}) async-start(bf16[8,128,256]{2,1,0:T(8,128)(2,1)} %bitcast.26), calls=%async_computation.1 | async-start | bytes 1048576 | tf_op jit(solution)/shard_map/all_to_all | solution.py:678
  106.8 14.9 %collective-permute-start.23 = (bf16[144,2048]{1,0:T(8,128)(2,1)}, bf16[144,2048]{1,0:T(8,128)(2,1)}, u32[]{:S(2)}, u32[]{:S(2)}) collective-permute-start(bf16[144,2048]{1,0:T(8,128)(2,1)} %collective-permute-done.22.refs_6_), channel_id=1, source_target_pairs={{0,1},{1,0},{2,3},{3,2},{4,5},{5,4},{6,7},{7,6},{8,9},{9,8},{10,11... | collective-permute-start | bytes 1769480 | tf_op jit(solution)/shard_map/ppermute | solution.py:375
  108.4 20.0 %collective-permute-start.25 = (bf16[128,2048]{1,0:T(8,128)(2,1)}, bf16[128,2048]{1,0:T(8,128)(2,1)}, u32[]{:S(2)}, u32[]{:S(2)}) collective-permute-start(bf16[128,2048]{1,0:T(8,128)(2,1)} %collective-permute-done.24.refs_6_), channel_id=1, source_target_pairs={{0,1},{1,0},{2,3},{3,2},{4,5},{5,4},{6,7},{7,6},{8,9},{9,8},{10,11... | collective-permute-start | bytes 1572872 | tf_op jit(solution)/shard_map/ppermute | solution.py:375
  116.8 11.6 %all-to-all-start = ((bf16[8,128,128]{2,1,0:T(8,128)(2,1)}), bf16[8,128,128]{2,1,0:T(8,128)(2,1)}, u32[]{:S(2)}, u32[]{:S(2)}) async-start(bf16[8,128,128]{2,1,0:T(8,128)(2,1)} %bitcast.27), calls=%async_computation | async-start | bytes 524288 | tf_op jit(solution)/shard_map/all_to_all | solution.py:682
  (13 other events, 18.8 us)

commit v2 on v1

--- a/solution.py
+++ b/solution.py
@@ -325,11 +325,10 @@
     )(q, k, v, bl)
 
 
-def along_kernel(place_ref, p0, p1, p2, p3, before_hbm, total_ref, held, kept, sems, out_sem):
+def along_kernel(place_ref, p0, p1, p2, p3, before_hbm, total_ref, held, kept, out_sem):
     me = place_ref[0]
-    pieces = ((0, p0), (2, p1), (3, p2), (1, p3))
-    for one in fetch(sems, *((piece, held.at[(me - j + 4) & 3]) for j, piece in pieces)):
-        one.wait()
+    for j, piece in ((0, p0), (2, p1), (3, p2), (1, p3)):
+        held[(me - j + 4) & 3] = piece[...]
     size = p0.shape[1] // 2
     nothing = (jnp.ones((1, 1), F32), jnp.zeros((size, size), F32), jnp.zeros((size, size), F32))
     before = nothing
@@ -346,13 +345,12 @@
 def along(place, state, *others):
     return pl.pallas_call(
         along_kernel,
-        in_specs=[scalars()] + [anywhere()] * 4,
+        in_specs=[scalars()] + [whole()] * 4,
         out_specs=[hbm(), whole()],
         out_shape=[pltpu.HBM(state.shape, BF16), pltpu.VMEM(state.shape, BF16)],
         scratch_shapes=[
             pltpu.VMEM((4,) + state.shape, BF16),
             pltpu.VMEM(state.shape, BF16),
-            pltpu.SemaphoreType.DMA((4,)),
             pltpu.SemaphoreType.DMA((1,)),
         ],
         compiler_params=params(4),
@@ -473,6 +471,17 @@
     )(home(gu), before, taps, home(cg))
 
 
+def add_slots(out_ref, slots, left, weights, start):
+    width = out_ref.shape[1]
+    size = weights.shape[1] - weights.shape[1] % 128
+    for base in range(0, width, 512):
+        here = slice(base, base + 512)
+        acc = jnp.zeros((out_ref.shape[0], 512), F32) if start is None else start[:, here]
+        for slot in slots:
+            acc = acc + dot(left(slot), weights[slot, 0:size, here])
+        out_ref[:, here] = acc.astype(out_ref.dtype)
+
+
 def conv_out_kernel(block_ref, got_hbm, *refs):
     sources, out_hbm = refs[:8], refs[8]
     got_ref, weights, mixed, out_ref, sems, out_sems = refs[9:]
@@ -486,37 +495,32 @@
         ),
     )
     load.wait()
-    total = jnp.zeros((rows, 1), F32)
-    total_square = jnp.zeros((rows, 1), F32)
+    total = jnp.zeros((rows, size), F32)
+    total_square = jnp.zeros((rows, size), F32)
     for g in range(groups):
         part = got_ref[g, :, 0:size].astype(F32)
-        total = total + jnp.sum(part, axis=1, keepdims=True)
-        total_square = total_square + jnp.sum(part * part, axis=1, keepdims=True)
+        total = total + part
+        total_square = total_square + part * part
     scale = 1.0 / (groups * size)
-    center = total * scale
-    variance = jnp.maximum(total_square * scale - center * center, 0.0)
-    factor = lax.rsqrt(variance + TINY_VAR)
-    for one in loads:
-        one.wait()
-    for slot in range(groups):
-        g = block_ref[slot]
-        extra = weights[slot, size : size + 16, :].astype(F32)
-        gain = extra[0:1, 0:size] + extra[1:2, 0:size] + extra[2:3, 0:size]
-        shift = extra[3:4, 0:size] + extra[4:5, 0:size] + extra[5:6, 0:size]
-        normed = (got_ref[g, :, 0:size].astype(F32) - center) * factor * gain + shift
-        gate = got_ref[g, :, size:].astype(F32)
-        mixed[slot] = low(jax.nn.silu(normed) * jax.nn.silu(gate))
-    width = out_ref.shape[1]
-    stores = []
-    for n, base in enumerate(range(0, width, 512)):
-        acc = jnp.zeros((rows, 512), F32)
-        for slot in range(groups):
-            acc = acc + dot(mixed[slot], weights[slot, 0:size, base : base + 512])
-        here = slice(base, base + 512)
-        out_ref[:, here] = acc
-        stores += fetch(out_sems.at[pl.ds(n, 1)], (out_ref.at[:, here], out_hbm.at[:, here]))
-    for one in stores:
-        one.wait()
+    center = jnp.sum(total, axis=1, keepdims=True) * scale
+    second = jnp.sum(total_square, axis=1, keepdims=True) * scale
+    factor = lax.rsqrt(jnp.maximum(second - center * center, 0.0) + TINY_VAR)
+    for half in range(2):
+        slots = range(half * 4, half * 4 + 4)
+        for slot in slots:
+            loads[slot].wait()
+            g = block_ref[slot]
+            extra = weights[slot, size : size + 16, :].astype(F32)
+            gain = extra[0:1, 0:size] + extra[1:2, 0:size] + extra[2:3, 0:size]
+            shift = extra[3:4, 0:size] + extra[4:5, 0:size] + extra[5:6, 0:size]
+            normed = (got_ref[g, :, 0:size].astype(F32) - center) * factor * gain + shift
+            gate = got_ref[g, :, size:].astype(F32)
+            mixed[slot] = low(jax.nn.silu(normed) * jax.nn.silu(gate))
+        add_slots(
+            out_ref, slots, lambda slot: mixed[slot], weights, out_ref if half else None
+        )
+    (store,) = fetch(out_sems, (out_ref, out_hbm))
+    store.wait()
 
 
 def conv_out(blocks, got, *sources):
@@ -533,7 +537,7 @@
             pltpu.VMEM((groups, rows, size), BF16),
             pltpu.VMEM((rows, width), F32),
             pltpu.SemaphoreType.DMA((9,)),
-            pltpu.SemaphoreType.DMA((4,)),
+            pltpu.SemaphoreType.DMA((1,)),
         ],
         compiler_params=params(12),
         cost_estimate=cost(2 * rows * 1024 * width, 6 << 20),
@@ -548,17 +552,22 @@
     loads = fetch(
         sems,
         (got_hbm, got_ref),
+        (conv_hbm, conv_ref),
         *((ref.at[pl.ds(0, size), :], weights.at[slot]) for slot, ref in enumerate(sources)),
-        (conv_hbm, conv_ref),
     )
-    for one in loads:
-        one.wait()
-    width = out_ref.shape[1]
-    for base in range(0, width, 512):
-        acc = conv_ref[:, base : base + 512]
-        for slot in range(len(sources)):
-            acc = acc + dot(got_ref[block_ref[slot]], weights[slot, :, base : base + 512])
-        out_ref[:, base : base + 512] = low(acc)
+    loads[0].wait()
+    loads[1].wait()
+    for half in range(2):
+        slots = range(half * 4, half * 4 + 4)
+        for slot in slots:
+            loads[2 + slot].wait()
+        add_slots(
+            out_ref if half else conv_ref,
+            slots,
+            lambda slot: got_ref[block_ref[slot]],
+            weights,
+            conv_ref,
+        )
 
 
 def delta_out(blocks, got, conv_part, *sources):
@@ -665,7 +674,8 @@
     far = shifted(total_z[:size, size:], "z", 4)
 
     ws = swapped(last)
-    wfa, wfb = cyclic(wr[:size], "y", 1), cyclic(wl[size:], "y", -1)
+    wr_top, wl_rest = wr[:size], wl[size:]
+    wfa, wfb = cyclic(wr_top, "y", 1), cyclic(wl_rest, "y", -1)
     wsr, wsl = swapped(wr), swapped(wl)
     wsfa, wsfb = swapped(wfa), swapped(wfb)
     near = [last, ws, wr, wsr, wl, wsl]

time: 134 us -> 134 us (level)
  no operation moved by 1% of the time
where the time goes in v2:
time: 134 us; the launch traced here: 133 us
  starting transfers between devices  57.8 us (43%)
  Pallas kernels  33.1 us (25%)
  waiting for transfers between devices  24.7 us (18%)
  local copies, waits for them, and re-layouts  14.9 us (11%)
    ppermute x11, waiting for transfers between devices, cyclic(): lax.ppermute(block, axis, [(i, (i + distance) % count) for i in range(cou...  16.9 us
    ppermute x10, starting transfers between devices, swapped(): return lax.ppermute(block, 'c', [(0, 1), (1, 0)])  14.8 us
    ppermute x11, starting transfers between devices, cyclic(): lax.ppermute(block, axis, [(i, (i + distance) % count) for i in range(cou...  13.2 us
    ppermute x1, starting transfers between devices, shifted(): lax.ppermute(block, axis, [(i, i + distance) for i in devices if i + dist...  11 us
    pallas_call x1, Pallas kernels, project(): pl.pallas_call(functools.partial(project_kernel, width_all, head_size), i...  9.4 us
    unnamed x36, local copies, waits for them, and re-layouts  8.86 us
    all_to_all x1, starting transfers between devices, local(): lax.all_to_all(filtered.reshape(groups, rows // groups, 2 * size), TP, 0,...  7.47 us
    pallas_call x1, Pallas kernels, delta(): pl.pallas_call(delta_kernel, in_specs=[whole()] * 4, out_specs=[hbm(), hb...  6.4 us
  transfers between devices with their start and end apart: 28, of which 11 were waited for; matrix products, arithmetic and copies ran while one was open for 6% of the time, Pallas kernels for 22%

profile of v2, /device:TPU:1, one launch (start us, length us, event | category | flops | bytes accessed | tf_op | source)
XLA Modules:
  0.0 132.8 jit_solution(13135349973289407524)
XLA Ops:
  0.0 3.2 %collective-permute-start = (bf16[1024,256]{1,0:T(8,128)(2,1)}, bf16[1024,256]{1,0:T(8,128)(2,1)S(1)}, u32[]{:S(2)}, u32[]{:S(2)}) collective-permute-start(bf16[1024,256]{1,0:T(8,128)(2,1)} %refs_0_.1), channel_id=1, source_target_pairs={{0,1},{1,0},{2,3},{3,2},{4,5},{5,4},{6,7},{7,6},{8,9},{9,8},{10,11... | collective-permute-start | bytes 1572872 | tf_op jit(solution)/shard_map/ppermute | solution.py:373
  3.2 2.7 %collective-permute-start.2 = (bf16[1024,256]{1,0:T(8,128)(2,1)}, bf16[1024,256]{1,0:T(8,128)(2,1)}, u32[]{:S(2)}, u32[]{:S(2)}) collective-permute-start(bf16[1024,256]{1,0:T(8,128)(2,1)} %refs_0_.1), channel_id=1, source_target_pairs={{0,6},{2,0},{4,2},{6,4},{1,7},{3,1},{5,3},{7,5},{8,14},{10,8},{12,... | collective-permute-start | bytes 1572872 | tf_op jit(solution)/shard_map/ppermute | solution.py:364
  7.5 1.1 maximum_maximum_fusion.refs_17_
  8.7 9.5 %collective-permute-done.1.refs_2_ = bf16[1024,256]{1,0:T(8,128)(2,1)} collective-permute-done((bf16[1024,256]{1,0:T(8,128)(2,1)}, bf16[1024,256]{1,0:T(8,128)(2,1)}, u32[]{:S(2)}, u32[]{:S(2)}) %collective-permute-start.1) | collective-permute-done | bytes 524320 | tf_op jit(solution)/shard_map/ppermute | solution.py:364
  21.1 2.8 %collective-permute-start.7 = (bf16[512,256]{1,0:T(8,128)(2,1)S(1)}, bf16[512,256]{1,0:T(8,128)(2,1)}, u32[]{:S(2)}, u32[]{:S(2)}) collective-permute-start(bf16[512,256]{1,0:T(8,128)(2,1)S(1)} %slice.19), channel_id=1, source_target_pairs={{0,6},{2,0},{4,2},{6,4},{1,7},{3,1},{5,3},{7,5},{8,14},{10,8},{12,... | collective-permute-start | bytes 786440 | tf_op jit(solution)/shard_map/ppermute | solution.py:364
  25.2 1.5 %collective-permute-start.20 = (bf16[272,2048]{1,0:T(8,128)(2,1)S(1)}, bf16[272,2048]{1,0:T(8,128)(2,1)S(1)}, u32[]{:S(2)}, u32[]{:S(2)}) collective-permute-start(bf16[272,2048]{1,0:T(8,128)(2,1)S(1)} %fusion.1.refs_0_), channel_id=1, source_target_pairs={{0,6},{2,0},{4,2},{6,4},{1,7},{3,1},{5,3},{7,5},{8,14},{10,8},{12,... | collective-permute-start | bytes 3342344 | tf_op jit(solution)/shard_map/ppermute | solution.py:364
  26.7 2.6 %collective-permute-done.5.refs_6_ = bf16[512,256]{1,0:T(8,128)(2,1)} collective-permute-done((bf16[512,256]{1,0:T(8,128)(2,1)S(1)}, bf16[512,256]{1,0:T(8,128)(2,1)}, u32[]{:S(2)}, u32[]{:S(2)}) %collective-permute-start.5) | collective-permute-done | bytes 262176 | tf_op jit(solution)/shard_map/ppermute | solution.py:364
  29.3 1.8 %collective-permute-start.6 = (bf16[512,256]{1,0:T(8,128)(2,1)}, bf16[512,256]{1,0:T(8,128)(2,1)}, u32[]{:S(2)}, u32[]{:S(2)}) collective-permute-start(bf16[512,256]{1,0:T(8,128)(2,1)} %collective-permute-done.5.refs_6_), channel_id=1, source_target_pairs={{0,1},{1,0},{2,3},{3,2},{4,5},{5,4},{6,7},{7,6},{8,9},{9,8},{10,11... | collective-permute-start | bytes 786440 | tf_op jit(solution)/shard_map/ppermute | solution.py:373
  33.8 1.0 copy-done.9
  34.8 1.0 copy-done.11
  35.9 9.4 %project.1 = (bf16[1024,128]{1,0:T(8,128)(2,1)S(1)}, bf16[1024,128]{1,0:T(8,128)(2,1)S(1)}, bf16[1024,128]{1,0:T(8,128)(2,1)S(1)}, f32[1024,128]{1,0:T(8,128)S(1...) custom-call(s32[8]{0:T(128)S(1)} %stack.63.block_ref, f32[1]{0:T(128)S(6)} %exp.3.rate_ref, ...), custom_call_target="tpu_custom_call" | custom-call | flops 4294967296 | bytes 12582912 | tf_op jit(solution)/shard_map/project/pallas_call | solution.py:170
  45.3 6.4 %delta.1 = (bf16[1024,128]{1,0:T(8,128)(2,1)}, f32[1024,128]{1,0:T(8,128)}, bf16[144,256]{1,0:T(8,128)(2,1)S(1)}) custom-call(bf16[1024,128]{1,0:T(8,128)(2,1)S(1)} %get-tuple-element.26.q_ref, bf16[1024,128]{1,0:T(8,128)(2,1)S(1)} %get-tuple-element.27.k_ref, bf16[1024,128]{1,0:T(8,128)(2,1)S(1)} %get-tuple-element.28.v_ref, ...), custom_call_target="tpu_custom_call" | custom-call | flops 2013265920 | bytes 3145728 | tf_op jit(solution)/shard_map/delta/pallas_call | solution.py:308
  51.7 2.1 %collective-permute-start.9 = (bf16[144,256]{1,0:T(8,128)(2,1)S(1)}, bf16[144,256]{1,0:T(8,128)(2,1)S(1)}, u32[]{:S(2)}, u32[]{:S(2)}) collective-permute-start(bf16[144,256]{1,0:T(8,128)(2,1)S(1)} %get-tuple-element.33.p0), channel_id=1, source_target_pairs={{0,16},{8,24},{16,0},{24,8},{1,17},{9,25},{17,1},{25,9},{2,18},{10... | collective-permute-start | bytes 221192 | tf_op jit(solution)/shard_map/ppermute | solution.py:364
  55.3 1.7 %collective-permute-done.9.p1 = bf16[144,256]{1,0:T(8,128)(2,1)S(1)} collective-permute-done((bf16[144,256]{1,0:T(8,128)(2,1)S(1)}, bf16[144,256]{1,0:T(8,128)(2,1)S(1)}, u32[]{:S(2)}, u32[]{:S(2)}) %collective-permute-start.9) | collective-permute-done | bytes 73760 | tf_op jit(solution)/shard_map/ppermute | solution.py:364
  60.1 1.9 %along.2 = (bf16[144,256]{1,0:T(8,128)(2,1)}, bf16[144,256]{1,0:T(8,128)(2,1)S(1)}) custom-call(s32[1]{0:T(128)} %bitcast.16.place_ref, bf16[144,256]{1,0:T(8,128)(2,1)S(1)} %get-tuple-element.33.p0, bf16[144,256]{1,0:T(8,128)(2,1)S(1)} %copy-done.5, bf16[144,256]{1,0:T(8,128)(2,1)} %collective-permute-done.10.p2, bf16[144,256]{1,0:T(8,128)(2,1)} %collective-permute-done.11.p3), custom_call_target="tpu_custom_call" | custom-call | flops 16777216 | bytes 262144 | tf_op jit(solution)/shard_map/along/pallas_call | solution.py:346
  62.0 3.3 %collective-permute-start.12 = (bf16[144,256]{1,0:T(8,128)(2,1)S(1)}, bf16[144,256]{1,0:T(8,128)(2,1)S(1)}, u32[]{:S(2)}, u32[]{:S(2)}) collective-permute-start(bf16[144,256]{1,0:T(8,128)(2,1)S(1)} %get-tuple-element.34.p0), channel_id=1, source_target_pairs={{0,64},{32,96},{64,0},{96,32},{128,192},{160,224},{192,128},{224,1... | collective-permute-start | bytes 221192 | tf_op jit(solution)/shard_map/ppermute | solution.py:672
  65.4 1.4 %collective-permute-start.13 = (bf16[144,256]{1,0:T(8,128)(2,1)S(1)}, bf16[144,256]{1,0:T(8,128)(2,1)S(1)}, u32[]{:S(2)}, u32[]{:S(2)}) collective-permute-start(bf16[144,256]{1,0:T(8,128)(2,1)S(1)} %get-tuple-element.34.p0), channel_id=1, source_target_pairs={{0,96},{32,0},{64,32},{96,64},{128,224},{160,128},{192,160},{224,1... | collective-permute-start | bytes 221192 | tf_op jit(solution)/shard_map/ppermute | solution.py:672
  67.7 2.6 %collective-permute-start.22 = (bf16[144,2048]{1,0:T(8,128)(2,1)}, bf16[144,2048]{1,0:T(8,128)(2,1)}, u32[]{:S(2)}, u32[]{:S(2)}) collective-permute-start(bf16[144,2048]{1,0:T(8,128)(2,1)} %slice.24), channel_id=1, source_target_pairs={{0,6},{2,0},{4,2},{6,4},{1,7},{3,1},{5,3},{7,5},{8,14},{10,8},{12,... | collective-permute-start | bytes 1769480 | tf_op jit(solution)/shard_map/ppermute | solution.py:364
  70.3 2.4 %collective-permute-start.17 = (bf16[272,2048]{1,0:T(8,128)(2,1)S(1)}, bf16[272,2048]{1,0:T(8,128)(2,1)}, u32[]{:S(2)}, u32[]{:S(2)}) collective-permute-start(bf16[272,2048]{1,0:T(8,128)(2,1)S(1)} %fusion.1.refs_0_), channel_id=1, source_target_pairs={{0,1},{1,0},{2,3},{3,2},{4,5},{5,4},{6,7},{7,6},{8,9},{9,8},{10,11... | collective-permute-start | bytes 3342344 | tf_op jit(solution)/shard_map/ppermute | solution.py:373
  74.8 4.5 %collective-permute-done.14.p3 = bf16[144,256]{1,0:T(8,128)(2,1)S(1)} collective-permute-done((bf16[144,256]{1,0:T(8,128)(2,1)S(1)}, bf16[144,256]{1,0:T(8,128)(2,1)S(1)}, u32[]{:S(2)}, u32[]{:S(2)}) %collective-permute-start.14) | collective-permute-done | bytes 73760 | tf_op jit(solution)/shard_map/ppermute | solution.py:672
  80.0 1.3 collective-permute-start.16
  83.1 1.0 along.3
  84.1 11.0 %collective-permute-start.15 = (bf16[128,128]{1,0:T(8,128)(2,1)S(1)}, bf16[128,128]{1,0:T(8,128)(2,1)S(1)}, u32[]{:S(2)}, u32[]{:S(2)}) collective-permute-start(bf16[128,128]{1,0:T(8,128)(2,1)S(1)} %slice.20), channel_id=1, source_target_pairs={{0,128},{32,160},{64,192},{96,224},{1,129},{33,161},{65,193},{97,2... | collective-permute-start | bytes 98312 | tf_op jit(solution)/shard_map/ppermute | solution.py:369
  96.2 3.0 %conv.1 = bf16[1024,256]{1,0:T(8,128)(2,1)} custom-call(bf16[1024,128]{1,0:T(8,128)(2,1)} %get-tuple-element.38.gu_hbm, bf16[32,128]{1,0:T(8,128)(2,1)S(1)} %collective-permute-done.16.before_any, bf16[31,128]{1,0:T(8,128)(2,1)S(1)} %copy-done.6, bf16[1024,128]{1,0:T(8,128)(2,1)} %get-tuple-element.39.cg_hbm), custom_call_target="tpu_custom_call" | custom-call | flops 268435456 | bytes 1048576 | tf_op jit(solution)/shard_map/conv/pallas_call | solution.py:455
  99.2 7.5 %all-to-all-start.1 = ((bf16[8,128,256]{2,1,0:T(8,128)(2,1)}), bf16[8,128,256]{2,1,0:T(8,128)(2,1)}, u32[]{:S(2)}, u32[]{:S(2)}) async-start(bf16[8,128,256]{2,1,0:T(8,128)(2,1)} %bitcast.26), calls=%async_computation.1 | async-start | bytes 1048576 | tf_op jit(solution)/shard_map/all_to_all | solution.py:688
  106.8 1.5 %collective-permute-done.24.refs_6_ = bf16[128,2048]{1,0:T(8,128)(2,1)} collective-permute-done((bf16[128,2048]{1,0:T(8,128)(2,1)}, bf16[128,2048]{1,0:T(8,128)(2,1)}, u32[]{:S(2)}, u32[]{:S(2)}) %collective-permute-start.24) | collective-permute-done | bytes 524320 | tf_op jit(solution)/shard_map/ppermute | solution.py:364
  108.2 5.4 %collective-permute-start.25 = (bf16[128,2048]{1,0:T(8,128)(2,1)}, bf16[128,2048]{1,0:T(8,128)(2,1)}, u32[]{:S(2)}, u32[]{:S(2)}) collective-permute-start(bf16[128,2048]{1,0:T(8,128)(2,1)} %collective-permute-done.24.refs_6_), channel_id=1, source_target_pairs={{0,1},{1,0},{2,3},{3,2},{4,5},{5,4},{6,7},{7,6},{8,9},{9,8},{10,11... | collective-permute-start | bytes 1572872 | tf_op jit(solution)/shard_map/ppermute | solution.py:373
  113.6 2.4 %finish.1 = bf16[1024,128]{1,0:T(8,128)(2,1)} custom-call(bf16[1024,128]{1,0:T(8,128)(2,1)} %get-tuple-element.30.coef_p_hbm, f32[1024,128]{1,0:T(8,128)} %get-tuple-element.31.coef_q_hbm, bf16[1024,128]{1,0:T(8,128)(2,1)} %get-tuple-element.32.dg_hbm, f32[1,128]{1,0:T(1,128)S(1)} %bitcast.25, bf16[144,256]{1,0:T(8,128)(2,1)} %get-tuple-element.35.reach_any, ...), custom_call_target="tpu_custom_call" | custom-call | flops 67108864 | bytes 2097152 | tf_op jit(solution)/shard_map/finish/pallas_call | solution.py:414
  116.6 4.9 %all-to-all-start = ((bf16[8,128,128]{2,1,0:T(8,128)(2,1)}), bf16[8,128,128]{2,1,0:T(8,128)(2,1)}, u32[]{:S(2)}, u32[]{:S(2)}) async-start(bf16[8,128,128]{2,1,0:T(8,128)(2,1)} %bitcast.27), calls=%async_computation | async-start | bytes 524288 | tf_op jit(solution)/shard_map/all_to_all | solution.py:692
  121.6 4.5 %conv_out.1.conv_hbm = f32[128,2048]{1,0:T(8,128)} custom-call(s32[8]{0:T(128)S(1)} %stack.63.block_ref, bf16[8,128,256]{2,1,0:T(8,128)(2,1)} %all-to-all-done.1.got_hbm, bf16[272,2048]{1,0:T(8,128)(2,1)S(1)} %fusion.1.refs_0_, bf16[272,2048]{1,0:T(8,128)(2,1)} %collective-permute-done.17.refs_1_, bf16[272,2048]{1,0:T(8,128)(2,1)S(1)} %collective-permute-done.18.refs_2_, ...), custom_call_target="tpu_custom_call" | custom-call | flops 536870912 | bytes 6291456 | tf_op jit(solution)/shard_map/conv_out/pallas_call | solution.py:529
  126.2 2.0 %all-to-all-done.got_hbm = bf16[8,128,128]{2,1,0:T(8,128)(2,1)} async-done(((bf16[8,128,128]{2,1,0:T(8,128)(2,1)}), bf16[8,128,128]{2,1,0:T(8,128)(2,1)}, u32[]{:S(2)}, u32[]{:S(2)}) %all-to-all-start) | async-done | bytes 262176 | tf_op jit(solution)/shard_map/all_to_all | solution.py:692
  128.2 4.4 %delta_out.1 = bf16[128,2048]{1,0:T(8,128)(2,1)} custom-call(s32[8]{0:T(128)S(1)} %stack.63.block_ref, bf16[8,128,128]{2,1,0:T(8,128)(2,1)} %all-to-all-done.got_hbm, f32[128,2048]{1,0:T(8,128)} %conv_out.1.conv_hbm, bf16[272,2048]{1,0:T(8,128)(2,1)S(1)} %fusion.1.refs_0_, bf16[272,2048]{1,0:T(8,128)(2,1)} %collective-permute-done.17.refs_1_, ...), custom_call_target="tpu_custom_call" | custom-call | flops 536870912 | bytes 6291456 | tf_op jit(solution)/shard_map/delta_out/pallas_call | solution.py:576
  (83 shorter events, 19.7 us)
Async XLA Ops:
  0.0 7.4 %copy-start.15 = (f32[128]{0:T(128)S(1)}, f32[128]{0:T(128)}, u32[]{:S(2)}) copy-start(f32[128]{0:T(128)} %param.31) | copy-start | bytes 1540
  0.0 24.4 %collective-permute-start = (bf16[1024,256]{1,0:T(8,128)(2,1)}, bf16[1024,256]{1,0:T(8,128)(2,1)S(1)}, u32[]{:S(2)}, u32[]{:S(2)}) collective-permute-start(bf16[1024,256]{1,0:T(8,128)(2,1)} %refs_0_.1), channel_id=1, source_target_pairs={{0,1},{1,0},{2,3},{3,2},{4,5},{5,4},{6,7},{7,6},{8,9},{9,8},{10,11... | collective-permute-start | bytes 1572872 | tf_op jit(solution)/shard_map/ppermute | solution.py:373
  3.2 15.0 %collective-permute-start.1 = (bf16[1024,256]{1,0:T(8,128)(2,1)}, bf16[1024,256]{1,0:T(8,128)(2,1)}, u32[]{:S(2)}, u32[]{:S(2)}) collective-permute-start(bf16[1024,256]{1,0:T(8,128)(2,1)} %refs_0_.1), channel_id=1, source_target_pairs={{0,2},{2,4},{4,6},{6,0},{1,3},{3,5},{5,7},{7,1},{8,10},{10,12},{12... | collective-permute-start | bytes 1572872 | tf_op jit(solution)/shard_map/ppermute | solution.py:364
  3.2 15.0 %collective-permute-start.2 = (bf16[1024,256]{1,0:T(8,128)(2,1)}, bf16[1024,256]{1,0:T(8,128)(2,1)}, u32[]{:S(2)}, u32[]{:S(2)}) collective-permute-start(bf16[1024,256]{1,0:T(8,128)(2,1)} %refs_0_.1), channel_id=1, source_target_pairs={{0,6},{2,0},{4,2},{6,4},{1,7},{3,1},{5,3},{7,5},{8,14},{10,8},{12,... | collective-permute-start | bytes 1572872 | tf_op jit(solution)/shard_map/ppermute | solution.py:364
  8.6 23.3 %copy-start.16 = (f32[8]{0:T(128)S(1)}, f32[8]{0:T(128)}, u32[]{:S(2)}) copy-start(f32[8]{0:T(128)} %param.27) | copy-start | bytes 100
  18.2 12.9 %collective-permute-start.3 = (bf16[1024,256]{1,0:T(8,128)(2,1)}, bf16[1024,256]{1,0:T(8,128)(2,1)S(1)}, u32[]{:S(2)}, u32[]{:S(2)}) collective-permute-start(bf16[1024,256]{1,0:T(8,128)(2,1)} %collective-permute-done.1.refs_2_), channel_id=1, source_target_pairs={{0,1},{1,0},{2,3},{3,2},{4,5},{5,4},{6,7},{7,6},{8,9},{9,8},{10,11... | collective-permute-start | bytes 1572872 | tf_op jit(solution)/shard_map/ppermute | solution.py:373
  20.0 9.3 %collective-permute-start.5 = (bf16[512,256]{1,0:T(8,128)(2,1)S(1)}, bf16[512,256]{1,0:T(8,128)(2,1)}, u32[]{:S(2)}, u32[]{:S(2)}) collective-permute-start(bf16[512,256]{1,0:T(8,128)(2,1)S(1)} %slice.18), channel_id=1, source_target_pairs={{0,2},{2,4},{4,6},{6,0},{1,3},{3,5},{5,7},{7,1},{8,10},{10,12},{12... | collective-permute-start | bytes 786440 | tf_op jit(solution)/shard_map/ppermute | solution.py:364
  21.1 8.2 %collective-permute-start.7 = (bf16[512,256]{1,0:T(8,128)(2,1)S(1)}, bf16[512,256]{1,0:T(8,128)(2,1)}, u32[]{:S(2)}, u32[]{:S(2)}) collective-permute-start(bf16[512,256]{1,0:T(8,128)(2,1)S(1)} %slice.19), channel_id=1, source_target_pairs={{0,6},{2,0},{4,2},{6,4},{1,7},{3,1},{5,3},{7,5},{8,14},{10,8},{12,... | collective-permute-start | bytes 786440 | tf_op jit(solution)/shard_map/ppermute | solution.py:364
  23.9 9.4 %collective-permute-start.4 = (bf16[1024,256]{1,0:T(8,128)(2,1)}, bf16[1024,256]{1,0:T(8,128)(2,1)}, u32[]{:S(2)}, u32[]{:S(2)}) collective-permute-start(bf16[1024,256]{1,0:T(8,128)(2,1)} %collective-permute-done.2.refs_4_), channel_id=1, source_target_pairs={{0,1},{1,0},{2,3},{3,2},{4,5},{5,4},{6,7},{7,6},{8,9},{9,8},{10,11... | collective-permute-start | bytes 1572872 | tf_op jit(solution)/shard_map/ppermute | solution.py:373
  25.2 41.6 %collective-permute-start.20 = (bf16[272,2048]{1,0:T(8,128)(2,1)S(1)}, bf16[272,2048]{1,0:T(8,128)(2,1)S(1)}, u32[]{:S(2)}, u32[]{:S(2)}) collective-permute-start(bf16[272,2048]{1,0:T(8,128)(2,1)S(1)} %fusion.1.refs_0_), channel_id=1, source_target_pairs={{0,6},{2,0},{4,2},{6,4},{1,7},{3,1},{5,3},{7,5},{8,14},{10,8},{12,... | collective-permute-start | bytes 3342344 | tf_op jit(solution)/shard_map/ppermute | solution.py:364
  29.3 43.4 %collective-permute-start.18 = (bf16[272,2048]{1,0:T(8,128)(2,1)S(1)}, bf16[272,2048]{1,0:T(8,128)(2,1)S(1)}, u32[]{:S(2)}, u32[]{:S(2)}) collective-permute-start(bf16[272,2048]{1,0:T(8,128)(2,1)S(1)} %fusion.1.refs_0_), channel_id=1, source_target_pairs={{0,2},{2,4},{4,6},{6,0},{1,3},{3,5},{5,7},{7,1},{8,10},{10,12},{12... | collective-permute-start | bytes 3342344 | tf_op jit(solution)/shard_map/ppermute | solution.py:364
  29.3 4.0 %collective-permute-start.6 = (bf16[512,256]{1,0:T(8,128)(2,1)}, bf16[512,256]{1,0:T(8,128)(2,1)}, u32[]{:S(2)}, u32[]{:S(2)}) collective-permute-start(bf16[512,256]{1,0:T(8,128)(2,1)} %collective-permute-done.5.refs_6_), channel_id=1, source_target_pairs={{0,1},{1,0},{2,3},{3,2},{4,5},{5,4},{6,7},{7,6},{8,9},{9,8},{10,11... | collective-permute-start | bytes 786440 | tf_op jit(solution)/shard_map/ppermute | solution.py:373
  31.9 1.9 %collective-permute-start.8 = (bf16[512,256]{1,0:T(8,128)(2,1)}, bf16[512,256]{1,0:T(8,128)(2,1)}, u32[]{:S(2)}, u32[]{:S(2)}) collective-permute-start(bf16[512,256]{1,0:T(8,128)(2,1)} %collective-permute-done.7.refs_8_), channel_id=1, source_target_pairs={{0,1},{1,0},{2,3},{3,2},{4,5},{5,4},{6,7},{7,6},{8,9},{9,8},{10,11... | collective-permute-start | bytes 786440 | tf_op jit(solution)/shard_map/ppermute | solution.py:373
  51.7 5.3 %collective-permute-start.9 = (bf16[144,256]{1,0:T(8,128)(2,1)S(1)}, bf16[144,256]{1,0:T(8,128)(2,1)S(1)}, u32[]{:S(2)}, u32[]{:S(2)}) collective-permute-start(bf16[144,256]{1,0:T(8,128)(2,1)S(1)} %get-tuple-element.33.p0), channel_id=1, source_target_pairs={{0,16},{8,24},{16,0},{24,8},{1,17},{9,25},{17,1},{25,9},{2,18},{10... | collective-permute-start | bytes 221192 | tf_op jit(solution)/shard_map/ppermute | solution.py:364
  53.8 4.4 %collective-permute-start.10 = (bf16[144,256]{1,0:T(8,128)(2,1)S(1)}, bf16[144,256]{1,0:T(8,128)(2,1)}, u32[]{:S(2)}, u32[]{:S(2)}) collective-permute-start(bf16[144,256]{1,0:T(8,128)(2,1)S(1)} %get-tuple-element.33.p0), channel_id=1, source_target_pairs={{0,24},{8,0},{16,8},{24,16},{1,25},{9,1},{17,9},{25,17},{2,26},{10... | collective-permute-start | bytes 221192 | tf_op jit(solution)/shard_map/ppermute | solution.py:364
  54.7 4.5 %collective-permute-start.11 = (bf16[144,256]{1,0:T(8,128)(2,1)S(1)}, bf16[144,256]{1,0:T(8,128)(2,1)}, u32[]{:S(2)}, u32[]{:S(2)}) collective-permute-start(bf16[144,256]{1,0:T(8,128)(2,1)S(1)} %get-tuple-element.33.p0), channel_id=1, source_target_pairs={{0,8},{8,16},{16,24},{24,0},{1,9},{9,17},{17,25},{25,1},{2,10},{10... | collective-permute-start | bytes 221192 | tf_op jit(solution)/shard_map/ppermute | solution.py:364
  62.0 34.1 %copy-start.6 = (bf16[31,128]{1,0:T(8,128)(2,1)S(1)}, bf16[31,128]{1,0:T(8,128)(2,1)}, u32[]{:S(2)}) copy-start(bf16[31,128]{1,0:T(8,128)(2,1)} %taps_ref.1) | copy-start | bytes 23812
  62.0 10.6 %collective-permute-start.12 = (bf16[144,256]{1,0:T(8,128)(2,1)S(1)}, bf16[144,256]{1,0:T(8,128)(2,1)S(1)}, u32[]{:S(2)}, u32[]{:S(2)}) collective-permute-start(bf16[144,256]{1,0:T(8,128)(2,1)S(1)} %get-tuple-element.34.p0), channel_id=1, source_target_pairs={{0,64},{32,96},{64,0},{96,32},{128,192},{160,224},{192,128},{224,1... | collective-permute-start | bytes 221192 | tf_op jit(solution)/shard_map/ppermute | solution.py:672
  65.4 7.8 %collective-permute-start.13 = (bf16[144,256]{1,0:T(8,128)(2,1)S(1)}, bf16[144,256]{1,0:T(8,128)(2,1)S(1)}, u32[]{:S(2)}, u32[]{:S(2)}) collective-permute-start(bf16[144,256]{1,0:T(8,128)(2,1)S(1)} %get-tuple-element.34.p0), channel_id=1, source_target_pairs={{0,96},{32,0},{64,32},{96,64},{128,224},{160,128},{192,160},{224,1... | collective-permute-start | bytes 221192 | tf_op jit(solution)/shard_map/ppermute | solution.py:672
  67.7 39.0 %collective-permute-start.22 = (bf16[144,2048]{1,0:T(8,128)(2,1)}, bf16[144,2048]{1,0:T(8,128)(2,1)}, u32[]{:S(2)}, u32[]{:S(2)}) collective-permute-start(bf16[144,2048]{1,0:T(8,128)(2,1)} %slice.24), channel_id=1, source_target_pairs={{0,6},{2,0},{4,2},{6,4},{1,7},{3,1},{5,3},{7,5},{8,14},{10,8},{12,... | collective-permute-start | bytes 1769480 | tf_op jit(solution)/shard_map/ppermute | solution.py:364
  70.3 51.3 %collective-permute-start.17 = (bf16[272,2048]{1,0:T(8,128)(2,1)S(1)}, bf16[272,2048]{1,0:T(8,128)(2,1)}, u32[]{:S(2)}, u32[]{:S(2)}) collective-permute-start(bf16[272,2048]{1,0:T(8,128)(2,1)S(1)} %fusion.1.refs_0_), channel_id=1, source_target_pairs={{0,1},{1,0},{2,3},{3,2},{4,5},{5,4},{6,7},{7,6},{8,9},{9,8},{10,11... | collective-permute-start | bytes 3342344 | tf_op jit(solution)/shard_map/ppermute | solution.py:373
  72.7 48.9 %collective-permute-start.19 = (bf16[272,2048]{1,0:T(8,128)(2,1)S(1)}, bf16[272,2048]{1,0:T(8,128)(2,1)}, u32[]{:S(2)}, u32[]{:S(2)}) collective-permute-start(bf16[272,2048]{1,0:T(8,128)(2,1)S(1)} %collective-permute-done.18.refs_2_), channel_id=1, source_target_pairs={{0,1},{1,0},{2,3},{3,2},{4,5},{5,4},{6,7},{7,6},{8,9},{9,8},{10,11... | collective-permute-start | bytes 3342344 | tf_op jit(solution)/shard_map/ppermute | solution.py:373
  72.7 48.9 %collective-permute-start.21 = (bf16[272,2048]{1,0:T(8,128)(2,1)S(1)}, bf16[272,2048]{1,0:T(8,128)(2,1)}, u32[]{:S(2)}, u32[]{:S(2)}) collective-permute-start(bf16[272,2048]{1,0:T(8,128)(2,1)S(1)} %collective-permute-done.20.refs_4_), channel_id=1, source_target_pairs={{0,1},{1,0},{2,3},{3,2},{4,5},{5,4},{6,7},{7,6},{8,9},{9,8},{10,11... | collective-permute-start | bytes 3342344 | tf_op jit(solution)/shard_map/ppermute | solution.py:373
  73.8 5.5 %collective-permute-start.14 = (bf16[144,256]{1,0:T(8,128)(2,1)S(1)}, bf16[144,256]{1,0:T(8,128)(2,1)S(1)}, u32[]{:S(2)}, u32[]{:S(2)}) collective-permute-start(bf16[144,256]{1,0:T(8,128)(2,1)S(1)} %get-tuple-element.34.p0), channel_id=1, source_target_pairs={{0,32},{32,64},{64,96},{96,0},{128,160},{160,192},{192,224},{224,1... | collective-permute-start | bytes 221192 | tf_op jit(solution)/shard_map/ppermute | solution.py:672
  80.0 4.1 %collective-permute-start.16 = (bf16[32,128]{1,0:T(8,128)(2,1)S(1)}, bf16[32,128]{1,0:T(8,128)(2,1)S(1)}, u32[]{:S(2)}, u32[]{:S(2)}) collective-permute-start(bf16[32,128]{1,0:T(8,128)(2,1)S(1)} %slice.21), channel_id=1, source_target_pairs={{0,8},{8,16},{16,24},{24,32},{32,40},{40,48},{48,56},{56,64},{64,7... | collective-permute-start | bytes 24584 | tf_op jit(solution)/shard_map/ppermute | solution.py:685
  84.1 12.1 %collective-permute-start.15 = (bf16[128,128]{1,0:T(8,128)(2,1)S(1)}, bf16[128,128]{1,0:T(8,128)(2,1)S(1)}, u32[]{:S(2)}, u32[]{:S(2)}) collective-permute-start(bf16[128,128]{1,0:T(8,128)(2,1)S(1)} %slice.20), channel_id=1, source_target_pairs={{0,128},{32,160},{64,192},{96,224},{1,129},{33,161},{65,193},{97,2... | collective-permute-start | bytes 98312 | tf_op jit(solution)/shard_map/ppermute | solution.py:369
  96.0 17.5 %copy-start.7 = (f32[128]{0:T(128)S(1)}, f32[128]{0:T(128)}, u32[]{:S(2)}) copy-start(f32[128]{0:T(128)} %param.28) | copy-start | bytes 1540
  96.2 12.1 %collective-permute-start.24 = (bf16[128,2048]{1,0:T(8,128)(2,1)}, bf16[128,2048]{1,0:T(8,128)(2,1)}, u32[]{:S(2)}, u32[]{:S(2)}) collective-permute-start(bf16[128,2048]{1,0:T(8,128)(2,1)} %slice.25), channel_id=1, source_target_pairs={{0,2},{2,4},{4,6},{6,0},{1,3},{3,5},{5,7},{7,1},{8,10},{10,12},{12... | collective-permute-start | bytes 1572872 | tf_op jit(solution)/shard_map/ppermute | solution.py:364
  99.2 17.4 %all-to-all-start.1 = ((bf16[8,128,256]{2,1,0:T(8,128)(2,1)}), bf16[8,128,256]{2,1,0:T(8,128)(2,1)}, u32[]{:S(2)}, u32[]{:S(2)}) async-start(bf16[8,128,256]{2,1,0:T(8,128)(2,1)} %bitcast.26), calls=%async_computation.1 | async-start | bytes 1048576 | tf_op jit(solution)/shard_map/all_to_all | solution.py:688
  106.7 14.9 %collective-permute-start.23 = (bf16[144,2048]{1,0:T(8,128)(2,1)}, bf16[144,2048]{1,0:T(8,128)(2,1)}, u32[]{:S(2)}, u32[]{:S(2)}) collective-permute-start(bf16[144,2048]{1,0:T(8,128)(2,1)} %collective-permute-done.22.refs_6_), channel_id=1, source_target_pairs={{0,1},{1,0},{2,3},{3,2},{4,5},{5,4},{6,7},{7,6},{8,9},{9,8},{10,11... | collective-permute-start | bytes 1769480 | tf_op jit(solution)/shard_map/ppermute | solution.py:373
  108.2 20.0 %collective-permute-start.25 = (bf16[128,2048]{1,0:T(8,128)(2,1)}, bf16[128,2048]{1,0:T(8,128)(2,1)}, u32[]{:S(2)}, u32[]{:S(2)}) collective-permute-start(bf16[128,2048]{1,0:T(8,128)(2,1)} %collective-permute-done.24.refs_6_), channel_id=1, source_target_pairs={{0,1},{1,0},{2,3},{3,2},{4,5},{5,4},{6,7},{7,6},{8,9},{9,8},{10,11... | collective-permute-start | bytes 1572872 | tf_op jit(solution)/shard_map/ppermute | solution.py:373
  116.6 11.5 %all-to-all-start = ((bf16[8,128,128]{2,1,0:T(8,128)(2,1)}), bf16[8,128,128]{2,1,0:T(8,128)(2,1)}, u32[]{:S(2)}, u32[]{:S(2)}) async-start(bf16[8,128,128]{2,1,0:T(8,128)(2,1)} %bitcast.27), calls=%async_computation | async-start | bytes 524288 | tf_op jit(solution)/shard_map/all_to_all | solution.py:692
  (13 other events, 18.8 us)

commit v3 on v2

--- a/solution.py
+++ b/solution.py
@@ -14,6 +14,8 @@
 TINY_NORM = 1e-06
 TINY_VAR = 1e-05
 CHUNK = 128
+STEPS = (0, 1, -1, 2)
+GOES_TO = (0, 1, 4, 5, 2, 3, 6, 7)
 F32 = jnp.float32
 BF16 = jnp.bfloat16
 
@@ -32,6 +34,10 @@
 
 def home(array):
     return pltpu.with_memory_space_constraint(array, pltpu.HBM)
+
+
+def near_core(array):
+    return pltpu.with_memory_space_constraint(array, pltpu.VMEM)
 
 
 def fetch(sems, *pairs):
@@ -91,7 +97,7 @@
     own, sw, r1, sr1, l1, sl1, fa, sfa, fb, sfb = refs[:10]
     sides = refs[10:18]
     q_ref, k_ref, v_ref, bl_ref, dg_hbm, gu_hbm, cg_hbm = refs[18:25]
-    gathered, weights, dg_ref, gu_ref, cg_ref, sems, out_sems = refs[25:]
+    gathered, weights, factors, dg_ref, gu_ref, cg_ref, sems, out_sems = refs[25:]
     rows, piece_width = own.shape[0], own.shape[1]
     half = rows // 2
     places = [slice(0, half), slice(half, rows)]
@@ -117,49 +123,57 @@
         wide = low(raw).astype(F32)
         return wide * lax.rsqrt(jnp.sum(wide * wide, axis=-1, keepdims=True) + TINY_NORM)
 
-    def factor_of(n, pieces):
-        for one in pieces:
-            one.wait()
-        wide = gathered[places[n], :].astype(F32)
+    def pair(n, here):
+        both = dot(gathered[here, :], weights[n]) * factors[here, :]
+        return both[:, :128], both[:, 128:]
+
+    def each_half(body):
+        def step(n, carry):
+            body(n, pl.ds(pl.multiple_of(n * half, half), half))
+            return carry
+
+        lax.fori_loop(0, 2, step, 0)
+
+    def gated(n, here):
+        for which, pieces in enumerate((first + loads[:2], second)):
+
+            @pl.when(n == which)
+            def _():
+                for one in pieces:
+                    one.wait()
+
+        wide = gathered[here, :].astype(F32)
         squares = jnp.sum(wide * wide, axis=1, keepdims=True)
-        return lax.rsqrt(squares / width_all + TINY_NORM)
-
-    def pair(n, here, factor):
-        both = dot(gathered[here, :], weights[n]) * factor
-        return both[:, :128], both[:, 128:]
-
-    factors = []
-    for n, here in enumerate(places):
-        factor = factor_of(n, second if n else first[:8])
-        factors.append(factor)
-        if n == 0:
-            loads[0].wait()
-            loads[1].wait()
-        gv, gg = pair(0, here, factor)
+        factors[here, :] = lax.rsqrt(squares / width_all + TINY_NORM)
+        gv, gg = pair(0, here)
         gu_ref[here, :] = low(low(gv).astype(F32) * jax.nn.sigmoid(low(gg).astype(F32)))
-    stores = fetch(out_sems, (gu_ref, gu_hbm))
-    for one in loads[2 : 4]:
-        one.wait()
-    for here, factor in zip(places, factors):
-        dg, cg = pair(1, here, factor)
+
+    def gates(n, here):
+        dg, cg = pair(1, here)
         dg_ref[here, :] = low(dg)
         cg_ref[here, :] = low(cg)
-    stores += fetch(out_sems.at[pl.ds(1, 2)], (dg_ref, dg_hbm), (cg_ref, cg_hbm))
-    for one in loads[4 : 6]:
-        one.wait()
-    for here, factor in zip(places, factors):
-        q, k = pair(2, here, factor)
+
+    def queries(n, here):
+        q, k = pair(2, here)
         q_ref[here, :] = low(unit_rows(q) * head_size ** (-0.5))
         k_ref[here, :] = low(unit_rows(k))
-    for one in loads[6 : 8]:
-        one.wait()
-    for here, factor in zip(places, factors):
-        v, bl = pair(3, here, factor)
+
+    def rest_of(n, here):
+        v, bl = pair(3, here)
         v_ref[here, :] = low(v)
         lane = lax.broadcasted_iota(jnp.int32, bl.shape, 1)
         bl_ref[here, :] = jnp.where(
             lane == 0, jax.nn.sigmoid(bl), -rate_ref[0] * jax.nn.softplus(bl)
         )
+
+    each_half(gated)
+    stores = fetch(out_sems, (gu_ref, gu_hbm))
+    for n, body in enumerate((gates, queries, rest_of)):
+        for one in loads[2 * n + 2 : 2 * n + 4]:
+            one.wait()
+        each_half(body)
+        if n == 0:
+            stores += fetch(out_sems.at[pl.ds(1, 2)], (dg_ref, dg_hbm), (cg_ref, cg_hbm))
     for one in stores:
         one.wait()
 
@@ -176,6 +190,7 @@
         scratch_shapes=[
             pltpu.VMEM((rows, width_all), BF16),
             pltpu.VMEM((4, width_all, 256), BF16),
+            pltpu.VMEM((rows, 1), F32),
         ]
         + [pltpu.VMEM((rows, 128), BF16)] * 3
         + [pltpu.SemaphoreType.DMA((24,)), pltpu.SemaphoreType.DMA((3,))],
@@ -325,8 +340,8 @@
     )(q, k, v, bl)
 
 
-def along_kernel(place_ref, p0, p1, p2, p3, before_hbm, total_ref, held, kept, out_sem):
-    me = place_ref[0]
+def along_kernel(which, place_ref, p0, p1, p2, p3, before_ref, total_ref, held):
+    me = place_ref[which]
     for j, piece in ((0, p0), (2, p1), (3, p2), (1, p3)):
         held[(me - j + 4) & 3] = piece[...]
     size = p0.shape[1] // 2
@@ -336,27 +351,24 @@
     for m in range(1, 4):
         before = tuple(jnp.where(me == m, a, b) for a, b in zip(so_far, before))
         so_far = compose(read_state(held.at[m]), so_far)
-    write_state(kept, before)
-    (store,) = fetch(out_sem, (kept, before_hbm))
+    write_state(before_ref, before)
     write_state(total_ref, so_far)
-    store.wait()
-
-
-def along(place, state, *others):
+
+
+def along(which, places, state, *others):
     return pl.pallas_call(
-        along_kernel,
+        functools.partial(along_kernel, which),
         in_specs=[scalars()] + [whole()] * 4,
-        out_specs=[hbm(), whole()],
-        out_shape=[pltpu.HBM(state.shape, BF16), pltpu.VMEM(state.shape, BF16)],
-        scratch_shapes=[
-            pltpu.VMEM((4,) + state.shape, BF16),
+        out_specs=[whole(), whole()],
+        out_shape=[
+            jax.ShapeDtypeStruct(state.shape, BF16),
             pltpu.VMEM(state.shape, BF16),
-            pltpu.SemaphoreType.DMA((1,)),
         ],
+        scratch_shapes=[pltpu.VMEM((4,) + state.shape, BF16)],
         compiler_params=params(4),
         cost_estimate=cost(16 << 20, 1 << 18),
         name="along",
-    )(place[None].astype(jnp.int32), state, *others)
+    )(places, *map(near_core, (state,) + others))
 
 
 def cyclic(block, axis, distance):
@@ -373,9 +385,19 @@
     return lax.ppermute(block, "c", [(0, 1), (1, 0)])
 
 
+def exchanged(parts):
+    got = [parts[0]]
+    for slot in range(1, 8):
+        step, side = STEPS[slot // 2], slot % 2
+        route = [(y * 2 + c, (y + step) % 4 * 2 + (c ^ side)) for y in range(4) for c in range(2)]
+        got.append(lax.ppermute(parts[slot], TP, route))
+    return got
+
+
 def finish_kernel(
-    coef_p_hbm, coef_q_hbm, dg_hbm, gain_ref, reach_any, far_any, before_hbm, out_hbm, *scratch
+    block_ref, coef_p_hbm, coef_q_hbm, dg_hbm, gain_ref, reach_any, far_any, before_hbm, *rest
 ):
+    outs, scratch = rest[:8], rest[8:]
     coef_p_ref, coef_q_ref, dg_ref, reach_ref, far_ref, before_ref, out_ref, sems, out_sems = scratch
     loads = fetch(
         sems,
@@ -395,36 +417,40 @@
     for one in loads[3:]:
         one.wait()
     stores = []
-    step = out_ref.shape[0] // 4
-    for n in range(4):
-        here = slice(n * step, (n + 1) * step)
+    step = out_ref.shape[1]
+    for slot in range(8):
+        here = pl.ds(pl.multiple_of(block_ref[GOES_TO[slot]] * step, step), step)
         result = coef_q_ref[here, :] + dot(coef_p_ref[here, :], state)
         mean = jnp.sum(result * result, axis=-1, keepdims=True) * (1.0 / result.shape[1])
         result = result * lax.rsqrt(mean + TINY_NORM) * gain_ref[...]
-        out_ref[here, :] = low(result * jax.nn.silu(dg_ref[here, :].astype(F32)))
-        stores += fetch(out_sems.at[pl.ds(n, 1)], (out_ref.at[here, :], out_hbm.at[here, :]))
+        out_ref[slot] = low(result * jax.nn.silu(dg_ref[here, :].astype(F32)))
+        stores += fetch(out_sems.at[pl.ds(slot, 1)], (out_ref.at[slot], outs[slot]))
     for one in stores:
         one.wait()
 
 
-def finish(coef_p, coef_q, dg, gain, reach, far, before):
-    coef_p, coef_q, dg, before, reach = map(home, (coef_p, coef_q, dg, before, reach))
+def finish(blocks, coef_p, coef_q, dg, gain, reach, far, before):
+    coef_p, coef_q, dg = map(home, (coef_p, coef_q, dg))
+    rows, size = dg.shape
     args = (coef_p, coef_q, dg, gain, reach, far, before)
-    copied = (coef_p, coef_q, dg, reach, far, before, dg)
+    copied = (coef_p, coef_q, dg, reach, far, before)
     return pl.pallas_call(
         finish_kernel,
-        in_specs=[hbm(), hbm(), hbm(), whole(), anywhere(), anywhere(), hbm()],
-        out_specs=hbm(),
-        out_shape=pltpu.HBM(dg.shape, BF16),
+        in_specs=[scalars(), hbm(), hbm(), hbm(), whole(), anywhere(), anywhere(), anywhere()],
+        out_specs=[hbm()] * 8,
+        out_shape=[pltpu.HBM((rows // 8, size), BF16)] * 8,
         scratch_shapes=[pltpu.VMEM(a.shape, a.dtype) for a in copied]
-        + [pltpu.SemaphoreType.DMA((6,)), pltpu.SemaphoreType.DMA((4,))],
+        + [pltpu.VMEM((8, rows // 8, size), BF16)]
+        + [pltpu.SemaphoreType.DMA((6,)), pltpu.SemaphoreType.DMA((8,))],
         compiler_params=params(8),
         cost_estimate=cost(64 << 20, 2 << 20),
         name="finish",
-    )(*args)
-
-
-def conv_kernel(gu_hbm, before_any, taps_ref, cg_hbm, out_hbm, gu_ref, before_ref, padded, out_ref, sems, out_sems):
+    )(blocks, *args)
+
+
+def conv_kernel(block_ref, gu_hbm, before_any, taps_ref, cg_hbm, *rest):
+    outs = rest[:8]
+    gu_ref, before_ref, padded, out_ref, sems, out_sems = rest[8:]
     rows, size = gu_ref.shape
     head = before_ref.shape[0]
     count = taps_ref.shape[0]
@@ -437,56 +463,99 @@
     taps = taps_ref[...].astype(F32)
     step = 64
     skip = head - (count - 1)
-    gate.wait()
-    stores = []
-    for n, base in enumerate(range(0, rows, step)):
+
+    def block(n, carry):
+        base = pl.multiple_of(n * step, step)
         total = jnp.zeros((step, size), F32)
         for j in range(count):
-            total = total + padded[base + skip + j : base + skip + j + step, :] * taps[j : j + 1, :]
-        here = slice(base, base + step)
-        out_ref[here, 0:size] = low(total)
-        stores += fetch(out_sems.at[pl.ds(n, 1)], (out_ref.at[here, :], out_hbm.at[here, :]))
-    for one in stores:
-        one.wait()
-
-
-def conv(gu, before, taps, cg):
+            total = total + padded[pl.ds(base + skip + j, step), :] * taps[j : j + 1, :]
+        out_ref[pl.ds(base, step), 0:size] = low(total)
+        return carry
+
+    lax.fori_loop(0, rows // step, block, 0)
+    gate.wait()
+    part = rows // 8
+    pairs = []
+    for slot in range(8):
+        here = pl.ds(pl.multiple_of(block_ref[GOES_TO[slot]] * part, part), part)
+        pairs.append((out_ref.at[here, :], outs[slot]))
+    for one in fetch(out_sems, *pairs):
+        one.wait()
+
+
+def conv(blocks, gu, before, taps, cg):
     rows, size = gu.shape
     return pl.pallas_call(
         conv_kernel,
-        in_specs=[hbm(), anywhere(), whole(), hbm()],
-        out_specs=hbm(),
-        out_shape=pltpu.HBM((rows, 2 * size), BF16),
+        in_specs=[scalars(), hbm(), anywhere(), whole(), hbm()],
+        out_specs=[hbm()] * 8,
+        out_shape=[pltpu.HBM((rows // 8, 2 * size), BF16)] * 8,
         scratch_shapes=[
             pltpu.VMEM(gu.shape, BF16),
             pltpu.VMEM(before.shape, BF16),
             pltpu.VMEM((rows + before.shape[0], size), F32),
             pltpu.VMEM((rows, 2 * size), BF16),
             pltpu.SemaphoreType.DMA((3,)),
-            pltpu.SemaphoreType.DMA((rows // 64,)),
+            pltpu.SemaphoreType.DMA((8,)),
         ],
         compiler_params=params(8),
         cost_estimate=cost(256 << 20, 1 << 20),
         name="conv",
-    )(home(gu), before, taps, home(cg))
+    )(blocks, home(gu), before, taps, home(cg))
 
 
 def add_slots(out_ref, slots, left, weights, start):
-    width = out_ref.shape[1]
     size = weights.shape[1] - weights.shape[1] % 128
-    for base in range(0, width, 512):
-        here = slice(base, base + 512)
+
+    def step(n, carry):
+        here = pl.ds(pl.multiple_of(n * 512, 512), 512)
         acc = jnp.zeros((out_ref.shape[0], 512), F32) if start is None else start[:, here]
         for slot in slots:
             acc = acc + dot(left(slot), weights[slot, 0:size, here])
         out_ref[:, here] = acc.astype(out_ref.dtype)
-
-
-def conv_out_kernel(block_ref, got_hbm, *refs):
-    sources, out_hbm = refs[:8], refs[8]
-    got_ref, weights, mixed, out_ref, sems, out_sems = refs[9:]
+        return carry
+
+    lax.fori_loop(0, out_ref.shape[1] // 512, step, 0)
+
+
+def cut_kernel(right_any, left_any, top_hbm, rest_hbm, top, rest, sems):
+    count = top.shape[0]
+    inward = fetch(
+        sems,
+        (right_any.at[pl.ds(0, count), :], top),
+        (left_any.at[pl.ds(count, rest.shape[0]), :], rest),
+    )
+    outward = []
+    for n, pair in enumerate(((top, top_hbm), (rest, rest_hbm))):
+        inward[n].wait()
+        outward += fetch(sems.at[pl.ds(2 + n, 1)], pair)
+    for one in outward:
+        one.wait()
+
+
+def cut(right, left, count):
+    rows, width = right.shape
+    shapes = [(count, width), (rows - count, width)]
+    return pl.pallas_call(
+        cut_kernel,
+        in_specs=[anywhere()] * 2,
+        out_specs=[hbm()] * 2,
+        out_shape=[pltpu.HBM(shape, BF16) for shape in shapes],
+        scratch_shapes=[pltpu.VMEM(shape, BF16) for shape in shapes]
+        + [pltpu.SemaphoreType.DMA((4,))],
+        compiler_params=params(4),
+        cost_estimate=cost(1 << 20, 4 << 20),
+        name="cut",
+    )(right, left)
+
+
+def conv_out_kernel(*refs):
+    got, sources, out_hbm = refs[:8], refs[8:16], refs[16]
+    got_ref, weights, mixed, out_ref, sems, out_sems = refs[17:]
     groups, rows, size = mixed.shape
-    (load,) = fetch(sems.at[pl.ds(8, 1)], (got_hbm, got_ref))
+    got_loads = fetch(
+        sems.at[pl.ds(8, 8)], *((ref, got_ref.at[slot]) for slot, ref in enumerate(got))
+    )
     loads = fetch(
         sems,
         *(
@@ -494,7 +563,8 @@
             for slot, ref in enumerate(sources)
         ),
     )
-    load.wait()
+    for one in got_loads:
+        one.wait()
     total = jnp.zeros((rows, size), F32)
     total_square = jnp.zeros((rows, size), F32)
     for g in range(groups):
@@ -509,12 +579,11 @@
         slots = range(half * 4, half * 4 + 4)
         for slot in slots:
             loads[slot].wait()
-            g = block_ref[slot]
             extra = weights[slot, size : size + 16, :].astype(F32)
             gain = extra[0:1, 0:size] + extra[1:2, 0:size] + extra[2:3, 0:size]
             shift = extra[3:4, 0:size] + extra[4:5, 0:size] + extra[5:6, 0:size]
-            normed = (got_ref[g, :, 0:size].astype(F32) - center) * factor * gain + shift
-            gate = got_ref[g, :, size:].astype(F32)
+            normed = (got_ref[slot, :, 0:size].astype(F32) - center) * factor * gain + shift
+            gate = got_ref[slot, :, size:].astype(F32)
             mixed[slot] = low(jax.nn.silu(normed) * jax.nn.silu(gate))
         add_slots(
             out_ref, slots, lambda slot: mixed[slot], weights, out_ref if half else None
@@ -523,71 +592,73 @@
     store.wait()
 
 
-def conv_out(blocks, got, *sources):
-    groups, rows, both = got.shape
+def conv_out(got, sources):
+    groups = len(got)
+    rows, both = got[0].shape
     size, width = both // 2, sources[0].shape[1]
     return pl.pallas_call(
         conv_out_kernel,
-        in_specs=[scalars()] + [anywhere()] * 9,
+        in_specs=[anywhere()] * 16,
         out_specs=hbm(),
         out_shape=pltpu.HBM((rows, width), F32),
         scratch_shapes=[
-            pltpu.VMEM(got.shape, BF16),
+            pltpu.VMEM((groups, rows, both), BF16),
             pltpu.VMEM((groups, size + 16, width), BF16),
             pltpu.VMEM((groups, rows, size), BF16),
             pltpu.VMEM((rows, width), F32),
-            pltpu.SemaphoreType.DMA((9,)),
+            pltpu.SemaphoreType.DMA((16,)),
             pltpu.SemaphoreType.DMA((1,)),
         ],
         compiler_params=params(12),
         cost_estimate=cost(2 * rows * 1024 * width, 6 << 20),
         name="conv_out",
-    )(blocks, got, *sources)
-
-
-def delta_out_kernel(block_ref, got_hbm, conv_hbm, *refs):
-    sources, out_ref = refs[:8], refs[8]
-    got_ref, weights, conv_ref, sems = refs[9:]
+    )(*got, *sources)
+
+
+def delta_out_kernel(conv_hbm, *refs):
+    got, sources, out_ref = refs[:8], refs[8:16], refs[16]
+    got_ref, weights, conv_ref, sems = refs[17:]
     size = got_ref.shape[1]
     loads = fetch(
         sems,
-        (got_hbm, got_ref),
         (conv_hbm, conv_ref),
+        *((ref, got_ref.at[slot]) for slot, ref in enumerate(got)),
         *((ref.at[pl.ds(0, size), :], weights.at[slot]) for slot, ref in enumerate(sources)),
     )
-    loads[0].wait()
-    loads[1].wait()
+    for one in loads[:9]:
+        one.wait()
     for half in range(2):
         slots = range(half * 4, half * 4 + 4)
         for slot in slots:
-            loads[2 + slot].wait()
+            loads[9 + slot].wait()
         add_slots(
             out_ref if half else conv_ref,
             slots,
-            lambda slot: got_ref[block_ref[slot]],
+            lambda slot: got_ref[slot],
             weights,
             conv_ref,
         )
 
 
-def delta_out(blocks, got, conv_part, *sources):
-    groups, rows, size = got.shape
+def delta_out(got, conv_part, sources):
+    groups = len(got)
+    rows, size = got[0].shape
     width = conv_part.shape[1]
     return pl.pallas_call(
         delta_out_kernel,
-        in_specs=[scalars()] + [anywhere()] * 10,
+        in_specs=[anywhere()] * 17,
         out_specs=whole(),
         out_shape=jax.ShapeDtypeStruct((rows, width), BF16),
         scratch_shapes=[
-            pltpu.VMEM(got.shape, BF16),
+            pltpu.VMEM((groups, rows, size), BF16),
             pltpu.VMEM((groups, size, width), BF16),
             pltpu.VMEM(conv_part.shape, F32),
-            pltpu.SemaphoreType.DMA((10,)),
+            pltpu.SemaphoreType.DMA((17,)),
         ],
         compiler_params=params(12),
         cost_estimate=cost(2 * rows * 1024 * width, 6 << 20),
         name="delta_out",
-    )(blocks, got, home(conv_part), *sources)
+    )(home(conv_part), *got, *sources)
 
 
 def local(
@@ -617,7 +688,8 @@
     count_y = lax.axis_size("y")
     head = y * 2 + core
     chips = [y, (y - 1) % count_y, (y + 1) % count_y, (y + 2) % count_y]
-    blocks = jnp.stack([chip * 2 + side for chip in chips for side in (core, 1 - core)])
+    slots = [chip * 2 + side for chip in chips for side in (core, 1 - core)]
+    blocks = jnp.stack(slots + [x, z % 4])
     blocks = blocks.astype(jnp.int32)
 
     beta_decay = jnp.concatenate(
@@ -665,16 +737,16 @@
     coef_p, coef_q, state = delta(q, k, v, bl)
 
 
-    before, total = along(x, state, *(cyclic(state, "x", j) for j in (2, 3, 1)))
+    before, total = along(8, blocks, state, *(cyclic(state, "x", j) for j in (2, 3, 1)))
     route = lambda j: [(h + i, h + (i + j) % 4) for h in (0, 4) for i in range(4)]
     around = []
     for j in (2, 3, 1):
         around.append(lax.ppermute(total, "z", route(j)))
-    before_z, total_z = along(z % 4, total, *around)
+    before_z, total_z = along(9, blocks, total, *around)
     far = shifted(total_z[:size, size:], "z", 4)
 
     ws = swapped(last)
-    wr_top, wl_rest = wr[:size], wl[size:]
+    wr_top, wl_rest = cut(wr, wl, size)
     wfa, wfb = cyclic(wr_top, "y", 1), cyclic(wl_rest, "y", -1)
     wsr, wsl = swapped(wr), swapped(wl)
     wsfa, wsfb = swapped(wfa), swapped(wfb)
@@ -683,14 +755,12 @@
     conv_weights = near + [wfb, wsfb]
 
     halo = lax.ppermute(gu[rows - 32 :], SP, [(i, i + 1) for i in range(31)])
-    filtered = conv(gu, halo, conv_taps, cg)
-    groups = 8
-    got = lax.all_to_all(filtered.reshape(groups, rows // groups, 2 * size), TP, 0, 0, tiled=True)
-    conv_part = conv_out(blocks, got, *conv_weights)
-
-    mixed = finish(coef_p, coef_q, dg, head_gain[None, :], before_z, far, before)
-    mixed = lax.all_to_all(mixed.reshape(groups, rows // groups, size), TP, 0, 0, tiled=True)
-    return delta_out(blocks, mixed, conv_part, *delta_weights)
+    filtered = conv(blocks, gu, halo, conv_taps, cg)
+    got = exchanged(filtered)
+    conv_part = conv_out(got, conv_weights)
+
+    mixed = finish(blocks, coef_p, coef_q, dg, head_gain[None, :], before_z, far, before)
+    return delta_out(exchanged(mixed), conv_part, delta_weights)
 
 
 def solution(mesh):

time: 134 us -> 144 us (1.075)
  the two profiles are of different devices: /device:TPU:1 before, /device:TPU:239 now
where the time goes in v3:
time: 144 us; the launch traced here: 143 us
  starting transfers between devices  53.6 us (37%)
  waiting for transfers between devices  41.2 us (29%)
  Pallas kernels  36 us (25%)
  local copies, waits for them, and re-layouts  10.1 us (7%)
    ppermute x11, waiting for transfers between devices, cyclic(): lax.ppermute(block, axis, [(i, (i + distance) % count) for i in range(cou...  23.7 us
    ppermute x14, starting transfers between devices, exchanged(): got.append(lax.ppermute(parts[slot], TP, route))  22 us
    ppermute x11, starting transfers between devices, cyclic(): lax.ppermute(block, axis, [(i, (i + distance) % count) for i in range(cou...  12 us
    ppermute x10, starting transfers between devices, swapped(): return lax.ppermute(block, 'c', [(0, 1), (1, 0)])  11.3 us
    pallas_call x1, Pallas kernels, project(): pl.pallas_call(functools.partial(project_kernel, width_all, head_size), i...  9.13 us
    ppermute x14, waiting for transfers between devices, exchanged(): got.append(lax.ppermute(parts[slot], TP, route))  6.98 us
    pallas_call x1, Pallas kernels, delta(): pl.pallas_call(delta_kernel, in_specs=[whole()] * 4, out_specs=[hbm(), hb...  6.41 us
    unnamed x36, local copies, waits for them, and re-layouts  5.81 us
  transfers between devices with their start and end apart: 40, of which 12 were waited for; matrix products, arithmetic and copies ran while one was open for 4% of the time, Pallas kernels for 22%

profile of v3, /device:TPU:239, one launch (start us, length us, event | category | flops | bytes accessed | tf_op | source)
XLA Modules:
  0.0 143.4 jit_solution(8955653312561408394)
XLA Ops:
  0.0 1.3 collective-permute-start.1
  5.6 7.6 %collective-permute-done.1.refs_2_ = bf16[1024,256]{1,0:T(8,128)(2,1)} collective-permute-done((bf16[1024,256]{1,0:T(8,128)(2,1)}, bf16[1024,256]{1,0:T(8,128)(2,1)}, u32[]{:S(2)}, u32[]{:S(2)}) %collective-permute-start.1) | collective-permute-done | bytes 524320 | tf_op jit(solution)/shard_map/ppermute | solution.py:376
  17.7 3.5 %collective-permute-done.5.refs_6_ = bf16[512,256]{1,0:T(8,128)(2,1)S(1)} collective-permute-done((bf16[512,256]{1,0:T(8,128)(2,1)S(1)}, bf16[512,256]{1,0:T(8,128)(2,1)S(1)}, u32[]{:S(2)}, u32[]{:S(2)}) %collective-permute-start.5) | collective-permute-done | bytes 262176 | tf_op jit(solution)/shard_map/ppermute | solution.py:376
  21.2 2.7 %collective-permute-start.6 = (bf16[512,256]{1,0:T(8,128)(2,1)S(1)}, bf16[512,256]{1,0:T(8,128)(2,1)S(1)}, u32[]{:S(2)}, u32[]{:S(2)}) collective-permute-start(bf16[512,256]{1,0:T(8,128)(2,1)S(1)} %collective-permute-done.5.refs_6_), channel_id=1, source_target_pairs={{0,1},{1,0},{2,3},{3,2},{4,5},{5,4},{6,7},{7,6},{8,9},{9,8},{10,11... | collective-permute-start | bytes 786440 | tf_op jit(solution)/shard_map/ppermute | solution.py:385
  33.2 9.1 %project.1 = (bf16[1024,128]{1,0:T(8,128)(2,1)S(1)}, bf16[1024,128]{1,0:T(8,128)(2,1)S(1)}, bf16[1024,128]{1,0:T(8,128)(2,1)S(1)}, f32[1024,128]{1,0:T(8,128)S(1...) custom-call(s32[10]{0:T(128)S(1)} %stack.71.block_ref.place_ref, ...), custom_call_target="tpu_custom_call" | custom-call | flops 4294967296 | bytes 12582912 | tf_op jit(solution)/shard_map/project/pallas_call | solution.py:184
  42.3 6.4 %delta.1 = (bf16[1024,128]{1,0:T(8,128)(2,1)}, f32[1024,128]{1,0:T(8,128)}, bf16[144,256]{1,0:T(8,128)(2,1)S(1)}) custom-call(bf16[1024,128]{1,0:T(8,128)(2,1)S(1)} %get-tuple-element.56.q_ref, bf16[1024,128]{1,0:T(8,128)(2,1)S(1)} %get-tuple-element.57.k_ref, bf16[1024,128]{1,0:T(8,128)(2,1)S(1)} %get-tuple-element.58.v_ref, ...), custom_call_target="tpu_custom_call" | custom-call | flops 2013265920 | bytes 3145728 | tf_op jit(solution)/shard_map/delta/pallas_call | solution.py:323
  51.9 3.5 %collective-permute-done.9.before_any = bf16[32,128]{1,0:T(8,128)(2,1)S(1)} collective-permute-done((bf16[32,128]{1,0:T(8,128)(2,1)S(1)}, bf16[32,128]{1,0:T(8,128)(2,1)S(1)}, u32[]{:S(2)}, u32[]{:S(2)}) %collective-permute-start.9) | collective-permute-done | bytes 8224 | tf_op jit(solution)/shard_map/ppermute | solution.py:757
  55.4 4.4 %collective-permute-start.26 = (bf16[144,256]{1,0:T(8,128)(2,1)S(1)}, bf16[144,256]{1,0:T(8,128)(2,1)S(1)}, u32[]{:S(2)}, u32[]{:S(2)}) collective-permute-start(bf16[144,256]{1,0:T(8,128)(2,1)S(1)} %get-tuple-element.63.p0), channel_id=1, source_target_pairs={{0,8},{8,16},{16,24},{24,0},{1,9},{9,17},{17,25},{25,1},{2,10},{10... | collective-permute-start | bytes 221192 | tf_op jit(solution)/shard_map/ppermute | solution.py:376
  59.8 4.0 %conv.1 = (bf16[128,256]{1,0:T(8,128)(2,1)}, bf16[128,256]{1,0:T(8,128)(2,1)}, bf16[128,256]{1,0:T(8,128)(2,1)}, bf16[128,256]{1,0:T(8,128)(2,1)}, bf16[128,256]...) custom-call(s32[10]{0:T(128)S(1)} %stack.71.block_ref.place_ref, ...), custom_call_target="tpu_custom_call" | custom-call | flops 268435456 | bytes 1048576 | tf_op jit(solution)/shard_map/conv/pallas_call | solution.py:488
  63.8 2.4 %collective-permute-start.10 = (bf16[128,256]{1,0:T(8,128)(2,1)}, bf16[128,256]{1,0:T(8,128)(2,1)S(1)}, u32[]{:S(2)}, u32[]{:S(2)}) collective-permute-start(bf16[128,256]{1,0:T(8,128)(2,1)} %get-tuple-element.47), channel_id=1, source_target_pairs={{0,1},{1,0},{2,3},{3,2},{4,5},{5,4},{6,7},{7,6},{8,9},{9,8},{10,11... | collective-permute-start | bytes 196616 | tf_op jit(solution)/shard_map/ppermute | solution.py:393
  67.2 1.7 %collective-permute-start.12 = (bf16[128,256]{1,0:T(8,128)(2,1)}, bf16[128,256]{1,0:T(8,128)(2,1)S(1)}, u32[]{:S(2)}, u32[]{:S(2)}) collective-permute-start(bf16[128,256]{1,0:T(8,128)(2,1)} %get-tuple-element.49), channel_id=1, source_target_pairs={{0,3},{1,2},{2,5},{3,4},{4,7},{5,6},{6,1},{7,0},{8,11},{9,10},{10,... | collective-permute-start | bytes 196616 | tf_op jit(solution)/shard_map/ppermute | solution.py:393
  70.0 1.5 %collective-permute-start.27 = (bf16[144,256]{1,0:T(8,128)(2,1)S(1)}, bf16[144,256]{1,0:T(8,128)(2,1)S(1)}, u32[]{:S(2)}, u32[]{:S(2)}) collective-permute-start(bf16[144,256]{1,0:T(8,128)(2,1)S(1)} %get-tuple-element.64.p0), channel_id=1, source_target_pairs={{0,64},{32,96},{64,0},{96,32},{128,192},{160,224},{192,128},{224,1... | collective-permute-start | bytes 221192 | tf_op jit(solution)/shard_map/ppermute | solution.py:744
  71.7 1.7 %collective-permute-start.28 = (bf16[144,256]{1,0:T(8,128)(2,1)S(1)}, bf16[144,256]{1,0:T(8,128)(2,1)S(1)}, u32[]{:S(2)}, u32[]{:S(2)}) collective-permute-start(bf16[144,256]{1,0:T(8,128)(2,1)S(1)} %get-tuple-element.64.p0), channel_id=1, source_target_pairs={{0,96},{32,0},{64,32},{96,64},{128,224},{160,128},{192,160},{224,1... | collective-permute-start | bytes 221192 | tf_op jit(solution)/shard_map/ppermute | solution.py:744
  73.4 2.5 %collective-permute-start.29 = (bf16[144,256]{1,0:T(8,128)(2,1)S(1)}, bf16[144,256]{1,0:T(8,128)(2,1)S(1)}, u32[]{:S(2)}, u32[]{:S(2)}) collective-permute-start(bf16[144,256]{1,0:T(8,128)(2,1)S(1)} %get-tuple-element.64.p0), channel_id=1, source_target_pairs={{0,32},{32,64},{64,96},{96,0},{128,160},{160,192},{192,224},{224,1... | collective-permute-start | bytes 221192 | tf_op jit(solution)/shard_map/ppermute | solution.py:744
  76.0 1.3 collective-permute-done.27.p1
  77.3 1.5 %collective-permute-start.13 = (bf16[128,256]{1,0:T(8,128)(2,1)}, bf16[128,256]{1,0:T(8,128)(2,1)S(1)}, u32[]{:S(2)}, u32[]{:S(2)}) collective-permute-start(bf16[128,256]{1,0:T(8,128)(2,1)} %get-tuple-element.50), channel_id=1, source_target_pairs={{0,6},{1,7},{2,0},{3,1},{4,2},{5,3},{6,4},{7,5},{8,14},{9,15},{10,... | collective-permute-start | bytes 196616 | tf_op jit(solution)/shard_map/ppermute | solution.py:393
  78.8 4.0 %collective-permute-start.14 = (bf16[128,256]{1,0:T(8,128)(2,1)}, bf16[128,256]{1,0:T(8,128)(2,1)S(1)}, u32[]{:S(2)}, u32[]{:S(2)}) collective-permute-start(bf16[128,256]{1,0:T(8,128)(2,1)} %get-tuple-element.51), channel_id=1, source_target_pairs={{0,7},{1,6},{2,1},{3,0},{4,3},{5,2},{6,5},{7,4},{8,15},{9,14},{10,... | collective-permute-start | bytes 196616 | tf_op jit(solution)/shard_map/ppermute | solution.py:393
  85.7 1.4 collective-permute-start.16
  88.2 1.3 collective-permute-start.30
  89.5 1.5 %collective-permute-start.17 = (bf16[272,2048]{1,0:T(8,128)(2,1)S(1)}, bf16[272,2048]{1,0:T(8,128)(2,1)S(1)}, u32[]{:S(2)}, u32[]{:S(2)}) collective-permute-start(bf16[272,2048]{1,0:T(8,128)(2,1)S(1)} %fusion.1.refs_8_), channel_id=1, source_target_pairs={{0,1},{1,0},{2,3},{3,2},{4,5},{5,4},{6,7},{7,6},{8,9},{9,8},{10,11... | collective-permute-start | bytes 3342344 | tf_op jit(solution)/shard_map/ppermute | solution.py:385
  91.1 5.7 %collective-permute-done.30.far_any = bf16[128,128]{1,0:T(8,128)(2,1)S(1)} collective-permute-done((bf16[128,128]{1,0:T(8,128)(2,1)S(1)}, bf16[128,128]{1,0:T(8,128)(2,1)S(1)}, u32[]{:S(2)}, u32[]{:S(2)}) %collective-permute-start.30) | collective-permute-done | bytes 32800 | tf_op jit(solution)/shard_map/ppermute | solution.py:381
  96.7 2.5 %collective-permute-start.21 = (bf16[272,2048]{1,0:T(8,128)(2,1)S(1)}, bf16[272,2048]{1,0:T(8,128)(2,1)S(1)}, u32[]{:S(2)}, u32[]{:S(2)}) collective-permute-start(bf16[272,2048]{1,0:T(8,128)(2,1)S(1)} %collective-permute-done.20.left_any.refs_12_), channel_id=1, source_target_pairs={{0,1},{1,0},{2,3},{3,2},{4,5},{5,4},{6,7},{7,6},{8,9},{9,8},{10,11... | collective-permute-start | bytes 3342344 | tf_op jit(solution)/shard_map/ppermute | solution.py:385
  99.3 3.1 %finish.1 = (bf16[128,128]{1,0:T(8,128)(2,1)}, bf16[128,128]{1,0:T(8,128)(2,1)}, bf16[128,128]{1,0:T(8,128)(2,1)}, bf16[128,128]{1,0:T(8,128)(2,1)}, bf16[128,12...) custom-call(s32[10]{0:T(128)S(1)} %stack.71.block_ref.place_ref, ...), custom_call_target="tpu_custom_call" | custom-call | flops 67108864 | bytes 2097152 | tf_op jit(solution)/shard_map/finish/pallas_call | solution.py:437
  104.9 2.4 %collective-permute-done.32.refs_2_ = bf16[128,128]{1,0:T(8,128)(2,1)S(1)} collective-permute-done((bf16[128,128]{1,0:T(8,128)(2,1)}, bf16[128,128]{1,0:T(8,128)(2,1)S(1)}, u32[]{:S(2)}, u32[]{:S(2)}) %collective-permute-start.32) | collective-permute-done | bytes 32800 | tf_op jit(solution)/shard_map/ppermute | solution.py:393
  107.3 1.7 %collective-permute-start.33 = (bf16[128,128]{1,0:T(8,128)(2,1)}, bf16[128,128]{1,0:T(8,128)(2,1)S(1)}, u32[]{:S(2)}, u32[]{:S(2)}) collective-permute-start(bf16[128,128]{1,0:T(8,128)(2,1)} %get-tuple-element.71), channel_id=1, source_target_pairs={{0,3},{1,2},{2,5},{3,4},{4,7},{5,6},{6,1},{7,0},{8,11},{9,10},{10,... | collective-permute-start | bytes 98312 | tf_op jit(solution)/shard_map/ppermute | solution.py:393
  109.1 3.2 %collective-permute-done.33.refs_3_ = bf16[128,128]{1,0:T(8,128)(2,1)S(1)} collective-permute-done((bf16[128,128]{1,0:T(8,128)(2,1)}, bf16[128,128]{1,0:T(8,128)(2,1)S(1)}, u32[]{:S(2)}, u32[]{:S(2)}) %collective-permute-start.33) | collective-permute-done | bytes 32800 | tf_op jit(solution)/shard_map/ppermute | solution.py:393
  113.3 11.6 %collective-permute-done.38.refs_14_ = bf16[128,2048]{1,0:T(8,128)(2,1)S(1)} collective-permute-done((bf16[128,2048]{1,0:T(8,128)(2,1)S(1)}, bf16[128,2048]{1,0:T(8,128)(2,1)S(1)}, u32[]{:S(2)}, u32[]{:S(2)}) %collective-permute-start.38) | collective-permute-done | bytes 524320 | tf_op jit(solution)/shard_map/ppermute | solution.py:376
  124.9 1.7 %collective-permute-start.39 = (bf16[128,2048]{1,0:T(8,128)(2,1)S(1)}, bf16[128,2048]{1,0:T(8,128)(2,1)S(1)}, u32[]{:S(2)}, u32[]{:S(2)}) collective-permute-start(bf16[128,2048]{1,0:T(8,128)(2,1)S(1)} %collective-permute-done.38.refs_14_), channel_id=1, source_target_pairs={{0,1},{1,0},{2,3},{3,2},{4,5},{5,4},{6,7},{7,6},{8,9},{9,8},{10,11... | collective-permute-start | bytes 1572872 | tf_op jit(solution)/shard_map/ppermute | solution.py:385
  126.6 2.5 %collective-permute-start.34 = (bf16[128,128]{1,0:T(8,128)(2,1)}, bf16[128,128]{1,0:T(8,128)(2,1)S(1)}, u32[]{:S(2)}, u32[]{:S(2)}) collective-permute-start(bf16[128,128]{1,0:T(8,128)(2,1)} %get-tuple-element.72), channel_id=1, source_target_pairs={{0,6},{1,7},{2,0},{3,1},{4,2},{5,3},{6,4},{7,5},{8,14},{9,15},{10,... | collective-permute-start | bytes 98312 | tf_op jit(solution)/shard_map/ppermute | solution.py:393
  129.4 3.5 %collective-permute-start.37 = (bf16[128,128]{1,0:T(8,128)(2,1)}, bf16[128,128]{1,0:T(8,128)(2,1)S(1)}, u32[]{:S(2)}, u32[]{:S(2)}) collective-permute-start(bf16[128,128]{1,0:T(8,128)(2,1)} %get-tuple-element.75), channel_id=1, source_target_pairs={{0,5},{1,4},{2,7},{3,6},{4,1},{5,0},{6,3},{7,2},{8,13},{9,12},{10,... | collective-permute-start | bytes 98312 | tf_op jit(solution)/shard_map/ppermute | solution.py:393
  133.0 5.7 %conv_out.1.conv_hbm = f32[128,2048]{1,0:T(8,128)} custom-call(bf16[128,256]{1,0:T(8,128)(2,1)S(1)} %copy-done, bf16[128,256]{1,0:T(8,128)(2,1)S(1)} %collective-permute-done.10.refs_1_, bf16[128,256]{1,0:T(8,128)(2,1)S(1)} %collective-permute-done.11.refs_2_, bf16[128,256]{1,0:T(8,128)(2,1)S(1)} %collective-permute-done.12.refs_3_, ...), custom_call_target="tpu_custom_call" | custom-call | flops 536870912 | bytes 6291456 | tf_op jit(solution)/shard_map/conv_out/pallas_call | solution.py:599
  138.7 4.5 %delta_out.1 = bf16[128,2048]{1,0:T(8,128)(2,1)} custom-call(f32[128,2048]{1,0:T(8,128)} %conv_out.1.conv_hbm, bf16[128,128]{1,0:T(8,128)(2,1)S(1)} %copy-done.1, bf16[128,128]{1,0:T(8,128)(2,1)S(1)} %collective-permute-done.31.refs_1_, bf16[128,128]{1,0:T(8,128)(2,1)S(1)} %collective-permute-done.32.refs_2_, ...), custom_call_target="tpu_custom_call" | custom-call | flops 536870912 | bytes 6291456 | tf_op jit(solution)/shard_map/delta_out/pallas_call | solution.py:647
  (106 shorter events, 30.8 us)
Async XLA Ops:
  0.0 13.1 %collective-permute-start.1 = (bf16[1024,256]{1,0:T(8,128)(2,1)}, bf16[1024,256]{1,0:T(8,128)(2,1)}, u32[]{:S(2)}, u32[]{:S(2)}) collective-permute-start(bf16[1024,256]{1,0:T(8,128)(2,1)} %refs_0_.1), channel_id=1, source_target_pairs={{0,2},{2,4},{4,6},{6,0},{1,3},{3,5},{5,7},{7,1},{8,10},{10,12},{12... | collective-permute-start | bytes 1572872 | tf_op jit(solution)/shard_map/ppermute | solution.py:376
  1.3 12.8 %collective-permute-start.2 = (bf16[1024,256]{1,0:T(8,128)(2,1)}, bf16[1024,256]{1,0:T(8,128)(2,1)}, u32[]{:S(2)}, u32[]{:S(2)}) collective-permute-start(bf16[1024,256]{1,0:T(8,128)(2,1)} %refs_0_.1), channel_id=1, source_target_pairs={{0,6},{2,0},{4,2},{6,4},{1,7},{3,1},{5,3},{7,5},{8,14},{10,8},{12,... | collective-permute-start | bytes 1572872 | tf_op jit(solution)/shard_map/ppermute | solution.py:376
  1.5 23.6 %collective-permute-start = (bf16[1024,256]{1,0:T(8,128)(2,1)}, bf16[1024,256]{1,0:T(8,128)(2,1)S(1)}, u32[]{:S(2)}, u32[]{:S(2)}) collective-permute-start(bf16[1024,256]{1,0:T(8,128)(2,1)} %refs_0_.1), channel_id=1, source_target_pairs={{0,1},{1,0},{2,3},{3,2},{4,5},{5,4},{6,7},{7,6},{8,9},{9,8},{10,11... | collective-permute-start | bytes 1572872 | tf_op jit(solution)/shard_map/ppermute | solution.py:385
  15.1 6.1 %collective-permute-start.5 = (bf16[512,256]{1,0:T(8,128)(2,1)S(1)}, bf16[512,256]{1,0:T(8,128)(2,1)S(1)}, u32[]{:S(2)}, u32[]{:S(2)}) collective-permute-start(bf16[512,256]{1,0:T(8,128)(2,1)S(1)} %slice.12), channel_id=1, source_target_pairs={{0,2},{2,4},{4,6},{6,0},{1,3},{3,5},{5,7},{7,1},{8,10},{10,12},{12... | collective-permute-start | bytes 786440 | tf_op jit(solution)/shard_map/ppermute | solution.py:376
  17.2 9.8 %collective-permute-start.7 = (bf16[512,256]{1,0:T(8,128)(2,1)S(1)}, bf16[512,256]{1,0:T(8,128)(2,1)}, u32[]{:S(2)}, u32[]{:S(2)}) collective-permute-start(bf16[512,256]{1,0:T(8,128)(2,1)S(1)} %slice.13), channel_id=1, source_target_pairs={{0,6},{2,0},{4,2},{6,4},{1,7},{3,1},{5,3},{7,5},{8,14},{10,8},{12,... | collective-permute-start | bytes 786440 | tf_op jit(solution)/shard_map/ppermute | solution.py:376
  21.2 6.4 %collective-permute-start.6 = (bf16[512,256]{1,0:T(8,128)(2,1)S(1)}, bf16[512,256]{1,0:T(8,128)(2,1)S(1)}, u32[]{:S(2)}, u32[]{:S(2)}) collective-permute-start(bf16[512,256]{1,0:T(8,128)(2,1)S(1)} %collective-permute-done.5.refs_6_), channel_id=1, source_target_pairs={{0,1},{1,0},{2,3},{3,2},{4,5},{5,4},{6,7},{7,6},{8,9},{9,8},{10,11... | collective-permute-start | bytes 786440 | tf_op jit(solution)/shard_map/ppermute | solution.py:385
  25.9 52.9 %collective-permute-start.18 = (bf16[272,2048]{1,0:T(8,128)(2,1)S(1)}, bf16[272,2048]{1,0:T(8,128)(2,1)S(1)}, u32[]{:S(2)}, u32[]{:S(2)}) collective-permute-start(bf16[272,2048]{1,0:T(8,128)(2,1)S(1)} %fusion.1.refs_8_), channel_id=1, source_target_pairs={{0,2},{2,4},{4,6},{6,0},{1,3},{3,5},{5,7},{7,1},{8,10},{10,12},{12... | collective-permute-start | bytes 3342344 | tf_op jit(solution)/shard_map/ppermute | solution.py:376
  26.9 55.8 %collective-permute-start.20 = (bf16[272,2048]{1,0:T(8,128)(2,1)S(1)}, bf16[272,2048]{1,0:T(8,128)(2,1)S(1)}, u32[]{:S(2)}, u32[]{:S(2)}) collective-permute-start(bf16[272,2048]{1,0:T(8,128)(2,1)S(1)} %fusion.1.refs_8_), channel_id=1, source_target_pairs={{0,6},{2,0},{4,2},{6,4},{1,7},{3,1},{5,3},{7,5},{8,14},{10,8},{12,... | collective-permute-start | bytes 3342344 | tf_op jit(solution)/shard_map/ppermute | solution.py:376
  48.7 15.1 %collective-permute-start.24 = (bf16[144,256]{1,0:T(8,128)(2,1)S(1)}, bf16[144,256]{1,0:T(8,128)(2,1)S(1)}, u32[]{:S(2)}, u32[]{:S(2)}) collective-permute-start(bf16[144,256]{1,0:T(8,128)(2,1)S(1)} %get-tuple-element.63.p0), channel_id=1, source_target_pairs={{0,16},{8,24},{16,0},{24,8},{1,17},{9,25},{17,1},{25,9},{2,18},{10... | collective-permute-start | bytes 221192 | tf_op jit(solution)/shard_map/ppermute | solution.py:376
  50.0 16.3 %collective-permute-start.25 = (bf16[144,256]{1,0:T(8,128)(2,1)S(1)}, bf16[144,256]{1,0:T(8,128)(2,1)S(1)}, u32[]{:S(2)}, u32[]{:S(2)}) collective-permute-start(bf16[144,256]{1,0:T(8,128)(2,1)S(1)} %get-tuple-element.63.p0), channel_id=1, source_target_pairs={{0,24},{8,0},{16,8},{24,16},{1,25},{9,1},{17,9},{25,17},{2,26},{10... | collective-permute-start | bytes 221192 | tf_op jit(solution)/shard_map/ppermute | solution.py:376
  55.4 11.9 %collective-permute-start.26 = (bf16[144,256]{1,0:T(8,128)(2,1)S(1)}, bf16[144,256]{1,0:T(8,128)(2,1)S(1)}, u32[]{:S(2)}, u32[]{:S(2)}) collective-permute-start(bf16[144,256]{1,0:T(8,128)(2,1)S(1)} %get-tuple-element.63.p0), channel_id=1, source_target_pairs={{0,8},{8,16},{16,24},{24,0},{1,9},{9,17},{17,25},{25,1},{2,10},{10... | collective-permute-start | bytes 221192 | tf_op jit(solution)/shard_map/ppermute | solution.py:376
  63.8 6.2 %collective-permute-start.10 = (bf16[128,256]{1,0:T(8,128)(2,1)}, bf16[128,256]{1,0:T(8,128)(2,1)S(1)}, u32[]{:S(2)}, u32[]{:S(2)}) collective-permute-start(bf16[128,256]{1,0:T(8,128)(2,1)} %get-tuple-element.47), channel_id=1, source_target_pairs={{0,1},{1,0},{2,3},{3,2},{4,5},{5,4},{6,7},{7,6},{8,9},{9,8},{10,11... | collective-permute-start | bytes 196616 | tf_op jit(solution)/shard_map/ppermute | solution.py:393
  67.2 6.2 %collective-permute-start.12 = (bf16[128,256]{1,0:T(8,128)(2,1)}, bf16[128,256]{1,0:T(8,128)(2,1)S(1)}, u32[]{:S(2)}, u32[]{:S(2)}) collective-permute-start(bf16[128,256]{1,0:T(8,128)(2,1)} %get-tuple-element.49), channel_id=1, source_target_pairs={{0,3},{1,2},{2,5},{3,4},{4,7},{5,6},{6,1},{7,0},{8,11},{9,10},{10,... | collective-permute-start | bytes 196616 | tf_op jit(solution)/shard_map/ppermute | solution.py:393
  70.0 7.3 %collective-permute-start.27 = (bf16[144,256]{1,0:T(8,128)(2,1)S(1)}, bf16[144,256]{1,0:T(8,128)(2,1)S(1)}, u32[]{:S(2)}, u32[]{:S(2)}) collective-permute-start(bf16[144,256]{1,0:T(8,128)(2,1)S(1)} %get-tuple-element.64.p0), channel_id=1, source_target_pairs={{0,64},{32,96},{64,0},{96,32},{128,192},{160,224},{192,128},{224,1... | collective-permute-start | bytes 221192 | tf_op jit(solution)/shard_map/ppermute | solution.py:744
  71.7 12.7 %collective-permute-start.28 = (bf16[144,256]{1,0:T(8,128)(2,1)S(1)}, bf16[144,256]{1,0:T(8,128)(2,1)S(1)}, u32[]{:S(2)}, u32[]{:S(2)}) collective-permute-start(bf16[144,256]{1,0:T(8,128)(2,1)S(1)} %get-tuple-element.64.p0), channel_id=1, source_target_pairs={{0,96},{32,0},{64,32},{96,64},{128,224},{160,128},{192,160},{224,1... | collective-permute-start | bytes 221192 | tf_op jit(solution)/shard_map/ppermute | solution.py:744
  73.4 12.3 %collective-permute-start.29 = (bf16[144,256]{1,0:T(8,128)(2,1)S(1)}, bf16[144,256]{1,0:T(8,128)(2,1)S(1)}, u32[]{:S(2)}, u32[]{:S(2)}) collective-permute-start(bf16[144,256]{1,0:T(8,128)(2,1)S(1)} %get-tuple-element.64.p0), channel_id=1, source_target_pairs={{0,32},{32,64},{64,96},{96,0},{128,160},{160,192},{192,224},{224,1... | collective-permute-start | bytes 221192 | tf_op jit(solution)/shard_map/ppermute | solution.py:744
  77.3 10.9 %collective-permute-start.13 = (bf16[128,256]{1,0:T(8,128)(2,1)}, bf16[128,256]{1,0:T(8,128)(2,1)S(1)}, u32[]{:S(2)}, u32[]{:S(2)}) collective-permute-start(bf16[128,256]{1,0:T(8,128)(2,1)} %get-tuple-element.50), channel_id=1, source_target_pairs={{0,6},{1,7},{2,0},{3,1},{4,2},{5,3},{6,4},{7,5},{8,14},{9,15},{10,... | collective-permute-start | bytes 196616 | tf_op jit(solution)/shard_map/ppermute | solution.py:393
  78.8 10.7 %collective-permute-start.14 = (bf16[128,256]{1,0:T(8,128)(2,1)}, bf16[128,256]{1,0:T(8,128)(2,1)S(1)}, u32[]{:S(2)}, u32[]{:S(2)}) collective-permute-start(bf16[128,256]{1,0:T(8,128)(2,1)} %get-tuple-element.51), channel_id=1, source_target_pairs={{0,7},{1,6},{2,1},{3,0},{4,3},{5,2},{6,5},{7,4},{8,15},{9,14},{10,... | collective-permute-start | bytes 196616 | tf_op jit(solution)/shard_map/ppermute | solution.py:393
  82.8 8.2 %collective-permute-start.15 = (bf16[128,256]{1,0:T(8,128)(2,1)}, bf16[128,256]{1,0:T(8,128)(2,1)S(1)}, u32[]{:S(2)}, u32[]{:S(2)}) collective-permute-start(bf16[128,256]{1,0:T(8,128)(2,1)} %get-tuple-element.52), channel_id=1, source_target_pairs={{0,4},{1,5},{2,6},{3,7},{4,0},{5,1},{6,2},{7,3},{8,12},{9,13},{10,... | collective-permute-start | bytes 196616 | tf_op jit(solution)/shard_map/ppermute | solution.py:393
  84.5 28.1 %collective-permute-start.22 = (bf16[144,2048]{1,0:T(8,128)(2,1)}, bf16[144,2048]{1,0:T(8,128)(2,1)S(1)}, u32[]{:S(2)}, u32[]{:S(2)}) collective-permute-start(bf16[144,2048]{1,0:T(8,128)(2,1)} %get-tuple-element.55), channel_id=1, source_target_pairs={{0,6},{2,0},{4,2},{6,4},{1,7},{3,1},{5,3},{7,5},{8,14},{10,8},{12,... | collective-permute-start | bytes 1769480 | tf_op jit(solution)/shard_map/ppermute | solution.py:376
  85.7 16.6 %collective-permute-start.16 = (bf16[128,256]{1,0:T(8,128)(2,1)S(1)}, bf16[128,256]{1,0:T(8,128)(2,1)S(1)}, u32[]{:S(2)}, u32[]{:S(2)}) collective-permute-start(bf16[128,256]{1,0:T(8,128)(2,1)S(1)} %copy-done.15), channel_id=1, source_target_pairs={{0,5},{1,4},{2,7},{3,6},{4,1},{5,0},{6,3},{7,2},{8,13},{9,12},{10,... | collective-permute-start | bytes 196616 | tf_op jit(solution)/shard_map/ppermute | solution.py:393
  88.2 8.6 %collective-permute-start.30 = (bf16[128,128]{1,0:T(8,128)(2,1)S(1)}, bf16[128,128]{1,0:T(8,128)(2,1)S(1)}, u32[]{:S(2)}, u32[]{:S(2)}) collective-permute-start(bf16[128,128]{1,0:T(8,128)(2,1)S(1)} %slice.15), channel_id=1, source_target_pairs={{0,128},{32,160},{64,192},{96,224},{1,129},{33,161},{65,193},{97,2... | collective-permute-start | bytes 98312 | tf_op jit(solution)/shard_map/ppermute | solution.py:381
  89.5 37.1 %collective-permute-start.17 = (bf16[272,2048]{1,0:T(8,128)(2,1)S(1)}, bf16[272,2048]{1,0:T(8,128)(2,1)S(1)}, u32[]{:S(2)}, u32[]{:S(2)}) collective-permute-start(bf16[272,2048]{1,0:T(8,128)(2,1)S(1)} %fusion.1.refs_8_), channel_id=1, source_target_pairs={{0,1},{1,0},{2,3},{3,2},{4,5},{5,4},{6,7},{7,6},{8,9},{9,8},{10,11... | collective-permute-start | bytes 3342344 | tf_op jit(solution)/shard_map/ppermute | solution.py:385
  91.0 38.1 %collective-permute-start.19 = (bf16[272,2048]{1,0:T(8,128)(2,1)S(1)}, bf16[272,2048]{1,0:T(8,128)(2,1)S(1)}, u32[]{:S(2)}, u32[]{:S(2)}) collective-permute-start(bf16[272,2048]{1,0:T(8,128)(2,1)S(1)} %collective-permute-done.18.right_any.refs_10_), channel_id=1, source_target_pairs={{0,1},{1,0},{2,3},{3,2},{4,5},{5,4},{6,7},{7,6},{8,9},{9,8},{10,11... | collective-permute-start | bytes 3342344 | tf_op jit(solution)/shard_map/ppermute | solution.py:385
  96.7 32.6 %collective-permute-start.21 = (bf16[272,2048]{1,0:T(8,128)(2,1)S(1)}, bf16[272,2048]{1,0:T(8,128)(2,1)S(1)}, u32[]{:S(2)}, u32[]{:S(2)}) collective-permute-start(bf16[272,2048]{1,0:T(8,128)(2,1)S(1)} %collective-permute-done.20.left_any.refs_12_), channel_id=1, source_target_pairs={{0,1},{1,0},{2,3},{3,2},{4,5},{5,4},{6,7},{7,6},{8,9},{9,8},{10,11... | collective-permute-start | bytes 3342344 | tf_op jit(solution)/shard_map/ppermute | solution.py:385
  112.3 12.6 %collective-permute-start.38 = (bf16[128,2048]{1,0:T(8,128)(2,1)S(1)}, bf16[128,2048]{1,0:T(8,128)(2,1)S(1)}, u32[]{:S(2)}, u32[]{:S(2)}) collective-permute-start(bf16[128,2048]{1,0:T(8,128)(2,1)S(1)} %copy-done.14), channel_id=1, source_target_pairs={{0,2},{2,4},{4,6},{6,0},{1,3},{3,5},{5,7},{7,1},{8,10},{10,12},{12... | collective-permute-start | bytes 1572872 | tf_op jit(solution)/shard_map/ppermute | solution.py:376
  112.6 16.8 %collective-permute-start.23 = (bf16[144,2048]{1,0:T(8,128)(2,1)S(1)}, bf16[144,2048]{1,0:T(8,128)(2,1)S(1)}, u32[]{:S(2)}, u32[]{:S(2)}) collective-permute-start(bf16[144,2048]{1,0:T(8,128)(2,1)S(1)} %collective-permute-done.22.refs_14_), channel_id=1, source_target_pairs={{0,1},{1,0},{2,3},{3,2},{4,5},{5,4},{6,7},{7,6},{8,9},{9,8},{10,11... | collective-permute-start | bytes 1769480 | tf_op jit(solution)/shard_map/ppermute | solution.py:385
  124.9 13.8 %collective-permute-start.39 = (bf16[128,2048]{1,0:T(8,128)(2,1)S(1)}, bf16[128,2048]{1,0:T(8,128)(2,1)S(1)}, u32[]{:S(2)}, u32[]{:S(2)}) collective-permute-start(bf16[128,2048]{1,0:T(8,128)(2,1)S(1)} %collective-permute-done.38.refs_14_), channel_id=1, source_target_pairs={{0,1},{1,0},{2,3},{3,2},{4,5},{5,4},{6,7},{7,6},{8,9},{9,8},{10,11... | collective-permute-start | bytes 1572872 | tf_op jit(solution)/shard_map/ppermute | solution.py:385
  126.6 12.0 %collective-permute-start.34 = (bf16[128,128]{1,0:T(8,128)(2,1)}, bf16[128,128]{1,0:T(8,128)(2,1)S(1)}, u32[]{:S(2)}, u32[]{:S(2)}) collective-permute-start(bf16[128,128]{1,0:T(8,128)(2,1)} %get-tuple-element.72), channel_id=1, source_target_pairs={{0,6},{1,7},{2,0},{3,1},{4,2},{5,3},{6,4},{7,5},{8,14},{9,15},{10,... | collective-permute-start | bytes 98312 | tf_op jit(solution)/shard_map/ppermute | solution.py:393
  129.1 9.6 %collective-permute-start.35 = (bf16[128,128]{1,0:T(8,128)(2,1)}, bf16[128,128]{1,0:T(8,128)(2,1)S(1)}, u32[]{:S(2)}, u32[]{:S(2)}) collective-permute-start(bf16[128,128]{1,0:T(8,128)(2,1)} %get-tuple-element.73), channel_id=1, source_target_pairs={{0,7},{1,6},{2,1},{3,0},{4,3},{5,2},{6,5},{7,4},{8,15},{9,14},{10,... | collective-permute-start | bytes 98312 | tf_op jit(solution)/shard_map/ppermute | solution.py:393
  129.3 9.3 %collective-permute-start.36 = (bf16[128,128]{1,0:T(8,128)(2,1)}, bf16[128,128]{1,0:T(8,128)(2,1)S(1)}, u32[]{:S(2)}, u32[]{:S(2)}) collective-permute-start(bf16[128,128]{1,0:T(8,128)(2,1)} %get-tuple-element.74), channel_id=1, source_target_pairs={{0,4},{1,5},{2,6},{3,7},{4,0},{5,1},{6,2},{7,3},{8,12},{9,13},{10,... | collective-permute-start | bytes 98312 | tf_op jit(solution)/shard_map/ppermute | solution.py:393
  129.4 9.2 %collective-permute-start.37 = (bf16[128,128]{1,0:T(8,128)(2,1)}, bf16[128,128]{1,0:T(8,128)(2,1)S(1)}, u32[]{:S(2)}, u32[]{:S(2)}) collective-permute-start(bf16[128,128]{1,0:T(8,128)(2,1)} %get-tuple-element.75), channel_id=1, source_target_pairs={{0,5},{1,4},{2,7},{3,6},{4,1},{5,0},{6,3},{7,2},{8,13},{9,12},{10,... | collective-permute-start | bytes 98312 | tf_op jit(solution)/shard_map/ppermute | solution.py:393
  (25 other events, 192.2 us)

commit v4 on v3

--- a/solution.py
+++ b/solution.py
@@ -14,6 +14,7 @@
 TINY_NORM = 1e-06
 TINY_VAR = 1e-05
 CHUNK = 128
+HALO = 32
 STEPS = (0, 1, -1, 2)
 GOES_TO = (0, 1, 4, 5, 2, 3, 6, 7)
 F32 = jnp.float32
@@ -96,8 +97,8 @@
 def project_kernel(width_all, head_size, block_ref, rate_ref, *refs):
     own, sw, r1, sr1, l1, sl1, fa, sfa, fb, sfb = refs[:10]
     sides = refs[10:18]
-    q_ref, k_ref, v_ref, bl_ref, dg_hbm, gu_hbm, cg_hbm = refs[18:25]
-    gathered, weights, factors, dg_ref, gu_ref, cg_ref, sems, out_sems = refs[25:]
+    q_ref, k_ref, v_ref, bl_ref, tail_ref, dg_hbm, gu_hbm, cg_hbm = refs[18:26]
+    gathered, weights, factors, dg_ref, gu_ref, cg_ref, sems, out_sems = refs[26:]
     rows, piece_width = own.shape[0], own.shape[1]
     half = rows // 2
     places = [slice(0, half), slice(half, rows)]
@@ -167,6 +168,7 @@
         )
 
     each_half(gated)
+    tail_ref[...] = gu_ref[rows - HALO :, :]
     stores = fetch(out_sems, (gu_ref, gu_hbm))
     for n, body in enumerate((gates, queries, rest_of)):
         for one in loads[2 * n + 2 : 2 * n + 4]:
@@ -184,8 +186,9 @@
     return pl.pallas_call(
         functools.partial(project_kernel, width_all, head_size),
         in_specs=[scalars(), scalars()] + [anywhere()] * 18,
-        out_specs=[whole()] * 4 + [hbm()] * 3,
+        out_specs=[whole()] * 5 + [hbm()] * 3,
         out_shape=[pltpu.VMEM((rows, 128), kind) for kind in kinds[:4]]
+        + [pltpu.VMEM((HALO, 128), BF16)]
         + [pltpu.HBM((rows, 128), kind) for kind in kinds[4:]],
         scratch_shapes=[
             pltpu.VMEM((rows, width_all), BF16),
@@ -340,7 +343,7 @@
     )(q, k, v, bl)
 
 
-def along_kernel(which, place_ref, p0, p1, p2, p3, before_ref, total_ref, held):
+def along_kernel(which, place_ref, p0, p1, p2, p3, before_ref, total_ref, made_ref, held):
     me = place_ref[which]
     for j, piece in ((0, p0), (2, p1), (3, p2), (1, p3)):
         held[(me - j + 4) & 3] = piece[...]
@@ -353,16 +356,18 @@
         so_far = compose(read_state(held.at[m]), so_far)
     write_state(before_ref, before)
     write_state(total_ref, so_far)
+    made_ref[...] = low(so_far[2])
 
 
 def along(which, places, state, *others):
     return pl.pallas_call(
         functools.partial(along_kernel, which),
         in_specs=[scalars()] + [whole()] * 4,
-        out_specs=[whole(), whole()],
+        out_specs=[whole()] * 3,
         out_shape=[
             jax.ShapeDtypeStruct(state.shape, BF16),
             pltpu.VMEM(state.shape, BF16),
+            pltpu.VMEM((state.shape[1] // 2,) * 2, BF16),
         ],
         scratch_shapes=[pltpu.VMEM((4,) + state.shape, BF16)],
         compiler_params=params(4),
@@ -398,7 +403,7 @@
     block_ref, coef_p_hbm, coef_q_hbm, dg_hbm, gain_ref, reach_any, far_any, before_hbm, *rest
 ):
     outs, scratch = rest[:8], rest[8:]
-    coef_p_ref, coef_q_ref, dg_ref, reach_ref, far_ref, before_ref, out_ref, sems, out_sems = scratch
+    coef_p_ref, coef_q_ref, dg_ref, reach_ref, far_ref, before_ref, sems = scratch
     loads = fetch(
         sems,
         (reach_any, reach_ref),
@@ -416,17 +421,13 @@
     state = low(total * state - dot(low(lost), low(state)) + made)
     for one in loads[3:]:
         one.wait()
-    stores = []
-    step = out_ref.shape[1]
+    step = outs[0].shape[0]
     for slot in range(8):
         here = pl.ds(pl.multiple_of(block_ref[GOES_TO[slot]] * step, step), step)
         result = coef_q_ref[here, :] + dot(coef_p_ref[here, :], state)
         mean = jnp.sum(result * result, axis=-1, keepdims=True) * (1.0 / result.shape[1])
         result = result * lax.rsqrt(mean + TINY_NORM) * gain_ref[...]
-        out_ref[slot] = low(result * jax.nn.silu(dg_ref[here, :].astype(F32)))
-        stores += fetch(out_sems.at[pl.ds(slot, 1)], (out_ref.at[slot], outs[slot]))
-    for one in stores:
-        one.wait()
+        outs[slot][...] = low(result * jax.nn.silu(dg_ref[here, :].astype(F32)))
 
 
 def finish(blocks, coef_p, coef_q, dg, gain, reach, far, before):
@@ -437,11 +438,10 @@
     return pl.pallas_call(
         finish_kernel,
         in_specs=[scalars(), hbm(), hbm(), hbm(), whole(), anywhere(), anywhere(), anywhere()],
-        out_specs=[hbm()] * 8,
-        out_shape=[pltpu.HBM((rows // 8, size), BF16)] * 8,
+        out_specs=[whole()] * 8,
+        out_shape=[pltpu.VMEM((rows // 8, size), BF16)] * 8,
         scratch_shapes=[pltpu.VMEM(a.shape, a.dtype) for a in copied]
-        + [pltpu.VMEM((8, rows // 8, size), BF16)]
-        + [pltpu.SemaphoreType.DMA((6,)), pltpu.SemaphoreType.DMA((8,))],
+        + [pltpu.SemaphoreType.DMA((6,))],
         compiler_params=params(8),
         cost_estimate=cost(64 << 20, 2 << 20),
         name="finish",
@@ -450,13 +450,12 @@
 
 def conv_kernel(block_ref, gu_hbm, before_any, taps_ref, cg_hbm, *rest):
     outs = rest[:8]
-    gu_ref, before_ref, padded, out_ref, sems, out_sems = rest[8:]
+    gu_ref, before_ref, padded, out_ref, cg_ref, sems = rest[8:]
     rows, size = gu_ref.shape
     head = before_ref.shape[0]
     count = taps_ref.shape[0]
-    gate = pltpu.make_async_copy(cg_hbm, out_ref.at[:, pl.ds(size, size)], sems.at[2])
-    gate.start()
-    for one in fetch(sems, (gu_hbm, gu_ref), (before_any, before_ref)):
+    loads = fetch(sems, (gu_hbm, gu_ref), (before_any, before_ref), (cg_hbm, cg_ref))
+    for one in loads[:2]:
         one.wait()
     padded[0:head, :] = before_ref[...].astype(F32)
     padded[head:, :] = gu_ref[...].astype(F32)
@@ -469,18 +468,16 @@
         total = jnp.zeros((step, size), F32)
         for j in range(count):
             total = total + padded[pl.ds(base + skip + j, step), :] * taps[j : j + 1, :]
-        out_ref[pl.ds(base, step), 0:size] = low(total)
+        out_ref[pl.ds(base, step), :] = low(total)
         return carry
 
     lax.fori_loop(0, rows // step, block, 0)
-    gate.wait()
+    loads[2].wait()
     part = rows // 8
-    pairs = []
     for slot in range(8):
         here = pl.ds(pl.multiple_of(block_ref[GOES_TO[slot]] * part, part), part)
-        pairs.append((out_ref.at[here, :], outs[slot]))
-    for one in fetch(out_sems, *pairs):
-        one.wait()
+        outs[slot][:, 0:size] = out_ref[here, :]
+        outs[slot][:, size:] = cg_ref[here, :]
 
 
 def conv(blocks, gu, before, taps, cg):
@@ -488,15 +485,15 @@
     return pl.pallas_call(
         conv_kernel,
         in_specs=[scalars(), hbm(), anywhere(), whole(), hbm()],
-        out_specs=[hbm()] * 8,
-        out_shape=[pltpu.HBM((rows // 8, 2 * size), BF16)] * 8,
+        out_specs=[whole()] * 8,
+        out_shape=[pltpu.VMEM((rows // 8, 2 * size), BF16)] * 8,
         scratch_shapes=[
             pltpu.VMEM(gu.shape, BF16),
             pltpu.VMEM(before.shape, BF16),
             pltpu.VMEM((rows + before.shape[0], size), F32),
-            pltpu.VMEM((rows, 2 * size), BF16),
+            pltpu.VMEM((rows, size), BF16),
+            pltpu.VMEM((rows, size), BF16),
             pltpu.SemaphoreType.DMA((3,)),
-            pltpu.SemaphoreType.DMA((8,)),
         ],
         compiler_params=params(8),
         cost_estimate=cost(256 << 20, 1 << 20),
@@ -518,8 +515,7 @@
     lax.fori_loop(0, out_ref.shape[1] // 512, step, 0)
 
 
-def cut_kernel(right_any, left_any, top_hbm, rest_hbm, top, rest, sems):
-    count = top.shape[0]
+def cut_kernel(count, right_any, left_any, top_hbm, rest_hbm, top, rest, sems):
     inward = fetch(
         sems,
         (right_any.at[pl.ds(0, count), :], top),
@@ -537,7 +533,7 @@
     rows, width = right.shape
     shapes = [(count, width), (rows - count, width)]
     return pl.pallas_call(
-        cut_kernel,
+        functools.partial(cut_kernel, count),
         in_specs=[anywhere()] * 2,
         out_specs=[hbm()] * 2,
         out_shape=[pltpu.HBM(shape, BF16) for shape in shapes],
@@ -550,8 +546,9 @@
 
 
 def conv_out_kernel(*refs):
-    got, sources, out_hbm = refs[:8], refs[8:16], refs[16]
-    got_ref, weights, mixed, out_ref, sems, out_sems = refs[17:]
+    got, sources, delta_sources = refs[:8], refs[8:16], refs[16:24]
+    out_ref, delta_weights = refs[24:26]
+    got_ref, weights, mixed, sems = refs[26:]
     groups, rows, size = mixed.shape
     got_loads = fetch(
         sems.at[pl.ds(8, 8)], *((ref, got_ref.at[slot]) for slot, ref in enumerate(got))
@@ -561,6 +558,13 @@
         *(
             (ref.at[pl.ds(0 if ref.shape[0] == size + 16 else size, size + 16), :], weights.at[slot])
             for slot, ref in enumerate(sources)
+        ),
+    )
+    more = fetch(
+        sems.at[pl.ds(16, 8)],
+        *(
+            (ref.at[pl.ds(0, size), :], delta_weights.at[slot])
+            for slot, ref in enumerate(delta_sources)
         ),
     )
     for one in got_loads:
@@ -588,77 +592,55 @@
         add_slots(
             out_ref, slots, lambda slot: mixed[slot], weights, out_ref if half else None
         )
-    (store,) = fetch(out_sems, (out_ref, out_hbm))
-    store.wait()
-
-
-def conv_out(got, sources):
+    for one in more:
+        one.wait()
+
+
+def conv_out(got, sources, delta_sources):
     groups = len(got)
     rows, both = got[0].shape
     size, width = both // 2, sources[0].shape[1]
     return pl.pallas_call(
         conv_out_kernel,
-        in_specs=[anywhere()] * 16,
-        out_specs=hbm(),
-        out_shape=pltpu.HBM((rows, width), F32),
+        in_specs=[anywhere()] * 24,
+        out_specs=[whole()] * 2,
+        out_shape=[pltpu.VMEM((rows, width), F32), pltpu.VMEM((groups, size, width), BF16)],
         scratch_shapes=[
             pltpu.VMEM((groups, rows, both), BF16),
             pltpu.VMEM((groups, size + 16, width), BF16),
             pltpu.VMEM((groups, rows, size), BF16),
-            pltpu.VMEM((rows, width), F32),
-            pltpu.SemaphoreType.DMA((16,)),
-            pltpu.SemaphoreType.DMA((1,)),
+            pltpu.SemaphoreType.DMA((24,)),
         ],
         compiler_params=params(12),
         cost_estimate=cost(2 * rows * 1024 * width, 6 << 20),
         name="conv_out",
-    )(*got, *sources)
-
-
-def delta_out_kernel(conv_hbm, *refs):
-    got, sources, out_ref = refs[:8], refs[8:16], refs[16]
-    got_ref, weights, conv_ref, sems = refs[17:]
-    size = got_ref.shape[1]
-    loads = fetch(
-        sems,
-        (conv_hbm, conv_ref),
-        *((ref, got_ref.at[slot]) for slot, ref in enumerate(got)),
-        *((ref.at[pl.ds(0, size), :], weights.at[slot]) for slot, ref in enumerate(sources)),
-    )
-    for one in loads[:9]:
-        one.wait()
-    for half in range(2):
-        slots = range(half * 4, half * 4 + 4)
-        for slot in slots:
-            loads[9 + slot].wait()
-        add_slots(
-            out_ref if half else conv_ref,
-            slots,
-            lambda slot: got_ref[slot],
-            weights,
-            conv_ref,
-        )
-
-
-def delta_out(got, conv_part, sources):
+    )(*got, *sources, *delta_sources)
+
+
+def delta_out_kernel(conv_ref, weights, *refs):
+    got, out_ref, got_ref, sems = refs[:8], refs[8], refs[9], refs[10]
+    for one in fetch(sems, *((ref, got_ref.at[slot]) for slot, ref in enumerate(got))):
+        one.wait()
+    add_slots(out_ref, range(8), lambda slot: got_ref[slot], weights, conv_ref)
+
+
+def delta_out(got, conv_part, weights):
     groups = len(got)
     rows, size = got[0].shape
     width = conv_part.shape[1]
     return pl.pallas_call(
         delta_out_kernel,
-        in_specs=[anywhere()] * 17,
+        in_specs=[whole()] * 2 + [anywhere()] * 8,
         out_specs=whole(),
         out_shape=jax.ShapeDtypeStruct((rows, width), BF16),
         scratch_shapes=[
             pltpu.VMEM((groups, rows, size), BF16),
-            pltpu.VMEM((groups, size, width), BF16),
-            pltpu.VMEM(conv_part.shape, F32),
-            pltpu.SemaphoreType.DMA((17,)),
+            pltpu.SemaphoreType.DMA((8,)),
         ],
         compiler_params=params(12),
         cost_estimate=cost(2 * rows * 1024 * width, 6 << 20),
         name="delta_out",
-    )(home(conv_part), *got, *sources)
+    )(near_core(conv_part), near_core(weights), *got)
 
 
 def local(
@@ -725,25 +707,28 @@
     own = tokens
     r1, l1 = cyclic(own, "y", 1), cyclic(own, "y", -1)
     sw = swapped(own)
-    r1, l1, beta_decay, last = lax.optimization_barrier((r1, l1, beta_decay, last))
+    r1, l1, beta_decay, last, blocks, rate = lax.optimization_barrier(
+        (r1, l1, beta_decay, last, blocks, rate)
+    )
     weights = weights[:7] + (beta_decay,)
-    fa, fb = cyclic(r1[:half], "y", 1), cyclic(l1[half:], "y", -1)
+    r1_top, l1_rest = cut(r1, l1, half)
+    fa, fb = cyclic(r1_top, "y", 1), cyclic(l1_rest, "y", -1)
     sr1, sl1 = swapped(r1), swapped(l1)
     sfa, sfb = swapped(fa), swapped(fb)
     pieces = [own, sw, r1, sr1, l1, sl1, fa, sfa, fb, sfb]
     wr, wl = cyclic(last, "y", 1), cyclic(last, "y", -1)
-    q, k, v, bl, dg, gu, cg = project(pieces, weights, blocks, rate, 2048, size)
+    q, k, v, bl, tail, dg, gu, cg = project(pieces, weights, blocks, rate, 2048, size)
 
     coef_p, coef_q, state = delta(q, k, v, bl)
 
 
-    before, total = along(8, blocks, state, *(cyclic(state, "x", j) for j in (2, 3, 1)))
+    before, total, _ = along(8, blocks, state, *(cyclic(state, "x", j) for j in (2, 3, 1)))
     route = lambda j: [(h + i, h + (i + j) % 4) for h in (0, 4) for i in range(4)]
     around = []
     for j in (2, 3, 1):
         around.append(lax.ppermute(total, "z", route(j)))
-    before_z, total_z = along(9, blocks, total, *around)
-    far = shifted(total_z[:size, size:], "z", 4)
+    before_z, _, made_z = along(9, blocks, total, *around)
+    far = shifted(made_z, "z", 4)
 
     ws = swapped(last)
     wr_top, wl_rest = cut(wr, wl, size)
@@ -754,13 +739,13 @@
     delta_weights = near + [wfa, wsfa]
     conv_weights = near + [wfb, wsfb]
 
-    halo = lax.ppermute(gu[rows - 32 :], SP, [(i, i + 1) for i in range(31)])
+    halo = lax.ppermute(tail, SP, [(i, i + 1) for i in range(31)])
     filtered = conv(blocks, gu, halo, conv_taps, cg)
     got = exchanged(filtered)
-    conv_part = conv_out(got, conv_weights)
+    conv_part, kept = conv_out(got, conv_weights, delta_weights)
 
     mixed = finish(blocks, coef_p, coef_q, dg, head_gain[None, :], before_z, far, before)
-    return delta_out(exchanged(mixed), conv_part, delta_weights)
+    return delta_out(exchanged(mixed), conv_part, kept)
 
 
 def solution(mesh):

time: 144 us -> 132 us (0.917)
  the two profiles are of different devices: /device:TPU:239 before, /device:TPU:1 now
where the time goes in v4:
time: 132 us; the launch traced here: 131 us
  starting transfers between devices  58.1 us (44%)
  Pallas kernels  34.3 us (26%)
  waiting for transfers between devices  33.9 us (26%)
  local copies, waits for them, and re-layouts  2.69 us (2%)
    ppermute x11, waiting for transfers between devices, cyclic(): lax.ppermute(block, axis, [(i, (i + distance) % count) for i in range(cou...  27.9 us
    ppermute x14, starting transfers between devices, exchanged(): got.append(lax.ppermute(parts[slot], TP, route))  19 us
    ppermute x11, starting transfers between devices, cyclic(): lax.ppermute(block, axis, [(i, (i + distance) % count) for i in range(cou...  12.7 us
    ppermute x10, starting transfers between devices, swapped(): return lax.ppermute(block, 'c', [(0, 1), (1, 0)])  9.25 us
    pallas_call x1, Pallas kernels, project(): pl.pallas_call(functools.partial(project_kernel, width_all, head_size), i...  8.99 us
    ppermute x3, starting transfers between devices, local(): around.append(lax.ppermute(total, 'z', route(j)))  8.13 us
    pallas_call x1, Pallas kernels, delta(): pl.pallas_call(delta_kernel, in_specs=[whole()] * 4, out_specs=[hbm(), hb...  6.44 us
    ppermute x1, starting transfers between devices, shifted(): lax.ppermute(block, axis, [(i, i + distance) for i in devices if i + dist...  6.11 us
  transfers between devices with their start and end apart: 40, of which 11 were waited for; matrix products, arithmetic and copies ran while one was open for 3% of the time, Pallas kernels for 24%

profile of v4, /device:TPU:1, one launch (start us, length us, event | category | flops | bytes accessed | tf_op | source)
XLA Modules:
  0.0 131.3 jit_solution(13187030490619865289)
XLA Ops:
  0.0 3.6 %collective-permute-start.1 = (bf16[1024,256]{1,0:T(8,128)(2,1)}, bf16[1024,256]{1,0:T(8,128)(2,1)S(1)}, u32[]{:S(2)}, u32[]{:S(2)}) collective-permute-start(bf16[1024,256]{1,0:T(8,128)(2,1)} %refs_0_.1), channel_id=1, source_target_pairs={{0,6},{2,0},{4,2},{6,4},{1,7},{3,1},{5,3},{7,5},{8,14},{10,8},{12,... | collective-permute-start | bytes 1572872 | tf_op jit(solution)/shard_map/ppermute | solution.py:381
  3.6 1.7 %collective-permute-start.2 = (bf16[1024,256]{1,0:T(8,128)(2,1)}, bf16[1024,256]{1,0:T(8,128)(2,1)S(1)}, u32[]{:S(2)}, u32[]{:S(2)}) collective-permute-start(bf16[1024,256]{1,0:T(8,128)(2,1)} %refs_0_.1), channel_id=1, source_target_pairs={{0,1},{1,0},{2,3},{3,2},{4,5},{5,4},{6,7},{7,6},{8,9},{9,8},{10,11... | collective-permute-start | bytes 1572872 | tf_op jit(solution)/shard_map/ppermute | solution.py:390
  9.9 4.6 %collective-permute-done.1.left_any.refs_4_ = bf16[1024,256]{1,0:T(8,128)(2,1)S(1)} collective-permute-done((bf16[1024,256]{1,0:T(8,128)(2,1)}, bf16[1024,256]{1,0:T(8,128)(2,1)S(1)}, u32[]{:S(2)}, u32[]{:S(2)}) %collective-permute-start.1) | collective-permute-done | bytes 524320 | tf_op jit(solution)/shard_map/ppermute | solution.py:381
  14.5 3.0 %collective-permute-done.right_any.refs_2_ = bf16[1024,256]{1,0:T(8,128)(2,1)S(1)} collective-permute-done((bf16[1024,256]{1,0:T(8,128)(2,1)}, bf16[1024,256]{1,0:T(8,128)(2,1)S(1)}, u32[]{:S(2)}, u32[]{:S(2)}) %collective-permute-start) | collective-permute-done | bytes 524320 | tf_op jit(solution)/shard_map/ppermute | solution.py:381
  18.5 2.7 %collective-permute-start.7 = (bf16[512,256]{1,0:T(8,128)(2,1)}, bf16[512,256]{1,0:T(8,128)(2,1)S(1)}, u32[]{:S(2)}, u32[]{:S(2)}) collective-permute-start(bf16[512,256]{1,0:T(8,128)(2,1)} %get-tuple-element.53), channel_id=1, source_target_pairs={{0,6},{2,0},{4,2},{6,4},{1,7},{3,1},{5,3},{7,5},{8,14},{10,8},{12,... | collective-permute-start | bytes 786440 | tf_op jit(solution)/shard_map/ppermute | solution.py:381
  21.1 4.8 %collective-permute-done.5.refs_6_ = bf16[512,256]{1,0:T(8,128)(2,1)S(1)} collective-permute-done((bf16[512,256]{1,0:T(8,128)(2,1)}, bf16[512,256]{1,0:T(8,128)(2,1)S(1)}, u32[]{:S(2)}, u32[]{:S(2)}) %collective-permute-start.5) | collective-permute-done | bytes 262176 | tf_op jit(solution)/shard_map/ppermute | solution.py:381
  25.9 2.7 %collective-permute-start.6 = (bf16[512,256]{1,0:T(8,128)(2,1)S(1)}, bf16[512,256]{1,0:T(8,128)(2,1)S(1)}, u32[]{:S(2)}, u32[]{:S(2)}) collective-permute-start(bf16[512,256]{1,0:T(8,128)(2,1)S(1)} %collective-permute-done.5.refs_6_), channel_id=1, source_target_pairs={{0,1},{1,0},{2,3},{3,2},{4,5},{5,4},{6,7},{7,6},{8,9},{9,8},{10,11... | collective-permute-start | bytes 786440 | tf_op jit(solution)/shard_map/ppermute | solution.py:390
  32.3 9.0 %project.1 = (bf16[1024,128]{1,0:T(8,128)(2,1)S(1)}, bf16[1024,128]{1,0:T(8,128)(2,1)S(1)}, bf16[1024,128]{1,0:T(8,128)(2,1)S(1)}, f32[1024,128]{1,0:T(8,128)S(1...) custom-call(s32[10]{0:T(128)S(1)} %stack.78.block_ref.place_ref, ...), custom_call_target="tpu_custom_call" | custom-call | flops 4294967296 | bytes 12582912 | tf_op jit(solution)/shard_map/project/pallas_call | solution.py:186
  41.3 6.4 %delta.1 = (bf16[1024,128]{1,0:T(8,128)(2,1)}, f32[1024,128]{1,0:T(8,128)}, bf16[144,256]{1,0:T(8,128)(2,1)S(1)}) custom-call(bf16[1024,128]{1,0:T(8,128)(2,1)S(1)} %get-tuple-element.71.q_ref, bf16[1024,128]{1,0:T(8,128)(2,1)S(1)} %get-tuple-element.72.k_ref, bf16[1024,128]{1,0:T(8,128)(2,1)S(1)} %get-tuple-element.73.v_ref, ...), custom_call_target="tpu_custom_call" | custom-call | flops 2013265920 | bytes 3145728 | tf_op jit(solution)/shard_map/delta/pallas_call | solution.py:326
  50.5 1.5 %collective-permute-start.26 = (bf16[144,256]{1,0:T(8,128)(2,1)S(1)}, bf16[144,256]{1,0:T(8,128)(2,1)S(1)}, u32[]{:S(2)}, u32[]{:S(2)}) collective-permute-start(bf16[144,256]{1,0:T(8,128)(2,1)S(1)} %get-tuple-element.78.p0), channel_id=1, source_target_pairs={{0,16},{8,24},{16,0},{24,8},{1,17},{9,25},{17,1},{25,9},{2,18},{10... | collective-permute-start | bytes 221192 | tf_op jit(solution)/shard_map/ppermute | solution.py:381
  52.6 2.7 %collective-permute-done.26.p1 = bf16[144,256]{1,0:T(8,128)(2,1)S(1)} collective-permute-done((bf16[144,256]{1,0:T(8,128)(2,1)S(1)}, bf16[144,256]{1,0:T(8,128)(2,1)S(1)}, u32[]{:S(2)}, u32[]{:S(2)}) %collective-permute-start.26) | collective-permute-done | bytes 73760 | tf_op jit(solution)/shard_map/ppermute | solution.py:381
  55.3 1.7 %along.2 = (bf16[144,256]{1,0:T(8,128)(2,1)S(1)}, bf16[144,256]{1,0:T(8,128)(2,1)S(1)}, bf16[128,128]{1,0:T(8,128)(2,1)}) custom-call(s32[10]{0:T(128)S(1)} %stack.78.block_ref.place_ref, bf16[144,256]{1,0:T(8,128)(2,1)S(1)} %get-tuple-element.78.p0, bf16[144,256]{1,0:T(8,128)(2,1)S(1)} %collective-permute-done.26.p1, ...), custom_call_target="tpu_custom_call" | custom-call | flops 16777216 | bytes 262144 | tf_op jit(solution)/shard_map/along/pallas_call | solution.py:363
  56.9 1.6 %collective-permute-start.31 = (bf16[144,256]{1,0:T(8,128)(2,1)S(1)}, bf16[144,256]{1,0:T(8,128)(2,1)S(1)}, u32[]{:S(2)}, u32[]{:S(2)}) collective-permute-start(bf16[144,256]{1,0:T(8,128)(2,1)S(1)} %get-tuple-element.79.p0), channel_id=1, source_target_pairs={{0,32},{32,64},{64,96},{96,0},{128,160},{160,192},{192,224},{224,1... | collective-permute-start | bytes 221192 | tf_op jit(solution)/shard_map/ppermute | solution.py:729
  58.5 3.0 %collective-permute-start.9 = (bf16[32,128]{1,0:T(8,128)(2,1)S(1)}, bf16[32,128]{1,0:T(8,128)(2,1)S(1)}, u32[]{:S(2)}, u32[]{:S(2)}) collective-permute-start(bf16[32,128]{1,0:T(8,128)(2,1)S(1)} %get-tuple-element.56), channel_id=1, source_target_pairs={{0,8},{8,16},{16,24},{24,32},{32,40},{40,48},{48,56},{56,64},{64,7... | collective-permute-start | bytes 24584 | tf_op jit(solution)/shard_map/ppermute | solution.py:742
  61.5 2.8 %collective-permute-start.30 = (bf16[144,256]{1,0:T(8,128)(2,1)S(1)}, bf16[144,256]{1,0:T(8,128)(2,1)S(1)}, u32[]{:S(2)}, u32[]{:S(2)}) collective-permute-start(bf16[144,256]{1,0:T(8,128)(2,1)S(1)} %get-tuple-element.79.p0), channel_id=1, source_target_pairs={{0,96},{32,0},{64,32},{96,64},{128,224},{160,128},{192,160},{224,1... | collective-permute-start | bytes 221192 | tf_op jit(solution)/shard_map/ppermute | solution.py:729
  64.3 3.7 %collective-permute-start.29 = (bf16[144,256]{1,0:T(8,128)(2,1)S(1)}, bf16[144,256]{1,0:T(8,128)(2,1)S(1)}, u32[]{:S(2)}, u32[]{:S(2)}) collective-permute-start(bf16[144,256]{1,0:T(8,128)(2,1)S(1)} %get-tuple-element.79.p0), channel_id=1, source_target_pairs={{0,64},{32,96},{64,0},{96,32},{128,192},{160,224},{192,128},{224,1... | collective-permute-start | bytes 221192 | tf_op jit(solution)/shard_map/ppermute | solution.py:729
  68.0 3.1 %conv.1 = (bf16[128,256]{1,0:T(8,128)(2,1)S(1)}, bf16[128,256]{1,0:T(8,128)(2,1)S(1)}, bf16[128,256]{1,0:T(8,128)(2,1)S(1)}, bf16[128,256]{1,0:T(8,128)(2,1)S(1)...) custom-call(s32[10]{0:T(128)S(1)} %stack.78.block_ref.place_ref, ...), custom_call_target="tpu_custom_call" | custom-call | flops 268435456 | bytes 1048576 | tf_op jit(solution)/shard_map/conv/pallas_call | solution.py:485
  71.1 4.1 %collective-permute-start.10 = (bf16[128,256]{1,0:T(8,128)(2,1)S(1)}, bf16[128,256]{1,0:T(8,128)(2,1)S(1)}, u32[]{:S(2)}, u32[]{:S(2)}) collective-permute-start(bf16[128,256]{1,0:T(8,128)(2,1)S(1)} %get-tuple-element.59), channel_id=1, source_target_pairs={{0,1},{1,0},{2,3},{3,2},{4,5},{5,4},{6,7},{7,6},{8,9},{9,8},{10,11... | collective-permute-start | bytes 196616 | tf_op jit(solution)/shard_map/ppermute | solution.py:398
  75.2 1.5 %collective-permute-start.12 = (bf16[128,256]{1,0:T(8,128)(2,1)S(1)}, bf16[128,256]{1,0:T(8,128)(2,1)S(1)}, u32[]{:S(2)}, u32[]{:S(2)}) collective-permute-start(bf16[128,256]{1,0:T(8,128)(2,1)S(1)} %get-tuple-element.61), channel_id=1, source_target_pairs={{0,3},{1,2},{2,5},{3,4},{4,7},{5,6},{6,1},{7,0},{8,11},{9,10},{10,... | collective-permute-start | bytes 196616 | tf_op jit(solution)/shard_map/ppermute | solution.py:398
  76.7 1.7 %along.3 = (bf16[144,256]{1,0:T(8,128)(2,1)S(1)}, bf16[144,256]{1,0:T(8,128)(2,1)}, bf16[128,128]{1,0:T(8,128)(2,1)S(1)}) custom-call(s32[10]{0:T(128)S(1)} %stack.78.block_ref.place_ref, bf16[144,256]{1,0:T(8,128)(2,1)S(1)} %get-tuple-element.79.p0, bf16[144,256]{1,0:T(8,128)(2,1)S(1)} %collective-permute-done.29.p1, ...), custom_call_target="tpu_custom_call" | custom-call | flops 16777216 | bytes 262144 | tf_op jit(solution)/shard_map/along/pallas_call | solution.py:363
  78.4 6.1 %collective-permute-start.32 = (bf16[128,128]{1,0:T(8,128)(2,1)S(1)}, bf16[128,128]{1,0:T(8,128)(2,1)S(1)}, u32[]{:S(2)}, u32[]{:S(2)}) collective-permute-start(bf16[128,128]{1,0:T(8,128)(2,1)S(1)} %get-tuple-element.81), channel_id=1, source_target_pairs={{0,128},{32,160},{64,192},{96,224},{1,129},{33,161},{65,193},{97,2... | collective-permute-start | bytes 98312 | tf_op jit(solution)/shard_map/ppermute | solution.py:386
  84.5 2.8 %collective-permute-start.13 = (bf16[128,256]{1,0:T(8,128)(2,1)S(1)}, bf16[128,256]{1,0:T(8,128)(2,1)S(1)}, u32[]{:S(2)}, u32[]{:S(2)}) collective-permute-start(bf16[128,256]{1,0:T(8,128)(2,1)S(1)} %get-tuple-element.62), channel_id=1, source_target_pairs={{0,6},{1,7},{2,0},{3,1},{4,2},{5,3},{6,4},{7,5},{8,14},{9,15},{10,... | collective-permute-start | bytes 196616 | tf_op jit(solution)/shard_map/ppermute | solution.py:398
  89.8 2.6 %collective-permute-start.16 = (bf16[128,256]{1,0:T(8,128)(2,1)S(1)}, bf16[128,256]{1,0:T(8,128)(2,1)S(1)}, u32[]{:S(2)}, u32[]{:S(2)}) collective-permute-start(bf16[128,256]{1,0:T(8,128)(2,1)S(1)} %get-tuple-element.65), channel_id=1, source_target_pairs={{0,5},{1,4},{2,7},{3,6},{4,1},{5,0},{6,3},{7,2},{8,13},{9,12},{10,... | collective-permute-start | bytes 196616 | tf_op jit(solution)/shard_map/ppermute | solution.py:398
  92.9 2.4 %finish.1 = (bf16[128,128]{1,0:T(8,128)(2,1)S(1)}, bf16[128,128]{1,0:T(8,128)(2,1)S(1)}, bf16[128,128]{1,0:T(8,128)(2,1)S(1)}, bf16[128,128]{1,0:T(8,128)(2,1)S(...) custom-call(s32[10]{0:T(128)S(1)} %stack.78.block_ref.place_ref, ...), custom_call_target="tpu_custom_call" | custom-call | flops 67108864 | bytes 2097152 | tf_op jit(solution)/shard_map/finish/pallas_call | solution.py:438
  97.9 3.0 %collective-permute-done.34.refs_2_ = bf16[128,128]{1,0:T(8,128)(2,1)S(1)} collective-permute-done((bf16[128,128]{1,0:T(8,128)(2,1)S(1)}, bf16[128,128]{1,0:T(8,128)(2,1)S(1)}, u32[]{:S(2)}, u32[]{:S(2)}) %collective-permute-start.34) | collective-permute-done | bytes 32800 | tf_op jit(solution)/shard_map/ppermute | solution.py:398
  100.9 6.9 %collective-permute-done.22.refs_14_ = bf16[144,2048]{1,0:T(8,128)(2,1)S(1)} collective-permute-done((bf16[144,2048]{1,0:T(8,128)(2,1)}, bf16[144,2048]{1,0:T(8,128)(2,1)S(1)}, u32[]{:S(2)}, u32[]{:S(2)}) %collective-permute-start.22) | collective-permute-done | bytes 589856 | tf_op jit(solution)/shard_map/ppermute | solution.py:381
  108.7 5.4 %collective-permute-done.24.refs_22_ = bf16[128,2048]{1,0:T(8,128)(2,1)S(1)} collective-permute-done((bf16[128,2048]{1,0:T(8,128)(2,1)S(1)}, bf16[128,2048]{1,0:T(8,128)(2,1)S(1)}, u32[]{:S(2)}, u32[]{:S(2)}) %collective-permute-start.24) | collective-permute-done | bytes 524320 | tf_op jit(solution)/shard_map/ppermute | solution.py:381
  114.1 2.4 %collective-permute-start.25 = (bf16[128,2048]{1,0:T(8,128)(2,1)S(1)}, bf16[128,2048]{1,0:T(8,128)(2,1)S(1)}, u32[]{:S(2)}, u32[]{:S(2)}) collective-permute-start(bf16[128,2048]{1,0:T(8,128)(2,1)S(1)} %collective-permute-done.24.refs_22_), channel_id=1, source_target_pairs={{0,1},{1,0},{2,3},{3,2},{4,5},{5,4},{6,7},{7,6},{8,9},{9,8},{10,11... | collective-permute-start | bytes 1572872 | tf_op jit(solution)/shard_map/ppermute | solution.py:390
  116.4 1.5 %collective-permute-done.25.refs_23_ = bf16[128,2048]{1,0:T(8,128)(2,1)S(1)} collective-permute-done((bf16[128,2048]{1,0:T(8,128)(2,1)S(1)}, bf16[128,2048]{1,0:T(8,128)(2,1)S(1)}, u32[]{:S(2)}, u32[]{:S(2)}) %collective-permute-start.25) | collective-permute-done | bytes 524320 | tf_op jit(solution)/shard_map/ppermute | solution.py:390
  119.5 2.3 %collective-permute-start.38 = (bf16[128,128]{1,0:T(8,128)(2,1)S(1)}, bf16[128,128]{1,0:T(8,128)(2,1)S(1)}, u32[]{:S(2)}, u32[]{:S(2)}) collective-permute-start(bf16[128,128]{1,0:T(8,128)(2,1)S(1)} %get-tuple-element.89), channel_id=1, source_target_pairs={{0,4},{1,5},{2,6},{3,7},{4,0},{5,1},{6,2},{7,3},{8,12},{9,13},{10,... | collective-permute-start | bytes 98312 | tf_op jit(solution)/shard_map/ppermute | solution.py:398
  123.0 5.1 %conv_out.1 = (f32[128,2048]{1,0:T(8,128)S(1)}, bf16[8,128,2048]{2,1,0:T(8,128)(2,1)S(1)}) custom-call(bf16[128,256]{1,0:T(8,128)(2,1)S(1)} %get-tuple-element.58.refs_0_, bf16[128,256]{1,0:T(8,128)(2,1)S(1)} %collective-permute-done.10.refs_1_, bf16[128,256]{1,0:T(8,128)(2,1)S(1)} %collective-permute-done.11.refs_2_, ...), custom_call_target="tpu_custom_call" | custom-call | flops 536870912 | bytes 6291456 | tf_op jit(solution)/shard_map/conv_out/pallas_call | solution.py:603
  128.2 2.9 %delta_out.1 = bf16[128,2048]{1,0:T(8,128)(2,1)} custom-call(f32[128,2048]{1,0:T(8,128)S(1)} %get-tuple-element.69.conv_ref, bf16[8,128,2048]{2,1,0:T(8,128)(2,1)S(1)} %get-tuple-element.70.weights, bf16[128,128]{1,0:T(8,128)(2,1)S(1)} %get-tuple-element.83.refs_0_, bf16[128,128]{1,0:T(8,128)(2,1)S(1)} %collective-permute-done.33.refs_1_, ...), custom_call_target="tpu_custom_call" | custom-call | flops 536870912 | bytes 6291456 | tf_op jit(solution)/shard_map/delta_out/pallas_call | solution.py:631
  (85 shorter events, 21.1 us)
Async XLA Ops:
  0.0 14.5 %collective-permute-start.1 = (bf16[1024,256]{1,0:T(8,128)(2,1)}, bf16[1024,256]{1,0:T(8,128)(2,1)S(1)}, u32[]{:S(2)}, u32[]{:S(2)}) collective-permute-start(bf16[1024,256]{1,0:T(8,128)(2,1)} %refs_0_.1), channel_id=1, source_target_pairs={{0,6},{2,0},{4,2},{6,4},{1,7},{3,1},{5,3},{7,5},{8,14},{10,8},{12,... | collective-permute-start | bytes 1572872 | tf_op jit(solution)/shard_map/ppermute | solution.py:381
  3.6 13.9 %collective-permute-start = (bf16[1024,256]{1,0:T(8,128)(2,1)}, bf16[1024,256]{1,0:T(8,128)(2,1)S(1)}, u32[]{:S(2)}, u32[]{:S(2)}) collective-permute-start(bf16[1024,256]{1,0:T(8,128)(2,1)} %refs_0_.1), channel_id=1, source_target_pairs={{0,2},{2,4},{4,6},{6,0},{1,3},{3,5},{5,7},{7,1},{8,10},{10,12},{12... | collective-permute-start | bytes 1572872 | tf_op jit(solution)/shard_map/ppermute | solution.py:381
  3.6 25.6 %collective-permute-start.2 = (bf16[1024,256]{1,0:T(8,128)(2,1)}, bf16[1024,256]{1,0:T(8,128)(2,1)S(1)}, u32[]{:S(2)}, u32[]{:S(2)}) collective-permute-start(bf16[1024,256]{1,0:T(8,128)(2,1)} %refs_0_.1), channel_id=1, source_target_pairs={{0,1},{1,0},{2,3},{3,2},{4,5},{5,4},{6,7},{7,6},{8,9},{9,8},{10,11... | collective-permute-start | bytes 1572872 | tf_op jit(solution)/shard_map/ppermute | solution.py:390
  18.4 7.6 %collective-permute-start.5 = (bf16[512,256]{1,0:T(8,128)(2,1)}, bf16[512,256]{1,0:T(8,128)(2,1)S(1)}, u32[]{:S(2)}, u32[]{:S(2)}) collective-permute-start(bf16[512,256]{1,0:T(8,128)(2,1)} %get-tuple-element.52), channel_id=1, source_target_pairs={{0,2},{2,4},{4,6},{6,0},{1,3},{3,5},{5,7},{7,1},{8,10},{10,12},{12... | collective-permute-start | bytes 786440 | tf_op jit(solution)/shard_map/ppermute | solution.py:381
  18.5 10.7 %collective-permute-start.7 = (bf16[512,256]{1,0:T(8,128)(2,1)}, bf16[512,256]{1,0:T(8,128)(2,1)S(1)}, u32[]{:S(2)}, u32[]{:S(2)}) collective-permute-start(bf16[512,256]{1,0:T(8,128)(2,1)} %get-tuple-element.53), channel_id=1, source_target_pairs={{0,6},{2,0},{4,2},{6,4},{1,7},{3,1},{5,3},{7,5},{8,14},{10,8},{12,... | collective-permute-start | bytes 786440 | tf_op jit(solution)/shard_map/ppermute | solution.py:381
  29.1 55.4 %collective-permute-start.20 = (bf16[272,2048]{1,0:T(8,128)(2,1)S(1)}, bf16[272,2048]{1,0:T(8,128)(2,1)S(1)}, u32[]{:S(2)}, u32[]{:S(2)}) collective-permute-start(bf16[272,2048]{1,0:T(8,128)(2,1)S(1)} %fusion.1.refs_8_.refs_16_), channel_id=1, source_target_pairs={{0,6},{2,0},{4,2},{6,4},{1,7},{3,1},{5,3},{7,5},{8,14},{10,8},{12,... | collective-permute-start | bytes 3342344 | tf_op jit(solution)/shard_map/ppermute | solution.py:381
  29.1 58.2 %collective-permute-start.18 = (bf16[272,2048]{1,0:T(8,128)(2,1)S(1)}, bf16[272,2048]{1,0:T(8,128)(2,1)S(1)}, u32[]{:S(2)}, u32[]{:S(2)}) collective-permute-start(bf16[272,2048]{1,0:T(8,128)(2,1)S(1)} %fusion.1.refs_8_.refs_16_), channel_id=1, source_target_pairs={{0,2},{2,4},{4,6},{6,0},{1,3},{3,5},{5,7},{7,1},{8,10},{10,12},{12... | collective-permute-start | bytes 3342344 | tf_op jit(solution)/shard_map/ppermute | solution.py:381
  47.8 4.8 %collective-permute-start.28 = (bf16[144,256]{1,0:T(8,128)(2,1)S(1)}, bf16[144,256]{1,0:T(8,128)(2,1)S(1)}, u32[]{:S(2)}, u32[]{:S(2)}) collective-permute-start(bf16[144,256]{1,0:T(8,128)(2,1)S(1)} %get-tuple-element.78.p0), channel_id=1, source_target_pairs={{0,8},{8,16},{16,24},{24,0},{1,9},{9,17},{17,25},{25,1},{2,10},{10... | collective-permute-start | bytes 221192 | tf_op jit(solution)/shard_map/ppermute | solution.py:381
  50.5 4.7 %collective-permute-start.26 = (bf16[144,256]{1,0:T(8,128)(2,1)S(1)}, bf16[144,256]{1,0:T(8,128)(2,1)S(1)}, u32[]{:S(2)}, u32[]{:S(2)}) collective-permute-start(bf16[144,256]{1,0:T(8,128)(2,1)S(1)} %get-tuple-element.78.p0), channel_id=1, source_target_pairs={{0,16},{8,24},{16,0},{24,8},{1,17},{9,25},{17,1},{25,9},{2,18},{10... | collective-permute-start | bytes 221192 | tf_op jit(solution)/shard_map/ppermute | solution.py:381
  56.9 14.2 %collective-permute-start.31 = (bf16[144,256]{1,0:T(8,128)(2,1)S(1)}, bf16[144,256]{1,0:T(8,128)(2,1)S(1)}, u32[]{:S(2)}, u32[]{:S(2)}) collective-permute-start(bf16[144,256]{1,0:T(8,128)(2,1)S(1)} %get-tuple-element.79.p0), channel_id=1, source_target_pairs={{0,32},{32,64},{64,96},{96,0},{128,160},{160,192},{192,224},{224,1... | collective-permute-start | bytes 221192 | tf_op jit(solution)/shard_map/ppermute | solution.py:729
  58.5 5.8 %collective-permute-start.9 = (bf16[32,128]{1,0:T(8,128)(2,1)S(1)}, bf16[32,128]{1,0:T(8,128)(2,1)S(1)}, u32[]{:S(2)}, u32[]{:S(2)}) collective-permute-start(bf16[32,128]{1,0:T(8,128)(2,1)S(1)} %get-tuple-element.56), channel_id=1, source_target_pairs={{0,8},{8,16},{16,24},{24,32},{32,40},{40,48},{48,56},{56,64},{64,7... | collective-permute-start | bytes 24584 | tf_op jit(solution)/shard_map/ppermute | solution.py:742
  61.5 13.7 %collective-permute-start.30 = (bf16[144,256]{1,0:T(8,128)(2,1)S(1)}, bf16[144,256]{1,0:T(8,128)(2,1)S(1)}, u32[]{:S(2)}, u32[]{:S(2)}) collective-permute-start(bf16[144,256]{1,0:T(8,128)(2,1)S(1)} %get-tuple-element.79.p0), channel_id=1, source_target_pairs={{0,96},{32,0},{64,32},{96,64},{128,224},{160,128},{192,160},{224,1... | collective-permute-start | bytes 221192 | tf_op jit(solution)/shard_map/ppermute | solution.py:729
  64.3 10.9 %collective-permute-start.29 = (bf16[144,256]{1,0:T(8,128)(2,1)S(1)}, bf16[144,256]{1,0:T(8,128)(2,1)S(1)}, u32[]{:S(2)}, u32[]{:S(2)}) collective-permute-start(bf16[144,256]{1,0:T(8,128)(2,1)S(1)} %get-tuple-element.79.p0), channel_id=1, source_target_pairs={{0,64},{32,96},{64,0},{96,32},{128,192},{160,224},{192,128},{224,1... | collective-permute-start | bytes 221192 | tf_op jit(solution)/shard_map/ppermute | solution.py:729
  71.1 7.3 %collective-permute-start.10 = (bf16[128,256]{1,0:T(8,128)(2,1)S(1)}, bf16[128,256]{1,0:T(8,128)(2,1)S(1)}, u32[]{:S(2)}, u32[]{:S(2)}) collective-permute-start(bf16[128,256]{1,0:T(8,128)(2,1)S(1)} %get-tuple-element.59), channel_id=1, source_target_pairs={{0,1},{1,0},{2,3},{3,2},{4,5},{5,4},{6,7},{7,6},{8,9},{9,8},{10,11... | collective-permute-start | bytes 196616 | tf_op jit(solution)/shard_map/ppermute | solution.py:398
  75.2 14.1 %collective-permute-start.11 = (bf16[128,256]{1,0:T(8,128)(2,1)S(1)}, bf16[128,256]{1,0:T(8,128)(2,1)S(1)}, u32[]{:S(2)}, u32[]{:S(2)}) collective-permute-start(bf16[128,256]{1,0:T(8,128)(2,1)S(1)} %get-tuple-element.60), channel_id=1, source_target_pairs={{0,2},{1,3},{2,4},{3,5},{4,6},{5,7},{6,0},{7,1},{8,10},{9,11},{10,... | collective-permute-start | bytes 196616 | tf_op jit(solution)/shard_map/ppermute | solution.py:398
  75.2 14.6 %collective-permute-start.12 = (bf16[128,256]{1,0:T(8,128)(2,1)S(1)}, bf16[128,256]{1,0:T(8,128)(2,1)S(1)}, u32[]{:S(2)}, u32[]{:S(2)}) collective-permute-start(bf16[128,256]{1,0:T(8,128)(2,1)S(1)} %get-tuple-element.61), channel_id=1, source_target_pairs={{0,3},{1,2},{2,5},{3,4},{4,7},{5,6},{6,1},{7,0},{8,11},{9,10},{10,... | collective-permute-start | bytes 196616 | tf_op jit(solution)/shard_map/ppermute | solution.py:398
  78.4 13.9 %collective-permute-start.32 = (bf16[128,128]{1,0:T(8,128)(2,1)S(1)}, bf16[128,128]{1,0:T(8,128)(2,1)S(1)}, u32[]{:S(2)}, u32[]{:S(2)}) collective-permute-start(bf16[128,128]{1,0:T(8,128)(2,1)S(1)} %get-tuple-element.81), channel_id=1, source_target_pairs={{0,128},{32,160},{64,192},{96,224},{1,129},{33,161},{65,193},{97,2... | collective-permute-start | bytes 98312 | tf_op jit(solution)/shard_map/ppermute | solution.py:386
  84.5 10.7 %collective-permute-start.13 = (bf16[128,256]{1,0:T(8,128)(2,1)S(1)}, bf16[128,256]{1,0:T(8,128)(2,1)S(1)}, u32[]{:S(2)}, u32[]{:S(2)}) collective-permute-start(bf16[128,256]{1,0:T(8,128)(2,1)S(1)} %get-tuple-element.62), channel_id=1, source_target_pairs={{0,6},{1,7},{2,0},{3,1},{4,2},{5,3},{6,4},{7,5},{8,14},{9,15},{10,... | collective-permute-start | bytes 196616 | tf_op jit(solution)/shard_map/ppermute | solution.py:398
  87.3 8.7 %collective-permute-start.14 = (bf16[128,256]{1,0:T(8,128)(2,1)S(1)}, bf16[128,256]{1,0:T(8,128)(2,1)S(1)}, u32[]{:S(2)}, u32[]{:S(2)}) collective-permute-start(bf16[128,256]{1,0:T(8,128)(2,1)S(1)} %get-tuple-element.63), channel_id=1, source_target_pairs={{0,7},{1,6},{2,1},{3,0},{4,3},{5,2},{6,5},{7,4},{8,15},{9,14},{10,... | collective-permute-start | bytes 196616 | tf_op jit(solution)/shard_map/ppermute | solution.py:398
  89.3 6.8 %collective-permute-start.15 = (bf16[128,256]{1,0:T(8,128)(2,1)S(1)}, bf16[128,256]{1,0:T(8,128)(2,1)S(1)}, u32[]{:S(2)}, u32[]{:S(2)}) collective-permute-start(bf16[128,256]{1,0:T(8,128)(2,1)S(1)} %get-tuple-element.64), channel_id=1, source_target_pairs={{0,4},{1,5},{2,6},{3,7},{4,0},{5,1},{6,2},{7,3},{8,12},{9,13},{10,... | collective-permute-start | bytes 196616 | tf_op jit(solution)/shard_map/ppermute | solution.py:398
  89.8 6.8 %collective-permute-start.16 = (bf16[128,256]{1,0:T(8,128)(2,1)S(1)}, bf16[128,256]{1,0:T(8,128)(2,1)S(1)}, u32[]{:S(2)}, u32[]{:S(2)}) collective-permute-start(bf16[128,256]{1,0:T(8,128)(2,1)S(1)} %get-tuple-element.65), channel_id=1, source_target_pairs={{0,5},{1,4},{2,7},{3,6},{4,1},{5,0},{6,3},{7,2},{8,13},{9,12},{10,... | collective-permute-start | bytes 196616 | tf_op jit(solution)/shard_map/ppermute | solution.py:398
  92.4 15.5 %collective-permute-start.22 = (bf16[144,2048]{1,0:T(8,128)(2,1)}, bf16[144,2048]{1,0:T(8,128)(2,1)S(1)}, u32[]{:S(2)}, u32[]{:S(2)}) collective-permute-start(bf16[144,2048]{1,0:T(8,128)(2,1)} %get-tuple-element.67), channel_id=1, source_target_pairs={{0,6},{2,0},{4,2},{6,4},{1,7},{3,1},{5,3},{7,5},{8,14},{10,8},{12,... | collective-permute-start | bytes 1769480 | tf_op jit(solution)/shard_map/ppermute | solution.py:381
  96.0 20.4 %collective-permute-start.17 = (bf16[272,2048]{1,0:T(8,128)(2,1)S(1)}, bf16[272,2048]{1,0:T(8,128)(2,1)S(1)}, u32[]{:S(2)}, u32[]{:S(2)}) collective-permute-start(bf16[272,2048]{1,0:T(8,128)(2,1)S(1)} %fusion.1.refs_8_.refs_16_), channel_id=1, source_target_pairs={{0,1},{1,0},{2,3},{3,2},{4,5},{5,4},{6,7},{7,6},{8,9},{9,8},{10,11... | collective-permute-start | bytes 3342344 | tf_op jit(solution)/shard_map/ppermute | solution.py:390
  96.2 22.9 %collective-permute-start.21 = (bf16[272,2048]{1,0:T(8,128)(2,1)S(1)}, bf16[272,2048]{1,0:T(8,128)(2,1)S(1)}, u32[]{:S(2)}, u32[]{:S(2)}) collective-permute-start(bf16[272,2048]{1,0:T(8,128)(2,1)S(1)} %collective-permute-done.20.left_any.refs_12_.refs_20_), channel_id=1, source_target_pairs={{0,1},{1,0},{2,3},{3,2},{4,5},{5,4},{6,7},{7,6},{8,9},{9,8},{10,11... | collective-permute-start | bytes 3342344 | tf_op jit(solution)/shard_map/ppermute | solution.py:390
  96.6 22.9 %collective-permute-start.19 = (bf16[272,2048]{1,0:T(8,128)(2,1)S(1)}, bf16[272,2048]{1,0:T(8,128)(2,1)S(1)}, u32[]{:S(2)}, u32[]{:S(2)}) collective-permute-start(bf16[272,2048]{1,0:T(8,128)(2,1)S(1)} %collective-permute-done.18.right_any.refs_10_.refs_18_), channel_id=1, source_target_pairs={{0,1},{1,0},{2,3},{3,2},{4,5},{5,4},{6,7},{7,6},{8,9},{9,8},{10,11... | collective-permute-start | bytes 3342344 | tf_op jit(solution)/shard_map/ppermute | solution.py:390
  100.9 13.2 %collective-permute-start.24 = (bf16[128,2048]{1,0:T(8,128)(2,1)S(1)}, bf16[128,2048]{1,0:T(8,128)(2,1)S(1)}, u32[]{:S(2)}, u32[]{:S(2)}) collective-permute-start(bf16[128,2048]{1,0:T(8,128)(2,1)S(1)} %copy-done.6), channel_id=1, source_target_pairs={{0,2},{2,4},{4,6},{6,0},{1,3},{3,5},{5,7},{7,1},{8,10},{10,12},{12... | collective-permute-start | bytes 1572872 | tf_op jit(solution)/shard_map/ppermute | solution.py:381
  107.9 13.9 %collective-permute-start.23 = (bf16[144,2048]{1,0:T(8,128)(2,1)S(1)}, bf16[144,2048]{1,0:T(8,128)(2,1)S(1)}, u32[]{:S(2)}, u32[]{:S(2)}) collective-permute-start(bf16[144,2048]{1,0:T(8,128)(2,1)S(1)} %collective-permute-done.22.refs_14_), channel_id=1, source_target_pairs={{0,1},{1,0},{2,3},{3,2},{4,5},{5,4},{6,7},{7,6},{8,9},{9,8},{10,11... | collective-permute-start | bytes 1769480 | tf_op jit(solution)/shard_map/ppermute | solution.py:390
  116.4 11.7 %collective-permute-start.35 = (bf16[128,128]{1,0:T(8,128)(2,1)S(1)}, bf16[128,128]{1,0:T(8,128)(2,1)S(1)}, u32[]{:S(2)}, u32[]{:S(2)}) collective-permute-start(bf16[128,128]{1,0:T(8,128)(2,1)S(1)} %get-tuple-element.86), channel_id=1, source_target_pairs={{0,3},{1,2},{2,5},{3,4},{4,7},{5,6},{6,1},{7,0},{8,11},{9,10},{10,... | collective-permute-start | bytes 98312 | tf_op jit(solution)/shard_map/ppermute | solution.py:398
  118.0 10.2 %collective-permute-start.36 = (bf16[128,128]{1,0:T(8,128)(2,1)S(1)}, bf16[128,128]{1,0:T(8,128)(2,1)S(1)}, u32[]{:S(2)}, u32[]{:S(2)}) collective-permute-start(bf16[128,128]{1,0:T(8,128)(2,1)S(1)} %get-tuple-element.87), channel_id=1, source_target_pairs={{0,6},{1,7},{2,0},{3,1},{4,2},{5,3},{6,4},{7,5},{8,14},{9,15},{10,... | collective-permute-start | bytes 98312 | tf_op jit(solution)/shard_map/ppermute | solution.py:398
  119.0 9.1 %collective-permute-start.37 = (bf16[128,128]{1,0:T(8,128)(2,1)S(1)}, bf16[128,128]{1,0:T(8,128)(2,1)S(1)}, u32[]{:S(2)}, u32[]{:S(2)}) collective-permute-start(bf16[128,128]{1,0:T(8,128)(2,1)S(1)} %get-tuple-element.88), channel_id=1, source_target_pairs={{0,7},{1,6},{2,1},{3,0},{4,3},{5,2},{6,5},{7,4},{8,15},{9,14},{10,... | collective-permute-start | bytes 98312 | tf_op jit(solution)/shard_map/ppermute | solution.py:398
  119.5 8.7 %collective-permute-start.38 = (bf16[128,128]{1,0:T(8,128)(2,1)S(1)}, bf16[128,128]{1,0:T(8,128)(2,1)S(1)}, u32[]{:S(2)}, u32[]{:S(2)}) collective-permute-start(bf16[128,128]{1,0:T(8,128)(2,1)S(1)} %get-tuple-element.89), channel_id=1, source_target_pairs={{0,4},{1,5},{2,6},{3,7},{4,0},{5,1},{6,2},{7,3},{8,12},{9,13},{10,... | collective-permute-start | bytes 98312 | tf_op jit(solution)/shard_map/ppermute | solution.py:398
  121.8 6.4 %collective-permute-start.39 = (bf16[128,128]{1,0:T(8,128)(2,1)S(1)}, bf16[128,128]{1,0:T(8,128)(2,1)S(1)}, u32[]{:S(2)}, u32[]{:S(2)}) collective-permute-start(bf16[128,128]{1,0:T(8,128)(2,1)S(1)} %get-tuple-element.90), channel_id=1, source_target_pairs={{0,5},{1,4},{2,7},{3,6},{4,1},{5,0},{6,3},{7,2},{8,13},{9,12},{10,... | collective-permute-start | bytes 98312 | tf_op jit(solution)/shard_map/ppermute | solution.py:398
  (16 other events, 87.5 us)

commit v5 on v4

--- a/solution.py
+++ b/solution.py
@@ -94,72 +94,90 @@
     return dot(a_high, b_high) + (dot(a_high, b_low) + dot(a_low, b_high))
 
 
+def pack_kernel(*refs):
+    sides, packed, sems = refs[:8], refs[8], refs[9]
+    for one in fetch(
+        sems,
+        *((ref, packed.at[n // 2, :, pl.ds(n % 2 * 128, 128)]) for n, ref in enumerate(sides)),
+    ):
+        one.wait()
+
+
+def pack(weights):
+    depth, width = weights[0].shape
+    return pl.pallas_call(
+        pack_kernel,
+        in_specs=[anywhere()] * 8,
+        out_specs=whole(),
+        out_shape=pltpu.VMEM((4, depth, 2 * width), BF16),
+        scratch_shapes=[pltpu.SemaphoreType.DMA((8,))],
+        compiler_params=params(4),
+        cost_estimate=cost(1 << 20, 8 << 20),
+        name="pack",
+    )(*map(home, weights))
+
+
 def project_kernel(width_all, head_size, block_ref, rate_ref, *refs):
-    own, sw, r1, sr1, l1, sl1, fa, sfa, fb, sfb = refs[:10]
-    sides = refs[10:18]
-    q_ref, k_ref, v_ref, bl_ref, tail_ref, dg_hbm, gu_hbm, cg_hbm = refs[18:26]
-    gathered, weights, factors, dg_ref, gu_ref, cg_ref, sems, out_sems = refs[26:]
-    rows, piece_width = own.shape[0], own.shape[1]
+    near, (fa, sfa, fb, sfb), weights = refs[:6], refs[6:10], refs[10]
+    q_ref, k_ref, v_ref, bl_ref, tail_ref, dg_ref, gu_ref, cg_ref = refs[11:19]
+    far, factors, sems = refs[19:]
+    rows, piece_width = near[0].shape
     half = rows // 2
-    places = [slice(0, half), slice(half, rows)]
-
-    def columns(slot):
-        return pl.ds(pl.multiple_of(block_ref[slot] * piece_width, piece_width), piece_width)
-
-    moves = [[], []]
-    for n, here in enumerate(places):
-        for slot, ref in enumerate((own, sw, r1, sr1, l1, sl1)):
-            moves[n].append((ref.at[here, :], gathered.at[here, columns(slot)]))
-        for slot, ref in enumerate(((fa, sfa), (fb, sfb))[n]):
-            moves[n].append((ref, gathered.at[here, columns(6 + slot)]))
-    parts = [
-        (ref, weights.at[n // 2, :, pl.ds(n % 2 * 128, 128)]) for n, ref in enumerate(sides)
-    ]
-    first = fetch(sems, *moves[0])
-    loads = fetch(sems.at[pl.ds(16, 2)], *parts[:2])
-    second = fetch(sems.at[pl.ds(8, 8)], *moves[1])
-    loads += fetch(sems.at[pl.ds(18, 6)], *parts[2:])
+    moves = fetch(
+        sems,
+        *(
+            (ref, far.at[side, pl.ds(n * half, half), :])
+            for n, pair in enumerate(((fa, sfa), (fb, sfb)))
+            for side, ref in enumerate(pair)
+        ),
+    )
 
     def unit_rows(raw):
         wide = low(raw).astype(F32)
         return wide * lax.rsqrt(jnp.sum(wide * wide, axis=-1, keepdims=True) + TINY_NORM)
 
+    def product(n, here, slots):
+        total = None
+        for slot in slots:
+            piece = near[slot][here, :] if slot < 6 else far[slot - 6, here, :]
+            offset = pl.multiple_of(block_ref[slot] * piece_width, piece_width)
+            term = dot(piece, weights[n, pl.ds(offset, piece_width), :])
+            total = term if total is None else total + term
+        return total
+
     def pair(n, here):
-        both = dot(gathered[here, :], weights[n]) * factors[here, :]
+        both = product(n, here, range(8)) * factors[here, :]
         return both[:, :128], both[:, 128:]
 
     def each_half(body):
         def step(n, carry):
-            body(n, pl.ds(pl.multiple_of(n * half, half), half))
+            body(pl.ds(pl.multiple_of(n * half, half), half))
             return carry
 
         lax.fori_loop(0, 2, step, 0)
 
-    def gated(n, here):
-        for which, pieces in enumerate((first + loads[:2], second)):
-
-            @pl.when(n == which)
-            def _():
-                for one in pieces:
-                    one.wait()
-
-        wide = gathered[here, :].astype(F32)
-        squares = jnp.sum(wide * wide, axis=1, keepdims=True)
+    def gated(here):
+        squares = jnp.zeros((half, piece_width), F32)
+        for slot in range(8):
+            piece = near[slot][here, :] if slot < 6 else far[slot - 6, here, :]
+            wide = piece.astype(F32)
+            squares = squares + wide * wide
+        squares = jnp.sum(squares, axis=1, keepdims=True)
         factors[here, :] = lax.rsqrt(squares / width_all + TINY_NORM)
         gv, gg = pair(0, here)
         gu_ref[here, :] = low(low(gv).astype(F32) * jax.nn.sigmoid(low(gg).astype(F32)))
 
-    def gates(n, here):
+    def gates(here):
         dg, cg = pair(1, here)
         dg_ref[here, :] = low(dg)
         cg_ref[here, :] = low(cg)
 
-    def queries(n, here):
+    def queries(here):
         q, k = pair(2, here)
         q_ref[here, :] = low(unit_rows(q) * head_size ** (-0.5))
         k_ref[here, :] = low(unit_rows(k))
 
-    def rest_of(n, here):
+    def rest_of(here):
         v, bl = pair(3, here)
         v_ref[here, :] = low(v)
         lane = lax.broadcasted_iota(jnp.int32, bl.shape, 1)
@@ -167,40 +185,32 @@
             lane == 0, jax.nn.sigmoid(bl), -rate_ref[0] * jax.nn.softplus(bl)
         )
 
-    each_half(gated)
+    for one in moves:
+        one.wait()
+    for body in (gated, gates, queries, rest_of):
+        each_half(body)
     tail_ref[...] = gu_ref[rows - HALO :, :]
-    stores = fetch(out_sems, (gu_ref, gu_hbm))
-    for n, body in enumerate((gates, queries, rest_of)):
-        for one in loads[2 * n + 2 : 2 * n + 4]:
-            one.wait()
-        each_half(body)
-        if n == 0:
-            stores += fetch(out_sems.at[pl.ds(1, 2)], (dg_ref, dg_hbm), (cg_ref, cg_hbm))
-    for one in stores:
-        one.wait()
 
 
 def project(pieces, weights, blocks, rate, width_all, head_size):
-    rows = pieces[0].shape[0]
+    rows, piece_width = pieces[0].shape
     kinds = [BF16] * 3 + [F32] + [BF16] * 3
     return pl.pallas_call(
         functools.partial(project_kernel, width_all, head_size),
-        in_specs=[scalars(), scalars()] + [anywhere()] * 18,
-        out_specs=[whole()] * 5 + [hbm()] * 3,
+        in_specs=[scalars(), scalars()] + [whole()] * 11,
+        out_specs=[whole()] * 8,
         out_shape=[pltpu.VMEM((rows, 128), kind) for kind in kinds[:4]]
         + [pltpu.VMEM((HALO, 128), BF16)]
-        + [pltpu.HBM((rows, 128), kind) for kind in kinds[4:]],
+        + [pltpu.VMEM((rows, 128), kind) for kind in kinds[4:]],
         scratch_shapes=[
-            pltpu.VMEM((rows, width_all), BF16),
-            pltpu.VMEM((4, width_all, 256), BF16),
+            pltpu.VMEM((2, rows, piece_width), BF16),
             pltpu.VMEM((rows, 1), F32),
-        ]
-        + [pltpu.VMEM((rows, 128), BF16)] * 3
-        + [pltpu.SemaphoreType.DMA((24,)), pltpu.SemaphoreType.DMA((3,))],
-        compiler_params=params(28),
+            pltpu.SemaphoreType.DMA((4,)),
+        ],
+        compiler_params=params(20),
         cost_estimate=cost(2 * rows * width_all * 1024, 12 << 20),
         name="project",
-    )(blocks, rate, home(pieces[0]), *pieces[1:], *map(home, weights))
+    )(blocks, rate, *map(near_core, pieces), near_core(weights))
 
 
 def write_state(ref, state):
@@ -236,7 +246,7 @@
 
 
 def delta_kernel(
-    q_ref, k_ref, v_ref, bl_ref, coef_p_hbm, coef_q_hbm, state_ref, coef_p_ref, coef_q_ref, sems
+    q_ref, k_ref, v_ref, bl_ref, coef_p_ref, coef_q_ref, state_ref
 ):
     rows, size = q_ref.shape
     chunks = rows // CHUNK
@@ -297,18 +307,12 @@
     carried = jnp.where(row == column, 1.0, 0.0)
     made = jnp.zeros((CHUNK, size), F32)
     log_total = jnp.zeros((1, CHUNK), F32)
-    stores = []
     for n in range(chunks):
         here = slice(n * CHUNK, (n + 1) * CHUNK)
         rounded = low(jnp.concatenate([carried, made], axis=1))
         seen = dot(queries[n], rounded)
         coef_p_ref[here, :] = low(seen[:, :size])
         coef_q_ref[here, :] = seen[:, size:] + starts[n]
-        stores += fetch(
-            sems.at[n],
-            (coef_p_ref.at[here, :], coef_p_hbm.at[here, :]),
-            (coef_q_ref.at[here, :], coef_q_hbm.at[here, :]),
-        )
         moved = dot(losts[n], rounded)
         keep = jnp.exp(tails[n])
         carried = carried * keep - moved[:, :size]
@@ -317,8 +321,6 @@
     total = jnp.exp(log_total)[:, 0:1]
     lost = jnp.where(row == column, total, 0.0) - carried
     write_state(state_ref, (total, lost, made))
-    for one in stores:
-        one.wait()
 
 
 def delta(q, k, v, bl):
@@ -326,21 +328,16 @@
     return pl.pallas_call(
         delta_kernel,
         in_specs=[whole()] * 4,
-        out_specs=[hbm(), hbm(), whole()],
+        out_specs=[whole()] * 3,
         out_shape=[
-            pltpu.HBM((rows, size), BF16),
-            pltpu.HBM((rows, size), F32),
-            pltpu.VMEM((size + 16, 2 * size), BF16),
-        ],
-        scratch_shapes=[
             pltpu.VMEM((rows, size), BF16),
             pltpu.VMEM((rows, size), F32),
-            pltpu.SemaphoreType.DMA((rows // CHUNK, 2)),
+            pltpu.VMEM((size + 16, 2 * size), BF16),
         ],
         compiler_params=params(16),
         cost_estimate=cost(2 * rows * size * size * 60, 3 << 20),
         name="delta",
-    )(q, k, v, bl)
+    )(*map(near_core, (q, k, v, bl)))
 
 
 def along_kernel(which, place_ref, p0, p1, p2, p3, before_ref, total_ref, made_ref, held):
@@ -400,27 +397,12 @@
 
 
 def finish_kernel(
-    block_ref, coef_p_hbm, coef_q_hbm, dg_hbm, gain_ref, reach_any, far_any, before_hbm, *rest
+    block_ref, coef_p_ref, coef_q_ref, dg_ref, gain_ref, reach_ref, far_ref, before_ref, *outs
 ):
-    outs, scratch = rest[:8], rest[8:]
-    coef_p_ref, coef_q_ref, dg_ref, reach_ref, far_ref, before_ref, sems = scratch
-    loads = fetch(
-        sems,
-        (reach_any, reach_ref),
-        (far_any, far_ref),
-        (before_hbm, before_ref),
-        (coef_p_hbm, coef_p_ref),
-        (coef_q_hbm, coef_q_ref),
-        (dg_hbm, dg_ref),
-    )
-    for one in loads[:3]:
-        one.wait()
     total, lost, made = read_state(reach_ref)
     state = total * far_ref[...].astype(F32) - dot(low(lost), far_ref[...]) + made
     total, lost, made = read_state(before_ref)
     state = low(total * state - dot(low(lost), low(state)) + made)
-    for one in loads[3:]:
-        one.wait()
     step = outs[0].shape[0]
     for slot in range(8):
         here = pl.ds(pl.multiple_of(block_ref[GOES_TO[slot]] * step, step), step)
@@ -430,33 +412,24 @@
         outs[slot][...] = low(result * jax.nn.silu(dg_ref[here, :].astype(F32)))
 
 
-def finish(blocks, coef_p, coef_q, dg, gain, reach, far, before):
-    coef_p, coef_q, dg = map(home, (coef_p, coef_q, dg))
-    rows, size = dg.shape
-    args = (coef_p, coef_q, dg, gain, reach, far, before)
-    copied = (coef_p, coef_q, dg, reach, far, before)
+def finish(blocks, *args):
+    rows, size = args[0].shape
     return pl.pallas_call(
         finish_kernel,
-        in_specs=[scalars(), hbm(), hbm(), hbm(), whole(), anywhere(), anywhere(), anywhere()],
+        in_specs=[scalars()] + [whole()] * 7,
         out_specs=[whole()] * 8,
         out_shape=[pltpu.VMEM((rows // 8, size), BF16)] * 8,
-        scratch_shapes=[pltpu.VMEM(a.shape, a.dtype) for a in copied]
-        + [pltpu.SemaphoreType.DMA((6,))],
-        compiler_params=params(8),
+        compiler_params=params(6),
         cost_estimate=cost(64 << 20, 2 << 20),
         name="finish",
-    )(blocks, *args)
-
-
-def conv_kernel(block_ref, gu_hbm, before_any, taps_ref, cg_hbm, *rest):
-    outs = rest[:8]
-    gu_ref, before_ref, padded, out_ref, cg_ref, sems = rest[8:]
+    )(blocks, *map(near_core, args))
+
+
+def conv_kernel(block_ref, gu_ref, before_ref, taps_ref, cg_ref, *rest):
+    outs, (padded, out_ref) = rest[:8], rest[8:]
     rows, size = gu_ref.shape
     head = before_ref.shape[0]
     count = taps_ref.shape[0]
-    loads = fetch(sems, (gu_hbm, gu_ref), (before_any, before_ref), (cg_hbm, cg_ref))
-    for one in loads[:2]:
-        one.wait()
     padded[0:head, :] = before_ref[...].astype(F32)
     padded[head:, :] = gu_ref[...].astype(F32)
     taps = taps_ref[...].astype(F32)
@@ -472,7 +445,6 @@
         return carry
 
     lax.fori_loop(0, rows // step, block, 0)
-    loads[2].wait()
     part = rows // 8
     for slot in range(8):
         here = pl.ds(pl.multiple_of(block_ref[GOES_TO[slot]] * part, part), part)
@@ -484,31 +456,27 @@
     rows, size = gu.shape
     return pl.pallas_call(
         conv_kernel,
-        in_specs=[scalars(), hbm(), anywhere(), whole(), hbm()],
+        in_specs=[scalars()] + [whole()] * 4,
         out_specs=[whole()] * 8,
         out_shape=[pltpu.VMEM((rows // 8, 2 * size), BF16)] * 8,
         scratch_shapes=[
-            pltpu.VMEM(gu.shape, BF16),
-            pltpu.VMEM(before.shape, BF16),
             pltpu.VMEM((rows + before.shape[0], size), F32),
             pltpu.VMEM((rows, size), BF16),
-            pltpu.VMEM((rows, size), BF16),
-            pltpu.SemaphoreType.DMA((3,)),
         ],
         compiler_params=params(8),
         cost_estimate=cost(256 << 20, 1 << 20),
         name="conv",
-    )(blocks, home(gu), before, taps, home(cg))
-
-
-def add_slots(out_ref, slots, left, weights, start):
-    size = weights.shape[1] - weights.shape[1] % 128
+    )(blocks, *map(near_core, (gu, before, taps, cg)))
+
+
+def add_slots(out_ref, left, weights, tops, start):
+    size = left[0].shape[1]
 
     def step(n, carry):
         here = pl.ds(pl.multiple_of(n * 512, 512), 512)
         acc = jnp.zeros((out_ref.shape[0], 512), F32) if start is None else start[:, here]
-        for slot in slots:
-            acc = acc + dot(left(slot), weights[slot, 0:size, here])
+        for part, ref, top in zip(left, weights, tops):
+            acc = acc + dot(part[...], ref[top : top + size, here])
         out_ref[:, here] = acc.astype(out_ref.dtype)
         return carry
 
@@ -546,101 +514,61 @@
 
 
 def conv_out_kernel(*refs):
-    got, sources, delta_sources = refs[:8], refs[8:16], refs[16:24]
-    out_ref, delta_weights = refs[24:26]
-    got_ref, weights, mixed, sems = refs[26:]
+    got, weights, out_ref, mixed = refs[:8], refs[8:16], refs[16], refs[17]
     groups, rows, size = mixed.shape
-    got_loads = fetch(
-        sems.at[pl.ds(8, 8)], *((ref, got_ref.at[slot]) for slot, ref in enumerate(got))
-    )
-    loads = fetch(
-        sems,
-        *(
-            (ref.at[pl.ds(0 if ref.shape[0] == size + 16 else size, size + 16), :], weights.at[slot])
-            for slot, ref in enumerate(sources)
-        ),
-    )
-    more = fetch(
-        sems.at[pl.ds(16, 8)],
-        *(
-            (ref.at[pl.ds(0, size), :], delta_weights.at[slot])
-            for slot, ref in enumerate(delta_sources)
-        ),
-    )
-    for one in got_loads:
-        one.wait()
+    tops = [0 if ref.shape[0] == size + 16 else size for ref in weights]
     total = jnp.zeros((rows, size), F32)
     total_square = jnp.zeros((rows, size), F32)
-    for g in range(groups):
-        part = got_ref[g, :, 0:size].astype(F32)
+    for ref in got:
+        part = ref[:, 0:size].astype(F32)
         total = total + part
         total_square = total_square + part * part
     scale = 1.0 / (groups * size)
     center = jnp.sum(total, axis=1, keepdims=True) * scale
     second = jnp.sum(total_square, axis=1, keepdims=True) * scale
     factor = lax.rsqrt(jnp.maximum(second - center * center, 0.0) + TINY_VAR)
-    for half in range(2):
-        slots = range(half * 4, half * 4 + 4)
-        for slot in slots:
-            loads[slot].wait()
-            extra = weights[slot, size : size + 16, :].astype(F32)
-            gain = extra[0:1, 0:size] + extra[1:2, 0:size] + extra[2:3, 0:size]
-            shift = extra[3:4, 0:size] + extra[4:5, 0:size] + extra[5:6, 0:size]
-            normed = (got_ref[slot, :, 0:size].astype(F32) - center) * factor * gain + shift
-            gate = got_ref[slot, :, size:].astype(F32)
-            mixed[slot] = low(jax.nn.silu(normed) * jax.nn.silu(gate))
-        add_slots(
-            out_ref, slots, lambda slot: mixed[slot], weights, out_ref if half else None
-        )
-    for one in more:
-        one.wait()
-
-
-def conv_out(got, sources, delta_sources):
+    for slot in range(groups):
+        top = tops[slot] + size
+        extra = weights[slot][top : top + 16, :].astype(F32)
+        gain = extra[0:1, 0:size] + extra[1:2, 0:size] + extra[2:3, 0:size]
+        shift = extra[3:4, 0:size] + extra[4:5, 0:size] + extra[5:6, 0:size]
+        normed = (got[slot][:, 0:size].astype(F32) - center) * factor * gain + shift
+        gate = got[slot][:, size:].astype(F32)
+        mixed[slot] = low(jax.nn.silu(normed) * jax.nn.silu(gate))
+    add_slots(out_ref, [mixed.at[slot] for slot in range(groups)], weights, tops, None)
+
+
+def conv_out(got, weights):
     groups = len(got)
     rows, both = got[0].shape
-    size, width = both // 2, sources[0].shape[1]
+    size, width = both // 2, weights[0].shape[1]
     return pl.pallas_call(
         conv_out_kernel,
-        in_specs=[anywhere()] * 24,
-        out_specs=[whole()] * 2,
-        out_shape=[pltpu.VMEM((rows, width), F32), pltpu.VMEM((groups, size, width), BF16)],
-        scratch_shapes=[
-            pltpu.VMEM((groups, rows, both), BF16),
-            pltpu.VMEM((groups, size + 16, width), BF16),
-            pltpu.VMEM((groups, rows, size), BF16),
-            pltpu.SemaphoreType.DMA((24,)),
-        ],
-        compiler_params=params(12),
+        in_specs=[whole()] * 16,
+        out_specs=whole(),
+        out_shape=pltpu.VMEM((rows, width), F32),
+        scratch_shapes=[pltpu.VMEM((groups, rows, size), BF16)],
+        compiler_params=params(8),
         cost_estimate=cost(2 * rows * 1024 * width, 6 << 20),
         name="conv_out",
-    )(*got, *sources, *delta_sources)
-
-
-def delta_out_kernel(conv_ref, weights, *refs):
-    got, out_ref, got_ref, sems = refs[:8], refs[8], refs[9], refs[10]
-    for one in fetch(sems, *((ref, got_ref.at[slot]) for slot, ref in enumerate(got))):
-        one.wait()
-    add_slots(out_ref, range(8), lambda slot: got_ref[slot], weights, conv_ref)
+    )(*map(near_core, got), *map(near_core, weights))
+
+
+def delta_out_kernel(conv_ref, *refs):
+    add_slots(refs[16], refs[:8], refs[8:16], [0] * 8, conv_ref)
 
 
 def delta_out(got, conv_part, weights):
-    groups = len(got)
-    rows, size = got[0].shape
-    width = conv_part.shape[1]
+    rows, width = conv_part.shape
     return pl.pallas_call(
         delta_out_kernel,
-        in_specs=[whole()] * 2 + [anywhere()] * 8,
+        in_specs=[whole()] * 17,
         out_specs=whole(),
         out_shape=jax.ShapeDtypeStruct((rows, width), BF16),
-        scratch_shapes=[
-            pltpu.VMEM((groups, rows, size), BF16),
-            pltpu.SemaphoreType.DMA((8,)),
-        ],
-        compiler_params=params(12),
+        compiler_params=params(8),
         cost_estimate=cost(2 * rows * 1024 * width, 6 << 20),
         name="delta_out",
-    )(near_core(conv_part), near_core(weights), *got)
+    )(near_core(conv_part), *map(near_core, got), *map(near_core, weights))
 
 
 def local(
@@ -707,10 +635,8 @@
     own = tokens
     r1, l1 = cyclic(own, "y", 1), cyclic(own, "y", -1)
     sw = swapped(own)
-    r1, l1, beta_decay, last, blocks, rate = lax.optimization_barrier(
-        (r1, l1, beta_decay, last, blocks, rate)
-    )
-    weights = weights[:7] + (beta_decay,)
+    blocks, rate, last, beta_decay = lax.optimization_barrier((blocks, rate, last, beta_decay))
+    weights = pack(weights[:7] + (beta_decay,))
     r1_top, l1_rest = cut(r1, l1, half)
     fa, fb = cyclic(r1_top, "y", 1), cyclic(l1_rest, "y", -1)
     sr1, sl1 = swapped(r1), swapped(l1)
@@ -742,10 +668,10 @@
     halo = lax.ppermute(tail, SP, [(i, i + 1) for i in range(31)])
     filtered = conv(blocks, gu, halo, conv_taps, cg)
     got = exchanged(filtered)
-    conv_part, kept = conv_out(got, conv_weights, delta_weights)
+    conv_part = conv_out(got, conv_weights)
 
     mixed = finish(blocks, coef_p, coef_q, dg, head_gain[None, :], before_z, far, before)
-    return delta_out(exchanged(mixed), conv_part, kept)
+    return delta_out(exchanged(mixed), conv_part, delta_weights)
 
 
 def solution(mesh):

time: 132 us -> 164 us (1.24)
  waiting for transfers between devices: 33.9 us -> 56.5 us
  starting transfers between devices: 58.1 us -> 73.2 us
  Pallas kernels: 34.3 us -> 28.7 us
    ppermute x14, waiting for transfers between devices: 3.26 us -> 23.1 us  [exchanged(): got.append(lax.ppermute(parts[slot], TP, route))]
    ppermute x14, starting transfers between devices: 19 us -> 26.2 us  [exchanged(): got.append(lax.ppermute(parts[slot], TP, route))]
    ppermute x3, waiting for transfers between devices: 0.01 us -> 6.98 us  [local(): around.append(lax.ppermute(total, 'z', route(j)))]
    ppermute x11, starting transfers between devices: 12.7 us -> 18.4 us  [cyclic(): lax.ppermute(block, axis, [(i, (i + distance) % count) for i in range(cou...]
    pallas_call x5 -> x6, Pallas kernels: 19.9 us -> 15.7 us  [the longest x1 5.61 us: delta(): pl.pallas_call(delta_kernel, in_specs=[whole()] * 4, out_specs=[whole()]...]
    ppermute x10, waiting for transfers between devices: 2.71 us -> 0.03 us  [swapped(): return lax.ppermute(block, 'c', [(0, 1), (1, 0)])]
    ppermute x11, waiting for transfers between devices: 27.9 us -> 25.4 us  [cyclic(): lax.ppermute(block, axis, [(i, (i + distance) % count) for i in range(cou...]
    ppermute x10, starting transfers between devices: 9.25 us -> 11.5 us  [swapped(): return lax.ppermute(block, 'c', [(0, 1), (1, 0)])]
  transfers between devices with their start and end apart: 40 -> 40, of which waited for: 11 -> 21; matrix products, arithmetic and copies ran while one was open for 3% -> 3% of each run, Pallas kernels for 24% -> 16%
where the time goes in v5:
time: 164 us
  starting transfers between devices  73.2 us (45%)
  waiting for transfers between devices  56.5 us (34%)
  Pallas kernels  28.7 us (18%)
  other arithmetic  2.44 us (1%)
  local copies, waits for them, and re-layouts  2.25 us (1%)
    ppermute x14, starting transfers between devices, exchanged(): got.append(lax.ppermute(parts[slot], TP, route))  26.2 us
    ppermute x11, waiting for transfers between devices, cyclic(): lax.ppermute(block, axis, [(i, (i + distance) % count) for i in range(cou...  25.4 us
    ppermute x14, waiting for transfers between devices, exchanged(): got.append(lax.ppermute(parts[slot], TP, route))  23.1 us
    ppermute x11, starting transfers between devices, cyclic(): lax.ppermute(block, axis, [(i, (i + distance) % count) for i in range(cou...  18.4 us
    ppermute x10, starting transfers between devices, swapped(): return lax.ppermute(block, 'c', [(0, 1), (1, 0)])  11.5 us
    pallas_call x1, Pallas kernels, project(): pl.pallas_call(functools.partial(project_kernel, width_all, head_size), i...  7.64 us
    ppermute x3, starting transfers between devices, local(): around.append(lax.ppermute(total, 'z', route(j)))  7.05 us
    ppermute x3, waiting for transfers between devices, local(): around.append(lax.ppermute(total, 'z', route(j)))  6.98 us
  transfers between devices with their start and end apart: 40, of which 21 were waited for; matrix products, arithmetic and copies ran while one was open for 3% of the time, Pallas kernels for 16%

profile of v5, /device:TPU:1, one launch (start us, length us, event | category | flops | bytes accessed | tf_op | source)
XLA Modules:
  0.0 164.1 jit_solution(14517999660256790878)
XLA Ops:
  0.0 2.1 %collective-permute-start.1 = (bf16[1024,256]{1,0:T(8,128)(2,1)}, bf16[1024,256]{1,0:T(8,128)(2,1)S(1)}, u32[]{:S(2)}, u32[]{:S(2)}) collective-permute-start(bf16[1024,256]{1,0:T(8,128)(2,1)} %refs_0_.3), channel_id=1, source_target_pairs={{0,2},{2,4},{4,6},{6,0},{1,3},{3,5},{5,7},{7,1},{8,10},{10,12},{12... | collective-permute-start | bytes 1572872 | tf_op jit(solution)/shard_map/ppermute | solution.py:378
  3.6 2.9 %collective-permute-start = (bf16[1024,256]{1,0:T(8,128)(2,1)}, bf16[1024,256]{1,0:T(8,128)(2,1)S(1)}, u32[]{:S(2)}, u32[]{:S(2)}) collective-permute-start(bf16[1024,256]{1,0:T(8,128)(2,1)} %refs_0_.3), channel_id=1, source_target_pairs={{0,1},{1,0},{2,3},{3,2},{4,5},{5,4},{6,7},{7,6},{8,9},{9,8},{10,11... | collective-permute-start | bytes 1572872 | tf_op jit(solution)/shard_map/ppermute | solution.py:387
  8.0 5.5 %collective-permute-done.1.right_any.refs_2_ = bf16[1024,256]{1,0:T(8,128)(2,1)S(1)} collective-permute-done((bf16[1024,256]{1,0:T(8,128)(2,1)}, bf16[1024,256]{1,0:T(8,128)(2,1)S(1)}, u32[]{:S(2)}, u32[]{:S(2)}) %collective-permute-start.1) | collective-permute-done | bytes 524320 | tf_op jit(solution)/shard_map/ppermute | solution.py:378
  19.5 3.5 %collective-permute-done.5.refs_6_ = bf16[512,256]{1,0:T(8,128)(2,1)S(1)} collective-permute-done((bf16[512,256]{1,0:T(8,128)(2,1)}, bf16[512,256]{1,0:T(8,128)(2,1)S(1)}, u32[]{:S(2)}, u32[]{:S(2)}) %collective-permute-start.5) | collective-permute-done | bytes 262176 | tf_op jit(solution)/shard_map/ppermute | solution.py:378
  23.0 2.8 %collective-permute-start.6 = (bf16[512,256]{1,0:T(8,128)(2,1)S(1)}, bf16[512,256]{1,0:T(8,128)(2,1)S(1)}, u32[]{:S(2)}, u32[]{:S(2)}) collective-permute-start(bf16[512,256]{1,0:T(8,128)(2,1)S(1)} %collective-permute-done.5.refs_6_), channel_id=1, source_target_pairs={{0,1},{1,0},{2,3},{3,2},{4,5},{5,4},{6,7},{7,6},{8,9},{9,8},{10,11... | collective-permute-start | bytes 786440 | tf_op jit(solution)/shard_map/ppermute | solution.py:387
  33.0 2.2 %pack.1.refs_10_ = bf16[4,2048,256]{2,1,0:T(8,128)(2,1)S(1)} custom-call(bf16[2048,128]{1,0:T(8,128)(2,1)} %refs_0_.2, bf16[2048,128]{1,0:T(8,128)(2,1)} %refs_1_.1, bf16[2048,128]{1,0:T(8,128)(2,1)} %refs_2_.1, bf16[2048,128]{1,0:T(8,128)(2,1)} %refs_3_.1, bf16[2048,128]{1,0:T(8,128)(2,1)} %refs_4_.1, bf16[2048,128]{1,0:T(8,128)(2,1)} %refs_5_.1, ...), custom_call_target="tpu_custom_call" | custom-call | flops 1048576 | bytes 8388608 | tf_op jit(solution)/shard_map/pack/pallas_call | solution.py:108
  35.2 7.6 %project.1 = (bf16[1024,128]{1,0:T(8,128)(2,1)S(1)}, bf16[1024,128]{1,0:T(8,128)(2,1)S(1)}, bf16[1024,128]{1,0:T(8,128)(2,1)S(1)}, f32[1024,128]{1,0:T(8,128)S(1...) custom-call(s32[10]{0:T(128)S(1)} %stack.71.block_ref.place_ref, ...), custom_call_target="tpu_custom_call" | custom-call | flops 4294967296 | bytes 12582912 | tf_op jit(solution)/shard_map/project/pallas_call | solution.py:198
  42.9 3.6 %collective-permute-start.9 = (bf16[32,128]{1,0:T(8,128)(2,1)S(1)}, bf16[32,128]{1,0:T(8,128)(2,1)S(1)}, u32[]{:S(2)}, u32[]{:S(2)}) collective-permute-start(bf16[32,128]{1,0:T(8,128)(2,1)S(1)} %get-tuple-element.50), channel_id=1, source_target_pairs={{0,8},{8,16},{16,24},{24,32},{32,40},{40,48},{48,56},{56,64},{64,7... | collective-permute-start | bytes 24584 | tf_op jit(solution)/shard_map/ppermute | solution.py:668
  46.4 9.5 %collective-permute-done.18.right_any.refs_10_ = bf16[272,2048]{1,0:T(8,128)(2,1)S(1)} collective-permute-done((bf16[272,2048]{1,0:T(8,128)(2,1)S(1)}, bf16[272,2048]{1,0:T(8,128)(2,1)S(1)}, u32[]{:S(2)}, u32[]{:S(2)}) %collective-permute-start.18) | collective-permute-done | bytes 1114144 | tf_op jit(solution)/shard_map/ppermute | solution.py:378
  57.2 2.7 %collective-permute-start.22 = (bf16[144,2048]{1,0:T(8,128)(2,1)}, bf16[144,2048]{1,0:T(8,128)(2,1)S(1)}, u32[]{:S(2)}, u32[]{:S(2)}) collective-permute-start(bf16[144,2048]{1,0:T(8,128)(2,1)} %get-tuple-element.61), channel_id=1, source_target_pairs={{0,6},{2,0},{4,2},{6,4},{1,7},{3,1},{5,3},{7,5},{8,14},{10,8},{12,... | collective-permute-start | bytes 1769480 | tf_op jit(solution)/shard_map/ppermute | solution.py:378
  61.5 5.6 %delta.1 = (bf16[1024,128]{1,0:T(8,128)(2,1)S(1)}, f32[1024,128]{1,0:T(8,128)S(1)}, bf16[144,256]{1,0:T(8,128)(2,1)S(1)}) custom-call(bf16[1024,128]{1,0:T(8,128)(2,1)S(1)} %get-tuple-element.62.q_ref, bf16[1024,128]{1,0:T(8,128)(2,1)S(1)} %get-tuple-element.63.k_ref, bf16[1024,128]{1,0:T(8,128)(2,1)S(1)} %get-tuple-element.64.v_ref, ...), custom_call_target="tpu_custom_call" | custom-call | flops 2013265920 | bytes 3145728 | tf_op jit(solution)/shard_map/delta/pallas_call | solution.py:328
  67.2 3.2 %collective-permute-start.24 = (bf16[144,256]{1,0:T(8,128)(2,1)S(1)}, bf16[144,256]{1,0:T(8,128)(2,1)S(1)}, u32[]{:S(2)}, u32[]{:S(2)}) collective-permute-start(bf16[144,256]{1,0:T(8,128)(2,1)S(1)} %get-tuple-element.69.p0), channel_id=1, source_target_pairs={{0,16},{8,24},{16,0},{24,8},{1,17},{9,25},{17,1},{25,9},{2,18},{10... | collective-permute-start | bytes 221192 | tf_op jit(solution)/shard_map/ppermute | solution.py:378
  72.1 2.7 %collective-permute-start.25 = (bf16[144,256]{1,0:T(8,128)(2,1)S(1)}, bf16[144,256]{1,0:T(8,128)(2,1)S(1)}, u32[]{:S(2)}, u32[]{:S(2)}) collective-permute-start(bf16[144,256]{1,0:T(8,128)(2,1)S(1)} %get-tuple-element.69.p0), channel_id=1, source_target_pairs={{0,24},{8,0},{16,8},{24,16},{1,25},{9,1},{17,9},{25,17},{2,26},{10... | collective-permute-start | bytes 221192 | tf_op jit(solution)/shard_map/ppermute | solution.py:378
  77.0 2.0 %conv.1 = (bf16[128,256]{1,0:T(8,128)(2,1)S(1)}, bf16[128,256]{1,0:T(8,128)(2,1)S(1)}, bf16[128,256]{1,0:T(8,128)(2,1)S(1)}, bf16[128,256]{1,0:T(8,128)(2,1)S(1)...) custom-call(s32[10]{0:T(128)S(1)} %stack.71.block_ref.place_ref, ...), custom_call_target="tpu_custom_call" | custom-call | flops 268435456 | bytes 1048576 | tf_op jit(solution)/shard_map/conv/pallas_call | solution.py:457
  79.0 2.5 %collective-permute-done.26.p3 = bf16[144,256]{1,0:T(8,128)(2,1)S(1)} collective-permute-done((bf16[144,256]{1,0:T(8,128)(2,1)S(1)}, bf16[144,256]{1,0:T(8,128)(2,1)S(1)}, u32[]{:S(2)}, u32[]{:S(2)}) %collective-permute-start.26) | collective-permute-done | bytes 73760 | tf_op jit(solution)/shard_map/ppermute | solution.py:378
  81.5 3.1 %collective-permute-start.10 = (bf16[128,256]{1,0:T(8,128)(2,1)S(1)}, bf16[128,256]{1,0:T(8,128)(2,1)S(1)}, u32[]{:S(2)}, u32[]{:S(2)}) collective-permute-start(bf16[128,256]{1,0:T(8,128)(2,1)S(1)} %get-tuple-element.53), channel_id=1, source_target_pairs={{0,1},{1,0},{2,3},{3,2},{4,5},{5,4},{6,7},{7,6},{8,9},{9,8},{10,11... | collective-permute-start | bytes 196616 | tf_op jit(solution)/shard_map/ppermute | solution.py:395
  85.5 4.3 %collective-permute-done.11.refs_2_ = bf16[128,256]{1,0:T(8,128)(2,1)S(1)} collective-permute-done((bf16[128,256]{1,0:T(8,128)(2,1)S(1)}, bf16[128,256]{1,0:T(8,128)(2,1)S(1)}, u32[]{:S(2)}, u32[]{:S(2)}) %collective-permute-start.11) | collective-permute-done | bytes 65568 | tf_op jit(solution)/shard_map/ppermute | solution.py:395
  89.9 4.8 %collective-permute-done.12.refs_3_ = bf16[128,256]{1,0:T(8,128)(2,1)S(1)} collective-permute-done((bf16[128,256]{1,0:T(8,128)(2,1)S(1)}, bf16[128,256]{1,0:T(8,128)(2,1)S(1)}, u32[]{:S(2)}, u32[]{:S(2)}) %collective-permute-start.12) | collective-permute-done | bytes 65568 | tf_op jit(solution)/shard_map/ppermute | solution.py:395
  97.9 3.5 %collective-permute-start.14 = (bf16[128,256]{1,0:T(8,128)(2,1)S(1)}, bf16[128,256]{1,0:T(8,128)(2,1)S(1)}, u32[]{:S(2)}, u32[]{:S(2)}) collective-permute-start(bf16[128,256]{1,0:T(8,128)(2,1)S(1)} %get-tuple-element.57), channel_id=1, source_target_pairs={{0,7},{1,6},{2,1},{3,0},{4,3},{5,2},{6,5},{7,4},{8,15},{9,14},{10,... | collective-permute-start | bytes 196616 | tf_op jit(solution)/shard_map/ppermute | solution.py:395
  103.0 3.0 %collective-permute-start.27 = (bf16[144,256]{1,0:T(8,128)(2,1)S(1)}, bf16[144,256]{1,0:T(8,128)(2,1)S(1)}, u32[]{:S(2)}, u32[]{:S(2)}) collective-permute-start(bf16[144,256]{1,0:T(8,128)(2,1)S(1)} %get-tuple-element.70.p0), channel_id=1, source_target_pairs={{0,64},{32,96},{64,0},{96,32},{128,192},{160,224},{192,128},{224,1... | collective-permute-start | bytes 221192 | tf_op jit(solution)/shard_map/ppermute | solution.py:655
  107.7 4.1 %collective-permute-start.28 = (bf16[144,256]{1,0:T(8,128)(2,1)S(1)}, bf16[144,256]{1,0:T(8,128)(2,1)S(1)}, u32[]{:S(2)}, u32[]{:S(2)}) collective-permute-start(bf16[144,256]{1,0:T(8,128)(2,1)S(1)} %get-tuple-element.70.p0), channel_id=1, source_target_pairs={{0,96},{32,0},{64,32},{96,64},{128,224},{160,128},{192,160},{224,1... | collective-permute-start | bytes 221192 | tf_op jit(solution)/shard_map/ppermute | solution.py:655
  113.2 5.3 %collective-permute-done.29.p3 = bf16[144,256]{1,0:T(8,128)(2,1)S(1)} collective-permute-done((bf16[144,256]{1,0:T(8,128)(2,1)S(1)}, bf16[144,256]{1,0:T(8,128)(2,1)S(1)}, u32[]{:S(2)}, u32[]{:S(2)}) %collective-permute-start.29) | collective-permute-done | bytes 73760 | tf_op jit(solution)/shard_map/ppermute | solution.py:655
  118.5 2.3 %collective-permute-start.15 = (bf16[128,256]{1,0:T(8,128)(2,1)S(1)}, bf16[128,256]{1,0:T(8,128)(2,1)S(1)}, u32[]{:S(2)}, u32[]{:S(2)}) collective-permute-start(bf16[128,256]{1,0:T(8,128)(2,1)S(1)} %get-tuple-element.58), channel_id=1, source_target_pairs={{0,4},{1,5},{2,6},{3,7},{4,0},{5,1},{6,2},{7,3},{8,12},{9,13},{10,... | collective-permute-start | bytes 196616 | tf_op jit(solution)/shard_map/ppermute | solution.py:395
  123.1 6.6 %collective-permute-start.30 = (bf16[128,128]{1,0:T(8,128)(2,1)S(1)}, bf16[128,128]{1,0:T(8,128)(2,1)S(1)}, u32[]{:S(2)}, u32[]{:S(2)}) collective-permute-start(bf16[128,128]{1,0:T(8,128)(2,1)S(1)} %get-tuple-element.72), channel_id=1, source_target_pairs={{0,128},{32,160},{64,192},{96,224},{1,129},{33,161},{65,193},{97,2... | collective-permute-start | bytes 98312 | tf_op jit(solution)/shard_map/ppermute | solution.py:383
  130.7 6.5 %collective-permute-start.16 = (bf16[128,256]{1,0:T(8,128)(2,1)S(1)}, bf16[128,256]{1,0:T(8,128)(2,1)S(1)}, u32[]{:S(2)}, u32[]{:S(2)}) collective-permute-start(bf16[128,256]{1,0:T(8,128)(2,1)S(1)} %get-tuple-element.59), channel_id=1, source_target_pairs={{0,5},{1,4},{2,7},{3,6},{4,1},{5,0},{6,3},{7,2},{8,13},{9,12},{10,... | collective-permute-start | bytes 196616 | tf_op jit(solution)/shard_map/ppermute | solution.py:395
  139.1 3.3 %collective-permute-start.31 = (bf16[128,128]{1,0:T(8,128)(2,1)S(1)}, bf16[128,128]{1,0:T(8,128)(2,1)S(1)}, u32[]{:S(2)}, u32[]{:S(2)}) collective-permute-start(bf16[128,128]{1,0:T(8,128)(2,1)S(1)} %get-tuple-element.75), channel_id=1, source_target_pairs={{0,1},{1,0},{2,3},{3,2},{4,5},{5,4},{6,7},{7,6},{8,9},{9,8},{10,11... | collective-permute-start | bytes 98312 | tf_op jit(solution)/shard_map/ppermute | solution.py:395
  144.2 3.0 %collective-permute-done.32.refs_2_ = bf16[128,128]{1,0:T(8,128)(2,1)S(1)} collective-permute-done((bf16[128,128]{1,0:T(8,128)(2,1)S(1)}, bf16[128,128]{1,0:T(8,128)(2,1)S(1)}, u32[]{:S(2)}, u32[]{:S(2)}) %collective-permute-start.32) | collective-permute-done | bytes 32800 | tf_op jit(solution)/shard_map/ppermute | solution.py:395
  148.3 3.4 %collective-permute-done.33.refs_3_ = bf16[128,128]{1,0:T(8,128)(2,1)S(1)} collective-permute-done((bf16[128,128]{1,0:T(8,128)(2,1)S(1)}, bf16[128,128]{1,0:T(8,128)(2,1)S(1)}, u32[]{:S(2)}, u32[]{:S(2)}) %collective-permute-start.33) | collective-permute-done | bytes 32800 | tf_op jit(solution)/shard_map/ppermute | solution.py:395
  153.0 3.7 %collective-permute-start.36 = (bf16[128,128]{1,0:T(8,128)(2,1)S(1)}, bf16[128,128]{1,0:T(8,128)(2,1)S(1)}, u32[]{:S(2)}, u32[]{:S(2)}) collective-permute-start(bf16[128,128]{1,0:T(8,128)(2,1)S(1)} %get-tuple-element.80), channel_id=1, source_target_pairs={{0,4},{1,5},{2,6},{3,7},{4,0},{5,1},{6,2},{7,3},{8,12},{9,13},{10,... | collective-permute-start | bytes 98312 | tf_op jit(solution)/shard_map/ppermute | solution.py:395
  156.7 2.1 %conv_out.1.conv_ref = f32[128,2048]{1,0:T(8,128)S(1)} custom-call(bf16[128,256]{1,0:T(8,128)(2,1)S(1)} %get-tuple-element.52.refs_0_, bf16[128,256]{1,0:T(8,128)(2,1)S(1)} %collective-permute-done.10.refs_1_, bf16[128,256]{1,0:T(8,128)(2,1)S(1)} %collective-permute-done.11.refs_2_, bf16[128,256]{1,0:T(8,128)(2,1)S(1)} %collective-permute-done.12.refs_3_, ...), custom_call_target="tpu_custom_call" | custom-call | flops 536870912 | bytes 6291456 | tf_op jit(solution)/shard_map/conv_out/pallas_call | solution.py:545
  158.8 2.7 %collective-permute-done.37.refs_7_ = bf16[128,128]{1,0:T(8,128)(2,1)S(1)} collective-permute-done((bf16[128,128]{1,0:T(8,128)(2,1)S(1)}, bf16[128,128]{1,0:T(8,128)(2,1)S(1)}, u32[]{:S(2)}, u32[]{:S(2)}) %collective-permute-start.37) | collective-permute-done | bytes 32800 | tf_op jit(solution)/shard_map/ppermute | solution.py:395
  161.5 2.5 %delta_out.1 = bf16[128,2048]{1,0:T(8,128)(2,1)} custom-call(f32[128,2048]{1,0:T(8,128)S(1)} %conv_out.1.conv_ref, bf16[128,128]{1,0:T(8,128)(2,1)S(1)} %get-tuple-element.74.refs_0_, bf16[128,128]{1,0:T(8,128)(2,1)S(1)} %collective-permute-done.31.refs_1_, bf16[128,128]{1,0:T(8,128)(2,1)S(1)} %collective-permute-done.32.refs_2_, ...), custom_call_target="tpu_custom_call" | custom-call | flops 536870912 | bytes 6291456 | tf_op jit(solution)/shard_map/delta_out/pallas_call | solution.py:563
  (84 shorter events, 40.6 us)
Async XLA Ops:
  0.0 13.5 %collective-permute-start.1 = (bf16[1024,256]{1,0:T(8,128)(2,1)}, bf16[1024,256]{1,0:T(8,128)(2,1)S(1)}, u32[]{:S(2)}, u32[]{:S(2)}) collective-permute-start(bf16[1024,256]{1,0:T(8,128)(2,1)} %refs_0_.3), channel_id=1, source_target_pairs={{0,2},{2,4},{4,6},{6,0},{1,3},{3,5},{5,7},{7,1},{8,10},{10,12},{12... | collective-permute-start | bytes 1572872 | tf_op jit(solution)/shard_map/ppermute | solution.py:378
  2.1 12.6 %collective-permute-start.3 = (bf16[1024,256]{1,0:T(8,128)(2,1)}, bf16[1024,256]{1,0:T(8,128)(2,1)S(1)}, u32[]{:S(2)}, u32[]{:S(2)}) collective-permute-start(bf16[1024,256]{1,0:T(8,128)(2,1)} %refs_0_.3), channel_id=1, source_target_pairs={{0,6},{2,0},{4,2},{6,4},{1,7},{3,1},{5,3},{7,5},{8,14},{10,8},{12,... | collective-permute-start | bytes 1572872 | tf_op jit(solution)/shard_map/ppermute | solution.py:378
  3.6 28.0 %collective-permute-start = (bf16[1024,256]{1,0:T(8,128)(2,1)}, bf16[1024,256]{1,0:T(8,128)(2,1)S(1)}, u32[]{:S(2)}, u32[]{:S(2)}) collective-permute-start(bf16[1024,256]{1,0:T(8,128)(2,1)} %refs_0_.3), channel_id=1, source_target_pairs={{0,1},{1,0},{2,3},{3,2},{4,5},{5,4},{6,7},{7,6},{8,9},{9,8},{10,11... | collective-permute-start | bytes 1572872 | tf_op jit(solution)/shard_map/ppermute | solution.py:387
  15.6 7.4 %collective-permute-start.5 = (bf16[512,256]{1,0:T(8,128)(2,1)}, bf16[512,256]{1,0:T(8,128)(2,1)S(1)}, u32[]{:S(2)}, u32[]{:S(2)}) collective-permute-start(bf16[512,256]{1,0:T(8,128)(2,1)} %get-tuple-element.46), channel_id=1, source_target_pairs={{0,2},{2,4},{4,6},{6,0},{1,3},{3,5},{5,7},{7,1},{8,10},{10,12},{12... | collective-permute-start | bytes 786440 | tf_op jit(solution)/shard_map/ppermute | solution.py:378
  17.1 8.7 %collective-permute-start.7 = (bf16[512,256]{1,0:T(8,128)(2,1)}, bf16[512,256]{1,0:T(8,128)(2,1)S(1)}, u32[]{:S(2)}, u32[]{:S(2)}) collective-permute-start(bf16[512,256]{1,0:T(8,128)(2,1)} %get-tuple-element.47), channel_id=1, source_target_pairs={{0,6},{2,0},{4,2},{6,4},{1,7},{3,1},{5,3},{7,5},{8,14},{10,8},{12,... | collective-permute-start | bytes 786440 | tf_op jit(solution)/shard_map/ppermute | solution.py:378
  23.0 9.4 %collective-permute-start.6 = (bf16[512,256]{1,0:T(8,128)(2,1)S(1)}, bf16[512,256]{1,0:T(8,128)(2,1)S(1)}, u32[]{:S(2)}, u32[]{:S(2)}) collective-permute-start(bf16[512,256]{1,0:T(8,128)(2,1)S(1)} %collective-permute-done.5.refs_6_), channel_id=1, source_target_pairs={{0,1},{1,0},{2,3},{3,2},{4,5},{5,4},{6,7},{7,6},{8,9},{9,8},{10,11... | collective-permute-start | bytes 786440 | tf_op jit(solution)/shard_map/ppermute | solution.py:387
  25.8 6.7 %collective-permute-start.8 = (bf16[512,256]{1,0:T(8,128)(2,1)S(1)}, bf16[512,256]{1,0:T(8,128)(2,1)}, u32[]{:S(2)}, u32[]{:S(2)}) collective-permute-start(bf16[512,256]{1,0:T(8,128)(2,1)S(1)} %collective-permute-done.7.refs_8_), channel_id=1, source_target_pairs={{0,1},{1,0},{2,3},{3,2},{4,5},{5,4},{6,7},{7,6},{8,9},{9,8},{10,11... | collective-permute-start | bytes 786440 | tf_op jit(solution)/shard_map/ppermute | solution.py:387
  28.8 27.1 %collective-permute-start.18 = (bf16[272,2048]{1,0:T(8,128)(2,1)S(1)}, bf16[272,2048]{1,0:T(8,128)(2,1)S(1)}, u32[]{:S(2)}, u32[]{:S(2)}) collective-permute-start(bf16[272,2048]{1,0:T(8,128)(2,1)S(1)} %fusion.1.refs_8_), channel_id=1, source_target_pairs={{0,2},{2,4},{4,6},{6,0},{1,3},{3,5},{5,7},{7,1},{8,10},{10,12},{12... | collective-permute-start | bytes 3342344 | tf_op jit(solution)/shard_map/ppermute | solution.py:378
  29.9 26.0 %collective-permute-start.20 = (bf16[272,2048]{1,0:T(8,128)(2,1)S(1)}, bf16[272,2048]{1,0:T(8,128)(2,1)S(1)}, u32[]{:S(2)}, u32[]{:S(2)}) collective-permute-start(bf16[272,2048]{1,0:T(8,128)(2,1)S(1)} %fusion.1.refs_8_), channel_id=1, source_target_pairs={{0,6},{2,0},{4,2},{6,4},{1,7},{3,1},{5,3},{7,5},{8,14},{10,8},{12,... | collective-permute-start | bytes 3342344 | tf_op jit(solution)/shard_map/ppermute | solution.py:378
  32.5 37.8 %collective-permute-start.17 = (bf16[272,2048]{1,0:T(8,128)(2,1)S(1)}, bf16[272,2048]{1,0:T(8,128)(2,1)S(1)}, u32[]{:S(2)}, u32[]{:S(2)}) collective-permute-start(bf16[272,2048]{1,0:T(8,128)(2,1)S(1)} %fusion.1.refs_8_), channel_id=1, source_target_pairs={{0,1},{1,0},{2,3},{3,2},{4,5},{5,4},{6,7},{7,6},{8,9},{9,8},{10,11... | collective-permute-start | bytes 3342344 | tf_op jit(solution)/shard_map/ppermute | solution.py:387
  42.9 24.3 %collective-permute-start.9 = (bf16[32,128]{1,0:T(8,128)(2,1)S(1)}, bf16[32,128]{1,0:T(8,128)(2,1)S(1)}, u32[]{:S(2)}, u32[]{:S(2)}) collective-permute-start(bf16[32,128]{1,0:T(8,128)(2,1)S(1)} %get-tuple-element.50), channel_id=1, source_target_pairs={{0,8},{8,16},{16,24},{24,32},{32,40},{40,48},{48,56},{56,64},{64,7... | collective-permute-start | bytes 24584 | tf_op jit(solution)/shard_map/ppermute | solution.py:668
  57.2 38.1 %collective-permute-start.22 = (bf16[144,2048]{1,0:T(8,128)(2,1)}, bf16[144,2048]{1,0:T(8,128)(2,1)S(1)}, u32[]{:S(2)}, u32[]{:S(2)}) collective-permute-start(bf16[144,2048]{1,0:T(8,128)(2,1)} %get-tuple-element.61), channel_id=1, source_target_pairs={{0,6},{2,0},{4,2},{6,4},{1,7},{3,1},{5,3},{7,5},{8,14},{10,8},{12,... | collective-permute-start | bytes 1769480 | tf_op jit(solution)/shard_map/ppermute | solution.py:378
  59.8 92.5 %collective-permute-start.19 = (bf16[272,2048]{1,0:T(8,128)(2,1)S(1)}, bf16[272,2048]{1,0:T(8,128)(2,1)S(1)}, u32[]{:S(2)}, u32[]{:S(2)}) collective-permute-start(bf16[272,2048]{1,0:T(8,128)(2,1)S(1)} %collective-permute-done.18.right_any.refs_10_), channel_id=1, source_target_pairs={{0,1},{1,0},{2,3},{3,2},{4,5},{5,4},{6,7},{7,6},{8,9},{9,8},{10,11... | collective-permute-start | bytes 3342344 | tf_op jit(solution)/shard_map/ppermute | solution.py:387
  61.5 91.5 %collective-permute-start.21 = (bf16[272,2048]{1,0:T(8,128)(2,1)S(1)}, bf16[272,2048]{1,0:T(8,128)(2,1)S(1)}, u32[]{:S(2)}, u32[]{:S(2)}) collective-permute-start(bf16[272,2048]{1,0:T(8,128)(2,1)S(1)} %collective-permute-done.20.left_any.refs_12_), channel_id=1, source_target_pairs={{0,1},{1,0},{2,3},{3,2},{4,5},{5,4},{6,7},{7,6},{8,9},{9,8},{10,11... | collective-permute-start | bytes 3342344 | tf_op jit(solution)/shard_map/ppermute | solution.py:387
  67.2 4.9 %collective-permute-start.24 = (bf16[144,256]{1,0:T(8,128)(2,1)S(1)}, bf16[144,256]{1,0:T(8,128)(2,1)S(1)}, u32[]{:S(2)}, u32[]{:S(2)}) collective-permute-start(bf16[144,256]{1,0:T(8,128)(2,1)S(1)} %get-tuple-element.69.p0), channel_id=1, source_target_pairs={{0,16},{8,24},{16,0},{24,8},{1,17},{9,25},{17,1},{25,9},{2,18},{10... | collective-permute-start | bytes 221192 | tf_op jit(solution)/shard_map/ppermute | solution.py:378
  70.3 35.6 %collective-permute-start.38 = (bf16[128,2048]{1,0:T(8,128)(2,1)S(1)}, bf16[128,2048]{1,0:T(8,128)(2,1)S(1)}, u32[]{:S(2)}, u32[]{:S(2)}) collective-permute-start(bf16[128,2048]{1,0:T(8,128)(2,1)S(1)} %copy-done.5), channel_id=1, source_target_pairs={{0,2},{2,4},{4,6},{6,0},{1,3},{3,5},{5,7},{7,1},{8,10},{10,12},{12... | collective-permute-start | bytes 1572872 | tf_op jit(solution)/shard_map/ppermute | solution.py:378
  76.2 5.3 %collective-permute-start.26 = (bf16[144,256]{1,0:T(8,128)(2,1)S(1)}, bf16[144,256]{1,0:T(8,128)(2,1)S(1)}, u32[]{:S(2)}, u32[]{:S(2)}) collective-permute-start(bf16[144,256]{1,0:T(8,128)(2,1)S(1)} %get-tuple-element.69.p0), channel_id=1, source_target_pairs={{0,8},{8,16},{16,24},{24,0},{1,9},{9,17},{17,25},{25,1},{2,10},{10... | collective-permute-start | bytes 221192 | tf_op jit(solution)/shard_map/ppermute | solution.py:378
  89.8 4.9 %collective-permute-start.12 = (bf16[128,256]{1,0:T(8,128)(2,1)S(1)}, bf16[128,256]{1,0:T(8,128)(2,1)S(1)}, u32[]{:S(2)}, u32[]{:S(2)}) collective-permute-start(bf16[128,256]{1,0:T(8,128)(2,1)S(1)} %get-tuple-element.55), channel_id=1, source_target_pairs={{0,3},{1,2},{2,5},{3,4},{4,7},{5,6},{6,1},{7,0},{8,11},{9,10},{10,... | collective-permute-start | bytes 196616 | tf_op jit(solution)/shard_map/ppermute | solution.py:395
  95.2 61.5 %collective-permute-start.23 = (bf16[144,2048]{1,0:T(8,128)(2,1)S(1)}, bf16[144,2048]{1,0:T(8,128)(2,1)S(1)}, u32[]{:S(2)}, u32[]{:S(2)}) collective-permute-start(bf16[144,2048]{1,0:T(8,128)(2,1)S(1)} %collective-permute-done.22.refs_14_), channel_id=1, source_target_pairs={{0,1},{1,0},{2,3},{3,2},{4,5},{5,4},{6,7},{7,6},{8,9},{9,8},{10,11... | collective-permute-start | bytes 1769480 | tf_op jit(solution)/shard_map/ppermute | solution.py:387
  97.9 5.1 %collective-permute-start.14 = (bf16[128,256]{1,0:T(8,128)(2,1)S(1)}, bf16[128,256]{1,0:T(8,128)(2,1)S(1)}, u32[]{:S(2)}, u32[]{:S(2)}) collective-permute-start(bf16[128,256]{1,0:T(8,128)(2,1)S(1)} %get-tuple-element.57), channel_id=1, source_target_pairs={{0,7},{1,6},{2,1},{3,0},{4,3},{5,2},{6,5},{7,4},{8,15},{9,14},{10,... | collective-permute-start | bytes 196616 | tf_op jit(solution)/shard_map/ppermute | solution.py:395
  103.0 4.7 %collective-permute-start.27 = (bf16[144,256]{1,0:T(8,128)(2,1)S(1)}, bf16[144,256]{1,0:T(8,128)(2,1)S(1)}, u32[]{:S(2)}, u32[]{:S(2)}) collective-permute-start(bf16[144,256]{1,0:T(8,128)(2,1)S(1)} %get-tuple-element.70.p0), channel_id=1, source_target_pairs={{0,64},{32,96},{64,0},{96,32},{128,192},{160,224},{192,128},{224,1... | collective-permute-start | bytes 221192 | tf_op jit(solution)/shard_map/ppermute | solution.py:655
  106.0 55.6 %collective-permute-start.39 = (bf16[128,2048]{1,0:T(8,128)(2,1)S(1)}, bf16[128,2048]{1,0:T(8,128)(2,1)S(1)}, u32[]{:S(2)}, u32[]{:S(2)}) collective-permute-start(bf16[128,2048]{1,0:T(8,128)(2,1)S(1)} %collective-permute-done.38.refs_14_), channel_id=1, source_target_pairs={{0,1},{1,0},{2,3},{3,2},{4,5},{5,4},{6,7},{7,6},{8,9},{9,8},{10,11... | collective-permute-start | bytes 1572872 | tf_op jit(solution)/shard_map/ppermute | solution.py:387
  107.7 5.5 %collective-permute-start.28 = (bf16[144,256]{1,0:T(8,128)(2,1)S(1)}, bf16[144,256]{1,0:T(8,128)(2,1)S(1)}, u32[]{:S(2)}, u32[]{:S(2)}) collective-permute-start(bf16[144,256]{1,0:T(8,128)(2,1)S(1)} %get-tuple-element.70.p0), channel_id=1, source_target_pairs={{0,96},{32,0},{64,32},{96,64},{128,224},{160,128},{192,160},{224,1... | collective-permute-start | bytes 221192 | tf_op jit(solution)/shard_map/ppermute | solution.py:655
  113.2 5.3 %collective-permute-start.29 = (bf16[144,256]{1,0:T(8,128)(2,1)S(1)}, bf16[144,256]{1,0:T(8,128)(2,1)S(1)}, u32[]{:S(2)}, u32[]{:S(2)}) collective-permute-start(bf16[144,256]{1,0:T(8,128)(2,1)S(1)} %get-tuple-element.70.p0), channel_id=1, source_target_pairs={{0,32},{32,64},{64,96},{96,0},{128,160},{160,192},{192,224},{224,1... | collective-permute-start | bytes 221192 | tf_op jit(solution)/shard_map/ppermute | solution.py:655
  118.5 4.6 %collective-permute-start.15 = (bf16[128,256]{1,0:T(8,128)(2,1)S(1)}, bf16[128,256]{1,0:T(8,128)(2,1)S(1)}, u32[]{:S(2)}, u32[]{:S(2)}) collective-permute-start(bf16[128,256]{1,0:T(8,128)(2,1)S(1)} %get-tuple-element.58), channel_id=1, source_target_pairs={{0,4},{1,5},{2,6},{3,7},{4,0},{5,1},{6,2},{7,3},{8,12},{9,13},{10,... | collective-permute-start | bytes 196616 | tf_op jit(solution)/shard_map/ppermute | solution.py:395
  123.1 7.6 %collective-permute-start.30 = (bf16[128,128]{1,0:T(8,128)(2,1)S(1)}, bf16[128,128]{1,0:T(8,128)(2,1)S(1)}, u32[]{:S(2)}, u32[]{:S(2)}) collective-permute-start(bf16[128,128]{1,0:T(8,128)(2,1)S(1)} %get-tuple-element.72), channel_id=1, source_target_pairs={{0,128},{32,160},{64,192},{96,224},{1,129},{33,161},{65,193},{97,2... | collective-permute-start | bytes 98312 | tf_op jit(solution)/shard_map/ppermute | solution.py:383
  130.7 8.4 %collective-permute-start.16 = (bf16[128,256]{1,0:T(8,128)(2,1)S(1)}, bf16[128,256]{1,0:T(8,128)(2,1)S(1)}, u32[]{:S(2)}, u32[]{:S(2)}) collective-permute-start(bf16[128,256]{1,0:T(8,128)(2,1)S(1)} %get-tuple-element.59), channel_id=1, source_target_pairs={{0,5},{1,4},{2,7},{3,6},{4,1},{5,0},{6,3},{7,2},{8,13},{9,12},{10,... | collective-permute-start | bytes 196616 | tf_op jit(solution)/shard_map/ppermute | solution.py:395
  147.2 4.6 %collective-permute-start.33 = (bf16[128,128]{1,0:T(8,128)(2,1)S(1)}, bf16[128,128]{1,0:T(8,128)(2,1)S(1)}, u32[]{:S(2)}, u32[]{:S(2)}) collective-permute-start(bf16[128,128]{1,0:T(8,128)(2,1)S(1)} %get-tuple-element.77), channel_id=1, source_target_pairs={{0,3},{1,2},{2,5},{3,4},{4,7},{5,6},{6,1},{7,0},{8,11},{9,10},{10,... | collective-permute-start | bytes 98312 | tf_op jit(solution)/shard_map/ppermute | solution.py:395
  151.8 7.0 %collective-permute-start.34 = (bf16[128,128]{1,0:T(8,128)(2,1)S(1)}, bf16[128,128]{1,0:T(8,128)(2,1)S(1)}, u32[]{:S(2)}, u32[]{:S(2)}) collective-permute-start(bf16[128,128]{1,0:T(8,128)(2,1)S(1)} %get-tuple-element.78), channel_id=1, source_target_pairs={{0,6},{1,7},{2,0},{3,1},{4,2},{5,3},{6,4},{7,5},{8,14},{9,15},{10,... | collective-permute-start | bytes 98312 | tf_op jit(solution)/shard_map/ppermute | solution.py:395
  152.3 6.5 %collective-permute-start.35 = (bf16[128,128]{1,0:T(8,128)(2,1)S(1)}, bf16[128,128]{1,0:T(8,128)(2,1)S(1)}, u32[]{:S(2)}, u32[]{:S(2)}) collective-permute-start(bf16[128,128]{1,0:T(8,128)(2,1)S(1)} %get-tuple-element.79), channel_id=1, source_target_pairs={{0,7},{1,6},{2,1},{3,0},{4,3},{5,2},{6,5},{7,4},{8,15},{9,14},{10,... | collective-permute-start | bytes 98312 | tf_op jit(solution)/shard_map/ppermute | solution.py:395
  153.0 5.8 %collective-permute-start.36 = (bf16[128,128]{1,0:T(8,128)(2,1)S(1)}, bf16[128,128]{1,0:T(8,128)(2,1)S(1)}, u32[]{:S(2)}, u32[]{:S(2)}) collective-permute-start(bf16[128,128]{1,0:T(8,128)(2,1)S(1)} %get-tuple-element.80), channel_id=1, source_target_pairs={{0,4},{1,5},{2,6},{3,7},{4,0},{5,1},{6,2},{7,3},{8,12},{9,13},{10,... | collective-permute-start | bytes 98312 | tf_op jit(solution)/shard_map/ppermute | solution.py:395
  156.7 4.8 %collective-permute-start.37 = (bf16[128,128]{1,0:T(8,128)(2,1)S(1)}, bf16[128,128]{1,0:T(8,128)(2,1)S(1)}, u32[]{:S(2)}, u32[]{:S(2)}) collective-permute-start(bf16[128,128]{1,0:T(8,128)(2,1)S(1)} %get-tuple-element.81), channel_id=1, source_target_pairs={{0,5},{1,4},{2,7},{3,6},{4,1},{5,0},{6,3},{7,2},{8,13},{9,12},{10,... | collective-permute-start | bytes 98312 | tf_op jit(solution)/shard_map/ppermute | solution.py:395
  (15 other events, 161.6 us)

commit v6 on v5

--- a/solution.py
+++ b/solution.py
@@ -187,8 +187,12 @@
 
     for one in moves:
         one.wait()
-    for body in (gated, gates, queries, rest_of):
-        each_half(body)
+
+    def everything(here):
+        for body in (gated, gates, queries, rest_of):
+            body(here)
+
+    each_half(everything)
     tail_ref[...] = gu_ref[rows - HALO :, :]
 
 
@@ -483,30 +487,23 @@
     lax.fori_loop(0, out_ref.shape[1] // 512, step, 0)
 
 
-def cut_kernel(count, right_any, left_any, top_hbm, rest_hbm, top, rest, sems):
-    inward = fetch(
+def cut_kernel(count, right_any, left_any, top_ref, rest_ref, sems):
+    for one in fetch(
         sems,
-        (right_any.at[pl.ds(0, count), :], top),
-        (left_any.at[pl.ds(count, rest.shape[0]), :], rest),
-    )
-    outward = []
-    for n, pair in enumerate(((top, top_hbm), (rest, rest_hbm))):
-        inward[n].wait()
-        outward += fetch(sems.at[pl.ds(2 + n, 1)], pair)
-    for one in outward:
+        (right_any.at[pl.ds(0, count), :], top_ref),
+        (left_any.at[pl.ds(count, rest_ref.shape[0]), :], rest_ref),
+    ):
         one.wait()
 
 
 def cut(right, left, count):
     rows, width = right.shape
-    shapes = [(count, width), (rows - count, width)]
     return pl.pallas_call(
         functools.partial(cut_kernel, count),
         in_specs=[anywhere()] * 2,
-        out_specs=[hbm()] * 2,
-        out_shape=[pltpu.HBM(shape, BF16) for shape in shapes],
-        scratch_shapes=[pltpu.VMEM(shape, BF16) for shape in shapes]
-        + [pltpu.SemaphoreType.DMA((4,))],
+        out_specs=[whole()] * 2,
+        out_shape=[pltpu.VMEM((count, width), BF16), pltpu.VMEM((rows - count, width), BF16)],
+        scratch_shapes=[pltpu.SemaphoreType.DMA((2,))],
         compiler_params=params(4),
         cost_estimate=cost(1 << 20, 4 << 20),
         name="cut",
@@ -555,7 +552,18 @@
 
 
 def delta_out_kernel(conv_ref, *refs):
-    add_slots(refs[16], refs[:8], refs[8:16], [0] * 8, conv_ref)
+    got, weights, out_hbm, staged, sems = refs[:8], refs[8:16], refs[16], refs[17], refs[18]
+    size = got[0].shape[1]
+    stores = []
+    for n, base in enumerate(range(0, staged.shape[1], 512)):
+        here = slice(base, base + 512)
+        acc = conv_ref[:, here]
+        for part, ref in zip(got, weights):
+            acc = acc + dot(part[...], ref[0:size, here])
+        staged[:, here] = low(acc)
+        stores += fetch(sems.at[pl.ds(n, 1)], (staged.at[:, here], out_hbm.at[:, here]))
+    for one in stores:
+        one.wait()
 
 
 def delta_out(got, conv_part, weights):
@@ -563,8 +571,9 @@
     return pl.pallas_call(
         delta_out_kernel,
         in_specs=[whole()] * 17,
-        out_specs=whole(),
+        out_specs=hbm(),
         out_shape=jax.ShapeDtypeStruct((rows, width), BF16),
+        scratch_shapes=[pltpu.VMEM((rows, width), BF16), pltpu.SemaphoreType.DMA((4,))],
         compiler_params=params(8),
         cost_estimate=cost(2 * rows * 1024 * width, 6 << 20),
         name="delta_out",

time: 164 us -> 162 us (0.988)
  Pallas kernels: 28.7 us -> 25.5 us
    pallas_call x2, Pallas kernels: 2.09 us -> 0.23 us  [cut(): pl.pallas_call(functools.partial(cut_kernel, count), in_specs=[anywhere()...]
  transfers between devices with their start and end apart: 40 -> 40, of which waited for: 21 -> 21; matrix products, arithmetic and copies ran while one was open for 3% -> 3% of each run, Pallas kernels for 16% -> 15%
where the time goes in v6:
time: 162 us
  starting transfers between devices  73 us (45%)
  waiting for transfers between devices  56.3 us (35%)
  Pallas kernels  25.5 us (16%)
  local copies, waits for them, and re-layouts  3.05 us (2%)
  other arithmetic  2.45 us (2%)
    ppermute x14, starting transfers between devices, exchanged(): got.append(lax.ppermute(parts[slot], TP, route))  26.2 us
    ppermute x11, waiting for transfers between devices, cyclic(): lax.ppermute(block, axis, [(i, (i + distance) % count) for i in range(cou...  25.2 us
    ppermute x14, waiting for transfers between devices, exchanged(): got.append(lax.ppermute(parts[slot], TP, route))  23.1 us
    ppermute x11, starting transfers between devices, cyclic(): lax.ppermute(block, axis, [(i, (i + distance) % count) for i in range(cou...  18.2 us
    ppermute x10, starting transfers between devices, swapped(): return lax.ppermute(block, 'c', [(0, 1), (1, 0)])  11.5 us
    ppermute x3, starting transfers between devices, local(): around.append(lax.ppermute(total, 'z', route(j)))  7.05 us
    ppermute x3, waiting for transfers between devices, local(): around.append(lax.ppermute(total, 'z', route(j)))  6.98 us
    pallas_call x1, Pallas kernels, project(): pl.pallas_call(functools.partial(project_kernel, width_all, head_size), i...  6.85 us
  transfers between devices with their start and end apart: 40, of which 21 were waited for; matrix products, arithmetic and copies ran while one was open for 3% of the time, Pallas kernels for 15%

profile of v6, /device:TPU:1, one launch (start us, length us, event | category | flops | bytes accessed | tf_op | source)
XLA Modules:
  0.0 161.5 jit_solution(7159984190714420349)
XLA Ops:
  0.0 2.1 %collective-permute-start.1 = (bf16[1024,256]{1,0:T(8,128)(2,1)}, bf16[1024,256]{1,0:T(8,128)(2,1)S(1)}, u32[]{:S(2)}, u32[]{:S(2)}) collective-permute-start(bf16[1024,256]{1,0:T(8,128)(2,1)} %refs_0_.3), channel_id=1, source_target_pairs={{0,2},{2,4},{4,6},{6,0},{1,3},{3,5},{5,7},{7,1},{8,10},{10,12},{12... | collective-permute-start | bytes 1572872 | tf_op jit(solution)/shard_map/ppermute | solution.py:382
  3.6 2.9 %collective-permute-start = (bf16[1024,256]{1,0:T(8,128)(2,1)}, bf16[1024,256]{1,0:T(8,128)(2,1)S(1)}, u32[]{:S(2)}, u32[]{:S(2)}) collective-permute-start(bf16[1024,256]{1,0:T(8,128)(2,1)} %refs_0_.3), channel_id=1, source_target_pairs={{0,1},{1,0},{2,3},{3,2},{4,5},{5,4},{6,7},{7,6},{8,9},{9,8},{10,11... | collective-permute-start | bytes 1572872 | tf_op jit(solution)/shard_map/ppermute | solution.py:391
  8.7 4.8 %collective-permute-done.1.right_any.refs_2_ = bf16[1024,256]{1,0:T(8,128)(2,1)S(1)} collective-permute-done((bf16[1024,256]{1,0:T(8,128)(2,1)}, bf16[1024,256]{1,0:T(8,128)(2,1)S(1)}, u32[]{:S(2)}, u32[]{:S(2)}) %collective-permute-start.1) | collective-permute-done | bytes 524320 | tf_op jit(solution)/shard_map/ppermute | solution.py:382
  18.7 3.3 %collective-permute-done.5.refs_6_ = bf16[512,256]{1,0:T(8,128)(2,1)S(1)} collective-permute-done((bf16[512,256]{1,0:T(8,128)(2,1)S(1)}, bf16[512,256]{1,0:T(8,128)(2,1)S(1)}, u32[]{:S(2)}, u32[]{:S(2)}) %collective-permute-start.5) | collective-permute-done | bytes 262176 | tf_op jit(solution)/shard_map/ppermute | solution.py:382
  22.0 2.8 %collective-permute-start.6 = (bf16[512,256]{1,0:T(8,128)(2,1)S(1)}, bf16[512,256]{1,0:T(8,128)(2,1)S(1)}, u32[]{:S(2)}, u32[]{:S(2)}) collective-permute-start(bf16[512,256]{1,0:T(8,128)(2,1)S(1)} %collective-permute-done.5.refs_6_), channel_id=1, source_target_pairs={{0,1},{1,0},{2,3},{3,2},{4,5},{5,4},{6,7},{7,6},{8,9},{9,8},{10,11... | collective-permute-start | bytes 786440 | tf_op jit(solution)/shard_map/ppermute | solution.py:391
  32.0 2.2 %pack.1.refs_10_ = bf16[4,2048,256]{2,1,0:T(8,128)(2,1)S(1)} custom-call(bf16[2048,128]{1,0:T(8,128)(2,1)} %refs_0_.2, bf16[2048,128]{1,0:T(8,128)(2,1)} %refs_1_.1, bf16[2048,128]{1,0:T(8,128)(2,1)} %refs_2_.1, bf16[2048,128]{1,0:T(8,128)(2,1)} %refs_3_.1, bf16[2048,128]{1,0:T(8,128)(2,1)} %refs_4_.1, bf16[2048,128]{1,0:T(8,128)(2,1)} %refs_5_.1, ...), custom_call_target="tpu_custom_call" | custom-call | flops 1048576 | bytes 8388608 | tf_op jit(solution)/shard_map/pack/pallas_call | solution.py:108
  34.3 6.9 %project.1 = (bf16[1024,128]{1,0:T(8,128)(2,1)S(1)}, bf16[1024,128]{1,0:T(8,128)(2,1)S(1)}, bf16[1024,128]{1,0:T(8,128)(2,1)S(1)}, f32[1024,128]{1,0:T(8,128)S(1...) custom-call(s32[10]{0:T(128)S(1)} %stack.71.block_ref.place_ref, ...), custom_call_target="tpu_custom_call" | custom-call | flops 4294967296 | bytes 12582912 | tf_op jit(solution)/shard_map/project/pallas_call | solution.py:202
  41.1 3.6 %collective-permute-start.9 = (bf16[32,128]{1,0:T(8,128)(2,1)S(1)}, bf16[32,128]{1,0:T(8,128)(2,1)S(1)}, u32[]{:S(2)}, u32[]{:S(2)}) collective-permute-start(bf16[32,128]{1,0:T(8,128)(2,1)S(1)} %get-tuple-element.50), channel_id=1, source_target_pairs={{0,8},{8,16},{16,24},{24,32},{32,40},{40,48},{48,56},{56,64},{64,7... | collective-permute-start | bytes 24584 | tf_op jit(solution)/shard_map/ppermute | solution.py:677
  44.7 10.3 %collective-permute-done.18.right_any.refs_10_ = bf16[272,2048]{1,0:T(8,128)(2,1)S(1)} collective-permute-done((bf16[272,2048]{1,0:T(8,128)(2,1)S(1)}, bf16[272,2048]{1,0:T(8,128)(2,1)S(1)}, u32[]{:S(2)}, u32[]{:S(2)}) %collective-permute-start.18) | collective-permute-done | bytes 1114144 | tf_op jit(solution)/shard_map/ppermute | solution.py:382
  55.2 2.5 %collective-permute-start.22 = (bf16[144,2048]{1,0:T(8,128)(2,1)S(1)}, bf16[144,2048]{1,0:T(8,128)(2,1)S(1)}, u32[]{:S(2)}, u32[]{:S(2)}) collective-permute-start(bf16[144,2048]{1,0:T(8,128)(2,1)S(1)} %get-tuple-element.61), channel_id=1, source_target_pairs={{0,6},{2,0},{4,2},{6,4},{1,7},{3,1},{5,3},{7,5},{8,14},{10,8},{12,... | collective-permute-start | bytes 1769480 | tf_op jit(solution)/shard_map/ppermute | solution.py:382
  59.4 5.6 %delta.1 = (bf16[1024,128]{1,0:T(8,128)(2,1)S(1)}, f32[1024,128]{1,0:T(8,128)S(1)}, bf16[144,256]{1,0:T(8,128)(2,1)S(1)}) custom-call(bf16[1024,128]{1,0:T(8,128)(2,1)S(1)} %get-tuple-element.62.q_ref, bf16[1024,128]{1,0:T(8,128)(2,1)S(1)} %get-tuple-element.63.k_ref, bf16[1024,128]{1,0:T(8,128)(2,1)S(1)} %get-tuple-element.64.v_ref, ...), custom_call_target="tpu_custom_call" | custom-call | flops 2013265920 | bytes 3145728 | tf_op jit(solution)/shard_map/delta/pallas_call | solution.py:332
  65.0 3.2 %collective-permute-start.24 = (bf16[144,256]{1,0:T(8,128)(2,1)S(1)}, bf16[144,256]{1,0:T(8,128)(2,1)S(1)}, u32[]{:S(2)}, u32[]{:S(2)}) collective-permute-start(bf16[144,256]{1,0:T(8,128)(2,1)S(1)} %get-tuple-element.69.p0), channel_id=1, source_target_pairs={{0,16},{8,24},{16,0},{24,8},{1,17},{9,25},{17,1},{25,9},{2,18},{10... | collective-permute-start | bytes 221192 | tf_op jit(solution)/shard_map/ppermute | solution.py:382
  69.9 2.7 %collective-permute-start.25 = (bf16[144,256]{1,0:T(8,128)(2,1)S(1)}, bf16[144,256]{1,0:T(8,128)(2,1)S(1)}, u32[]{:S(2)}, u32[]{:S(2)}) collective-permute-start(bf16[144,256]{1,0:T(8,128)(2,1)S(1)} %get-tuple-element.69.p0), channel_id=1, source_target_pairs={{0,24},{8,0},{16,8},{24,16},{1,25},{9,1},{17,9},{25,17},{2,26},{10... | collective-permute-start | bytes 221192 | tf_op jit(solution)/shard_map/ppermute | solution.py:382
  74.9 2.0 %conv.1 = (bf16[128,256]{1,0:T(8,128)(2,1)S(1)}, bf16[128,256]{1,0:T(8,128)(2,1)S(1)}, bf16[128,256]{1,0:T(8,128)(2,1)S(1)}, bf16[128,256]{1,0:T(8,128)(2,1)S(1)...) custom-call(s32[10]{0:T(128)S(1)} %stack.71.block_ref.place_ref, ...), custom_call_target="tpu_custom_call" | custom-call | flops 268435456 | bytes 1048576 | tf_op jit(solution)/shard_map/conv/pallas_call | solution.py:461
  76.9 2.5 %collective-permute-done.26.p3 = bf16[144,256]{1,0:T(8,128)(2,1)S(1)} collective-permute-done((bf16[144,256]{1,0:T(8,128)(2,1)S(1)}, bf16[144,256]{1,0:T(8,128)(2,1)S(1)}, u32[]{:S(2)}, u32[]{:S(2)}) %collective-permute-start.26) | collective-permute-done | bytes 73760 | tf_op jit(solution)/shard_map/ppermute | solution.py:382
  79.4 3.1 %collective-permute-start.10 = (bf16[128,256]{1,0:T(8,128)(2,1)S(1)}, bf16[128,256]{1,0:T(8,128)(2,1)S(1)}, u32[]{:S(2)}, u32[]{:S(2)}) collective-permute-start(bf16[128,256]{1,0:T(8,128)(2,1)S(1)} %get-tuple-element.53), channel_id=1, source_target_pairs={{0,1},{1,0},{2,3},{3,2},{4,5},{5,4},{6,7},{7,6},{8,9},{9,8},{10,11... | collective-permute-start | bytes 196616 | tf_op jit(solution)/shard_map/ppermute | solution.py:399
  83.4 4.3 %collective-permute-done.11.refs_2_ = bf16[128,256]{1,0:T(8,128)(2,1)S(1)} collective-permute-done((bf16[128,256]{1,0:T(8,128)(2,1)S(1)}, bf16[128,256]{1,0:T(8,128)(2,1)S(1)}, u32[]{:S(2)}, u32[]{:S(2)}) %collective-permute-start.11) | collective-permute-done | bytes 65568 | tf_op jit(solution)/shard_map/ppermute | solution.py:399
  87.8 4.8 %collective-permute-done.12.refs_3_ = bf16[128,256]{1,0:T(8,128)(2,1)S(1)} collective-permute-done((bf16[128,256]{1,0:T(8,128)(2,1)S(1)}, bf16[128,256]{1,0:T(8,128)(2,1)S(1)}, u32[]{:S(2)}, u32[]{:S(2)}) %collective-permute-start.12) | collective-permute-done | bytes 65568 | tf_op jit(solution)/shard_map/ppermute | solution.py:399
  95.7 3.5 %collective-permute-start.14 = (bf16[128,256]{1,0:T(8,128)(2,1)S(1)}, bf16[128,256]{1,0:T(8,128)(2,1)S(1)}, u32[]{:S(2)}, u32[]{:S(2)}) collective-permute-start(bf16[128,256]{1,0:T(8,128)(2,1)S(1)} %get-tuple-element.57), channel_id=1, source_target_pairs={{0,7},{1,6},{2,1},{3,0},{4,3},{5,2},{6,5},{7,4},{8,15},{9,14},{10,... | collective-permute-start | bytes 196616 | tf_op jit(solution)/shard_map/ppermute | solution.py:399
  100.8 3.0 %collective-permute-start.27 = (bf16[144,256]{1,0:T(8,128)(2,1)S(1)}, bf16[144,256]{1,0:T(8,128)(2,1)S(1)}, u32[]{:S(2)}, u32[]{:S(2)}) collective-permute-start(bf16[144,256]{1,0:T(8,128)(2,1)S(1)} %get-tuple-element.70.p0), channel_id=1, source_target_pairs={{0,64},{32,96},{64,0},{96,32},{128,192},{160,224},{192,128},{224,1... | collective-permute-start | bytes 221192 | tf_op jit(solution)/shard_map/ppermute | solution.py:664
  105.6 4.1 %collective-permute-start.28 = (bf16[144,256]{1,0:T(8,128)(2,1)S(1)}, bf16[144,256]{1,0:T(8,128)(2,1)S(1)}, u32[]{:S(2)}, u32[]{:S(2)}) collective-permute-start(bf16[144,256]{1,0:T(8,128)(2,1)S(1)} %get-tuple-element.70.p0), channel_id=1, source_target_pairs={{0,96},{32,0},{64,32},{96,64},{128,224},{160,128},{192,160},{224,1... | collective-permute-start | bytes 221192 | tf_op jit(solution)/shard_map/ppermute | solution.py:664
  111.0 5.3 %collective-permute-done.29.p3 = bf16[144,256]{1,0:T(8,128)(2,1)S(1)} collective-permute-done((bf16[144,256]{1,0:T(8,128)(2,1)S(1)}, bf16[144,256]{1,0:T(8,128)(2,1)S(1)}, u32[]{:S(2)}, u32[]{:S(2)}) %collective-permute-start.29) | collective-permute-done | bytes 73760 | tf_op jit(solution)/shard_map/ppermute | solution.py:664
  116.4 2.3 %collective-permute-start.15 = (bf16[128,256]{1,0:T(8,128)(2,1)S(1)}, bf16[128,256]{1,0:T(8,128)(2,1)S(1)}, u32[]{:S(2)}, u32[]{:S(2)}) collective-permute-start(bf16[128,256]{1,0:T(8,128)(2,1)S(1)} %get-tuple-element.58), channel_id=1, source_target_pairs={{0,4},{1,5},{2,6},{3,7},{4,0},{5,1},{6,2},{7,3},{8,12},{9,13},{10,... | collective-permute-start | bytes 196616 | tf_op jit(solution)/shard_map/ppermute | solution.py:399
  121.0 6.6 %collective-permute-start.30 = (bf16[128,128]{1,0:T(8,128)(2,1)S(1)}, bf16[128,128]{1,0:T(8,128)(2,1)S(1)}, u32[]{:S(2)}, u32[]{:S(2)}) collective-permute-start(bf16[128,128]{1,0:T(8,128)(2,1)S(1)} %get-tuple-element.72), channel_id=1, source_target_pairs={{0,128},{32,160},{64,192},{96,224},{1,129},{33,161},{65,193},{97,2... | collective-permute-start | bytes 98312 | tf_op jit(solution)/shard_map/ppermute | solution.py:387
  128.6 6.5 %collective-permute-start.16 = (bf16[128,256]{1,0:T(8,128)(2,1)S(1)}, bf16[128,256]{1,0:T(8,128)(2,1)S(1)}, u32[]{:S(2)}, u32[]{:S(2)}) collective-permute-start(bf16[128,256]{1,0:T(8,128)(2,1)S(1)} %get-tuple-element.59), channel_id=1, source_target_pairs={{0,5},{1,4},{2,7},{3,6},{4,1},{5,0},{6,3},{7,2},{8,13},{9,12},{10,... | collective-permute-start | bytes 196616 | tf_op jit(solution)/shard_map/ppermute | solution.py:399
  137.0 3.3 %collective-permute-start.31 = (bf16[128,128]{1,0:T(8,128)(2,1)S(1)}, bf16[128,128]{1,0:T(8,128)(2,1)S(1)}, u32[]{:S(2)}, u32[]{:S(2)}) collective-permute-start(bf16[128,128]{1,0:T(8,128)(2,1)S(1)} %get-tuple-element.75), channel_id=1, source_target_pairs={{0,1},{1,0},{2,3},{3,2},{4,5},{5,4},{6,7},{7,6},{8,9},{9,8},{10,11... | collective-permute-start | bytes 98312 | tf_op jit(solution)/shard_map/ppermute | solution.py:399
  142.0 3.0 %collective-permute-done.32.refs_2_ = bf16[128,128]{1,0:T(8,128)(2,1)S(1)} collective-permute-done((bf16[128,128]{1,0:T(8,128)(2,1)S(1)}, bf16[128,128]{1,0:T(8,128)(2,1)S(1)}, u32[]{:S(2)}, u32[]{:S(2)}) %collective-permute-start.32) | collective-permute-done | bytes 32800 | tf_op jit(solution)/shard_map/ppermute | solution.py:399
  146.2 3.4 %collective-permute-done.33.refs_3_ = bf16[128,128]{1,0:T(8,128)(2,1)S(1)} collective-permute-done((bf16[128,128]{1,0:T(8,128)(2,1)S(1)}, bf16[128,128]{1,0:T(8,128)(2,1)S(1)}, u32[]{:S(2)}, u32[]{:S(2)}) %collective-permute-start.33) | collective-permute-done | bytes 32800 | tf_op jit(solution)/shard_map/ppermute | solution.py:399
  150.9 3.7 %collective-permute-start.36 = (bf16[128,128]{1,0:T(8,128)(2,1)S(1)}, bf16[128,128]{1,0:T(8,128)(2,1)S(1)}, u32[]{:S(2)}, u32[]{:S(2)}) collective-permute-start(bf16[128,128]{1,0:T(8,128)(2,1)S(1)} %get-tuple-element.80), channel_id=1, source_target_pairs={{0,4},{1,5},{2,6},{3,7},{4,0},{5,1},{6,2},{7,3},{8,12},{9,13},{10,... | collective-permute-start | bytes 98312 | tf_op jit(solution)/shard_map/ppermute | solution.py:399
  154.6 2.1 %conv_out.1.conv_ref = f32[128,2048]{1,0:T(8,128)S(1)} custom-call(bf16[128,256]{1,0:T(8,128)(2,1)S(1)} %get-tuple-element.52.refs_0_, bf16[128,256]{1,0:T(8,128)(2,1)S(1)} %collective-permute-done.10.refs_1_, bf16[128,256]{1,0:T(8,128)(2,1)S(1)} %collective-permute-done.11.refs_2_, bf16[128,256]{1,0:T(8,128)(2,1)S(1)} %collective-permute-done.12.refs_3_, ...), custom_call_target="tpu_custom_call" | custom-call | flops 536870912 | bytes 6291456 | tf_op jit(solution)/shard_map/conv_out/pallas_call | solution.py:542
  156.7 2.7 %collective-permute-done.37.refs_7_ = bf16[128,128]{1,0:T(8,128)(2,1)S(1)} collective-permute-done((bf16[128,128]{1,0:T(8,128)(2,1)S(1)}, bf16[128,128]{1,0:T(8,128)(2,1)S(1)}, u32[]{:S(2)}, u32[]{:S(2)}) %collective-permute-start.37) | collective-permute-done | bytes 32800 | tf_op jit(solution)/shard_map/ppermute | solution.py:399
  159.4 1.9 %delta_out.1 = bf16[128,2048]{1,0:T(8,128)(2,1)} custom-call(f32[128,2048]{1,0:T(8,128)S(1)} %conv_out.1.conv_ref, bf16[128,128]{1,0:T(8,128)(2,1)S(1)} %get-tuple-element.74.refs_0_, bf16[128,128]{1,0:T(8,128)(2,1)S(1)} %collective-permute-done.31.refs_1_, bf16[128,128]{1,0:T(8,128)(2,1)S(1)} %collective-permute-done.32.refs_2_, ...), custom_call_target="tpu_custom_call" | custom-call | flops 536870912 | bytes 6291456 | tf_op jit(solution)/shard_map/delta_out/pallas_call | solution.py:571
  (84 shorter events, 39.6 us)
Async XLA Ops:
  0.0 13.5 %collective-permute-start.1 = (bf16[1024,256]{1,0:T(8,128)(2,1)}, bf16[1024,256]{1,0:T(8,128)(2,1)S(1)}, u32[]{:S(2)}, u32[]{:S(2)}) collective-permute-start(bf16[1024,256]{1,0:T(8,128)(2,1)} %refs_0_.3), channel_id=1, source_target_pairs={{0,2},{2,4},{4,6},{6,0},{1,3},{3,5},{5,7},{7,1},{8,10},{10,12},{12... | collective-permute-start | bytes 1572872 | tf_op jit(solution)/shard_map/ppermute | solution.py:382
  2.1 12.6 %collective-permute-start.3 = (bf16[1024,256]{1,0:T(8,128)(2,1)}, bf16[1024,256]{1,0:T(8,128)(2,1)S(1)}, u32[]{:S(2)}, u32[]{:S(2)}) collective-permute-start(bf16[1024,256]{1,0:T(8,128)(2,1)} %refs_0_.3), channel_id=1, source_target_pairs={{0,6},{2,0},{4,2},{6,4},{1,7},{3,1},{5,3},{7,5},{8,14},{10,8},{12,... | collective-permute-start | bytes 1572872 | tf_op jit(solution)/shard_map/ppermute | solution.py:382
  3.6 27.1 %collective-permute-start = (bf16[1024,256]{1,0:T(8,128)(2,1)}, bf16[1024,256]{1,0:T(8,128)(2,1)S(1)}, u32[]{:S(2)}, u32[]{:S(2)}) collective-permute-start(bf16[1024,256]{1,0:T(8,128)(2,1)} %refs_0_.3), channel_id=1, source_target_pairs={{0,1},{1,0},{2,3},{3,2},{4,5},{5,4},{6,7},{7,6},{8,9},{9,8},{10,11... | collective-permute-start | bytes 1572872 | tf_op jit(solution)/shard_map/ppermute | solution.py:391
  14.8 7.2 %collective-permute-start.5 = (bf16[512,256]{1,0:T(8,128)(2,1)S(1)}, bf16[512,256]{1,0:T(8,128)(2,1)S(1)}, u32[]{:S(2)}, u32[]{:S(2)}) collective-permute-start(bf16[512,256]{1,0:T(8,128)(2,1)S(1)} %get-tuple-element.46), channel_id=1, source_target_pairs={{0,2},{2,4},{4,6},{6,0},{1,3},{3,5},{5,7},{7,1},{8,10},{10,12},{12... | collective-permute-start | bytes 786440 | tf_op jit(solution)/shard_map/ppermute | solution.py:382
  16.3 8.5 %collective-permute-start.7 = (bf16[512,256]{1,0:T(8,128)(2,1)S(1)}, bf16[512,256]{1,0:T(8,128)(2,1)S(1)}, u32[]{:S(2)}, u32[]{:S(2)}) collective-permute-start(bf16[512,256]{1,0:T(8,128)(2,1)S(1)} %get-tuple-element.47), channel_id=1, source_target_pairs={{0,6},{2,0},{4,2},{6,4},{1,7},{3,1},{5,3},{7,5},{8,14},{10,8},{12,... | collective-permute-start | bytes 786440 | tf_op jit(solution)/shard_map/ppermute | solution.py:382
  22.0 9.5 %collective-permute-start.6 = (bf16[512,256]{1,0:T(8,128)(2,1)S(1)}, bf16[512,256]{1,0:T(8,128)(2,1)S(1)}, u32[]{:S(2)}, u32[]{:S(2)}) collective-permute-start(bf16[512,256]{1,0:T(8,128)(2,1)S(1)} %collective-permute-done.5.refs_6_), channel_id=1, source_target_pairs={{0,1},{1,0},{2,3},{3,2},{4,5},{5,4},{6,7},{7,6},{8,9},{9,8},{10,11... | collective-permute-start | bytes 786440 | tf_op jit(solution)/shard_map/ppermute | solution.py:391
  24.8 6.8 %collective-permute-start.8 = (bf16[512,256]{1,0:T(8,128)(2,1)S(1)}, bf16[512,256]{1,0:T(8,128)(2,1)}, u32[]{:S(2)}, u32[]{:S(2)}) collective-permute-start(bf16[512,256]{1,0:T(8,128)(2,1)S(1)} %collective-permute-done.7.refs_8_), channel_id=1, source_target_pairs={{0,1},{1,0},{2,3},{3,2},{4,5},{5,4},{6,7},{7,6},{8,9},{9,8},{10,11... | collective-permute-start | bytes 786440 | tf_op jit(solution)/shard_map/ppermute | solution.py:391
  27.9 27.1 %collective-permute-start.18 = (bf16[272,2048]{1,0:T(8,128)(2,1)S(1)}, bf16[272,2048]{1,0:T(8,128)(2,1)S(1)}, u32[]{:S(2)}, u32[]{:S(2)}) collective-permute-start(bf16[272,2048]{1,0:T(8,128)(2,1)S(1)} %fusion.1.refs_8_), channel_id=1, source_target_pairs={{0,2},{2,4},{4,6},{6,0},{1,3},{3,5},{5,7},{7,1},{8,10},{10,12},{12... | collective-permute-start | bytes 3342344 | tf_op jit(solution)/shard_map/ppermute | solution.py:382
  29.0 26.0 %collective-permute-start.20 = (bf16[272,2048]{1,0:T(8,128)(2,1)S(1)}, bf16[272,2048]{1,0:T(8,128)(2,1)S(1)}, u32[]{:S(2)}, u32[]{:S(2)}) collective-permute-start(bf16[272,2048]{1,0:T(8,128)(2,1)S(1)} %fusion.1.refs_8_), channel_id=1, source_target_pairs={{0,6},{2,0},{4,2},{6,4},{1,7},{3,1},{5,3},{7,5},{8,14},{10,8},{12,... | collective-permute-start | bytes 3342344 | tf_op jit(solution)/shard_map/ppermute | solution.py:382
  31.6 36.6 %collective-permute-start.17 = (bf16[272,2048]{1,0:T(8,128)(2,1)S(1)}, bf16[272,2048]{1,0:T(8,128)(2,1)S(1)}, u32[]{:S(2)}, u32[]{:S(2)}) collective-permute-start(bf16[272,2048]{1,0:T(8,128)(2,1)S(1)} %fusion.1.refs_8_), channel_id=1, source_target_pairs={{0,1},{1,0},{2,3},{3,2},{4,5},{5,4},{6,7},{7,6},{8,9},{9,8},{10,11... | collective-permute-start | bytes 3342344 | tf_op jit(solution)/shard_map/ppermute | solution.py:391
  41.1 23.9 %collective-permute-start.9 = (bf16[32,128]{1,0:T(8,128)(2,1)S(1)}, bf16[32,128]{1,0:T(8,128)(2,1)S(1)}, u32[]{:S(2)}, u32[]{:S(2)}) collective-permute-start(bf16[32,128]{1,0:T(8,128)(2,1)S(1)} %get-tuple-element.50), channel_id=1, source_target_pairs={{0,8},{8,16},{16,24},{24,32},{32,40},{40,48},{48,56},{56,64},{64,7... | collective-permute-start | bytes 24584 | tf_op jit(solution)/shard_map/ppermute | solution.py:677
  55.2 37.9 %collective-permute-start.22 = (bf16[144,2048]{1,0:T(8,128)(2,1)S(1)}, bf16[144,2048]{1,0:T(8,128)(2,1)S(1)}, u32[]{:S(2)}, u32[]{:S(2)}) collective-permute-start(bf16[144,2048]{1,0:T(8,128)(2,1)S(1)} %get-tuple-element.61), channel_id=1, source_target_pairs={{0,6},{2,0},{4,2},{6,4},{1,7},{3,1},{5,3},{7,5},{8,14},{10,8},{12,... | collective-permute-start | bytes 1769480 | tf_op jit(solution)/shard_map/ppermute | solution.py:382
  57.7 92.5 %collective-permute-start.19 = (bf16[272,2048]{1,0:T(8,128)(2,1)S(1)}, bf16[272,2048]{1,0:T(8,128)(2,1)S(1)}, u32[]{:S(2)}, u32[]{:S(2)}) collective-permute-start(bf16[272,2048]{1,0:T(8,128)(2,1)S(1)} %collective-permute-done.18.right_any.refs_10_), channel_id=1, source_target_pairs={{0,1},{1,0},{2,3},{3,2},{4,5},{5,4},{6,7},{7,6},{8,9},{9,8},{10,11... | collective-permute-start | bytes 3342344 | tf_op jit(solution)/shard_map/ppermute | solution.py:391
  59.4 91.5 %collective-permute-start.21 = (bf16[272,2048]{1,0:T(8,128)(2,1)S(1)}, bf16[272,2048]{1,0:T(8,128)(2,1)S(1)}, u32[]{:S(2)}, u32[]{:S(2)}) collective-permute-start(bf16[272,2048]{1,0:T(8,128)(2,1)S(1)} %collective-permute-done.20.left_any.refs_12_), channel_id=1, source_target_pairs={{0,1},{1,0},{2,3},{3,2},{4,5},{5,4},{6,7},{7,6},{8,9},{9,8},{10,11... | collective-permute-start | bytes 3342344 | tf_op jit(solution)/shard_map/ppermute | solution.py:391
  65.0 4.9 %collective-permute-start.24 = (bf16[144,256]{1,0:T(8,128)(2,1)S(1)}, bf16[144,256]{1,0:T(8,128)(2,1)S(1)}, u32[]{:S(2)}, u32[]{:S(2)}) collective-permute-start(bf16[144,256]{1,0:T(8,128)(2,1)S(1)} %get-tuple-element.69.p0), channel_id=1, source_target_pairs={{0,16},{8,24},{16,0},{24,8},{1,17},{9,25},{17,1},{25,9},{2,18},{10... | collective-permute-start | bytes 221192 | tf_op jit(solution)/shard_map/ppermute | solution.py:382
  68.2 35.6 %collective-permute-start.38 = (bf16[128,2048]{1,0:T(8,128)(2,1)S(1)}, bf16[128,2048]{1,0:T(8,128)(2,1)S(1)}, u32[]{:S(2)}, u32[]{:S(2)}) collective-permute-start(bf16[128,2048]{1,0:T(8,128)(2,1)S(1)} %get-tuple-element.82), channel_id=1, source_target_pairs={{0,2},{2,4},{4,6},{6,0},{1,3},{3,5},{5,7},{7,1},{8,10},{10,12},{12... | collective-permute-start | bytes 1572872 | tf_op jit(solution)/shard_map/ppermute | solution.py:382
  74.0 5.3 %collective-permute-start.26 = (bf16[144,256]{1,0:T(8,128)(2,1)S(1)}, bf16[144,256]{1,0:T(8,128)(2,1)S(1)}, u32[]{:S(2)}, u32[]{:S(2)}) collective-permute-start(bf16[144,256]{1,0:T(8,128)(2,1)S(1)} %get-tuple-element.69.p0), channel_id=1, source_target_pairs={{0,8},{8,16},{16,24},{24,0},{1,9},{9,17},{17,25},{25,1},{2,10},{10... | collective-permute-start | bytes 221192 | tf_op jit(solution)/shard_map/ppermute | solution.py:382
  87.7 4.9 %collective-permute-start.12 = (bf16[128,256]{1,0:T(8,128)(2,1)S(1)}, bf16[128,256]{1,0:T(8,128)(2,1)S(1)}, u32[]{:S(2)}, u32[]{:S(2)}) collective-permute-start(bf16[128,256]{1,0:T(8,128)(2,1)S(1)} %get-tuple-element.55), channel_id=1, source_target_pairs={{0,3},{1,2},{2,5},{3,4},{4,7},{5,6},{6,1},{7,0},{8,11},{9,10},{10,... | collective-permute-start | bytes 196616 | tf_op jit(solution)/shard_map/ppermute | solution.py:399
  93.1 61.5 %collective-permute-start.23 = (bf16[144,2048]{1,0:T(8,128)(2,1)S(1)}, bf16[144,2048]{1,0:T(8,128)(2,1)S(1)}, u32[]{:S(2)}, u32[]{:S(2)}) collective-permute-start(bf16[144,2048]{1,0:T(8,128)(2,1)S(1)} %collective-permute-done.22.refs_14_), channel_id=1, source_target_pairs={{0,1},{1,0},{2,3},{3,2},{4,5},{5,4},{6,7},{7,6},{8,9},{9,8},{10,11... | collective-permute-start | bytes 1769480 | tf_op jit(solution)/shard_map/ppermute | solution.py:391
  95.7 5.1 %collective-permute-start.14 = (bf16[128,256]{1,0:T(8,128)(2,1)S(1)}, bf16[128,256]{1,0:T(8,128)(2,1)S(1)}, u32[]{:S(2)}, u32[]{:S(2)}) collective-permute-start(bf16[128,256]{1,0:T(8,128)(2,1)S(1)} %get-tuple-element.57), channel_id=1, source_target_pairs={{0,7},{1,6},{2,1},{3,0},{4,3},{5,2},{6,5},{7,4},{8,15},{9,14},{10,... | collective-permute-start | bytes 196616 | tf_op jit(solution)/shard_map/ppermute | solution.py:399
  100.8 4.7 %collective-permute-start.27 = (bf16[144,256]{1,0:T(8,128)(2,1)S(1)}, bf16[144,256]{1,0:T(8,128)(2,1)S(1)}, u32[]{:S(2)}, u32[]{:S(2)}) collective-permute-start(bf16[144,256]{1,0:T(8,128)(2,1)S(1)} %get-tuple-element.70.p0), channel_id=1, source_target_pairs={{0,64},{32,96},{64,0},{96,32},{128,192},{160,224},{192,128},{224,1... | collective-permute-start | bytes 221192 | tf_op jit(solution)/shard_map/ppermute | solution.py:664
  103.8 55.6 %collective-permute-start.39 = (bf16[128,2048]{1,0:T(8,128)(2,1)S(1)}, bf16[128,2048]{1,0:T(8,128)(2,1)S(1)}, u32[]{:S(2)}, u32[]{:S(2)}) collective-permute-start(bf16[128,2048]{1,0:T(8,128)(2,1)S(1)} %collective-permute-done.38.refs_14_), channel_id=1, source_target_pairs={{0,1},{1,0},{2,3},{3,2},{4,5},{5,4},{6,7},{7,6},{8,9},{9,8},{10,11... | collective-permute-start | bytes 1572872 | tf_op jit(solution)/shard_map/ppermute | solution.py:391
  105.6 5.5 %collective-permute-start.28 = (bf16[144,256]{1,0:T(8,128)(2,1)S(1)}, bf16[144,256]{1,0:T(8,128)(2,1)S(1)}, u32[]{:S(2)}, u32[]{:S(2)}) collective-permute-start(bf16[144,256]{1,0:T(8,128)(2,1)S(1)} %get-tuple-element.70.p0), channel_id=1, source_target_pairs={{0,96},{32,0},{64,32},{96,64},{128,224},{160,128},{192,160},{224,1... | collective-permute-start | bytes 221192 | tf_op jit(solution)/shard_map/ppermute | solution.py:664
  111.0 5.3 %collective-permute-start.29 = (bf16[144,256]{1,0:T(8,128)(2,1)S(1)}, bf16[144,256]{1,0:T(8,128)(2,1)S(1)}, u32[]{:S(2)}, u32[]{:S(2)}) collective-permute-start(bf16[144,256]{1,0:T(8,128)(2,1)S(1)} %get-tuple-element.70.p0), channel_id=1, source_target_pairs={{0,32},{32,64},{64,96},{96,0},{128,160},{160,192},{192,224},{224,1... | collective-permute-start | bytes 221192 | tf_op jit(solution)/shard_map/ppermute | solution.py:664
  116.4 4.6 %collective-permute-start.15 = (bf16[128,256]{1,0:T(8,128)(2,1)S(1)}, bf16[128,256]{1,0:T(8,128)(2,1)S(1)}, u32[]{:S(2)}, u32[]{:S(2)}) collective-permute-start(bf16[128,256]{1,0:T(8,128)(2,1)S(1)} %get-tuple-element.58), channel_id=1, source_target_pairs={{0,4},{1,5},{2,6},{3,7},{4,0},{5,1},{6,2},{7,3},{8,12},{9,13},{10,... | collective-permute-start | bytes 196616 | tf_op jit(solution)/shard_map/ppermute | solution.py:399
  121.0 7.6 %collective-permute-start.30 = (bf16[128,128]{1,0:T(8,128)(2,1)S(1)}, bf16[128,128]{1,0:T(8,128)(2,1)S(1)}, u32[]{:S(2)}, u32[]{:S(2)}) collective-permute-start(bf16[128,128]{1,0:T(8,128)(2,1)S(1)} %get-tuple-element.72), channel_id=1, source_target_pairs={{0,128},{32,160},{64,192},{96,224},{1,129},{33,161},{65,193},{97,2... | collective-permute-start | bytes 98312 | tf_op jit(solution)/shard_map/ppermute | solution.py:387
  128.6 8.4 %collective-permute-start.16 = (bf16[128,256]{1,0:T(8,128)(2,1)S(1)}, bf16[128,256]{1,0:T(8,128)(2,1)S(1)}, u32[]{:S(2)}, u32[]{:S(2)}) collective-permute-start(bf16[128,256]{1,0:T(8,128)(2,1)S(1)} %get-tuple-element.59), channel_id=1, source_target_pairs={{0,5},{1,4},{2,7},{3,6},{4,1},{5,0},{6,3},{7,2},{8,13},{9,12},{10,... | collective-permute-start | bytes 196616 | tf_op jit(solution)/shard_map/ppermute | solution.py:399
  145.1 4.6 %collective-permute-start.33 = (bf16[128,128]{1,0:T(8,128)(2,1)S(1)}, bf16[128,128]{1,0:T(8,128)(2,1)S(1)}, u32[]{:S(2)}, u32[]{:S(2)}) collective-permute-start(bf16[128,128]{1,0:T(8,128)(2,1)S(1)} %get-tuple-element.77), channel_id=1, source_target_pairs={{0,3},{1,2},{2,5},{3,4},{4,7},{5,6},{6,1},{7,0},{8,11},{9,10},{10,... | collective-permute-start | bytes 98312 | tf_op jit(solution)/shard_map/ppermute | solution.py:399
  149.6 7.0 %collective-permute-start.34 = (bf16[128,128]{1,0:T(8,128)(2,1)S(1)}, bf16[128,128]{1,0:T(8,128)(2,1)S(1)}, u32[]{:S(2)}, u32[]{:S(2)}) collective-permute-start(bf16[128,128]{1,0:T(8,128)(2,1)S(1)} %get-tuple-element.78), channel_id=1, source_target_pairs={{0,6},{1,7},{2,0},{3,1},{4,2},{5,3},{6,4},{7,5},{8,14},{9,15},{10,... | collective-permute-start | bytes 98312 | tf_op jit(solution)/shard_map/ppermute | solution.py:399
  150.2 6.5 %collective-permute-start.35 = (bf16[128,128]{1,0:T(8,128)(2,1)S(1)}, bf16[128,128]{1,0:T(8,128)(2,1)S(1)}, u32[]{:S(2)}, u32[]{:S(2)}) collective-permute-start(bf16[128,128]{1,0:T(8,128)(2,1)S(1)} %get-tuple-element.79), channel_id=1, source_target_pairs={{0,7},{1,6},{2,1},{3,0},{4,3},{5,2},{6,5},{7,4},{8,15},{9,14},{10,... | collective-permute-start | bytes 98312 | tf_op jit(solution)/shard_map/ppermute | solution.py:399
  150.9 5.8 %collective-permute-start.36 = (bf16[128,128]{1,0:T(8,128)(2,1)S(1)}, bf16[128,128]{1,0:T(8,128)(2,1)S(1)}, u32[]{:S(2)}, u32[]{:S(2)}) collective-permute-start(bf16[128,128]{1,0:T(8,128)(2,1)S(1)} %get-tuple-element.80), channel_id=1, source_target_pairs={{0,4},{1,5},{2,6},{3,7},{4,0},{5,1},{6,2},{7,3},{8,12},{9,13},{10,... | collective-permute-start | bytes 98312 | tf_op jit(solution)/shard_map/ppermute | solution.py:399
  154.5 4.8 %collective-permute-start.37 = (bf16[128,128]{1,0:T(8,128)(2,1)S(1)}, bf16[128,128]{1,0:T(8,128)(2,1)S(1)}, u32[]{:S(2)}, u32[]{:S(2)}) collective-permute-start(bf16[128,128]{1,0:T(8,128)(2,1)S(1)} %get-tuple-element.81), channel_id=1, source_target_pairs={{0,5},{1,4},{2,7},{3,6},{4,1},{5,0},{6,3},{7,2},{8,13},{9,12},{10,... | collective-permute-start | bytes 98312 | tf_op jit(solution)/shard_map/ppermute | solution.py:399
  (15 other events, 158.4 us)

commit v7 on v6

--- a/solution.py
+++ b/solution.py
@@ -151,6 +151,13 @@
 
     def each_half(body):
         def step(n, carry):
+            for which in range(2):
+
+                @pl.when(n == which)
+                def _():
+                    for one in moves[2 * which : 2 * which + 2]:
+                        one.wait()
+
             body(pl.ds(pl.multiple_of(n * half, half), half))
             return carry
 
@@ -184,9 +191,6 @@
         bl_ref[here, :] = jnp.where(
             lane == 0, jax.nn.sigmoid(bl), -rate_ref[0] * jax.nn.softplus(bl)
         )
-
-    for one in moves:
-        one.wait()
 
     def everything(here):
         for body in (gated, gates, queries, rest_of):
@@ -283,7 +287,7 @@
         shift = level.bit_length() - 1
         part = row >> shift
         below = ((part & 1) == 1) & ((column >> shift) == part - 1)
-        multiply = dot_fine if level >= 16 else (lambda a, b: dot(low(a), low(b)))
+        multiply = dot_fine if level >= 32 else (lambda a, b: dot(low(a), low(b)))
         moved = [
             multiply(inverse, jnp.where(below, lower, 0.0))
             for inverse, lower in zip(inverses, lowers)
@@ -344,7 +348,7 @@
     )(*map(near_core, (q, k, v, bl)))
 
 
-def along_kernel(which, place_ref, p0, p1, p2, p3, before_ref, total_ref, made_ref, held):
+def along_kernel(which, place_ref, p0, p1, p2, p3, before_ref, out_ref, held):
     me = place_ref[which]
     for j, piece in ((0, p0), (2, p1), (3, p2), (1, p3)):
         held[(me - j + 4) & 3] = piece[...]
@@ -356,20 +360,18 @@
         before = tuple(jnp.where(me == m, a, b) for a, b in zip(so_far, before))
         so_far = compose(read_state(held.at[m]), so_far)
     write_state(before_ref, before)
-    write_state(total_ref, so_far)
-    made_ref[...] = low(so_far[2])
-
-
-def along(which, places, state, *others):
+    if out_ref.shape == p0.shape:
+        write_state(out_ref, so_far)
+    else:
+        out_ref[...] = low(so_far[2])
+
+
+def along(which, places, out_shape, state, *others):
     return pl.pallas_call(
         functools.partial(along_kernel, which),
         in_specs=[scalars()] + [whole()] * 4,
-        out_specs=[whole()] * 3,
-        out_shape=[
-            jax.ShapeDtypeStruct(state.shape, BF16),
-            pltpu.VMEM(state.shape, BF16),
-            pltpu.VMEM((state.shape[1] // 2,) * 2, BF16),
-        ],
+        out_specs=[whole()] * 2,
+        out_shape=[pltpu.VMEM(state.shape, BF16), pltpu.VMEM(out_shape, BF16)],
         scratch_shapes=[pltpu.VMEM((4,) + state.shape, BF16)],
         compiler_params=params(4),
         cost_estimate=cost(16 << 20, 1 << 18),
@@ -657,12 +659,12 @@
     coef_p, coef_q, state = delta(q, k, v, bl)
 
 
-    before, total, _ = along(8, blocks, state, *(cyclic(state, "x", j) for j in (2, 3, 1)))
+    before, total = along(8, blocks, state.shape, state, *(cyclic(state, "x", j) for j in (2, 3, 1)))
     route = lambda j: [(h + i, h + (i + j) % 4) for h in (0, 4) for i in range(4)]
     around = []
     for j in (2, 3, 1):
         around.append(lax.ppermute(total, "z", route(j)))
-    before_z, _, made_z = along(9, blocks, total, *around)
+    before_z, made_z = along(9, blocks, (size, size), total, *around)
     far = shifted(made_z, "z", 4)
 
     ws = swapped(last)

time: 162 us -> 162 us (level)
  transfers between devices with their start and end apart: 40 -> 40, of which waited for: 21 -> 21; matrix products, arithmetic and copies ran while one was open for 3% -> 3% of each run, Pallas kernels for 15% -> 14%
where the time goes in v7:
time: 162 us; the launch traced here: 161 us
  starting transfers between devices  73.8 us (46%)
  waiting for transfers between devices  56.8 us (35%)
  Pallas kernels  24 us (15%)
  local copies, waits for them, and re-layouts  3.05 us (2%)
  other arithmetic  2.45 us (2%)
    ppermute x14, starting transfers between devices, exchanged(): got.append(lax.ppermute(parts[slot], TP, route))  26.7 us
    ppermute x11, waiting for transfers between devices, cyclic(): lax.ppermute(block, axis, [(i, (i + distance) % count) for i in range(cou...  25.2 us
    ppermute x14, waiting for transfers between devices, exchanged(): got.append(lax.ppermute(parts[slot], TP, route))  23.8 us
    ppermute x11, starting transfers between devices, cyclic(): lax.ppermute(block, axis, [(i, (i + distance) % count) for i in range(cou...  18.2 us
    ppermute x10, starting transfers between devices, swapped(): return lax.ppermute(block, 'c', [(0, 1), (1, 0)])  11.8 us
    ppermute x3, starting transfers between devices, local(): around.append(lax.ppermute(total, 'z', route(j)))  7.01 us
    pallas_call x1, Pallas kernels, project(): pl.pallas_call(functools.partial(project_kernel, width_all, head_size), i...  6.86 us
    ppermute x3, waiting for transfers between devices, local(): around.append(lax.ppermute(total, 'z', route(j)))  6.74 us
  transfers between devices with their start and end apart: 40, of which 21 were waited for; matrix products, arithmetic and copies ran while one was open for 3% of the time, Pallas kernels for 14%

profile of v7, /device:TPU:1, one launch (start us, length us, event | category | flops | bytes accessed | tf_op | source)
XLA Modules:
  0.0 161.3 jit_solution(9642519017097594976)
XLA Ops:
  0.0 2.1 %collective-permute-start.1 = (bf16[1024,256]{1,0:T(8,128)(2,1)}, bf16[1024,256]{1,0:T(8,128)(2,1)S(1)}, u32[]{:S(2)}, u32[]{:S(2)}) collective-permute-start(bf16[1024,256]{1,0:T(8,128)(2,1)} %refs_0_.3), channel_id=1, source_target_pairs={{0,2},{2,4},{4,6},{6,0},{1,3},{3,5},{5,7},{7,1},{8,10},{10,12},{12... | collective-permute-start | bytes 1572872 | tf_op jit(solution)/shard_map/ppermute | solution.py:384
  3.6 2.9 %collective-permute-start = (bf16[1024,256]{1,0:T(8,128)(2,1)}, bf16[1024,256]{1,0:T(8,128)(2,1)S(1)}, u32[]{:S(2)}, u32[]{:S(2)}) collective-permute-start(bf16[1024,256]{1,0:T(8,128)(2,1)} %refs_0_.3), channel_id=1, source_target_pairs={{0,1},{1,0},{2,3},{3,2},{4,5},{5,4},{6,7},{7,6},{8,9},{9,8},{10,11... | collective-permute-start | bytes 1572872 | tf_op jit(solution)/shard_map/ppermute | solution.py:393
  8.7 4.8 %collective-permute-done.1.right_any.refs_2_ = bf16[1024,256]{1,0:T(8,128)(2,1)S(1)} collective-permute-done((bf16[1024,256]{1,0:T(8,128)(2,1)}, bf16[1024,256]{1,0:T(8,128)(2,1)S(1)}, u32[]{:S(2)}, u32[]{:S(2)}) %collective-permute-start.1) | collective-permute-done | bytes 524320 | tf_op jit(solution)/shard_map/ppermute | solution.py:384
  18.7 3.3 %collective-permute-done.5.refs_6_ = bf16[512,256]{1,0:T(8,128)(2,1)S(1)} collective-permute-done((bf16[512,256]{1,0:T(8,128)(2,1)S(1)}, bf16[512,256]{1,0:T(8,128)(2,1)S(1)}, u32[]{:S(2)}, u32[]{:S(2)}) %collective-permute-start.5) | collective-permute-done | bytes 262176 | tf_op jit(solution)/shard_map/ppermute | solution.py:384
  22.0 2.8 %collective-permute-start.6 = (bf16[512,256]{1,0:T(8,128)(2,1)S(1)}, bf16[512,256]{1,0:T(8,128)(2,1)S(1)}, u32[]{:S(2)}, u32[]{:S(2)}) collective-permute-start(bf16[512,256]{1,0:T(8,128)(2,1)S(1)} %collective-permute-done.5.refs_6_), channel_id=1, source_target_pairs={{0,1},{1,0},{2,3},{3,2},{4,5},{5,4},{6,7},{7,6},{8,9},{9,8},{10,11... | collective-permute-start | bytes 786440 | tf_op jit(solution)/shard_map/ppermute | solution.py:393
  32.0 2.2 %pack.1.refs_10_ = bf16[4,2048,256]{2,1,0:T(8,128)(2,1)S(1)} custom-call(bf16[2048,128]{1,0:T(8,128)(2,1)} %refs_0_.2, bf16[2048,128]{1,0:T(8,128)(2,1)} %refs_1_.1, bf16[2048,128]{1,0:T(8,128)(2,1)} %refs_2_.1, bf16[2048,128]{1,0:T(8,128)(2,1)} %refs_3_.1, bf16[2048,128]{1,0:T(8,128)(2,1)} %refs_4_.1, bf16[2048,128]{1,0:T(8,128)(2,1)} %refs_5_.1, ...), custom_call_target="tpu_custom_call" | custom-call | flops 1048576 | bytes 8388608 | tf_op jit(solution)/shard_map/pack/pallas_call | solution.py:108
  34.3 6.9 %project.1 = (bf16[1024,128]{1,0:T(8,128)(2,1)S(1)}, bf16[1024,128]{1,0:T(8,128)(2,1)S(1)}, bf16[1024,128]{1,0:T(8,128)(2,1)S(1)}, f32[1024,128]{1,0:T(8,128)S(1...) custom-call(s32[10]{0:T(128)S(1)} %stack.71.block_ref.place_ref, ...), custom_call_target="tpu_custom_call" | custom-call | flops 4294967296 | bytes 12582912 | tf_op jit(solution)/shard_map/project/pallas_call | solution.py:206
  41.1 3.6 %collective-permute-start.9 = (bf16[32,128]{1,0:T(8,128)(2,1)S(1)}, bf16[32,128]{1,0:T(8,128)(2,1)S(1)}, u32[]{:S(2)}, u32[]{:S(2)}) collective-permute-start(bf16[32,128]{1,0:T(8,128)(2,1)S(1)} %get-tuple-element.50), channel_id=1, source_target_pairs={{0,8},{8,16},{16,24},{24,32},{32,40},{40,48},{48,56},{56,64},{64,7... | collective-permute-start | bytes 24584 | tf_op jit(solution)/shard_map/ppermute | solution.py:679
  44.7 10.3 %collective-permute-done.18.right_any.refs_10_ = bf16[272,2048]{1,0:T(8,128)(2,1)S(1)} collective-permute-done((bf16[272,2048]{1,0:T(8,128)(2,1)S(1)}, bf16[272,2048]{1,0:T(8,128)(2,1)S(1)}, u32[]{:S(2)}, u32[]{:S(2)}) %collective-permute-start.18) | collective-permute-done | bytes 1114144 | tf_op jit(solution)/shard_map/ppermute | solution.py:384
  55.2 2.5 %collective-permute-start.22 = (bf16[144,2048]{1,0:T(8,128)(2,1)S(1)}, bf16[144,2048]{1,0:T(8,128)(2,1)S(1)}, u32[]{:S(2)}, u32[]{:S(2)}) collective-permute-start(bf16[144,2048]{1,0:T(8,128)(2,1)S(1)} %get-tuple-element.61), channel_id=1, source_target_pairs={{0,6},{2,0},{4,2},{6,4},{1,7},{3,1},{5,3},{7,5},{8,14},{10,8},{12,... | collective-permute-start | bytes 1769480 | tf_op jit(solution)/shard_map/ppermute | solution.py:384
  59.4 5.4 %delta.1 = (bf16[1024,128]{1,0:T(8,128)(2,1)S(1)}, f32[1024,128]{1,0:T(8,128)S(1)}, bf16[144,256]{1,0:T(8,128)(2,1)S(1)}) custom-call(bf16[1024,128]{1,0:T(8,128)(2,1)S(1)} %get-tuple-element.62.q_ref, bf16[1024,128]{1,0:T(8,128)(2,1)S(1)} %get-tuple-element.63.k_ref, bf16[1024,128]{1,0:T(8,128)(2,1)S(1)} %get-tuple-element.64.v_ref, ...), custom_call_target="tpu_custom_call" | custom-call | flops 2013265920 | bytes 3145728 | tf_op jit(solution)/shard_map/delta/pallas_call | solution.py:336
  64.8 3.2 %collective-permute-start.24 = (bf16[144,256]{1,0:T(8,128)(2,1)S(1)}, bf16[144,256]{1,0:T(8,128)(2,1)S(1)}, u32[]{:S(2)}, u32[]{:S(2)}) collective-permute-start(bf16[144,256]{1,0:T(8,128)(2,1)S(1)} %get-tuple-element.69.p0), channel_id=1, source_target_pairs={{0,16},{8,24},{16,0},{24,8},{1,17},{9,25},{17,1},{25,9},{2,18},{10... | collective-permute-start | bytes 221192 | tf_op jit(solution)/shard_map/ppermute | solution.py:384
  69.7 2.7 %collective-permute-start.25 = (bf16[144,256]{1,0:T(8,128)(2,1)S(1)}, bf16[144,256]{1,0:T(8,128)(2,1)S(1)}, u32[]{:S(2)}, u32[]{:S(2)}) collective-permute-start(bf16[144,256]{1,0:T(8,128)(2,1)S(1)} %get-tuple-element.69.p0), channel_id=1, source_target_pairs={{0,24},{8,0},{16,8},{24,16},{1,25},{9,1},{17,9},{25,17},{2,26},{10... | collective-permute-start | bytes 221192 | tf_op jit(solution)/shard_map/ppermute | solution.py:384
  74.7 2.0 %conv.1 = (bf16[128,256]{1,0:T(8,128)(2,1)S(1)}, bf16[128,256]{1,0:T(8,128)(2,1)S(1)}, bf16[128,256]{1,0:T(8,128)(2,1)S(1)}, bf16[128,256]{1,0:T(8,128)(2,1)S(1)...) custom-call(s32[10]{0:T(128)S(1)} %stack.71.block_ref.place_ref, ...), custom_call_target="tpu_custom_call" | custom-call | flops 268435456 | bytes 1048576 | tf_op jit(solution)/shard_map/conv/pallas_call | solution.py:463
  76.7 2.5 %collective-permute-done.26.p3 = bf16[144,256]{1,0:T(8,128)(2,1)S(1)} collective-permute-done((bf16[144,256]{1,0:T(8,128)(2,1)S(1)}, bf16[144,256]{1,0:T(8,128)(2,1)S(1)}, u32[]{:S(2)}, u32[]{:S(2)}) %collective-permute-start.26) | collective-permute-done | bytes 73760 | tf_op jit(solution)/shard_map/ppermute | solution.py:384
  79.2 3.1 %collective-permute-start.10 = (bf16[128,256]{1,0:T(8,128)(2,1)S(1)}, bf16[128,256]{1,0:T(8,128)(2,1)S(1)}, u32[]{:S(2)}, u32[]{:S(2)}) collective-permute-start(bf16[128,256]{1,0:T(8,128)(2,1)S(1)} %get-tuple-element.53), channel_id=1, source_target_pairs={{0,1},{1,0},{2,3},{3,2},{4,5},{5,4},{6,7},{7,6},{8,9},{9,8},{10,11... | collective-permute-start | bytes 196616 | tf_op jit(solution)/shard_map/ppermute | solution.py:401
  83.2 4.3 %collective-permute-done.11.refs_2_ = bf16[128,256]{1,0:T(8,128)(2,1)S(1)} collective-permute-done((bf16[128,256]{1,0:T(8,128)(2,1)S(1)}, bf16[128,256]{1,0:T(8,128)(2,1)S(1)}, u32[]{:S(2)}, u32[]{:S(2)}) %collective-permute-start.11) | collective-permute-done | bytes 65568 | tf_op jit(solution)/shard_map/ppermute | solution.py:401
  87.6 4.8 %collective-permute-done.12.refs_3_ = bf16[128,256]{1,0:T(8,128)(2,1)S(1)} collective-permute-done((bf16[128,256]{1,0:T(8,128)(2,1)S(1)}, bf16[128,256]{1,0:T(8,128)(2,1)S(1)}, u32[]{:S(2)}, u32[]{:S(2)}) %collective-permute-start.12) | collective-permute-done | bytes 65568 | tf_op jit(solution)/shard_map/ppermute | solution.py:401
  95.5 3.5 %collective-permute-start.14 = (bf16[128,256]{1,0:T(8,128)(2,1)S(1)}, bf16[128,256]{1,0:T(8,128)(2,1)S(1)}, u32[]{:S(2)}, u32[]{:S(2)}) collective-permute-start(bf16[128,256]{1,0:T(8,128)(2,1)S(1)} %get-tuple-element.57), channel_id=1, source_target_pairs={{0,7},{1,6},{2,1},{3,0},{4,3},{5,2},{6,5},{7,4},{8,15},{9,14},{10,... | collective-permute-start | bytes 196616 | tf_op jit(solution)/shard_map/ppermute | solution.py:401
  100.3 3.0 %collective-permute-start.27 = (bf16[144,256]{1,0:T(8,128)(2,1)S(1)}, bf16[144,256]{1,0:T(8,128)(2,1)S(1)}, u32[]{:S(2)}, u32[]{:S(2)}) collective-permute-start(bf16[144,256]{1,0:T(8,128)(2,1)S(1)} %get-tuple-element.70.p0), channel_id=1, source_target_pairs={{0,64},{32,96},{64,0},{96,32},{128,192},{160,224},{192,128},{224,1... | collective-permute-start | bytes 221192 | tf_op jit(solution)/shard_map/ppermute | solution.py:666
  105.1 4.0 %collective-permute-start.28 = (bf16[144,256]{1,0:T(8,128)(2,1)S(1)}, bf16[144,256]{1,0:T(8,128)(2,1)S(1)}, u32[]{:S(2)}, u32[]{:S(2)}) collective-permute-start(bf16[144,256]{1,0:T(8,128)(2,1)S(1)} %get-tuple-element.70.p0), channel_id=1, source_target_pairs={{0,96},{32,0},{64,32},{96,64},{128,224},{160,128},{192,160},{224,1... | collective-permute-start | bytes 221192 | tf_op jit(solution)/shard_map/ppermute | solution.py:666
  110.5 5.3 %collective-permute-done.29.p3 = bf16[144,256]{1,0:T(8,128)(2,1)S(1)} collective-permute-done((bf16[144,256]{1,0:T(8,128)(2,1)S(1)}, bf16[144,256]{1,0:T(8,128)(2,1)S(1)}, u32[]{:S(2)}, u32[]{:S(2)}) %collective-permute-start.29) | collective-permute-done | bytes 73760 | tf_op jit(solution)/shard_map/ppermute | solution.py:666
  115.9 2.6 %collective-permute-start.15 = (bf16[128,256]{1,0:T(8,128)(2,1)S(1)}, bf16[128,256]{1,0:T(8,128)(2,1)S(1)}, u32[]{:S(2)}, u32[]{:S(2)}) collective-permute-start(bf16[128,256]{1,0:T(8,128)(2,1)S(1)} %get-tuple-element.58), channel_id=1, source_target_pairs={{0,4},{1,5},{2,6},{3,7},{4,0},{5,1},{6,2},{7,3},{8,12},{9,13},{10,... | collective-permute-start | bytes 196616 | tf_op jit(solution)/shard_map/ppermute | solution.py:401
  120.5 6.6 %collective-permute-start.30 = (bf16[128,128]{1,0:T(8,128)(2,1)S(1)}, bf16[128,128]{1,0:T(8,128)(2,1)S(1)}, u32[]{:S(2)}, u32[]{:S(2)}) collective-permute-start(bf16[128,128]{1,0:T(8,128)(2,1)S(1)} %get-tuple-element.72), channel_id=1, source_target_pairs={{0,128},{32,160},{64,192},{96,224},{1,129},{33,161},{65,193},{97,2... | collective-permute-start | bytes 98312 | tf_op jit(solution)/shard_map/ppermute | solution.py:389
  128.1 6.8 %collective-permute-start.16 = (bf16[128,256]{1,0:T(8,128)(2,1)S(1)}, bf16[128,256]{1,0:T(8,128)(2,1)S(1)}, u32[]{:S(2)}, u32[]{:S(2)}) collective-permute-start(bf16[128,256]{1,0:T(8,128)(2,1)S(1)} %get-tuple-element.59), channel_id=1, source_target_pairs={{0,5},{1,4},{2,7},{3,6},{4,1},{5,0},{6,3},{7,2},{8,13},{9,12},{10,... | collective-permute-start | bytes 196616 | tf_op jit(solution)/shard_map/ppermute | solution.py:401
  136.8 3.3 %collective-permute-start.31 = (bf16[128,128]{1,0:T(8,128)(2,1)S(1)}, bf16[128,128]{1,0:T(8,128)(2,1)S(1)}, u32[]{:S(2)}, u32[]{:S(2)}) collective-permute-start(bf16[128,128]{1,0:T(8,128)(2,1)S(1)} %get-tuple-element.75), channel_id=1, source_target_pairs={{0,1},{1,0},{2,3},{3,2},{4,5},{5,4},{6,7},{7,6},{8,9},{9,8},{10,11... | collective-permute-start | bytes 98312 | tf_op jit(solution)/shard_map/ppermute | solution.py:401
  141.8 3.1 %collective-permute-done.32.refs_2_ = bf16[128,128]{1,0:T(8,128)(2,1)S(1)} collective-permute-done((bf16[128,128]{1,0:T(8,128)(2,1)S(1)}, bf16[128,128]{1,0:T(8,128)(2,1)S(1)}, u32[]{:S(2)}, u32[]{:S(2)}) %collective-permute-start.32) | collective-permute-done | bytes 32800 | tf_op jit(solution)/shard_map/ppermute | solution.py:401
  146.0 3.5 %collective-permute-done.33.refs_3_ = bf16[128,128]{1,0:T(8,128)(2,1)S(1)} collective-permute-done((bf16[128,128]{1,0:T(8,128)(2,1)S(1)}, bf16[128,128]{1,0:T(8,128)(2,1)S(1)}, u32[]{:S(2)}, u32[]{:S(2)}) %collective-permute-start.33) | collective-permute-done | bytes 32800 | tf_op jit(solution)/shard_map/ppermute | solution.py:401
  150.7 3.7 %collective-permute-start.36 = (bf16[128,128]{1,0:T(8,128)(2,1)S(1)}, bf16[128,128]{1,0:T(8,128)(2,1)S(1)}, u32[]{:S(2)}, u32[]{:S(2)}) collective-permute-start(bf16[128,128]{1,0:T(8,128)(2,1)S(1)} %get-tuple-element.80), channel_id=1, source_target_pairs={{0,4},{1,5},{2,6},{3,7},{4,0},{5,1},{6,2},{7,3},{8,12},{9,13},{10,... | collective-permute-start | bytes 98312 | tf_op jit(solution)/shard_map/ppermute | solution.py:401
  154.4 2.1 %conv_out.1.conv_ref = f32[128,2048]{1,0:T(8,128)S(1)} custom-call(bf16[128,256]{1,0:T(8,128)(2,1)S(1)} %get-tuple-element.52.refs_0_, bf16[128,256]{1,0:T(8,128)(2,1)S(1)} %collective-permute-done.10.refs_1_, bf16[128,256]{1,0:T(8,128)(2,1)S(1)} %collective-permute-done.11.refs_2_, bf16[128,256]{1,0:T(8,128)(2,1)S(1)} %collective-permute-done.12.refs_3_, ...), custom_call_target="tpu_custom_call" | custom-call | flops 536870912 | bytes 6291456 | tf_op jit(solution)/shard_map/conv_out/pallas_call | solution.py:544
  156.5 2.7 %collective-permute-done.37.refs_7_ = bf16[128,128]{1,0:T(8,128)(2,1)S(1)} collective-permute-done((bf16[128,128]{1,0:T(8,128)(2,1)S(1)}, bf16[128,128]{1,0:T(8,128)(2,1)S(1)}, u32[]{:S(2)}, u32[]{:S(2)}) %collective-permute-start.37) | collective-permute-done | bytes 32800 | tf_op jit(solution)/shard_map/ppermute | solution.py:401
  159.2 1.9 %delta_out.1 = bf16[128,2048]{1,0:T(8,128)(2,1)} custom-call(f32[128,2048]{1,0:T(8,128)S(1)} %conv_out.1.conv_ref, bf16[128,128]{1,0:T(8,128)(2,1)S(1)} %get-tuple-element.74.refs_0_, bf16[128,128]{1,0:T(8,128)(2,1)S(1)} %collective-permute-done.31.refs_1_, bf16[128,128]{1,0:T(8,128)(2,1)S(1)} %collective-permute-done.32.refs_2_, ...), custom_call_target="tpu_custom_call" | custom-call | flops 536870912 | bytes 6291456 | tf_op jit(solution)/shard_map/delta_out/pallas_call | solution.py:573
  (84 shorter events, 38.9 us)
Async XLA Ops:
  0.0 13.5 %collective-permute-start.1 = (bf16[1024,256]{1,0:T(8,128)(2,1)}, bf16[1024,256]{1,0:T(8,128)(2,1)S(1)}, u32[]{:S(2)}, u32[]{:S(2)}) collective-permute-start(bf16[1024,256]{1,0:T(8,128)(2,1)} %refs_0_.3), channel_id=1, source_target_pairs={{0,2},{2,4},{4,6},{6,0},{1,3},{3,5},{5,7},{7,1},{8,10},{10,12},{12... | collective-permute-start | bytes 1572872 | tf_op jit(solution)/shard_map/ppermute | solution.py:384
  2.1 12.6 %collective-permute-start.3 = (bf16[1024,256]{1,0:T(8,128)(2,1)}, bf16[1024,256]{1,0:T(8,128)(2,1)S(1)}, u32[]{:S(2)}, u32[]{:S(2)}) collective-permute-start(bf16[1024,256]{1,0:T(8,128)(2,1)} %refs_0_.3), channel_id=1, source_target_pairs={{0,6},{2,0},{4,2},{6,4},{1,7},{3,1},{5,3},{7,5},{8,14},{10,8},{12,... | collective-permute-start | bytes 1572872 | tf_op jit(solution)/shard_map/ppermute | solution.py:384
  3.6 27.1 %collective-permute-start = (bf16[1024,256]{1,0:T(8,128)(2,1)}, bf16[1024,256]{1,0:T(8,128)(2,1)S(1)}, u32[]{:S(2)}, u32[]{:S(2)}) collective-permute-start(bf16[1024,256]{1,0:T(8,128)(2,1)} %refs_0_.3), channel_id=1, source_target_pairs={{0,1},{1,0},{2,3},{3,2},{4,5},{5,4},{6,7},{7,6},{8,9},{9,8},{10,11... | collective-permute-start | bytes 1572872 | tf_op jit(solution)/shard_map/ppermute | solution.py:393
  14.8 7.2 %collective-permute-start.5 = (bf16[512,256]{1,0:T(8,128)(2,1)S(1)}, bf16[512,256]{1,0:T(8,128)(2,1)S(1)}, u32[]{:S(2)}, u32[]{:S(2)}) collective-permute-start(bf16[512,256]{1,0:T(8,128)(2,1)S(1)} %get-tuple-element.46), channel_id=1, source_target_pairs={{0,2},{2,4},{4,6},{6,0},{1,3},{3,5},{5,7},{7,1},{8,10},{10,12},{12... | collective-permute-start | bytes 786440 | tf_op jit(solution)/shard_map/ppermute | solution.py:384
  16.3 8.5 %collective-permute-start.7 = (bf16[512,256]{1,0:T(8,128)(2,1)S(1)}, bf16[512,256]{1,0:T(8,128)(2,1)S(1)}, u32[]{:S(2)}, u32[]{:S(2)}) collective-permute-start(bf16[512,256]{1,0:T(8,128)(2,1)S(1)} %get-tuple-element.47), channel_id=1, source_target_pairs={{0,6},{2,0},{4,2},{6,4},{1,7},{3,1},{5,3},{7,5},{8,14},{10,8},{12,... | collective-permute-start | bytes 786440 | tf_op jit(solution)/shard_map/ppermute | solution.py:384
  22.0 9.5 %collective-permute-start.6 = (bf16[512,256]{1,0:T(8,128)(2,1)S(1)}, bf16[512,256]{1,0:T(8,128)(2,1)S(1)}, u32[]{:S(2)}, u32[]{:S(2)}) collective-permute-start(bf16[512,256]{1,0:T(8,128)(2,1)S(1)} %collective-permute-done.5.refs_6_), channel_id=1, source_target_pairs={{0,1},{1,0},{2,3},{3,2},{4,5},{5,4},{6,7},{7,6},{8,9},{9,8},{10,11... | collective-permute-start | bytes 786440 | tf_op jit(solution)/shard_map/ppermute | solution.py:393
  24.8 6.8 %collective-permute-start.8 = (bf16[512,256]{1,0:T(8,128)(2,1)S(1)}, bf16[512,256]{1,0:T(8,128)(2,1)}, u32[]{:S(2)}, u32[]{:S(2)}) collective-permute-start(bf16[512,256]{1,0:T(8,128)(2,1)S(1)} %collective-permute-done.7.refs_8_), channel_id=1, source_target_pairs={{0,1},{1,0},{2,3},{3,2},{4,5},{5,4},{6,7},{7,6},{8,9},{9,8},{10,11... | collective-permute-start | bytes 786440 | tf_op jit(solution)/shard_map/ppermute | solution.py:393
  27.9 27.1 %collective-permute-start.18 = (bf16[272,2048]{1,0:T(8,128)(2,1)S(1)}, bf16[272,2048]{1,0:T(8,128)(2,1)S(1)}, u32[]{:S(2)}, u32[]{:S(2)}) collective-permute-start(bf16[272,2048]{1,0:T(8,128)(2,1)S(1)} %fusion.1.refs_8_), channel_id=1, source_target_pairs={{0,2},{2,4},{4,6},{6,0},{1,3},{3,5},{5,7},{7,1},{8,10},{10,12},{12... | collective-permute-start | bytes 3342344 | tf_op jit(solution)/shard_map/ppermute | solution.py:384
  29.0 26.0 %collective-permute-start.20 = (bf16[272,2048]{1,0:T(8,128)(2,1)S(1)}, bf16[272,2048]{1,0:T(8,128)(2,1)S(1)}, u32[]{:S(2)}, u32[]{:S(2)}) collective-permute-start(bf16[272,2048]{1,0:T(8,128)(2,1)S(1)} %fusion.1.refs_8_), channel_id=1, source_target_pairs={{0,6},{2,0},{4,2},{6,4},{1,7},{3,1},{5,3},{7,5},{8,14},{10,8},{12,... | collective-permute-start | bytes 3342344 | tf_op jit(solution)/shard_map/ppermute | solution.py:384
  31.6 36.4 %collective-permute-start.17 = (bf16[272,2048]{1,0:T(8,128)(2,1)S(1)}, bf16[272,2048]{1,0:T(8,128)(2,1)S(1)}, u32[]{:S(2)}, u32[]{:S(2)}) collective-permute-start(bf16[272,2048]{1,0:T(8,128)(2,1)S(1)} %fusion.1.refs_8_), channel_id=1, source_target_pairs={{0,1},{1,0},{2,3},{3,2},{4,5},{5,4},{6,7},{7,6},{8,9},{9,8},{10,11... | collective-permute-start | bytes 3342344 | tf_op jit(solution)/shard_map/ppermute | solution.py:393
  41.1 23.7 %collective-permute-start.9 = (bf16[32,128]{1,0:T(8,128)(2,1)S(1)}, bf16[32,128]{1,0:T(8,128)(2,1)S(1)}, u32[]{:S(2)}, u32[]{:S(2)}) collective-permute-start(bf16[32,128]{1,0:T(8,128)(2,1)S(1)} %get-tuple-element.50), channel_id=1, source_target_pairs={{0,8},{8,16},{16,24},{24,32},{32,40},{40,48},{48,56},{56,64},{64,7... | collective-permute-start | bytes 24584 | tf_op jit(solution)/shard_map/ppermute | solution.py:679
  55.2 37.7 %collective-permute-start.22 = (bf16[144,2048]{1,0:T(8,128)(2,1)S(1)}, bf16[144,2048]{1,0:T(8,128)(2,1)S(1)}, u32[]{:S(2)}, u32[]{:S(2)}) collective-permute-start(bf16[144,2048]{1,0:T(8,128)(2,1)S(1)} %get-tuple-element.61), channel_id=1, source_target_pairs={{0,6},{2,0},{4,2},{6,4},{1,7},{3,1},{5,3},{7,5},{8,14},{10,8},{12,... | collective-permute-start | bytes 1769480 | tf_op jit(solution)/shard_map/ppermute | solution.py:384
  57.7 92.3 %collective-permute-start.19 = (bf16[272,2048]{1,0:T(8,128)(2,1)S(1)}, bf16[272,2048]{1,0:T(8,128)(2,1)S(1)}, u32[]{:S(2)}, u32[]{:S(2)}) collective-permute-start(bf16[272,2048]{1,0:T(8,128)(2,1)S(1)} %collective-permute-done.18.right_any.refs_10_), channel_id=1, source_target_pairs={{0,1},{1,0},{2,3},{3,2},{4,5},{5,4},{6,7},{7,6},{8,9},{9,8},{10,11... | collective-permute-start | bytes 3342344 | tf_op jit(solution)/shard_map/ppermute | solution.py:393
  59.4 91.3 %collective-permute-start.21 = (bf16[272,2048]{1,0:T(8,128)(2,1)S(1)}, bf16[272,2048]{1,0:T(8,128)(2,1)S(1)}, u32[]{:S(2)}, u32[]{:S(2)}) collective-permute-start(bf16[272,2048]{1,0:T(8,128)(2,1)S(1)} %collective-permute-done.20.left_any.refs_12_), channel_id=1, source_target_pairs={{0,1},{1,0},{2,3},{3,2},{4,5},{5,4},{6,7},{7,6},{8,9},{9,8},{10,11... | collective-permute-start | bytes 3342344 | tf_op jit(solution)/shard_map/ppermute | solution.py:393
  64.8 4.9 %collective-permute-start.24 = (bf16[144,256]{1,0:T(8,128)(2,1)S(1)}, bf16[144,256]{1,0:T(8,128)(2,1)S(1)}, u32[]{:S(2)}, u32[]{:S(2)}) collective-permute-start(bf16[144,256]{1,0:T(8,128)(2,1)S(1)} %get-tuple-element.69.p0), channel_id=1, source_target_pairs={{0,16},{8,24},{16,0},{24,8},{1,17},{9,25},{17,1},{25,9},{2,18},{10... | collective-permute-start | bytes 221192 | tf_op jit(solution)/shard_map/ppermute | solution.py:384
  68.0 35.3 %collective-permute-start.38 = (bf16[128,2048]{1,0:T(8,128)(2,1)S(1)}, bf16[128,2048]{1,0:T(8,128)(2,1)S(1)}, u32[]{:S(2)}, u32[]{:S(2)}) collective-permute-start(bf16[128,2048]{1,0:T(8,128)(2,1)S(1)} %get-tuple-element.82), channel_id=1, source_target_pairs={{0,2},{2,4},{4,6},{6,0},{1,3},{3,5},{5,7},{7,1},{8,10},{10,12},{12... | collective-permute-start | bytes 1572872 | tf_op jit(solution)/shard_map/ppermute | solution.py:384
  73.8 5.3 %collective-permute-start.26 = (bf16[144,256]{1,0:T(8,128)(2,1)S(1)}, bf16[144,256]{1,0:T(8,128)(2,1)S(1)}, u32[]{:S(2)}, u32[]{:S(2)}) collective-permute-start(bf16[144,256]{1,0:T(8,128)(2,1)S(1)} %get-tuple-element.69.p0), channel_id=1, source_target_pairs={{0,8},{8,16},{16,24},{24,0},{1,9},{9,17},{17,25},{25,1},{2,10},{10... | collective-permute-start | bytes 221192 | tf_op jit(solution)/shard_map/ppermute | solution.py:384
  87.5 4.9 %collective-permute-start.12 = (bf16[128,256]{1,0:T(8,128)(2,1)S(1)}, bf16[128,256]{1,0:T(8,128)(2,1)S(1)}, u32[]{:S(2)}, u32[]{:S(2)}) collective-permute-start(bf16[128,256]{1,0:T(8,128)(2,1)S(1)} %get-tuple-element.55), channel_id=1, source_target_pairs={{0,3},{1,2},{2,5},{3,4},{4,7},{5,6},{6,1},{7,0},{8,11},{9,10},{10,... | collective-permute-start | bytes 196616 | tf_op jit(solution)/shard_map/ppermute | solution.py:401
  92.9 61.5 %collective-permute-start.23 = (bf16[144,2048]{1,0:T(8,128)(2,1)S(1)}, bf16[144,2048]{1,0:T(8,128)(2,1)S(1)}, u32[]{:S(2)}, u32[]{:S(2)}) collective-permute-start(bf16[144,2048]{1,0:T(8,128)(2,1)S(1)} %collective-permute-done.22.refs_14_), channel_id=1, source_target_pairs={{0,1},{1,0},{2,3},{3,2},{4,5},{5,4},{6,7},{7,6},{8,9},{9,8},{10,11... | collective-permute-start | bytes 1769480 | tf_op jit(solution)/shard_map/ppermute | solution.py:393
  95.5 4.8 %collective-permute-start.14 = (bf16[128,256]{1,0:T(8,128)(2,1)S(1)}, bf16[128,256]{1,0:T(8,128)(2,1)S(1)}, u32[]{:S(2)}, u32[]{:S(2)}) collective-permute-start(bf16[128,256]{1,0:T(8,128)(2,1)S(1)} %get-tuple-element.57), channel_id=1, source_target_pairs={{0,7},{1,6},{2,1},{3,0},{4,3},{5,2},{6,5},{7,4},{8,15},{9,14},{10,... | collective-permute-start | bytes 196616 | tf_op jit(solution)/shard_map/ppermute | solution.py:401
  100.3 4.8 %collective-permute-start.27 = (bf16[144,256]{1,0:T(8,128)(2,1)S(1)}, bf16[144,256]{1,0:T(8,128)(2,1)S(1)}, u32[]{:S(2)}, u32[]{:S(2)}) collective-permute-start(bf16[144,256]{1,0:T(8,128)(2,1)S(1)} %get-tuple-element.70.p0), channel_id=1, source_target_pairs={{0,64},{32,96},{64,0},{96,32},{128,192},{160,224},{192,128},{224,1... | collective-permute-start | bytes 221192 | tf_op jit(solution)/shard_map/ppermute | solution.py:666
  103.3 55.9 %collective-permute-start.39 = (bf16[128,2048]{1,0:T(8,128)(2,1)S(1)}, bf16[128,2048]{1,0:T(8,128)(2,1)S(1)}, u32[]{:S(2)}, u32[]{:S(2)}) collective-permute-start(bf16[128,2048]{1,0:T(8,128)(2,1)S(1)} %collective-permute-done.38.refs_14_), channel_id=1, source_target_pairs={{0,1},{1,0},{2,3},{3,2},{4,5},{5,4},{6,7},{7,6},{8,9},{9,8},{10,11... | collective-permute-start | bytes 1572872 | tf_op jit(solution)/shard_map/ppermute | solution.py:393
  105.1 5.4 %collective-permute-start.28 = (bf16[144,256]{1,0:T(8,128)(2,1)S(1)}, bf16[144,256]{1,0:T(8,128)(2,1)S(1)}, u32[]{:S(2)}, u32[]{:S(2)}) collective-permute-start(bf16[144,256]{1,0:T(8,128)(2,1)S(1)} %get-tuple-element.70.p0), channel_id=1, source_target_pairs={{0,96},{32,0},{64,32},{96,64},{128,224},{160,128},{192,160},{224,1... | collective-permute-start | bytes 221192 | tf_op jit(solution)/shard_map/ppermute | solution.py:666
  110.5 5.3 %collective-permute-start.29 = (bf16[144,256]{1,0:T(8,128)(2,1)S(1)}, bf16[144,256]{1,0:T(8,128)(2,1)S(1)}, u32[]{:S(2)}, u32[]{:S(2)}) collective-permute-start(bf16[144,256]{1,0:T(8,128)(2,1)S(1)} %get-tuple-element.70.p0), channel_id=1, source_target_pairs={{0,32},{32,64},{64,96},{96,0},{128,160},{160,192},{192,224},{224,1... | collective-permute-start | bytes 221192 | tf_op jit(solution)/shard_map/ppermute | solution.py:666
  115.9 4.6 %collective-permute-start.15 = (bf16[128,256]{1,0:T(8,128)(2,1)S(1)}, bf16[128,256]{1,0:T(8,128)(2,1)S(1)}, u32[]{:S(2)}, u32[]{:S(2)}) collective-permute-start(bf16[128,256]{1,0:T(8,128)(2,1)S(1)} %get-tuple-element.58), channel_id=1, source_target_pairs={{0,4},{1,5},{2,6},{3,7},{4,0},{5,1},{6,2},{7,3},{8,12},{9,13},{10,... | collective-permute-start | bytes 196616 | tf_op jit(solution)/shard_map/ppermute | solution.py:401
  120.5 7.6 %collective-permute-start.30 = (bf16[128,128]{1,0:T(8,128)(2,1)S(1)}, bf16[128,128]{1,0:T(8,128)(2,1)S(1)}, u32[]{:S(2)}, u32[]{:S(2)}) collective-permute-start(bf16[128,128]{1,0:T(8,128)(2,1)S(1)} %get-tuple-element.72), channel_id=1, source_target_pairs={{0,128},{32,160},{64,192},{96,224},{1,129},{33,161},{65,193},{97,2... | collective-permute-start | bytes 98312 | tf_op jit(solution)/shard_map/ppermute | solution.py:389
  128.1 8.7 %collective-permute-start.16 = (bf16[128,256]{1,0:T(8,128)(2,1)S(1)}, bf16[128,256]{1,0:T(8,128)(2,1)S(1)}, u32[]{:S(2)}, u32[]{:S(2)}) collective-permute-start(bf16[128,256]{1,0:T(8,128)(2,1)S(1)} %get-tuple-element.59), channel_id=1, source_target_pairs={{0,5},{1,4},{2,7},{3,6},{4,1},{5,0},{6,3},{7,2},{8,13},{9,12},{10,... | collective-permute-start | bytes 196616 | tf_op jit(solution)/shard_map/ppermute | solution.py:401
  144.9 4.6 %collective-permute-start.33 = (bf16[128,128]{1,0:T(8,128)(2,1)S(1)}, bf16[128,128]{1,0:T(8,128)(2,1)S(1)}, u32[]{:S(2)}, u32[]{:S(2)}) collective-permute-start(bf16[128,128]{1,0:T(8,128)(2,1)S(1)} %get-tuple-element.77), channel_id=1, source_target_pairs={{0,3},{1,2},{2,5},{3,4},{4,7},{5,6},{6,1},{7,0},{8,11},{9,10},{10,... | collective-permute-start | bytes 98312 | tf_op jit(solution)/shard_map/ppermute | solution.py:401
  149.4 7.0 %collective-permute-start.34 = (bf16[128,128]{1,0:T(8,128)(2,1)S(1)}, bf16[128,128]{1,0:T(8,128)(2,1)S(1)}, u32[]{:S(2)}, u32[]{:S(2)}) collective-permute-start(bf16[128,128]{1,0:T(8,128)(2,1)S(1)} %get-tuple-element.78), channel_id=1, source_target_pairs={{0,6},{1,7},{2,0},{3,1},{4,2},{5,3},{6,4},{7,5},{8,14},{9,15},{10,... | collective-permute-start | bytes 98312 | tf_op jit(solution)/shard_map/ppermute | solution.py:401
  150.0 6.5 %collective-permute-start.35 = (bf16[128,128]{1,0:T(8,128)(2,1)S(1)}, bf16[128,128]{1,0:T(8,128)(2,1)S(1)}, u32[]{:S(2)}, u32[]{:S(2)}) collective-permute-start(bf16[128,128]{1,0:T(8,128)(2,1)S(1)} %get-tuple-element.79), channel_id=1, source_target_pairs={{0,7},{1,6},{2,1},{3,0},{4,3},{5,2},{6,5},{7,4},{8,15},{9,14},{10,... | collective-permute-start | bytes 98312 | tf_op jit(solution)/shard_map/ppermute | solution.py:401
  150.7 5.8 %collective-permute-start.36 = (bf16[128,128]{1,0:T(8,128)(2,1)S(1)}, bf16[128,128]{1,0:T(8,128)(2,1)S(1)}, u32[]{:S(2)}, u32[]{:S(2)}) collective-permute-start(bf16[128,128]{1,0:T(8,128)(2,1)S(1)} %get-tuple-element.80), channel_id=1, source_target_pairs={{0,4},{1,5},{2,6},{3,7},{4,0},{5,1},{6,2},{7,3},{8,12},{9,13},{10,... | collective-permute-start | bytes 98312 | tf_op jit(solution)/shard_map/ppermute | solution.py:401
  154.4 4.8 %collective-permute-start.37 = (bf16[128,128]{1,0:T(8,128)(2,1)S(1)}, bf16[128,128]{1,0:T(8,128)(2,1)S(1)}, u32[]{:S(2)}, u32[]{:S(2)}) collective-permute-start(bf16[128,128]{1,0:T(8,128)(2,1)S(1)} %get-tuple-element.81), channel_id=1, source_target_pairs={{0,5},{1,4},{2,7},{3,6},{4,1},{5,0},{6,3},{7,2},{8,13},{9,12},{10,... | collective-permute-start | bytes 98312 | tf_op jit(solution)/shard_map/ppermute | solution.py:401
  (15 other events, 158.2 us)

commit v8 on v7

--- a/solution.py
+++ b/solution.py
@@ -120,17 +120,9 @@
 def project_kernel(width_all, head_size, block_ref, rate_ref, *refs):
     near, (fa, sfa, fb, sfb), weights = refs[:6], refs[6:10], refs[10]
     q_ref, k_ref, v_ref, bl_ref, tail_ref, dg_ref, gu_ref, cg_ref = refs[11:19]
-    far, factors, sems = refs[19:]
+    far, factors = refs[19:]
     rows, piece_width = near[0].shape
     half = rows // 2
-    moves = fetch(
-        sems,
-        *(
-            (ref, far.at[side, pl.ds(n * half, half), :])
-            for n, pair in enumerate(((fa, sfa), (fb, sfb)))
-            for side, ref in enumerate(pair)
-        ),
-    )
 
     def unit_rows(raw):
         wide = low(raw).astype(F32)
@@ -139,7 +131,7 @@
     def product(n, here, slots):
         total = None
         for slot in slots:
-            piece = near[slot][here, :] if slot < 6 else far[slot - 6, here, :]
+            piece = near[slot][here, :] if slot < 6 else far[slot - 6]
             offset = pl.multiple_of(block_ref[slot] * piece_width, piece_width)
             term = dot(piece, weights[n, pl.ds(offset, piece_width), :])
             total = term if total is None else total + term
@@ -151,13 +143,8 @@
 
     def each_half(body):
         def step(n, carry):
-            for which in range(2):
-
-                @pl.when(n == which)
-                def _():
-                    for one in moves[2 * which : 2 * which + 2]:
-                        one.wait()
-
+            far[0] = jnp.where(n == 0, fa[...], fb[...])
+            far[1] = jnp.where(n == 0, sfa[...], sfb[...])
             body(pl.ds(pl.multiple_of(n * half, half), half))
             return carry
 
@@ -166,7 +153,7 @@
     def gated(here):
         squares = jnp.zeros((half, piece_width), F32)
         for slot in range(8):
-            piece = near[slot][here, :] if slot < 6 else far[slot - 6, here, :]
+            piece = near[slot][here, :] if slot < 6 else far[slot - 6]
             wide = piece.astype(F32)
             squares = squares + wide * wide
         squares = jnp.sum(squares, axis=1, keepdims=True)
@@ -211,9 +198,8 @@
         + [pltpu.VMEM((HALO, 128), BF16)]
         + [pltpu.VMEM((rows, 128), kind) for kind in kinds[4:]],
         scratch_shapes=[
-            pltpu.VMEM((2, rows, piece_width), BF16),
+            pltpu.VMEM((2, rows // 2, piece_width), BF16),
             pltpu.VMEM((rows, 1), F32),
-            pltpu.SemaphoreType.DMA((4,)),
         ],
         compiler_params=params(20),
         cost_estimate=cost(2 * rows * width_all * 1024, 12 << 20),
@@ -432,7 +418,7 @@
 
 
 def conv_kernel(block_ref, gu_ref, before_ref, taps_ref, cg_ref, *rest):
-    outs, (padded, out_ref) = rest[:8], rest[8:]
+    outs, (padded, out_ref) = rest[:4], rest[4:]
     rows, size = gu_ref.shape
     head = before_ref.shape[0]
     count = taps_ref.shape[0]
@@ -454,8 +440,9 @@
     part = rows // 8
     for slot in range(8):
         here = pl.ds(pl.multiple_of(block_ref[GOES_TO[slot]] * part, part), part)
-        outs[slot][:, 0:size] = out_ref[here, :]
-        outs[slot][:, size:] = cg_ref[here, :]
+        there = slice(slot % 2 * part, (slot % 2 + 1) * part)
+        outs[slot // 2][there, 0:size] = out_ref[here, :]
+        outs[slot // 2][there, size:] = cg_ref[here, :]
 
 
 def conv(blocks, gu, before, taps, cg):
@@ -463,8 +450,8 @@
     return pl.pallas_call(
         conv_kernel,
         in_specs=[scalars()] + [whole()] * 4,
-        out_specs=[whole()] * 8,
-        out_shape=[pltpu.VMEM((rows // 8, 2 * size), BF16)] * 8,
+        out_specs=[whole()] * 4,
+        out_shape=[pltpu.VMEM((rows // 4, 2 * size), BF16)] * 4,
         scratch_shapes=[
             pltpu.VMEM((rows + before.shape[0], size), F32),
             pltpu.VMEM((rows, size), BF16),
@@ -513,8 +500,9 @@
 
 
 def conv_out_kernel(*refs):
-    got, weights, out_ref, mixed = refs[:8], refs[8:16], refs[16], refs[17]
+    both, weights, out_ref, mixed = refs[:8], refs[8:16], refs[16], refs[17]
     groups, rows, size = mixed.shape
+    got = [ref.at[slot % 2 * rows : (slot % 2 + 1) * rows, :] for slot, ref in enumerate(both)]
     tops = [0 if ref.shape[0] == size + 16 else size for ref in weights]
     total = jnp.zeros((rows, size), F32)
     total_square = jnp.zeros((rows, size), F32)
@@ -540,7 +528,7 @@
 def conv_out(got, weights):
     groups = len(got)
     rows, both = got[0].shape
-    size, width = both // 2, weights[0].shape[1]
+    rows, size, width = rows // 2, both // 2, weights[0].shape[1]
     return pl.pallas_call(
         conv_out_kernel,
         in_specs=[whole()] * 16,
@@ -678,7 +666,11 @@
 
     halo = lax.ppermute(tail, SP, [(i, i + 1) for i in range(31)])
     filtered = conv(blocks, gu, halo, conv_taps, cg)
-    got = exchanged(filtered)
+    got = []
+    for chip, part in enumerate(filtered):
+        if chip:
+            part = cyclic(part, "y", STEPS[chip])
+        got += [part, swapped(part)]
     conv_part = conv_out(got, conv_weights)
 
     mixed = finish(blocks, coef_p, coef_q, dg, head_gain[None, :], before_z, far, before)

time: 162 us -> 139 us (0.86)
  waiting for transfers between devices: 56.8 us -> 37.8 us
  starting transfers between devices: 73.8 us -> 70 us
    ppermute x14 -> x7, starting transfers between devices: 26.7 us -> 6.53 us  [exchanged(): got.append(lax.ppermute(parts[slot], TP, route))]
    ppermute x14 -> x7, waiting for transfers between devices: 23.8 us -> 9.85 us  [exchanged(): got.append(lax.ppermute(parts[slot], TP, route))]
    ppermute x11 -> x14, waiting for transfers between devices: 25.2 us -> 15 us  [cyclic(): lax.ppermute(block, axis, [(i, (i + distance) % count) for i in range(cou...]
    ppermute x10 -> x14, starting transfers between devices: 11.8 us -> 19.4 us  [swapped(): return lax.ppermute(block, 'c', [(0, 1), (1, 0)])]
    ppermute x11 -> x14, starting transfers between devices: 18.2 us -> 22.1 us  [cyclic(): lax.ppermute(block, axis, [(i, (i + distance) % count) for i in range(cou...]
    ppermute x3, starting transfers between devices: 7.01 us -> 10.2 us  [local(): around.append(lax.ppermute(total, 'z', route(j)))]
    ppermute x10 -> x14, waiting for transfers between devices: 0.03 us -> 2.99 us  [swapped(): return lax.ppermute(block, 'c', [(0, 1), (1, 0)])]
    ppermute x1, starting transfers between devices: 6.56 us -> 8.59 us  [shifted(): lax.ppermute(block, axis, [(i, i + distance) for i in devices if i + dist...]
  transfers between devices with their start and end apart: 40 -> 40, of which waited for: 21 -> 17; matrix products, arithmetic and copies ran while one was open for 3% -> 4% of each run, Pallas kernels for 14% -> 16%
where the time goes in v8:
time: 139 us
  starting transfers between devices  70 us (50%)
  waiting for transfers between devices  37.8 us (27%)
  Pallas kernels  24.3 us (17%)
  local copies, waits for them, and re-layouts  3.06 us (2%)
  other arithmetic  2.45 us (2%)
    ppermute x14, starting transfers between devices, cyclic(): lax.ppermute(block, axis, [(i, (i + distance) % count) for i in range(cou...  22.1 us
    ppermute x14, starting transfers between devices, swapped(): return lax.ppermute(block, 'c', [(0, 1), (1, 0)])  19.4 us
    ppermute x14, waiting for transfers between devices, cyclic(): lax.ppermute(block, axis, [(i, (i + distance) % count) for i in range(cou...  15 us
    ppermute x3, starting transfers between devices, local(): around.append(lax.ppermute(total, 'z', route(j)))  10.2 us
    ppermute x7, waiting for transfers between devices, exchanged(): got.append(lax.ppermute(parts[slot], TP, route))  9.85 us
    ppermute x1, starting transfers between devices, shifted(): lax.ppermute(block, axis, [(i, i + distance) for i in devices if i + dist...  8.59 us
    ppermute x3, waiting for transfers between devices, local(): around.append(lax.ppermute(total, 'z', route(j)))  8.48 us
    pallas_call x1, Pallas kernels, project(): pl.pallas_call(functools.partial(project_kernel, width_all, head_size), i...  7.15 us
  transfers between devices with their start and end apart: 40, of which 17 were waited for; matrix products, arithmetic and copies ran while one was open for 4% of the time, Pallas kernels for 16%

profile of v8, /device:TPU:1, one launch (start us, length us, event | category | flops | bytes accessed | tf_op | source)
XLA Modules:
  0.0 139.0 jit_solution(4567671824838442201)
XLA Ops:
  0.0 2.1 %collective-permute-start.1 = (bf16[1024,256]{1,0:T(8,128)(2,1)}, bf16[1024,256]{1,0:T(8,128)(2,1)S(1)}, u32[]{:S(2)}, u32[]{:S(2)}) collective-permute-start(bf16[1024,256]{1,0:T(8,128)(2,1)} %refs_0_.3), channel_id=1, source_target_pairs={{0,2},{2,4},{4,6},{6,0},{1,3},{3,5},{5,7},{7,1},{8,10},{10,12},{12... | collective-permute-start | bytes 1572872 | tf_op jit(solution)/shard_map/ppermute | solution.py:370
  3.6 2.9 %collective-permute-start = (bf16[1024,256]{1,0:T(8,128)(2,1)}, bf16[1024,256]{1,0:T(8,128)(2,1)S(1)}, u32[]{:S(2)}, u32[]{:S(2)}) collective-permute-start(bf16[1024,256]{1,0:T(8,128)(2,1)} %refs_0_.3), channel_id=1, source_target_pairs={{0,1},{1,0},{2,3},{3,2},{4,5},{5,4},{6,7},{7,6},{8,9},{9,8},{10,11... | collective-permute-start | bytes 1572872 | tf_op jit(solution)/shard_map/ppermute | solution.py:379
  8.7 4.8 %collective-permute-done.1.right_any.refs_2_ = bf16[1024,256]{1,0:T(8,128)(2,1)S(1)} collective-permute-done((bf16[1024,256]{1,0:T(8,128)(2,1)}, bf16[1024,256]{1,0:T(8,128)(2,1)S(1)}, u32[]{:S(2)}, u32[]{:S(2)}) %collective-permute-start.1) | collective-permute-done | bytes 524320 | tf_op jit(solution)/shard_map/ppermute | solution.py:370
  14.8 1.5 %collective-permute-start.5 = (bf16[512,256]{1,0:T(8,128)(2,1)S(1)}, bf16[512,256]{1,0:T(8,128)(2,1)S(1)}, u32[]{:S(2)}, u32[]{:S(2)}) collective-permute-start(bf16[512,256]{1,0:T(8,128)(2,1)S(1)} %get-tuple-element.42), channel_id=1, source_target_pairs={{0,2},{2,4},{4,6},{6,0},{1,3},{3,5},{5,7},{7,1},{8,10},{10,12},{12... | collective-permute-start | bytes 786440 | tf_op jit(solution)/shard_map/ppermute | solution.py:370
  18.7 3.3 %collective-permute-done.5.refs_6_ = bf16[512,256]{1,0:T(8,128)(2,1)S(1)} collective-permute-done((bf16[512,256]{1,0:T(8,128)(2,1)S(1)}, bf16[512,256]{1,0:T(8,128)(2,1)S(1)}, u32[]{:S(2)}, u32[]{:S(2)}) %collective-permute-start.5) | collective-permute-done | bytes 262176 | tf_op jit(solution)/shard_map/ppermute | solution.py:370
  22.0 2.8 %collective-permute-start.6 = (bf16[512,256]{1,0:T(8,128)(2,1)S(1)}, bf16[512,256]{1,0:T(8,128)(2,1)}, u32[]{:S(2)}, u32[]{:S(2)}) collective-permute-start(bf16[512,256]{1,0:T(8,128)(2,1)S(1)} %collective-permute-done.5.refs_6_), channel_id=1, source_target_pairs={{0,1},{1,0},{2,3},{3,2},{4,5},{5,4},{6,7},{7,6},{8,9},{9,8},{10,11... | collective-permute-start | bytes 786440 | tf_op jit(solution)/shard_map/ppermute | solution.py:379
  29.1 2.1 %collective-permute-start.20 = (bf16[272,2048]{1,0:T(8,128)(2,1)S(1)}, bf16[272,2048]{1,0:T(8,128)(2,1)S(1)}, u32[]{:S(2)}, u32[]{:S(2)}) collective-permute-start(bf16[272,2048]{1,0:T(8,128)(2,1)S(1)} %fusion.1.refs_8_), channel_id=1, source_target_pairs={{0,6},{2,0},{4,2},{6,4},{1,7},{3,1},{5,3},{7,5},{8,14},{10,8},{12,... | collective-permute-start | bytes 3342344 | tf_op jit(solution)/shard_map/ppermute | solution.py:370
  32.2 2.2 %pack.1.refs_10_ = bf16[4,2048,256]{2,1,0:T(8,128)(2,1)S(1)} custom-call(bf16[2048,128]{1,0:T(8,128)(2,1)} %refs_0_.2, bf16[2048,128]{1,0:T(8,128)(2,1)} %refs_1_.1, bf16[2048,128]{1,0:T(8,128)(2,1)} %refs_2_.1, bf16[2048,128]{1,0:T(8,128)(2,1)} %refs_3_.1, bf16[2048,128]{1,0:T(8,128)(2,1)} %refs_4_.1, bf16[2048,128]{1,0:T(8,128)(2,1)} %refs_5_.1, ...), custom_call_target="tpu_custom_call" | custom-call | flops 1048576 | bytes 8388608 | tf_op jit(solution)/shard_map/pack/pallas_call | solution.py:108
  34.4 7.1 %project.1 = (bf16[1024,128]{1,0:T(8,128)(2,1)S(1)}, bf16[1024,128]{1,0:T(8,128)(2,1)S(1)}, bf16[1024,128]{1,0:T(8,128)(2,1)S(1)}, f32[1024,128]{1,0:T(8,128)S(1...) custom-call(s32[10]{0:T(128)S(1)} %stack.71.block_ref.place_ref, ...), custom_call_target="tpu_custom_call" | custom-call | flops 4294967296 | bytes 12582912 | tf_op jit(solution)/shard_map/project/pallas_call | solution.py:193
  41.6 5.4 %delta.1 = (bf16[1024,128]{1,0:T(8,128)(2,1)S(1)}, f32[1024,128]{1,0:T(8,128)S(1)}, bf16[144,256]{1,0:T(8,128)(2,1)S(1)}) custom-call(bf16[1024,128]{1,0:T(8,128)(2,1)S(1)} %get-tuple-element.54.q_ref, bf16[1024,128]{1,0:T(8,128)(2,1)S(1)} %get-tuple-element.55.k_ref, bf16[1024,128]{1,0:T(8,128)(2,1)S(1)} %get-tuple-element.56.v_ref, ...), custom_call_target="tpu_custom_call" | custom-call | flops 2013265920 | bytes 3145728 | tf_op jit(solution)/shard_map/delta/pallas_call | solution.py:322
  47.1 3.3 %collective-permute-start.24 = (bf16[144,256]{1,0:T(8,128)(2,1)S(1)}, bf16[144,256]{1,0:T(8,128)(2,1)S(1)}, u32[]{:S(2)}, u32[]{:S(2)}) collective-permute-start(bf16[144,256]{1,0:T(8,128)(2,1)S(1)} %get-tuple-element.61.p0), channel_id=1, source_target_pairs={{0,16},{8,24},{16,0},{24,8},{1,17},{9,25},{17,1},{25,9},{2,18},{10... | collective-permute-start | bytes 221192 | tf_op jit(solution)/shard_map/ppermute | solution.py:370
  51.2 4.3 %collective-permute-done.18.right_any.refs_10_ = bf16[272,2048]{1,0:T(8,128)(2,1)S(1)} collective-permute-done((bf16[272,2048]{1,0:T(8,128)(2,1)S(1)}, bf16[272,2048]{1,0:T(8,128)(2,1)S(1)}, u32[]{:S(2)}, u32[]{:S(2)}) %collective-permute-start.18) | collective-permute-done | bytes 1114144 | tf_op jit(solution)/shard_map/ppermute | solution.py:370
  55.5 1.7 %collective-permute-start.26 = (bf16[144,256]{1,0:T(8,128)(2,1)S(1)}, bf16[144,256]{1,0:T(8,128)(2,1)S(1)}, u32[]{:S(2)}, u32[]{:S(2)}) collective-permute-start(bf16[144,256]{1,0:T(8,128)(2,1)S(1)} %get-tuple-element.61.p0), channel_id=1, source_target_pairs={{0,8},{8,16},{16,24},{24,0},{1,9},{9,17},{17,25},{25,1},{2,10},{10... | collective-permute-start | bytes 221192 | tf_op jit(solution)/shard_map/ppermute | solution.py:370
  57.1 3.2 %collective-permute-start.9 = (bf16[32,128]{1,0:T(8,128)(2,1)S(1)}, bf16[32,128]{1,0:T(8,128)(2,1)S(1)}, u32[]{:S(2)}, u32[]{:S(2)}) collective-permute-start(bf16[32,128]{1,0:T(8,128)(2,1)S(1)} %get-tuple-element.46), channel_id=1, source_target_pairs={{0,8},{8,16},{16,24},{24,32},{32,40},{40,48},{48,56},{56,64},{64,7... | collective-permute-start | bytes 24584 | tf_op jit(solution)/shard_map/ppermute | solution.py:667
  62.4 2.0 %conv.1 = (bf16[256,256]{1,0:T(8,128)(2,1)S(1)}, bf16[256,256]{1,0:T(8,128)(2,1)S(1)}, bf16[256,256]{1,0:T(8,128)(2,1)S(1)}, bf16[256,256]{1,0:T(8,128)(2,1)S(1)}) custom-call(s32[10]{0:T(128)S(1)} %stack.71.block_ref.place_ref, bf16[1024,128]{1,0:T(8,128)(2,1)S(1)} %get-tuple-element.45.gu_ref, bf16[32,128]{1,0:T(8,128)(2,1)S(1)} %collective-permute-done.9.before_ref, ...), custom_call_target="tpu_custom_call" | custom-call | flops 268435456 | bytes 1048576 | tf_op jit(solution)/shard_map/conv/pallas_call | solution.py:450
  64.8 2.4 %collective-permute-start.13 = (bf16[256,256]{1,0:T(8,128)(2,1)S(1)}, bf16[256,256]{1,0:T(8,128)(2,1)S(1)}, u32[]{:S(2)}, u32[]{:S(2)}) collective-permute-start(bf16[256,256]{1,0:T(8,128)(2,1)S(1)} %get-tuple-element.50), channel_id=1, source_target_pairs={{0,6},{2,0},{4,2},{6,4},{1,7},{3,1},{5,3},{7,5},{8,14},{10,8},{12,... | collective-permute-start | bytes 393224 | tf_op jit(solution)/shard_map/ppermute | solution.py:370
  67.2 3.2 %collective-permute-start.19 = (bf16[272,2048]{1,0:T(8,128)(2,1)S(1)}, bf16[272,2048]{1,0:T(8,128)(2,1)S(1)}, u32[]{:S(2)}, u32[]{:S(2)}) collective-permute-start(bf16[272,2048]{1,0:T(8,128)(2,1)S(1)} %collective-permute-done.18.right_any.refs_10_), channel_id=1, source_target_pairs={{0,1},{1,0},{2,3},{3,2},{4,5},{5,4},{6,7},{7,6},{8,9},{9,8},{10,11... | collective-permute-start | bytes 3342344 | tf_op jit(solution)/shard_map/ppermute | solution.py:379
  71.5 6.2 %collective-permute-start.27 = (bf16[144,256]{1,0:T(8,128)(2,1)S(1)}, bf16[144,256]{1,0:T(8,128)(2,1)S(1)}, u32[]{:S(2)}, u32[]{:S(2)}) collective-permute-start(bf16[144,256]{1,0:T(8,128)(2,1)S(1)} %get-tuple-element.62.p0), channel_id=1, source_target_pairs={{0,64},{32,96},{64,0},{96,32},{128,192},{160,224},{192,128},{224,1... | collective-permute-start | bytes 221192 | tf_op jit(solution)/shard_map/ppermute | solution.py:654
  77.7 1.7 %collective-permute-done.27.p1 = bf16[144,256]{1,0:T(8,128)(2,1)S(1)} collective-permute-done((bf16[144,256]{1,0:T(8,128)(2,1)S(1)}, bf16[144,256]{1,0:T(8,128)(2,1)S(1)}, u32[]{:S(2)}, u32[]{:S(2)}) %collective-permute-start.27) | collective-permute-done | bytes 73760 | tf_op jit(solution)/shard_map/ppermute | solution.py:654
  79.5 4.0 %collective-permute-start.28 = (bf16[144,256]{1,0:T(8,128)(2,1)S(1)}, bf16[144,256]{1,0:T(8,128)(2,1)S(1)}, u32[]{:S(2)}, u32[]{:S(2)}) collective-permute-start(bf16[144,256]{1,0:T(8,128)(2,1)S(1)} %get-tuple-element.62.p0), channel_id=1, source_target_pairs={{0,96},{32,0},{64,32},{96,64},{128,224},{160,128},{192,160},{224,1... | collective-permute-start | bytes 221192 | tf_op jit(solution)/shard_map/ppermute | solution.py:654
  84.9 5.3 %collective-permute-done.29.p3 = bf16[144,256]{1,0:T(8,128)(2,1)S(1)} collective-permute-done((bf16[144,256]{1,0:T(8,128)(2,1)S(1)}, bf16[144,256]{1,0:T(8,128)(2,1)S(1)}, u32[]{:S(2)}, u32[]{:S(2)}) %collective-permute-start.29) | collective-permute-done | bytes 73760 | tf_op jit(solution)/shard_map/ppermute | solution.py:654
  90.3 3.2 %collective-permute-start.15 = (bf16[256,256]{1,0:T(8,128)(2,1)S(1)}, bf16[256,256]{1,0:T(8,128)(2,1)S(1)}, u32[]{:S(2)}, u32[]{:S(2)}) collective-permute-start(bf16[256,256]{1,0:T(8,128)(2,1)S(1)} %get-tuple-element.51), channel_id=1, source_target_pairs={{0,4},{2,6},{4,0},{6,2},{1,5},{3,7},{5,1},{7,3},{8,12},{10,14},{12... | collective-permute-start | bytes 393224 | tf_op jit(solution)/shard_map/ppermute | solution.py:370
  95.8 8.6 %collective-permute-start.30 = (bf16[128,128]{1,0:T(8,128)(2,1)S(1)}, bf16[128,128]{1,0:T(8,128)(2,1)S(1)}, u32[]{:S(2)}, u32[]{:S(2)}) collective-permute-start(bf16[128,128]{1,0:T(8,128)(2,1)S(1)} %get-tuple-element.64), channel_id=1, source_target_pairs={{0,128},{32,160},{64,192},{96,224},{1,129},{33,161},{65,193},{97,2... | collective-permute-start | bytes 98312 | tf_op jit(solution)/shard_map/ppermute | solution.py:375
  105.5 6.4 %collective-permute-start.10 = (bf16[256,256]{1,0:T(8,128)(2,1)S(1)}, bf16[256,256]{1,0:T(8,128)(2,1)S(1)}, u32[]{:S(2)}, u32[]{:S(2)}) collective-permute-start(bf16[256,256]{1,0:T(8,128)(2,1)S(1)} %get-tuple-element.48.refs_0_), channel_id=1, source_target_pairs={{0,1},{1,0},{2,3},{3,2},{4,5},{5,4},{6,7},{7,6},{8,9},{9,8},{10,11... | collective-permute-start | bytes 393224 | tf_op jit(solution)/shard_map/ppermute | solution.py:379
  114.8 3.7 %collective-permute-done.32.refs_2_ = bf16[128,128]{1,0:T(8,128)(2,1)S(1)} collective-permute-done((bf16[128,128]{1,0:T(8,128)(2,1)S(1)}, bf16[128,128]{1,0:T(8,128)(2,1)S(1)}, u32[]{:S(2)}, u32[]{:S(2)}) %collective-permute-start.32) | collective-permute-done | bytes 32800 | tf_op jit(solution)/shard_map/ppermute | solution.py:387
  119.5 3.5 %collective-permute-done.33.refs_3_ = bf16[128,128]{1,0:T(8,128)(2,1)S(1)} collective-permute-done((bf16[128,128]{1,0:T(8,128)(2,1)S(1)}, bf16[128,128]{1,0:T(8,128)(2,1)S(1)}, u32[]{:S(2)}, u32[]{:S(2)}) %collective-permute-start.33) | collective-permute-done | bytes 32800 | tf_op jit(solution)/shard_map/ppermute | solution.py:387
  123.0 1.5 %collective-permute-start.12 = (bf16[256,256]{1,0:T(8,128)(2,1)S(1)}, bf16[256,256]{1,0:T(8,128)(2,1)S(1)}, u32[]{:S(2)}, u32[]{:S(2)}) collective-permute-start(bf16[256,256]{1,0:T(8,128)(2,1)S(1)} %collective-permute-done.11.refs_2_), channel_id=1, source_target_pairs={{0,1},{1,0},{2,3},{3,2},{4,5},{5,4},{6,7},{7,6},{8,9},{9,8},{10,11... | collective-permute-start | bytes 393224 | tf_op jit(solution)/shard_map/ppermute | solution.py:379
  128.4 1.4 %collective-permute-start.35 = (bf16[128,128]{1,0:T(8,128)(2,1)S(1)}, bf16[128,128]{1,0:T(8,128)(2,1)S(1)}, u32[]{:S(2)}, u32[]{:S(2)}) collective-permute-start(bf16[128,128]{1,0:T(8,128)(2,1)S(1)} %get-tuple-element.71), channel_id=1, source_target_pairs={{0,7},{1,6},{2,1},{3,0},{4,3},{5,2},{6,5},{7,4},{8,15},{9,14},{10,... | collective-permute-start | bytes 98312 | tf_op jit(solution)/shard_map/ppermute | solution.py:387
  129.9 2.1 %collective-permute-start.36 = (bf16[128,128]{1,0:T(8,128)(2,1)S(1)}, bf16[128,128]{1,0:T(8,128)(2,1)S(1)}, u32[]{:S(2)}, u32[]{:S(2)}) collective-permute-start(bf16[128,128]{1,0:T(8,128)(2,1)S(1)} %get-tuple-element.72), channel_id=1, source_target_pairs={{0,4},{1,5},{2,6},{3,7},{4,0},{5,1},{6,2},{7,3},{8,12},{9,13},{10,... | collective-permute-start | bytes 98312 | tf_op jit(solution)/shard_map/ppermute | solution.py:387
  132.9 2.1 %conv_out.1.conv_ref = f32[128,2048]{1,0:T(8,128)S(1)} custom-call(bf16[256,256]{1,0:T(8,128)(2,1)S(1)} %get-tuple-element.48.refs_0_, bf16[256,256]{1,0:T(8,128)(2,1)S(1)} %collective-permute-done.10.refs_1_, bf16[256,256]{1,0:T(8,128)(2,1)S(1)} %collective-permute-done.11.refs_2_, bf16[256,256]{1,0:T(8,128)(2,1)S(1)} %collective-permute-done.12.refs_3_, ...), custom_call_target="tpu_custom_call" | custom-call | flops 536870912 | bytes 6291456 | tf_op jit(solution)/shard_map/conv_out/pallas_call | solution.py:532
  135.0 1.9 %collective-permute-done.37.refs_7_ = bf16[128,128]{1,0:T(8,128)(2,1)S(1)} collective-permute-done((bf16[128,128]{1,0:T(8,128)(2,1)S(1)}, bf16[128,128]{1,0:T(8,128)(2,1)S(1)}, u32[]{:S(2)}, u32[]{:S(2)}) %collective-permute-start.37) | collective-permute-done | bytes 32800 | tf_op jit(solution)/shard_map/ppermute | solution.py:387
  136.9 1.9 %delta_out.1 = bf16[128,2048]{1,0:T(8,128)(2,1)} custom-call(f32[128,2048]{1,0:T(8,128)S(1)} %conv_out.1.conv_ref, bf16[128,128]{1,0:T(8,128)(2,1)S(1)} %get-tuple-element.66.refs_0_, bf16[128,128]{1,0:T(8,128)(2,1)S(1)} %collective-permute-done.31.refs_1_, bf16[128,128]{1,0:T(8,128)(2,1)S(1)} %collective-permute-done.32.refs_2_, ...), custom_call_target="tpu_custom_call" | custom-call | flops 536870912 | bytes 6291456 | tf_op jit(solution)/shard_map/delta_out/pallas_call | solution.py:561
  (84 shorter events, 29.6 us)
Async XLA Ops:
  0.0 13.5 %collective-permute-start.1 = (bf16[1024,256]{1,0:T(8,128)(2,1)}, bf16[1024,256]{1,0:T(8,128)(2,1)S(1)}, u32[]{:S(2)}, u32[]{:S(2)}) collective-permute-start(bf16[1024,256]{1,0:T(8,128)(2,1)} %refs_0_.3), channel_id=1, source_target_pairs={{0,2},{2,4},{4,6},{6,0},{1,3},{3,5},{5,7},{7,1},{8,10},{10,12},{12... | collective-permute-start | bytes 1572872 | tf_op jit(solution)/shard_map/ppermute | solution.py:370
  2.1 12.6 %collective-permute-start.3 = (bf16[1024,256]{1,0:T(8,128)(2,1)}, bf16[1024,256]{1,0:T(8,128)(2,1)S(1)}, u32[]{:S(2)}, u32[]{:S(2)}) collective-permute-start(bf16[1024,256]{1,0:T(8,128)(2,1)} %refs_0_.3), channel_id=1, source_target_pairs={{0,6},{2,0},{4,2},{6,4},{1,7},{3,1},{5,3},{7,5},{8,14},{10,8},{12,... | collective-permute-start | bytes 1572872 | tf_op jit(solution)/shard_map/ppermute | solution.py:370
  3.6 24.9 %collective-permute-start = (bf16[1024,256]{1,0:T(8,128)(2,1)}, bf16[1024,256]{1,0:T(8,128)(2,1)S(1)}, u32[]{:S(2)}, u32[]{:S(2)}) collective-permute-start(bf16[1024,256]{1,0:T(8,128)(2,1)} %refs_0_.3), channel_id=1, source_target_pairs={{0,1},{1,0},{2,3},{3,2},{4,5},{5,4},{6,7},{7,6},{8,9},{9,8},{10,11... | collective-permute-start | bytes 1572872 | tf_op jit(solution)/shard_map/ppermute | solution.py:379
  14.8 7.2 %collective-permute-start.5 = (bf16[512,256]{1,0:T(8,128)(2,1)S(1)}, bf16[512,256]{1,0:T(8,128)(2,1)S(1)}, u32[]{:S(2)}, u32[]{:S(2)}) collective-permute-start(bf16[512,256]{1,0:T(8,128)(2,1)S(1)} %get-tuple-element.42), channel_id=1, source_target_pairs={{0,2},{2,4},{4,6},{6,0},{1,3},{3,5},{5,7},{7,1},{8,10},{10,12},{12... | collective-permute-start | bytes 786440 | tf_op jit(solution)/shard_map/ppermute | solution.py:370
  16.3 9.2 %collective-permute-start.7 = (bf16[512,256]{1,0:T(8,128)(2,1)S(1)}, bf16[512,256]{1,0:T(8,128)(2,1)}, u32[]{:S(2)}, u32[]{:S(2)}) collective-permute-start(bf16[512,256]{1,0:T(8,128)(2,1)S(1)} %get-tuple-element.43), channel_id=1, source_target_pairs={{0,6},{2,0},{4,2},{6,4},{1,7},{3,1},{5,3},{7,5},{8,14},{10,8},{12,... | collective-permute-start | bytes 786440 | tf_op jit(solution)/shard_map/ppermute | solution.py:370
  22.0 7.1 %collective-permute-start.6 = (bf16[512,256]{1,0:T(8,128)(2,1)S(1)}, bf16[512,256]{1,0:T(8,128)(2,1)}, u32[]{:S(2)}, u32[]{:S(2)}) collective-permute-start(bf16[512,256]{1,0:T(8,128)(2,1)S(1)} %collective-permute-done.5.refs_6_), channel_id=1, source_target_pairs={{0,1},{1,0},{2,3},{3,2},{4,5},{5,4},{6,7},{7,6},{8,9},{9,8},{10,11... | collective-permute-start | bytes 786440 | tf_op jit(solution)/shard_map/ppermute | solution.py:379
  24.8 9.6 %collective-permute-start.2 = (bf16[1024,256]{1,0:T(8,128)(2,1)S(1)}, bf16[1024,256]{1,0:T(8,128)(2,1)S(1)}, u32[]{:S(2)}, u32[]{:S(2)}) collective-permute-start(bf16[1024,256]{1,0:T(8,128)(2,1)S(1)} %collective-permute-done.1.right_any.refs_2_), channel_id=1, source_target_pairs={{0,1},{1,0},{2,3},{3,2},{4,5},{5,4},{6,7},{7,6},{8,9},{9,8},{10,11... | collective-permute-start | bytes 1572872 | tf_op jit(solution)/shard_map/ppermute | solution.py:379
  24.9 9.5 %collective-permute-start.4 = (bf16[1024,256]{1,0:T(8,128)(2,1)S(1)}, bf16[1024,256]{1,0:T(8,128)(2,1)}, u32[]{:S(2)}, u32[]{:S(2)}) collective-permute-start(bf16[1024,256]{1,0:T(8,128)(2,1)S(1)} %collective-permute-done.3.left_any.refs_4_), channel_id=1, source_target_pairs={{0,1},{1,0},{2,3},{3,2},{4,5},{5,4},{6,7},{7,6},{8,9},{9,8},{10,11... | collective-permute-start | bytes 1572872 | tf_op jit(solution)/shard_map/ppermute | solution.py:379
  25.5 5.8 %collective-permute-start.8 = (bf16[512,256]{1,0:T(8,128)(2,1)}, bf16[512,256]{1,0:T(8,128)(2,1)}, u32[]{:S(2)}, u32[]{:S(2)}) collective-permute-start(bf16[512,256]{1,0:T(8,128)(2,1)} %collective-permute-done.7.refs_8_), channel_id=1, source_target_pairs={{0,1},{1,0},{2,3},{3,2},{4,5},{5,4},{6,7},{7,6},{8,9},{9,8},{10,11... | collective-permute-start | bytes 786440 | tf_op jit(solution)/shard_map/ppermute | solution.py:379
  28.5 27.0 %collective-permute-start.18 = (bf16[272,2048]{1,0:T(8,128)(2,1)S(1)}, bf16[272,2048]{1,0:T(8,128)(2,1)S(1)}, u32[]{:S(2)}, u32[]{:S(2)}) collective-permute-start(bf16[272,2048]{1,0:T(8,128)(2,1)S(1)} %fusion.1.refs_8_), channel_id=1, source_target_pairs={{0,2},{2,4},{4,6},{6,0},{1,3},{3,5},{5,7},{7,1},{8,10},{10,12},{12... | collective-permute-start | bytes 3342344 | tf_op jit(solution)/shard_map/ppermute | solution.py:370
  29.1 28.0 %collective-permute-start.20 = (bf16[272,2048]{1,0:T(8,128)(2,1)S(1)}, bf16[272,2048]{1,0:T(8,128)(2,1)S(1)}, u32[]{:S(2)}, u32[]{:S(2)}) collective-permute-start(bf16[272,2048]{1,0:T(8,128)(2,1)S(1)} %fusion.1.refs_8_), channel_id=1, source_target_pairs={{0,6},{2,0},{4,2},{6,4},{1,7},{3,1},{5,3},{7,5},{8,14},{10,8},{12,... | collective-permute-start | bytes 3342344 | tf_op jit(solution)/shard_map/ppermute | solution.py:370
  31.2 33.2 %collective-permute-start.17 = (bf16[272,2048]{1,0:T(8,128)(2,1)S(1)}, bf16[272,2048]{1,0:T(8,128)(2,1)S(1)}, u32[]{:S(2)}, u32[]{:S(2)}) collective-permute-start(bf16[272,2048]{1,0:T(8,128)(2,1)S(1)} %fusion.1.refs_8_), channel_id=1, source_target_pairs={{0,1},{1,0},{2,3},{3,2},{4,5},{5,4},{6,7},{7,6},{8,9},{9,8},{10,11... | collective-permute-start | bytes 3342344 | tf_op jit(solution)/shard_map/ppermute | solution.py:379
  47.1 17.7 %collective-permute-start.24 = (bf16[144,256]{1,0:T(8,128)(2,1)S(1)}, bf16[144,256]{1,0:T(8,128)(2,1)S(1)}, u32[]{:S(2)}, u32[]{:S(2)}) collective-permute-start(bf16[144,256]{1,0:T(8,128)(2,1)S(1)} %get-tuple-element.61.p0), channel_id=1, source_target_pairs={{0,16},{8,24},{16,0},{24,8},{1,17},{9,25},{17,1},{25,9},{2,18},{10... | collective-permute-start | bytes 221192 | tf_op jit(solution)/shard_map/ppermute | solution.py:370
  50.3 16.8 %collective-permute-start.25 = (bf16[144,256]{1,0:T(8,128)(2,1)S(1)}, bf16[144,256]{1,0:T(8,128)(2,1)S(1)}, u32[]{:S(2)}, u32[]{:S(2)}) collective-permute-start(bf16[144,256]{1,0:T(8,128)(2,1)S(1)} %get-tuple-element.61.p0), channel_id=1, source_target_pairs={{0,24},{8,0},{16,8},{24,16},{1,25},{9,1},{17,9},{25,17},{2,26},{10... | collective-permute-start | bytes 221192 | tf_op jit(solution)/shard_map/ppermute | solution.py:370
  55.5 14.9 %collective-permute-start.26 = (bf16[144,256]{1,0:T(8,128)(2,1)S(1)}, bf16[144,256]{1,0:T(8,128)(2,1)S(1)}, u32[]{:S(2)}, u32[]{:S(2)}) collective-permute-start(bf16[144,256]{1,0:T(8,128)(2,1)S(1)} %get-tuple-element.61.p0), channel_id=1, source_target_pairs={{0,8},{8,16},{16,24},{24,0},{1,9},{9,17},{17,25},{25,1},{2,10},{10... | collective-permute-start | bytes 221192 | tf_op jit(solution)/shard_map/ppermute | solution.py:370
  61.2 50.7 %collective-permute-start.22 = (bf16[144,2048]{1,0:T(8,128)(2,1)S(1)}, bf16[144,2048]{1,0:T(8,128)(2,1)S(1)}, u32[]{:S(2)}, u32[]{:S(2)}) collective-permute-start(bf16[144,2048]{1,0:T(8,128)(2,1)S(1)} %get-tuple-element.53), channel_id=1, source_target_pairs={{0,6},{2,0},{4,2},{6,4},{1,7},{3,1},{5,3},{7,5},{8,14},{10,8},{12,... | collective-permute-start | bytes 1769480 | tf_op jit(solution)/shard_map/ppermute | solution.py:370
  64.4 7.1 %collective-permute-start.11 = (bf16[256,256]{1,0:T(8,128)(2,1)S(1)}, bf16[256,256]{1,0:T(8,128)(2,1)S(1)}, u32[]{:S(2)}, u32[]{:S(2)}) collective-permute-start(bf16[256,256]{1,0:T(8,128)(2,1)S(1)} %get-tuple-element.49), channel_id=1, source_target_pairs={{0,2},{2,4},{4,6},{6,0},{1,3},{3,5},{5,7},{7,1},{8,10},{10,12},{12... | collective-permute-start | bytes 393224 | tf_op jit(solution)/shard_map/ppermute | solution.py:370
  64.8 13.0 %collective-permute-start.13 = (bf16[256,256]{1,0:T(8,128)(2,1)S(1)}, bf16[256,256]{1,0:T(8,128)(2,1)S(1)}, u32[]{:S(2)}, u32[]{:S(2)}) collective-permute-start(bf16[256,256]{1,0:T(8,128)(2,1)S(1)} %get-tuple-element.50), channel_id=1, source_target_pairs={{0,6},{2,0},{4,2},{6,4},{1,7},{3,1},{5,3},{7,5},{8,14},{10,8},{12,... | collective-permute-start | bytes 393224 | tf_op jit(solution)/shard_map/ppermute | solution.py:370
  67.2 61.2 %collective-permute-start.19 = (bf16[272,2048]{1,0:T(8,128)(2,1)S(1)}, bf16[272,2048]{1,0:T(8,128)(2,1)S(1)}, u32[]{:S(2)}, u32[]{:S(2)}) collective-permute-start(bf16[272,2048]{1,0:T(8,128)(2,1)S(1)} %collective-permute-done.18.right_any.refs_10_), channel_id=1, source_target_pairs={{0,1},{1,0},{2,3},{3,2},{4,5},{5,4},{6,7},{7,6},{8,9},{9,8},{10,11... | collective-permute-start | bytes 3342344 | tf_op jit(solution)/shard_map/ppermute | solution.py:379
  70.4 59.5 %collective-permute-start.21 = (bf16[272,2048]{1,0:T(8,128)(2,1)S(1)}, bf16[272,2048]{1,0:T(8,128)(2,1)S(1)}, u32[]{:S(2)}, u32[]{:S(2)}) collective-permute-start(bf16[272,2048]{1,0:T(8,128)(2,1)S(1)} %collective-permute-done.20.left_any.refs_12_), channel_id=1, source_target_pairs={{0,1},{1,0},{2,3},{3,2},{4,5},{5,4},{6,7},{7,6},{8,9},{9,8},{10,11... | collective-permute-start | bytes 3342344 | tf_op jit(solution)/shard_map/ppermute | solution.py:379
  71.5 7.9 %collective-permute-start.27 = (bf16[144,256]{1,0:T(8,128)(2,1)S(1)}, bf16[144,256]{1,0:T(8,128)(2,1)S(1)}, u32[]{:S(2)}, u32[]{:S(2)}) collective-permute-start(bf16[144,256]{1,0:T(8,128)(2,1)S(1)} %get-tuple-element.62.p0), channel_id=1, source_target_pairs={{0,64},{32,96},{64,0},{96,32},{128,192},{160,224},{192,128},{224,1... | collective-permute-start | bytes 221192 | tf_op jit(solution)/shard_map/ppermute | solution.py:654
  77.7 35.9 %collective-permute-start.38 = (bf16[128,2048]{1,0:T(8,128)(2,1)S(1)}, bf16[128,2048]{1,0:T(8,128)(2,1)S(1)}, u32[]{:S(2)}, u32[]{:S(2)}) collective-permute-start(bf16[128,2048]{1,0:T(8,128)(2,1)S(1)} %get-tuple-element.74), channel_id=1, source_target_pairs={{0,2},{2,4},{4,6},{6,0},{1,3},{3,5},{5,7},{7,1},{8,10},{10,12},{12... | collective-permute-start | bytes 1572872 | tf_op jit(solution)/shard_map/ppermute | solution.py:370
  79.5 5.5 %collective-permute-start.28 = (bf16[144,256]{1,0:T(8,128)(2,1)S(1)}, bf16[144,256]{1,0:T(8,128)(2,1)S(1)}, u32[]{:S(2)}, u32[]{:S(2)}) collective-permute-start(bf16[144,256]{1,0:T(8,128)(2,1)S(1)} %get-tuple-element.62.p0), channel_id=1, source_target_pairs={{0,96},{32,0},{64,32},{96,64},{128,224},{160,128},{192,160},{224,1... | collective-permute-start | bytes 221192 | tf_op jit(solution)/shard_map/ppermute | solution.py:654
  84.9 5.3 %collective-permute-start.29 = (bf16[144,256]{1,0:T(8,128)(2,1)S(1)}, bf16[144,256]{1,0:T(8,128)(2,1)S(1)}, u32[]{:S(2)}, u32[]{:S(2)}) collective-permute-start(bf16[144,256]{1,0:T(8,128)(2,1)S(1)} %get-tuple-element.62.p0), channel_id=1, source_target_pairs={{0,32},{32,64},{64,96},{96,0},{128,160},{160,192},{192,224},{224,1... | collective-permute-start | bytes 221192 | tf_op jit(solution)/shard_map/ppermute | solution.py:654
  90.3 5.6 %collective-permute-start.15 = (bf16[256,256]{1,0:T(8,128)(2,1)S(1)}, bf16[256,256]{1,0:T(8,128)(2,1)S(1)}, u32[]{:S(2)}, u32[]{:S(2)}) collective-permute-start(bf16[256,256]{1,0:T(8,128)(2,1)S(1)} %get-tuple-element.51), channel_id=1, source_target_pairs={{0,4},{2,6},{4,0},{6,2},{1,5},{3,7},{5,1},{7,3},{8,12},{10,14},{12... | collective-permute-start | bytes 393224 | tf_op jit(solution)/shard_map/ppermute | solution.py:370
  95.8 9.6 %collective-permute-start.30 = (bf16[128,128]{1,0:T(8,128)(2,1)S(1)}, bf16[128,128]{1,0:T(8,128)(2,1)S(1)}, u32[]{:S(2)}, u32[]{:S(2)}) collective-permute-start(bf16[128,128]{1,0:T(8,128)(2,1)S(1)} %get-tuple-element.64), channel_id=1, source_target_pairs={{0,128},{32,160},{64,192},{96,224},{1,129},{33,161},{65,193},{97,2... | collective-permute-start | bytes 98312 | tf_op jit(solution)/shard_map/ppermute | solution.py:375
  105.5 7.6 %collective-permute-start.10 = (bf16[256,256]{1,0:T(8,128)(2,1)S(1)}, bf16[256,256]{1,0:T(8,128)(2,1)S(1)}, u32[]{:S(2)}, u32[]{:S(2)}) collective-permute-start(bf16[256,256]{1,0:T(8,128)(2,1)S(1)} %get-tuple-element.48.refs_0_), channel_id=1, source_target_pairs={{0,1},{1,0},{2,3},{3,2},{4,5},{5,4},{6,7},{7,6},{8,9},{9,8},{10,11... | collective-permute-start | bytes 393224 | tf_op jit(solution)/shard_map/ppermute | solution.py:379
  111.8 20.2 %collective-permute-start.23 = (bf16[144,2048]{1,0:T(8,128)(2,1)S(1)}, bf16[144,2048]{1,0:T(8,128)(2,1)S(1)}, u32[]{:S(2)}, u32[]{:S(2)}) collective-permute-start(bf16[144,2048]{1,0:T(8,128)(2,1)S(1)} %collective-permute-done.22.refs_14_), channel_id=1, source_target_pairs={{0,1},{1,0},{2,3},{3,2},{4,5},{5,4},{6,7},{7,6},{8,9},{9,8},{10,11... | collective-permute-start | bytes 1769480 | tf_op jit(solution)/shard_map/ppermute | solution.py:379
  113.7 23.2 %collective-permute-start.39 = (bf16[128,2048]{1,0:T(8,128)(2,1)S(1)}, bf16[128,2048]{1,0:T(8,128)(2,1)S(1)}, u32[]{:S(2)}, u32[]{:S(2)}) collective-permute-start(bf16[128,2048]{1,0:T(8,128)(2,1)S(1)} %collective-permute-done.38.refs_14_), channel_id=1, source_target_pairs={{0,1},{1,0},{2,3},{3,2},{4,5},{5,4},{6,7},{7,6},{8,9},{9,8},{10,11... | collective-permute-start | bytes 1572872 | tf_op jit(solution)/shard_map/ppermute | solution.py:379
  128.2 6.7 %collective-permute-start.34 = (bf16[128,128]{1,0:T(8,128)(2,1)S(1)}, bf16[128,128]{1,0:T(8,128)(2,1)S(1)}, u32[]{:S(2)}, u32[]{:S(2)}) collective-permute-start(bf16[128,128]{1,0:T(8,128)(2,1)S(1)} %get-tuple-element.70), channel_id=1, source_target_pairs={{0,6},{1,7},{2,0},{3,1},{4,2},{5,3},{6,4},{7,5},{8,14},{9,15},{10,... | collective-permute-start | bytes 98312 | tf_op jit(solution)/shard_map/ppermute | solution.py:387
  128.4 6.5 %collective-permute-start.35 = (bf16[128,128]{1,0:T(8,128)(2,1)S(1)}, bf16[128,128]{1,0:T(8,128)(2,1)S(1)}, u32[]{:S(2)}, u32[]{:S(2)}) collective-permute-start(bf16[128,128]{1,0:T(8,128)(2,1)S(1)} %get-tuple-element.71), channel_id=1, source_target_pairs={{0,7},{1,6},{2,1},{3,0},{4,3},{5,2},{6,5},{7,4},{8,15},{9,14},{10,... | collective-permute-start | bytes 98312 | tf_op jit(solution)/shard_map/ppermute | solution.py:387
  129.9 5.1 %collective-permute-start.36 = (bf16[128,128]{1,0:T(8,128)(2,1)S(1)}, bf16[128,128]{1,0:T(8,128)(2,1)S(1)}, u32[]{:S(2)}, u32[]{:S(2)}) collective-permute-start(bf16[128,128]{1,0:T(8,128)(2,1)S(1)} %get-tuple-element.72), channel_id=1, source_target_pairs={{0,4},{1,5},{2,6},{3,7},{4,0},{5,1},{6,2},{7,3},{8,12},{9,13},{10,... | collective-permute-start | bytes 98312 | tf_op jit(solution)/shard_map/ppermute | solution.py:387
  (15 other events, 129.8 us)

commit v9 on v8

--- a/solution.py
+++ b/solution.py
@@ -380,11 +380,11 @@
 
 
 def exchanged(parts):
-    got = [parts[0]]
-    for slot in range(1, 8):
-        step, side = STEPS[slot // 2], slot % 2
-        route = [(y * 2 + c, (y + step) % 4 * 2 + (c ^ side)) for y in range(4) for c in range(2)]
-        got.append(lax.ppermute(parts[slot], TP, route))
+    got = []
+    for chip, part in enumerate(parts):
+        if chip:
+            part = cyclic(part, "y", STEPS[chip])
+        got += [part, swapped(part)]
     return got
 
 
@@ -395,13 +395,14 @@
     state = total * far_ref[...].astype(F32) - dot(low(lost), far_ref[...]) + made
     total, lost, made = read_state(before_ref)
     state = low(total * state - dot(low(lost), low(state)) + made)
-    step = outs[0].shape[0]
+    step = outs[0].shape[0] // 2
     for slot in range(8):
         here = pl.ds(pl.multiple_of(block_ref[GOES_TO[slot]] * step, step), step)
         result = coef_q_ref[here, :] + dot(coef_p_ref[here, :], state)
         mean = jnp.sum(result * result, axis=-1, keepdims=True) * (1.0 / result.shape[1])
         result = result * lax.rsqrt(mean + TINY_NORM) * gain_ref[...]
-        outs[slot][...] = low(result * jax.nn.silu(dg_ref[here, :].astype(F32)))
+        there = slice(slot % 2 * step, (slot % 2 + 1) * step)
+        outs[slot // 2][there, :] = low(result * jax.nn.silu(dg_ref[here, :].astype(F32)))
 
 
 def finish(blocks, *args):
@@ -409,8 +410,8 @@
     return pl.pallas_call(
         finish_kernel,
         in_specs=[scalars()] + [whole()] * 7,
-        out_specs=[whole()] * 8,
-        out_shape=[pltpu.VMEM((rows // 8, size), BF16)] * 8,
+        out_specs=[whole()] * 4,
+        out_shape=[pltpu.VMEM((rows // 4, size), BF16)] * 4,
         compiler_params=params(6),
         cost_estimate=cost(64 << 20, 2 << 20),
         name="finish",
@@ -543,13 +544,14 @@
 
 def delta_out_kernel(conv_ref, *refs):
     got, weights, out_hbm, staged, sems = refs[:8], refs[8:16], refs[16], refs[17], refs[18]
-    size = got[0].shape[1]
+    rows, size = staged.shape[0], got[0].shape[1]
     stores = []
     for n, base in enumerate(range(0, staged.shape[1], 512)):
         here = slice(base, base + 512)
         acc = conv_ref[:, here]
-        for part, ref in zip(got, weights):
-            acc = acc + dot(part[...], ref[0:size, here])
+        for slot, (part, ref) in enumerate(zip(got, weights)):
+            top = slot % 2 * rows
+            acc = acc + dot(part[top : top + rows, :], ref[0:size, here])
         staged[:, here] = low(acc)
         stores += fetch(sems.at[pl.ds(n, 1)], (staged.at[:, here], out_hbm.at[:, here]))
     for one in stores:
@@ -666,11 +668,7 @@
 
     halo = lax.ppermute(tail, SP, [(i, i + 1) for i in range(31)])
     filtered = conv(blocks, gu, halo, conv_taps, cg)
-    got = []
-    for chip, part in enumerate(filtered):
-        if chip:
-            part = cyclic(part, "y", STEPS[chip])
-        got += [part, swapped(part)]
+    got = exchanged(filtered)
     conv_part = conv_out(got, conv_weights)
 
     mixed = finish(blocks, coef_p, coef_q, dg, head_gain[None, :], before_z, far, before)

time: 139 us -> 136 us (0.978)
  the two profiles are of different devices: /device:TPU:1 before, /device:TPU:2 now
where the time goes in v9:
time: 136 us; the launch traced here: 133 us
  waiting for transfers between devices  56.7 us (42%)
  starting transfers between devices  45.5 us (33%)
  Pallas kernels  24.3 us (18%)
  local copies, waits for them, and re-layouts  3.06 us (2%)
  other arithmetic  2.45 us (2%)
    ppermute x17, waiting for transfers between devices, cyclic(): lax.ppermute(block, axis, [(i, (i + distance) % count) for i in range(cou...  39 us
    ppermute x17, starting transfers between devices, cyclic(): lax.ppermute(block, axis, [(i, (i + distance) % count) for i in range(cou...  23.1 us
    ppermute x3, starting transfers between devices, local(): around.append(lax.ppermute(total, 'z', route(j)))  11.1 us
    ppermute x3, waiting for transfers between devices, local(): around.append(lax.ppermute(total, 'z', route(j)))  8.58 us
    pallas_call x1, Pallas kernels, project(): pl.pallas_call(functools.partial(project_kernel, width_all, head_size), i...  7.14 us
    ppermute x1, starting transfers between devices, shifted(): lax.ppermute(block, axis, [(i, i + distance) for i in devices if i + dist...  6.39 us
    pallas_call x1, Pallas kernels, delta(): pl.pallas_call(delta_kernel, in_specs=[whole()] * 4, out_specs=[whole()]...  5.44 us
    ppermute x18, waiting for transfers between devices, swapped(): return lax.ppermute(block, 'c', [(0, 1), (1, 0)])  3.92 us
  transfers between devices with their start and end apart: 40, of which 17 were waited for; matrix products, arithmetic and copies ran while one was open for 4% of the time, Pallas kernels for 17%

profile of v9, /device:TPU:2, one launch (start us, length us, event | category | flops | bytes accessed | tf_op | source)
XLA Modules:
  0.0 133.3 jit_solution(15920201322676671763)
XLA Ops:
  0.0 1.6 %collective-permute-start.1 = (bf16[1024,256]{1,0:T(8,128)(2,1)}, bf16[1024,256]{1,0:T(8,128)(2,1)S(1)}, u32[]{:S(2)}, u32[]{:S(2)}) collective-permute-start(bf16[1024,256]{1,0:T(8,128)(2,1)} %refs_0_.3), channel_id=1, source_target_pairs={{0,2},{2,4},{4,6},{6,0},{1,3},{3,5},{5,7},{7,1},{8,10},{10,12},{12... | collective-permute-start | bytes 1572872 | tf_op jit(solution)/shard_map/ppermute | solution.py:370
  1.6 1.7 %collective-permute-start.3 = (bf16[1024,256]{1,0:T(8,128)(2,1)}, bf16[1024,256]{1,0:T(8,128)(2,1)S(1)}, u32[]{:S(2)}, u32[]{:S(2)}) collective-permute-start(bf16[1024,256]{1,0:T(8,128)(2,1)} %refs_0_.3), channel_id=1, source_target_pairs={{0,6},{2,0},{4,2},{6,4},{1,7},{3,1},{5,3},{7,5},{8,14},{10,8},{12,... | collective-permute-start | bytes 1572872 | tf_op jit(solution)/shard_map/ppermute | solution.py:370
  5.5 9.6 %collective-permute-done.1.right_any.refs_2_ = bf16[1024,256]{1,0:T(8,128)(2,1)S(1)} collective-permute-done((bf16[1024,256]{1,0:T(8,128)(2,1)}, bf16[1024,256]{1,0:T(8,128)(2,1)S(1)}, u32[]{:S(2)}, u32[]{:S(2)}) %collective-permute-start.1) | collective-permute-done | bytes 524320 | tf_op jit(solution)/shard_map/ppermute | solution.py:370
  15.2 1.7 %collective-permute-start.5 = (bf16[512,256]{1,0:T(8,128)(2,1)S(1)}, bf16[512,256]{1,0:T(8,128)(2,1)S(1)}, u32[]{:S(2)}, u32[]{:S(2)}) collective-permute-start(bf16[512,256]{1,0:T(8,128)(2,1)S(1)} %get-tuple-element.38), channel_id=1, source_target_pairs={{0,2},{2,4},{4,6},{6,0},{1,3},{3,5},{5,7},{7,1},{8,10},{10,12},{12... | collective-permute-start | bytes 786440 | tf_op jit(solution)/shard_map/ppermute | solution.py:370
  16.9 1.7 %collective-permute-start.7 = (bf16[512,256]{1,0:T(8,128)(2,1)S(1)}, bf16[512,256]{1,0:T(8,128)(2,1)}, u32[]{:S(2)}, u32[]{:S(2)}) collective-permute-start(bf16[512,256]{1,0:T(8,128)(2,1)S(1)} %get-tuple-element.39), channel_id=1, source_target_pairs={{0,6},{2,0},{4,2},{6,4},{1,7},{3,1},{5,3},{7,5},{8,14},{10,8},{12,... | collective-permute-start | bytes 786440 | tf_op jit(solution)/shard_map/ppermute | solution.py:370
  19.7 4.1 %collective-permute-done.5.refs_6_ = bf16[512,256]{1,0:T(8,128)(2,1)S(1)} collective-permute-done((bf16[512,256]{1,0:T(8,128)(2,1)S(1)}, bf16[512,256]{1,0:T(8,128)(2,1)S(1)}, u32[]{:S(2)}, u32[]{:S(2)}) %collective-permute-start.5) | collective-permute-done | bytes 262176 | tf_op jit(solution)/shard_map/ppermute | solution.py:370
  28.0 3.2 %collective-permute-start.20 = (bf16[272,2048]{1,0:T(8,128)(2,1)S(1)}, bf16[272,2048]{1,0:T(8,128)(2,1)S(1)}, u32[]{:S(2)}, u32[]{:S(2)}) collective-permute-start(bf16[272,2048]{1,0:T(8,128)(2,1)S(1)} %fusion.1.refs_8_), channel_id=1, source_target_pairs={{0,6},{2,0},{4,2},{6,4},{1,7},{3,1},{5,3},{7,5},{8,14},{10,8},{12,... | collective-permute-start | bytes 3342344 | tf_op jit(solution)/shard_map/ppermute | solution.py:370
  31.2 2.2 %pack.1.refs_10_ = bf16[4,2048,256]{2,1,0:T(8,128)(2,1)S(1)} custom-call(bf16[2048,128]{1,0:T(8,128)(2,1)} %refs_0_.2, bf16[2048,128]{1,0:T(8,128)(2,1)} %refs_1_.1, bf16[2048,128]{1,0:T(8,128)(2,1)} %refs_2_.1, bf16[2048,128]{1,0:T(8,128)(2,1)} %refs_3_.1, bf16[2048,128]{1,0:T(8,128)(2,1)} %refs_4_.1, bf16[2048,128]{1,0:T(8,128)(2,1)} %refs_5_.1, ...), custom_call_target="tpu_custom_call" | custom-call | flops 1048576 | bytes 8388608 | tf_op jit(solution)/shard_map/pack/pallas_call | solution.py:108
  33.4 7.1 %project.1 = (bf16[1024,128]{1,0:T(8,128)(2,1)S(1)}, bf16[1024,128]{1,0:T(8,128)(2,1)S(1)}, bf16[1024,128]{1,0:T(8,128)(2,1)S(1)}, f32[1024,128]{1,0:T(8,128)S(1...) custom-call(s32[10]{0:T(128)S(1)} %stack.71.block_ref.place_ref, ...), custom_call_target="tpu_custom_call" | custom-call | flops 4294967296 | bytes 12582912 | tf_op jit(solution)/shard_map/project/pallas_call | solution.py:193
  40.6 5.4 %delta.1 = (bf16[1024,128]{1,0:T(8,128)(2,1)S(1)}, f32[1024,128]{1,0:T(8,128)S(1)}, bf16[144,256]{1,0:T(8,128)(2,1)S(1)}) custom-call(bf16[1024,128]{1,0:T(8,128)(2,1)S(1)} %get-tuple-element.50.q_ref, bf16[1024,128]{1,0:T(8,128)(2,1)S(1)} %get-tuple-element.51.k_ref, bf16[1024,128]{1,0:T(8,128)(2,1)S(1)} %get-tuple-element.52.v_ref, ...), custom_call_target="tpu_custom_call" | custom-call | flops 2013265920 | bytes 3145728 | tf_op jit(solution)/shard_map/delta/pallas_call | solution.py:322
  46.0 2.2 %collective-permute-start.24 = (bf16[144,256]{1,0:T(8,128)(2,1)S(1)}, bf16[144,256]{1,0:T(8,128)(2,1)S(1)}, u32[]{:S(2)}, u32[]{:S(2)}) collective-permute-start(bf16[144,256]{1,0:T(8,128)(2,1)S(1)} %get-tuple-element.57.p0), channel_id=1, source_target_pairs={{0,16},{8,24},{16,0},{24,8},{1,17},{9,25},{17,1},{25,9},{2,18},{10... | collective-permute-start | bytes 221192 | tf_op jit(solution)/shard_map/ppermute | solution.py:370
  48.2 1.9 %collective-permute-start.9 = (bf16[32,128]{1,0:T(8,128)(2,1)S(1)}, bf16[32,128]{1,0:T(8,128)(2,1)S(1)}, u32[]{:S(2)}, u32[]{:S(2)}) collective-permute-start(bf16[32,128]{1,0:T(8,128)(2,1)S(1)} %get-tuple-element.42), channel_id=1, source_target_pairs={{0,8},{8,16},{16,24},{24,32},{32,40},{40,48},{48,56},{56,64},{64,7... | collective-permute-start | bytes 24584 | tf_op jit(solution)/shard_map/ppermute | solution.py:669
  50.2 3.6 %collective-permute-done.9.before_ref = bf16[32,128]{1,0:T(8,128)(2,1)S(1)} collective-permute-done((bf16[32,128]{1,0:T(8,128)(2,1)S(1)}, bf16[32,128]{1,0:T(8,128)(2,1)S(1)}, u32[]{:S(2)}, u32[]{:S(2)}) %collective-permute-start.9) | collective-permute-done | bytes 8224 | tf_op jit(solution)/shard_map/ppermute | solution.py:669
  53.8 2.0 %conv.1 = (bf16[256,256]{1,0:T(8,128)(2,1)S(1)}, bf16[256,256]{1,0:T(8,128)(2,1)S(1)}, bf16[256,256]{1,0:T(8,128)(2,1)S(1)}, bf16[256,256]{1,0:T(8,128)(2,1)S(1)}) custom-call(s32[10]{0:T(128)S(1)} %stack.71.block_ref.place_ref, bf16[1024,128]{1,0:T(8,128)(2,1)S(1)} %get-tuple-element.41.gu_ref, bf16[32,128]{1,0:T(8,128)(2,1)S(1)} %collective-permute-done.9.before_ref, ...), custom_call_target="tpu_custom_call" | custom-call | flops 268435456 | bytes 1048576 | tf_op jit(solution)/shard_map/conv/pallas_call | solution.py:451
  55.8 2.1 %collective-permute-start.26 = (bf16[144,256]{1,0:T(8,128)(2,1)S(1)}, bf16[144,256]{1,0:T(8,128)(2,1)S(1)}, u32[]{:S(2)}, u32[]{:S(2)}) collective-permute-start(bf16[144,256]{1,0:T(8,128)(2,1)S(1)} %get-tuple-element.57.p0), channel_id=1, source_target_pairs={{0,8},{8,16},{16,24},{24,0},{1,9},{9,17},{17,25},{25,1},{2,10},{10... | collective-permute-start | bytes 221192 | tf_op jit(solution)/shard_map/ppermute | solution.py:370
  58.1 3.3 %collective-permute-start.22 = (bf16[144,2048]{1,0:T(8,128)(2,1)S(1)}, bf16[144,2048]{1,0:T(8,128)(2,1)S(1)}, u32[]{:S(2)}, u32[]{:S(2)}) collective-permute-start(bf16[144,2048]{1,0:T(8,128)(2,1)S(1)} %get-tuple-element.49), channel_id=1, source_target_pairs={{0,6},{2,0},{4,2},{6,4},{1,7},{3,1},{5,3},{7,5},{8,14},{10,8},{12,... | collective-permute-start | bytes 1769480 | tf_op jit(solution)/shard_map/ppermute | solution.py:370
  64.1 4.9 %collective-permute-start.27 = (bf16[144,256]{1,0:T(8,128)(2,1)S(1)}, bf16[144,256]{1,0:T(8,128)(2,1)S(1)}, u32[]{:S(2)}, u32[]{:S(2)}) collective-permute-start(bf16[144,256]{1,0:T(8,128)(2,1)S(1)} %get-tuple-element.58.p0), channel_id=1, source_target_pairs={{0,64},{32,96},{64,0},{96,32},{128,192},{160,224},{192,128},{224,1... | collective-permute-start | bytes 221192 | tf_op jit(solution)/shard_map/ppermute | solution.py:656
  69.0 6.5 %collective-permute-done.13.refs_4_ = bf16[256,256]{1,0:T(8,128)(2,1)S(1)} collective-permute-done((bf16[256,256]{1,0:T(8,128)(2,1)S(1)}, bf16[256,256]{1,0:T(8,128)(2,1)S(1)}, u32[]{:S(2)}, u32[]{:S(2)}) %collective-permute-start.13) | collective-permute-done | bytes 131104 | tf_op jit(solution)/shard_map/ppermute | solution.py:370
  75.5 6.2 %collective-permute-start.28 = (bf16[144,256]{1,0:T(8,128)(2,1)S(1)}, bf16[144,256]{1,0:T(8,128)(2,1)S(1)}, u32[]{:S(2)}, u32[]{:S(2)}) collective-permute-start(bf16[144,256]{1,0:T(8,128)(2,1)S(1)} %get-tuple-element.58.p0), channel_id=1, source_target_pairs={{0,96},{32,0},{64,32},{96,64},{128,224},{160,128},{192,160},{224,1... | collective-permute-start | bytes 221192 | tf_op jit(solution)/shard_map/ppermute | solution.py:656
  81.8 2.0 %collective-permute-done.28.p2 = bf16[144,256]{1,0:T(8,128)(2,1)S(1)} collective-permute-done((bf16[144,256]{1,0:T(8,128)(2,1)S(1)}, bf16[144,256]{1,0:T(8,128)(2,1)S(1)}, u32[]{:S(2)}, u32[]{:S(2)}) %collective-permute-start.28) | collective-permute-done | bytes 73760 | tf_op jit(solution)/shard_map/ppermute | solution.py:656
  83.8 6.6 %collective-permute-done.29.p3 = bf16[144,256]{1,0:T(8,128)(2,1)S(1)} collective-permute-done((bf16[144,256]{1,0:T(8,128)(2,1)S(1)}, bf16[144,256]{1,0:T(8,128)(2,1)S(1)}, u32[]{:S(2)}, u32[]{:S(2)}) %collective-permute-start.29) | collective-permute-done | bytes 73760 | tf_op jit(solution)/shard_map/ppermute | solution.py:656
  90.4 2.7 %collective-permute-start.15 = (bf16[256,256]{1,0:T(8,128)(2,1)S(1)}, bf16[256,256]{1,0:T(8,128)(2,1)S(1)}, u32[]{:S(2)}, u32[]{:S(2)}) collective-permute-start(bf16[256,256]{1,0:T(8,128)(2,1)S(1)} %get-tuple-element.47), channel_id=1, source_target_pairs={{0,4},{2,6},{4,0},{6,2},{1,5},{3,7},{5,1},{7,3},{8,12},{10,14},{12... | collective-permute-start | bytes 393224 | tf_op jit(solution)/shard_map/ppermute | solution.py:370
  94.1 4.8 %collective-permute-done.15.refs_6_ = bf16[256,256]{1,0:T(8,128)(2,1)S(1)} collective-permute-done((bf16[256,256]{1,0:T(8,128)(2,1)S(1)}, bf16[256,256]{1,0:T(8,128)(2,1)S(1)}, u32[]{:S(2)}, u32[]{:S(2)}) %collective-permute-start.15) | collective-permute-done | bytes 131104 | tf_op jit(solution)/shard_map/ppermute | solution.py:370
  98.9 6.4 %collective-permute-start.30 = (bf16[128,128]{1,0:T(8,128)(2,1)S(1)}, bf16[128,128]{1,0:T(8,128)(2,1)S(1)}, u32[]{:S(2)}, u32[]{:S(2)}) collective-permute-start(bf16[128,128]{1,0:T(8,128)(2,1)S(1)} %get-tuple-element.60), channel_id=1, source_target_pairs={{0,128},{32,160},{64,192},{96,224},{1,129},{33,161},{65,193},{97,2... | collective-permute-start | bytes 98312 | tf_op jit(solution)/shard_map/ppermute | solution.py:375
  105.3 1.6 %collective-permute-done.30.far_ref = bf16[128,128]{1,0:T(8,128)(2,1)S(1)} collective-permute-done((bf16[128,128]{1,0:T(8,128)(2,1)S(1)}, bf16[128,128]{1,0:T(8,128)(2,1)S(1)}, u32[]{:S(2)}, u32[]{:S(2)}) %collective-permute-start.30) | collective-permute-done | bytes 32800 | tf_op jit(solution)/shard_map/ppermute | solution.py:375
  108.8 5.1 %collective-permute-done.32.refs_2_ = bf16[256,128]{1,0:T(8,128)(2,1)S(1)} collective-permute-done((bf16[256,128]{1,0:T(8,128)(2,1)S(1)}, bf16[256,128]{1,0:T(8,128)(2,1)S(1)}, u32[]{:S(2)}, u32[]{:S(2)}) %collective-permute-start.32) | collective-permute-done | bytes 65568 | tf_op jit(solution)/shard_map/ppermute | solution.py:370
  113.9 1.6 %collective-permute-start.34 = (bf16[256,128]{1,0:T(8,128)(2,1)S(1)}, bf16[256,128]{1,0:T(8,128)(2,1)S(1)}, u32[]{:S(2)}, u32[]{:S(2)}) collective-permute-start(bf16[256,128]{1,0:T(8,128)(2,1)S(1)} %get-tuple-element.64), channel_id=1, source_target_pairs={{0,6},{2,0},{4,2},{6,4},{1,7},{3,1},{5,3},{7,5},{8,14},{10,8},{12,... | collective-permute-start | bytes 196616 | tf_op jit(solution)/shard_map/ppermute | solution.py:370
  115.5 2.7 %collective-permute-done.34.refs_4_ = bf16[256,128]{1,0:T(8,128)(2,1)S(1)} collective-permute-done((bf16[256,128]{1,0:T(8,128)(2,1)S(1)}, bf16[256,128]{1,0:T(8,128)(2,1)S(1)}, u32[]{:S(2)}, u32[]{:S(2)}) %collective-permute-start.34) | collective-permute-done | bytes 65568 | tf_op jit(solution)/shard_map/ppermute | solution.py:370
  119.2 4.7 %collective-permute-done.36.refs_6_ = bf16[256,128]{1,0:T(8,128)(2,1)S(1)} collective-permute-done((bf16[256,128]{1,0:T(8,128)(2,1)S(1)}, bf16[256,128]{1,0:T(8,128)(2,1)S(1)}, u32[]{:S(2)}, u32[]{:S(2)}) %collective-permute-start.36) | collective-permute-done | bytes 65568 | tf_op jit(solution)/shard_map/ppermute | solution.py:370
  123.9 1.3 %collective-permute-done.12.refs_3_ = bf16[256,256]{1,0:T(8,128)(2,1)S(1)} collective-permute-done((bf16[256,256]{1,0:T(8,128)(2,1)S(1)}, bf16[256,256]{1,0:T(8,128)(2,1)S(1)}, u32[]{:S(2)}, u32[]{:S(2)}) %collective-permute-start.12) | collective-permute-done | bytes 131104 | tf_op jit(solution)/shard_map/ppermute | solution.py:379
  129.0 2.1 %conv_out.1.conv_ref = f32[128,2048]{1,0:T(8,128)S(1)} custom-call(bf16[256,256]{1,0:T(8,128)(2,1)S(1)} %get-tuple-element.44.refs_0_, bf16[256,256]{1,0:T(8,128)(2,1)S(1)} %collective-permute-done.10.refs_1_, bf16[256,256]{1,0:T(8,128)(2,1)S(1)} %collective-permute-done.11.refs_2_, bf16[256,256]{1,0:T(8,128)(2,1)S(1)} %collective-permute-done.12.refs_3_, ...), custom_call_target="tpu_custom_call" | custom-call | flops 536870912 | bytes 6291456 | tf_op jit(solution)/shard_map/conv_out/pallas_call | solution.py:533
  131.1 1.9 %delta_out.1 = bf16[128,2048]{1,0:T(8,128)(2,1)} custom-call(f32[128,2048]{1,0:T(8,128)S(1)} %conv_out.1.conv_ref, bf16[256,128]{1,0:T(8,128)(2,1)S(1)} %get-tuple-element.62.refs_0_, bf16[256,128]{1,0:T(8,128)(2,1)S(1)} %collective-permute-done.31.refs_1_, bf16[256,128]{1,0:T(8,128)(2,1)S(1)} %collective-permute-done.32.refs_2_, ...), custom_call_target="tpu_custom_call" | custom-call | flops 536870912 | bytes 6291456 | tf_op jit(solution)/shard_map/delta_out/pallas_call | solution.py:563
  (84 shorter events, 17.4 us)
Async XLA Ops:
  0.0 15.1 %collective-permute-start.1 = (bf16[1024,256]{1,0:T(8,128)(2,1)}, bf16[1024,256]{1,0:T(8,128)(2,1)S(1)}, u32[]{:S(2)}, u32[]{:S(2)}) collective-permute-start(bf16[1024,256]{1,0:T(8,128)(2,1)} %refs_0_.3), channel_id=1, source_target_pairs={{0,2},{2,4},{4,6},{6,0},{1,3},{3,5},{5,7},{7,1},{8,10},{10,12},{12... | collective-permute-start | bytes 1572872 | tf_op jit(solution)/shard_map/ppermute | solution.py:370
  1.6 13.6 %collective-permute-start.3 = (bf16[1024,256]{1,0:T(8,128)(2,1)}, bf16[1024,256]{1,0:T(8,128)(2,1)S(1)}, u32[]{:S(2)}, u32[]{:S(2)}) collective-permute-start(bf16[1024,256]{1,0:T(8,128)(2,1)} %refs_0_.3), channel_id=1, source_target_pairs={{0,6},{2,0},{4,2},{6,4},{1,7},{3,1},{5,3},{7,5},{8,14},{10,8},{12,... | collective-permute-start | bytes 1572872 | tf_op jit(solution)/shard_map/ppermute | solution.py:370
  3.2 24.6 %collective-permute-start = (bf16[1024,256]{1,0:T(8,128)(2,1)}, bf16[1024,256]{1,0:T(8,128)(2,1)S(1)}, u32[]{:S(2)}, u32[]{:S(2)}) collective-permute-start(bf16[1024,256]{1,0:T(8,128)(2,1)} %refs_0_.3), channel_id=1, source_target_pairs={{0,1},{1,0},{2,3},{3,2},{4,5},{5,4},{6,7},{7,6},{8,9},{9,8},{10,11... | collective-permute-start | bytes 1572872 | tf_op jit(solution)/shard_map/ppermute | solution.py:379
  15.2 8.5 %collective-permute-start.5 = (bf16[512,256]{1,0:T(8,128)(2,1)S(1)}, bf16[512,256]{1,0:T(8,128)(2,1)S(1)}, u32[]{:S(2)}, u32[]{:S(2)}) collective-permute-start(bf16[512,256]{1,0:T(8,128)(2,1)S(1)} %get-tuple-element.38), channel_id=1, source_target_pairs={{0,2},{2,4},{4,6},{6,0},{1,3},{3,5},{5,7},{7,1},{8,10},{10,12},{12... | collective-permute-start | bytes 786440 | tf_op jit(solution)/shard_map/ppermute | solution.py:370
  16.9 7.6 %collective-permute-start.7 = (bf16[512,256]{1,0:T(8,128)(2,1)S(1)}, bf16[512,256]{1,0:T(8,128)(2,1)}, u32[]{:S(2)}, u32[]{:S(2)}) collective-permute-start(bf16[512,256]{1,0:T(8,128)(2,1)S(1)} %get-tuple-element.39), channel_id=1, source_target_pairs={{0,6},{2,0},{4,2},{6,4},{1,7},{3,1},{5,3},{7,5},{8,14},{10,8},{12,... | collective-permute-start | bytes 786440 | tf_op jit(solution)/shard_map/ppermute | solution.py:370
  23.8 4.2 %collective-permute-start.6 = (bf16[512,256]{1,0:T(8,128)(2,1)S(1)}, bf16[512,256]{1,0:T(8,128)(2,1)}, u32[]{:S(2)}, u32[]{:S(2)}) collective-permute-start(bf16[512,256]{1,0:T(8,128)(2,1)S(1)} %collective-permute-done.5.refs_6_), channel_id=1, source_target_pairs={{0,1},{1,0},{2,3},{3,2},{4,5},{5,4},{6,7},{7,6},{8,9},{9,8},{10,11... | collective-permute-start | bytes 786440 | tf_op jit(solution)/shard_map/ppermute | solution.py:379
  23.8 9.6 %collective-permute-start.2 = (bf16[1024,256]{1,0:T(8,128)(2,1)S(1)}, bf16[1024,256]{1,0:T(8,128)(2,1)S(1)}, u32[]{:S(2)}, u32[]{:S(2)}) collective-permute-start(bf16[1024,256]{1,0:T(8,128)(2,1)S(1)} %collective-permute-done.1.right_any.refs_2_), channel_id=1, source_target_pairs={{0,1},{1,0},{2,3},{3,2},{4,5},{5,4},{6,7},{7,6},{8,9},{9,8},{10,11... | collective-permute-start | bytes 1572872 | tf_op jit(solution)/shard_map/ppermute | solution.py:379
  24.4 9.0 %collective-permute-start.4 = (bf16[1024,256]{1,0:T(8,128)(2,1)S(1)}, bf16[1024,256]{1,0:T(8,128)(2,1)}, u32[]{:S(2)}, u32[]{:S(2)}) collective-permute-start(bf16[1024,256]{1,0:T(8,128)(2,1)S(1)} %collective-permute-done.3.left_any.refs_4_), channel_id=1, source_target_pairs={{0,1},{1,0},{2,3},{3,2},{4,5},{5,4},{6,7},{7,6},{8,9},{9,8},{10,11... | collective-permute-start | bytes 1572872 | tf_op jit(solution)/shard_map/ppermute | solution.py:379
  24.5 6.6 %collective-permute-start.8 = (bf16[512,256]{1,0:T(8,128)(2,1)}, bf16[512,256]{1,0:T(8,128)(2,1)}, u32[]{:S(2)}, u32[]{:S(2)}) collective-permute-start(bf16[512,256]{1,0:T(8,128)(2,1)} %collective-permute-done.7.refs_8_), channel_id=1, source_target_pairs={{0,1},{1,0},{2,3},{3,2},{4,5},{5,4},{6,7},{7,6},{8,9},{9,8},{10,11... | collective-permute-start | bytes 786440 | tf_op jit(solution)/shard_map/ppermute | solution.py:379
  27.8 28.0 %collective-permute-start.18 = (bf16[272,2048]{1,0:T(8,128)(2,1)S(1)}, bf16[272,2048]{1,0:T(8,128)(2,1)S(1)}, u32[]{:S(2)}, u32[]{:S(2)}) collective-permute-start(bf16[272,2048]{1,0:T(8,128)(2,1)S(1)} %fusion.1.refs_8_), channel_id=1, source_target_pairs={{0,2},{2,4},{4,6},{6,0},{1,3},{3,5},{5,7},{7,1},{8,10},{10,12},{12... | collective-permute-start | bytes 3342344 | tf_op jit(solution)/shard_map/ppermute | solution.py:370
  28.0 30.0 %collective-permute-start.20 = (bf16[272,2048]{1,0:T(8,128)(2,1)S(1)}, bf16[272,2048]{1,0:T(8,128)(2,1)S(1)}, u32[]{:S(2)}, u32[]{:S(2)}) collective-permute-start(bf16[272,2048]{1,0:T(8,128)(2,1)S(1)} %fusion.1.refs_8_), channel_id=1, source_target_pairs={{0,6},{2,0},{4,2},{6,4},{1,7},{3,1},{5,3},{7,5},{8,14},{10,8},{12,... | collective-permute-start | bytes 3342344 | tf_op jit(solution)/shard_map/ppermute | solution.py:370
  31.2 27.0 %collective-permute-start.17 = (bf16[272,2048]{1,0:T(8,128)(2,1)S(1)}, bf16[272,2048]{1,0:T(8,128)(2,1)S(1)}, u32[]{:S(2)}, u32[]{:S(2)}) collective-permute-start(bf16[272,2048]{1,0:T(8,128)(2,1)S(1)} %fusion.1.refs_8_), channel_id=1, source_target_pairs={{0,1},{1,0},{2,3},{3,2},{4,5},{5,4},{6,7},{7,6},{8,9},{9,8},{10,11... | collective-permute-start | bytes 3342344 | tf_op jit(solution)/shard_map/ppermute | solution.py:379
  46.0 15.4 %collective-permute-start.24 = (bf16[144,256]{1,0:T(8,128)(2,1)S(1)}, bf16[144,256]{1,0:T(8,128)(2,1)S(1)}, u32[]{:S(2)}, u32[]{:S(2)}) collective-permute-start(bf16[144,256]{1,0:T(8,128)(2,1)S(1)} %get-tuple-element.57.p0), channel_id=1, source_target_pairs={{0,16},{8,24},{16,0},{24,8},{1,17},{9,25},{17,1},{25,9},{2,18},{10... | collective-permute-start | bytes 221192 | tf_op jit(solution)/shard_map/ppermute | solution.py:370
  48.2 5.5 %collective-permute-start.9 = (bf16[32,128]{1,0:T(8,128)(2,1)S(1)}, bf16[32,128]{1,0:T(8,128)(2,1)S(1)}, u32[]{:S(2)}, u32[]{:S(2)}) collective-permute-start(bf16[32,128]{1,0:T(8,128)(2,1)S(1)} %get-tuple-element.42), channel_id=1, source_target_pairs={{0,8},{8,16},{16,24},{24,32},{32,40},{40,48},{48,56},{56,64},{64,7... | collective-permute-start | bytes 24584 | tf_op jit(solution)/shard_map/ppermute | solution.py:669
  53.8 7.8 %collective-permute-start.25 = (bf16[144,256]{1,0:T(8,128)(2,1)S(1)}, bf16[144,256]{1,0:T(8,128)(2,1)S(1)}, u32[]{:S(2)}, u32[]{:S(2)}) collective-permute-start(bf16[144,256]{1,0:T(8,128)(2,1)S(1)} %get-tuple-element.57.p0), channel_id=1, source_target_pairs={{0,24},{8,0},{16,8},{24,16},{1,25},{9,1},{17,9},{25,17},{2,26},{10... | collective-permute-start | bytes 221192 | tf_op jit(solution)/shard_map/ppermute | solution.py:370
  55.8 6.1 %collective-permute-start.26 = (bf16[144,256]{1,0:T(8,128)(2,1)S(1)}, bf16[144,256]{1,0:T(8,128)(2,1)S(1)}, u32[]{:S(2)}, u32[]{:S(2)}) collective-permute-start(bf16[144,256]{1,0:T(8,128)(2,1)S(1)} %get-tuple-element.57.p0), channel_id=1, source_target_pairs={{0,8},{8,16},{16,24},{24,0},{1,9},{9,17},{17,25},{25,1},{2,10},{10... | collective-permute-start | bytes 221192 | tf_op jit(solution)/shard_map/ppermute | solution.py:370
  57.9 6.2 %collective-permute-start.11 = (bf16[256,256]{1,0:T(8,128)(2,1)S(1)}, bf16[256,256]{1,0:T(8,128)(2,1)S(1)}, u32[]{:S(2)}, u32[]{:S(2)}) collective-permute-start(bf16[256,256]{1,0:T(8,128)(2,1)S(1)} %get-tuple-element.45), channel_id=1, source_target_pairs={{0,2},{2,4},{4,6},{6,0},{1,3},{3,5},{5,7},{7,1},{8,10},{10,12},{12... | collective-permute-start | bytes 393224 | tf_op jit(solution)/shard_map/ppermute | solution.py:370
  58.1 50.3 %collective-permute-start.22 = (bf16[144,2048]{1,0:T(8,128)(2,1)S(1)}, bf16[144,2048]{1,0:T(8,128)(2,1)S(1)}, u32[]{:S(2)}, u32[]{:S(2)}) collective-permute-start(bf16[144,2048]{1,0:T(8,128)(2,1)S(1)} %get-tuple-element.49), channel_id=1, source_target_pairs={{0,6},{2,0},{4,2},{6,4},{1,7},{3,1},{5,3},{7,5},{8,14},{10,8},{12,... | collective-permute-start | bytes 1769480 | tf_op jit(solution)/shard_map/ppermute | solution.py:370
  61.4 14.1 %collective-permute-start.13 = (bf16[256,256]{1,0:T(8,128)(2,1)S(1)}, bf16[256,256]{1,0:T(8,128)(2,1)S(1)}, u32[]{:S(2)}, u32[]{:S(2)}) collective-permute-start(bf16[256,256]{1,0:T(8,128)(2,1)S(1)} %get-tuple-element.46), channel_id=1, source_target_pairs={{0,6},{2,0},{4,2},{6,4},{1,7},{3,1},{5,3},{7,5},{8,14},{10,8},{12,... | collective-permute-start | bytes 393224 | tf_op jit(solution)/shard_map/ppermute | solution.py:370
  61.5 66.6 %collective-permute-start.19 = (bf16[272,2048]{1,0:T(8,128)(2,1)S(1)}, bf16[272,2048]{1,0:T(8,128)(2,1)S(1)}, u32[]{:S(2)}, u32[]{:S(2)}) collective-permute-start(bf16[272,2048]{1,0:T(8,128)(2,1)S(1)} %collective-permute-done.18.right_any.refs_10_), channel_id=1, source_target_pairs={{0,1},{1,0},{2,3},{3,2},{4,5},{5,4},{6,7},{7,6},{8,9},{9,8},{10,11... | collective-permute-start | bytes 3342344 | tf_op jit(solution)/shard_map/ppermute | solution.py:379
  62.0 66.5 %collective-permute-start.21 = (bf16[272,2048]{1,0:T(8,128)(2,1)S(1)}, bf16[272,2048]{1,0:T(8,128)(2,1)S(1)}, u32[]{:S(2)}, u32[]{:S(2)}) collective-permute-start(bf16[272,2048]{1,0:T(8,128)(2,1)S(1)} %collective-permute-done.20.left_any.refs_12_), channel_id=1, source_target_pairs={{0,1},{1,0},{2,3},{3,2},{4,5},{5,4},{6,7},{7,6},{8,9},{9,8},{10,11... | collective-permute-start | bytes 3342344 | tf_op jit(solution)/shard_map/ppermute | solution.py:379
  64.1 17.7 %collective-permute-start.27 = (bf16[144,256]{1,0:T(8,128)(2,1)S(1)}, bf16[144,256]{1,0:T(8,128)(2,1)S(1)}, u32[]{:S(2)}, u32[]{:S(2)}) collective-permute-start(bf16[144,256]{1,0:T(8,128)(2,1)S(1)} %get-tuple-element.58.p0), channel_id=1, source_target_pairs={{0,64},{32,96},{64,0},{96,32},{128,192},{160,224},{192,128},{224,1... | collective-permute-start | bytes 221192 | tf_op jit(solution)/shard_map/ppermute | solution.py:656
  75.5 8.2 %collective-permute-start.28 = (bf16[144,256]{1,0:T(8,128)(2,1)S(1)}, bf16[144,256]{1,0:T(8,128)(2,1)S(1)}, u32[]{:S(2)}, u32[]{:S(2)}) collective-permute-start(bf16[144,256]{1,0:T(8,128)(2,1)S(1)} %get-tuple-element.58.p0), channel_id=1, source_target_pairs={{0,96},{32,0},{64,32},{96,64},{128,224},{160,128},{192,160},{224,1... | collective-permute-start | bytes 221192 | tf_op jit(solution)/shard_map/ppermute | solution.py:656
  81.8 37.4 %collective-permute-start.38 = (bf16[128,2048]{1,0:T(8,128)(2,1)S(1)}, bf16[128,2048]{1,0:T(8,128)(2,1)S(1)}, u32[]{:S(2)}, u32[]{:S(2)}) collective-permute-start(bf16[128,2048]{1,0:T(8,128)(2,1)S(1)} %get-tuple-element.66), channel_id=1, source_target_pairs={{0,2},{2,4},{4,6},{6,0},{1,3},{3,5},{5,7},{7,1},{8,10},{10,12},{12... | collective-permute-start | bytes 1572872 | tf_op jit(solution)/shard_map/ppermute | solution.py:370
  83.8 6.6 %collective-permute-start.29 = (bf16[144,256]{1,0:T(8,128)(2,1)S(1)}, bf16[144,256]{1,0:T(8,128)(2,1)S(1)}, u32[]{:S(2)}, u32[]{:S(2)}) collective-permute-start(bf16[144,256]{1,0:T(8,128)(2,1)S(1)} %get-tuple-element.58.p0), channel_id=1, source_target_pairs={{0,32},{32,64},{64,96},{96,0},{128,160},{160,192},{192,224},{224,1... | collective-permute-start | bytes 221192 | tf_op jit(solution)/shard_map/ppermute | solution.py:656
  90.4 8.6 %collective-permute-start.15 = (bf16[256,256]{1,0:T(8,128)(2,1)S(1)}, bf16[256,256]{1,0:T(8,128)(2,1)S(1)}, u32[]{:S(2)}, u32[]{:S(2)}) collective-permute-start(bf16[256,256]{1,0:T(8,128)(2,1)S(1)} %get-tuple-element.47), channel_id=1, source_target_pairs={{0,4},{2,6},{4,0},{6,2},{1,5},{3,7},{5,1},{7,3},{8,12},{10,14},{12... | collective-permute-start | bytes 393224 | tf_op jit(solution)/shard_map/ppermute | solution.py:370
  98.9 8.0 %collective-permute-start.30 = (bf16[128,128]{1,0:T(8,128)(2,1)S(1)}, bf16[128,128]{1,0:T(8,128)(2,1)S(1)}, u32[]{:S(2)}, u32[]{:S(2)}) collective-permute-start(bf16[128,128]{1,0:T(8,128)(2,1)S(1)} %get-tuple-element.60), channel_id=1, source_target_pairs={{0,128},{32,160},{64,192},{96,224},{1,129},{33,161},{65,193},{97,2... | collective-permute-start | bytes 98312 | tf_op jit(solution)/shard_map/ppermute | solution.py:375
  108.2 5.7 %collective-permute-start.32 = (bf16[256,128]{1,0:T(8,128)(2,1)S(1)}, bf16[256,128]{1,0:T(8,128)(2,1)S(1)}, u32[]{:S(2)}, u32[]{:S(2)}) collective-permute-start(bf16[256,128]{1,0:T(8,128)(2,1)S(1)} %get-tuple-element.63), channel_id=1, source_target_pairs={{0,2},{2,4},{4,6},{6,0},{1,3},{3,5},{5,7},{7,1},{8,10},{10,12},{12... | collective-permute-start | bytes 196616 | tf_op jit(solution)/shard_map/ppermute | solution.py:370
  108.4 20.3 %collective-permute-start.23 = (bf16[144,2048]{1,0:T(8,128)(2,1)S(1)}, bf16[144,2048]{1,0:T(8,128)(2,1)S(1)}, u32[]{:S(2)}, u32[]{:S(2)}) collective-permute-start(bf16[144,2048]{1,0:T(8,128)(2,1)S(1)} %collective-permute-done.22.refs_14_), channel_id=1, source_target_pairs={{0,1},{1,0},{2,3},{3,2},{4,5},{5,4},{6,7},{7,6},{8,9},{9,8},{10,11... | collective-permute-start | bytes 1769480 | tf_op jit(solution)/shard_map/ppermute | solution.py:379
  113.9 4.3 %collective-permute-start.34 = (bf16[256,128]{1,0:T(8,128)(2,1)S(1)}, bf16[256,128]{1,0:T(8,128)(2,1)S(1)}, u32[]{:S(2)}, u32[]{:S(2)}) collective-permute-start(bf16[256,128]{1,0:T(8,128)(2,1)S(1)} %get-tuple-element.64), channel_id=1, source_target_pairs={{0,6},{2,0},{4,2},{6,4},{1,7},{3,1},{5,3},{7,5},{8,14},{10,8},{12,... | collective-permute-start | bytes 196616 | tf_op jit(solution)/shard_map/ppermute | solution.py:370
  118.2 5.8 %collective-permute-start.36 = (bf16[256,128]{1,0:T(8,128)(2,1)S(1)}, bf16[256,128]{1,0:T(8,128)(2,1)S(1)}, u32[]{:S(2)}, u32[]{:S(2)}) collective-permute-start(bf16[256,128]{1,0:T(8,128)(2,1)S(1)} %get-tuple-element.65), channel_id=1, source_target_pairs={{0,4},{2,6},{4,0},{6,2},{1,5},{3,7},{5,1},{7,3},{8,12},{10,14},{12... | collective-permute-start | bytes 196616 | tf_op jit(solution)/shard_map/ppermute | solution.py:370
  119.2 11.9 %collective-permute-start.39 = (bf16[128,2048]{1,0:T(8,128)(2,1)S(1)}, bf16[128,2048]{1,0:T(8,128)(2,1)S(1)}, u32[]{:S(2)}, u32[]{:S(2)}) collective-permute-start(bf16[128,2048]{1,0:T(8,128)(2,1)S(1)} %collective-permute-done.38.refs_14_), channel_id=1, source_target_pairs={{0,1},{1,0},{2,3},{3,2},{4,5},{5,4},{6,7},{7,6},{8,9},{9,8},{10,11... | collective-permute-start | bytes 1572872 | tf_op jit(solution)/shard_map/ppermute | solution.py:379
  (15 other events, 136.5 us)
